TPU v7x, 256 devices: a whole 4x4x8 slice. The times are simulated.
256 devices in a mesh: sp: 16 (over y, x), tp: 16 (over z, core).
Axes of the slice: x: 4, y: 4, z: 8, core: 2. Of those that a mesh axis runs over, the one named last changes fastest.
Arguments:
- mix_in: bfloat16 [16384, 2048], P('sp', 'tp'), may hold values from -8 to 8
- gate_in: bfloat16 [16384, 2048], P('sp', 'tp'), may hold values from -6 to 6
- conv_w: float32 [4, 2048], P(None, 'tp'), may hold values from -3 to 3
- conv_b: float32 [2048], P('tp'), may hold values from -3 to 3
- decay_param: float32 [2, 2048], P(None, 'tp')
- recur_gate: float32 [2, 32, 64, 64], P(None, 'tp'), may hold values from -0.75 to 0.75
- recur_bias: float32 [2, 2048], P(None, 'tp'), may hold values from -4 to 4
- input_gate: float32 [2, 32, 64, 64], P(None, 'tp'), may hold values from -0.75 to 0.75
- input_bias: float32 [2, 2048], P(None, 'tp'), may hold values from -4 to 4
- residual: bfloat16 [16384, 2048], P(('sp', 'tp')), may hold values from -6 to 6
- out_proj: bfloat16 [2048, 2048], replicated, may hold values from -0.125 to 0.125
- norm_gain: float32 [3, 2048], replicated, may hold values from 0.1 to 1.9
- routes: int32 [16384, 2], P('sp'), may hold values from 0 to 15, all different within a row; in each aligned block of 64 rows (0 to 63, 64 to 127, ...) at most 16 rows name the same one
- route_wt: float32 [16384, 2], P('sp'), may hold values from 0.1 to 1
- exp_gate: bfloat16 [16, 2048, 1024], P('sp', None, 'tp'), may hold values from -0.125 to 0.125
- exp_up: bfloat16 [16, 2048, 1024], P('sp', None, 'tp'), may hold values from -0.125 to 0.125
- exp_down: bfloat16 [16, 1024, 2048], P('sp', 'tp'), may hold values from -0.1875 to 0.1875
Outputs:
- final: bfloat16 [16384, 2048], P(('sp', 'tp'))
Inputs may be any that keep to these rules, and one draw needn't show every extreme that they name: `routes`: in each aligned block of 64 tokens (the rows of one device in the expert layer) no expert is named more than 16 times, and in some block some expert exactly 16 times; a token's 2 experts differ.
All inputs are finite; a program needn't handle non-finite values.
Results may differ from a plain program's by a relative error of at most 0.008.
Values may be sent and summed in bfloat16 or wider, within the bound.
No kernel may reach another device: no remote copies, remote signals or barrier semaphores. Data moves between devices by JAX's collectives and lax.ppermute only.
A program may use at most 128 MiB of HBM per device.

v0:
```python
import jax
import jax.numpy as jnp
from jax import lax
from jax.sharding import PartitionSpec as P

EPSILON = 1e-06
HIGHEST_MODE = lax.Precision.HIGHEST


def extended(cells, sides, width):
    for axis, dim in sides:
        count = lax.axis_size(axis)
        ends = count - 1
        head = lax.slice_in_dim(cells, 0, width, axis=dim)
        tail = lax.slice_in_dim(cells, cells.shape[dim] - width, cells.shape[dim], axis=dim)
        cells = jnp.concatenate(
            [
                lax.ppermute(tail, axis, [(i, (i + 1) % count) for i in range(ends)]),
                cells,
                lax.ppermute(head, axis, [((i + 1) % count, i) for i in range(ends)]),
            ],
            axis=dim,
        )
    return cells


def copy_for_each(array, axis):
    copies = jnp.broadcast_to(array, (lax.axis_size(axis), *array.shape))
    return lax.all_to_all(copies, axis, split_axis=0, concat_axis=0, tiled=True)


def collected_together(array, axis):
    leaves = jax.tree.leaves(array)
    order = sorted(range(len(leaves)), key=lambda k: -leaves[k].size)
    width = (1, *leaves[order[0]].shape)[-1]
    lines = [
        jnp.pad(leaves[k].reshape(-1), (0, -leaves[k].size % width)).reshape(-1, width)
        for k in order
    ]
    both, at, found = (copy_for_each(jnp.concatenate(lines), axis), 0, {})
    for k, line in zip(order, lines):
        piece = both[:, at : at + len(line)].reshape(len(both), -1)
        found[k] = piece[:, : leaves[k].size].reshape(-1, *leaves[k].shape)
        at += len(line)
    numbers = iter(range(len(leaves)))
    return jax.tree.map(lambda _: found[next(numbers)], array)


def folded_in_pairs(pieces, combine):
    while len(jax.tree.leaves(pieces)[0]) > 1:
        pieces = jax.vmap(combine)(
            *(jax.tree.map(lambda part: part[side::2], pieces) for side in (0, 1))
        )
    return jax.tree.map(lambda part: part[0], pieces)


def carried_in(array, axis, combine, identity, reverse):
    length, here = (lax.axis_size(axis), lax.axis_index(axis))
    passed = jnp.arange(length) > here if reverse else jnp.arange(length) < here

    def kept(part, zero, own):
        part = jnp.where(
            passed.reshape(-1, *(1 for _ in own.shape)), part, jnp.asarray(zero, own.dtype)
        )
        return part[::-1] if reverse else part

    pieces = collected_together(array, axis)
    return folded_in_pairs(jax.tree.map(kept, pieces, identity, array), combine)


def gather_turned(arrays, axis, dims):
    turned = [jnp.moveaxis(a, dim, 0) for a, dim in zip(arrays, dims)]
    widths = [t[0].size for t in turned]
    both = jnp.concatenate([t.reshape(-1, w) for t, w in zip(turned, widths)], axis=1)
    filled = lax.all_gather(both, axis, axis=0, tiled=True)
    tiles = jnp.split(filled, [sum(widths[:k]) for k in range(1, len(widths))], axis=1)
    return tuple(
        (
            jnp.moveaxis(b.reshape(-1, *t.shape[1:]), 0, dim)
            for b, t, dim in zip(tiles, turned, dims)
        )
    )


def norm_rows(values, gain):
    floats = values.astype(jnp.float32)
    return floats * lax.rsqrt(jnp.mean(floats * floats, axis=-1, keepdims=True) + EPSILON) * gain


def pair_join(earlier, later_pair):
    return (earlier[0] * later_pair[0], later_pair[0] * earlier[1] + later_pair[1])


def slot_table(route_rows, experts, capacity):
    row_count, top_count = route_rows.shape
    flattened = route_rows.reshape(row_count * top_count)
    matches = (flattened[:, None] == jnp.arange(experts, dtype=jnp.int32)[None, :]).astype(
        jnp.int32
    )
    earlier_hits = jnp.cumsum(matches, axis=0) - matches
    position = jnp.sum(earlier_hits * matches, axis=1)
    return (flattened * capacity + position).reshape(row_count, top_count)


def weight_table(slots, route_weights, total_slots):
    matches = slots[..., None] == jnp.arange(total_slots, dtype=jnp.int32)
    return jnp.sum(jnp.where(matches, route_weights[..., None], 0.0), axis=-2)


def block_matrix(blocks):
    heads, head_dim, _ = blocks.shape
    identity = jnp.eye(heads, dtype=blocks.dtype)
    return jnp.einsum("hij,hg->higj", blocks, identity).reshape(heads * head_dim, heads * head_dim)


def coefficients(conv_out, recur_blocks, recur_bias, input_blocks, input_bias, decay_param):
    recur_pre = jnp.dot(conv_out, block_matrix(recur_blocks), precision=HIGHEST_MODE)
    input_pre = jnp.dot(conv_out, block_matrix(input_blocks), precision=HIGHEST_MODE)
    recur_act = jax.nn.sigmoid(recur_pre + recur_bias)
    input_act = jax.nn.sigmoid(input_pre + input_bias)
    log_decay = -8.0 * recur_act * jax.nn.softplus(-decay_param)
    return (jnp.exp(log_decay), jnp.sqrt(-jnp.expm1(2.0 * log_decay)) * (input_act * conv_out))


def on_device(
    mix_in,
    gate_in,
    conv_w,
    conv_b,
    decay_param,
    recur_gate,
    recur_bias,
    input_gate,
    input_bias,
    residual,
    out_proj,
    norm_gain,
    routes,
    route_wt,
    exp_gate,
    exp_up,
    exp_down,
):
    seq_len = mix_in.shape[0]
    padded = extended(mix_in, (("sp", 0),), 2).astype(jnp.float32)
    conv_out = conv_b + padded[0:seq_len] * conv_w[0]
    for tap in range(1, conv_w.shape[0]):
        conv_out = conv_out + padded[tap : tap + seq_len] * conv_w[tap]
    fwd_decay, fwd_drive = coefficients(
        conv_out, recur_gate[0], recur_bias[0], input_gate[0], input_bias[0], decay_param[0]
    )
    bwd_decay, bwd_drive = coefficients(
        conv_out, recur_gate[1], recur_bias[1], input_gate[1], input_bias[1], decay_param[1]
    )
    fwd_prod, fwd_state = lax.associative_scan(pair_join, (fwd_decay, fwd_drive), axis=0)
    bwd_prod, bwd_state = lax.associative_scan(
        pair_join, (jnp.flip(bwd_decay, 0), jnp.flip(bwd_drive, 0)), axis=0
    )
    identity = (jnp.ones_like(fwd_prod[-1]), jnp.zeros_like(fwd_state[-1]))
    fwd_enter = carried_in((fwd_prod[-1], fwd_state[-1]), "sp", pair_join, identity, False)[1]
    bwd_enter = carried_in((bwd_prod[-1], bwd_state[-1]), "sp", pair_join, identity, True)[1]
    state_sum = fwd_state + fwd_prod * fwd_enter + jnp.flip(bwd_state + bwd_prod * bwd_enter, 0)
    mixed = (state_sum * jax.nn.gelu(gate_in.astype(jnp.float32))).astype(jnp.bfloat16)
    tok_rows = lax.all_to_all(mixed, "tp", split_axis=0, concat_axis=1, tiled=True)
    proj = jnp.dot(tok_rows, out_proj, preferred_element_type=jnp.float32).astype(jnp.bfloat16)
    proj = lax.optimization_barrier(proj)
    stream = (residual.astype(jnp.float32) + norm_rows(proj, norm_gain[0])).astype(jnp.bfloat16)
    stream = lax.optimization_barrier(stream)
    normed = norm_rows(stream, norm_gain[1]).astype(jnp.bfloat16)
    sp_count = lax.axis_size("sp")
    row_count = residual.shape[0]
    width_model = residual.shape[1]
    top_count = routes.shape[1]
    local_experts = exp_gate.shape[0]
    experts = local_experts * sp_count
    capacity = 2 * row_count * top_count // experts
    total_slots = experts * capacity
    own_start = lax.axis_index("tp") * row_count
    own_routes = lax.dynamic_slice_in_dim(routes, own_start, row_count, 0)
    own_weights = lax.dynamic_slice_in_dim(route_wt, own_start, row_count, 0)
    own_slots = slot_table(own_routes, experts, capacity)
    selector = jnp.sum(
        (own_slots[:, :, None] == jnp.arange(total_slots, dtype=jnp.int32)).astype(jnp.bfloat16),
        axis=1,
    )
    outgoing = jnp.einsum("rs,rd->sd", selector, normed, preferred_element_type=jnp.float32).astype(
        jnp.bfloat16
    )
    arrived = lax.all_to_all(
        outgoing.reshape(experts, capacity, width_model),
        "sp",
        split_axis=0,
        concat_axis=1,
        tiled=True,
    )
    gate_full, up_full = gather_turned((exp_gate, exp_up), "tp", (2, 2))
    gate_act = jnp.einsum("emd,edf->emf", arrived, gate_full, preferred_element_type=jnp.float32)
    up_act = jnp.einsum("emd,edf->emf", arrived, up_full, preferred_element_type=jnp.float32)
    hidden = (jax.nn.silu(gate_act) * up_act).astype(jnp.bfloat16)
    summed = jnp.einsum(
        "emf,efd->emd",
        hidden,
        lax.all_gather(exp_down, "tp", axis=1, tiled=True),
        preferred_element_type=jnp.float32,
    )
    out_rows = summed.astype(jnp.bfloat16).reshape(local_experts, sp_count, capacity, width_model)
    returned = lax.all_to_all(out_rows, "sp", split_axis=1, concat_axis=0, tiled=True)
    values = returned.reshape(total_slots, width_model).astype(jnp.float32)
    own_table = weight_table(own_slots, own_weights, total_slots)
    mixture = jnp.dot(own_table, values, precision=HIGHEST_MODE).astype(jnp.bfloat16)
    mixture = lax.optimization_barrier(mixture)
    return (stream.astype(jnp.float32) + norm_rows(mixture, norm_gain[2])).astype(jnp.bfloat16)


def solution(mesh):
    return jax.shard_map(
        on_device,
        mesh=mesh,
        in_specs=(
            P("sp", "tp"),
            P("sp", "tp"),
            P(None, "tp"),
            P("tp"),
            P(None, "tp"),
            P(None, "tp", None, None),
            P(None, "tp"),
            P(None, "tp", None, None),
            P(None, "tp"),
            P(("sp", "tp"), None),
            P(),
            P(),
            P("sp", None),
            P("sp", None),
            P("sp", None, "tp"),
            P("sp", None, "tp"),
            P("sp", "tp", None),
        ),
        out_specs=P(("sp", "tp"), None),
        check_vma=False,
    )
```

profile of v0, /device:TPU:1, one launch (start us, length us, event | category | flops | bytes accessed | tf_op | source)
XLA Modules:
  0.0 247.0 jit_solution(15840716906587601891)
XLA Ops:
  6.5 1.9 pad_maximum_fusion
  9.2 3.9 %collective-permute-start = (bf16[2,128]{1,0:T(2,128)(2,1)S(1)}, bf16[2,128]{1,0:T(2,128)(2,1)S(1)}, u32[]{:S(2)}, u32[]{:S(2)}) collective-permute-start(bf16[2,128]{1,0:T(2,128)(2,1)S(1)} %get-tuple-element.14), channel_id=1, source_target_pairs={{0,16},{16,32},{32,48},{48,64},{64,80},{80,96},{96,112},{112,128},... | collective-permute-start | bytes 1544 | tf_op jit(solution)/shard_map/ppermute | solution.py:18
  20.7 2.0 concatenate.120
  49.8 1.7 fusion.91
  51.5 2.1 fusion.14
  97.8 7.7 %all-to-all-start = ((f32[16,2,128]{2,1,0:T(2,128)}), f32[16,2,128]{2,1,0:T(2,128)}, u32[]{:S(2)}, u32[]{:S(2)}) async-start(f32[16,2,128]{2,1,0:T(2,128)} %broadcast_in_dim.59), calls=%async_computation | async-start | bytes 32768 | tf_op jit(solution)/shard_map/all_to_all | solution.py:29
  123.1 3.0 %slice.1014 = f32[511,128]{1,0:T(8,128)} reverse(f32[511,128]{1,0:T(8,128)} %slice.1013), dimensions={0} | reverse | bytes 523264 | tf_op jit(solution)/shard_map/slice | solution.py:156
  126.1 1.4 slice.936
  130.1 1.4 pad_maximum_fusion.3
  132.6 1.6 pad.303
  134.3 2.7 %pad.302 = f32[1024,128]{1,0:T(8,128)} pad(f32[512,128]{1,0:T(8,128)} %pad_maximum_fusion.3, f32[]{:T(128)} %constant.17.clone.1), padding=0_1_1x0_0_0 | pad | bytes 786436 | tf_op jit(solution)/shard_map/pad | solution.py:156
  138.3 6.6 %all-to-all-start.1 = ((f32[16,2,128]{2,1,0:T(2,128)}), f32[16,2,128]{2,1,0:T(2,128)S(1)}, u32[]{:S(2)}, u32[]{:S(2)}) async-start(f32[16,2,128]{2,1,0:T(2,128)} %broadcast_in_dim.63), calls=%async_computation.1 | async-start | bytes 32768 | tf_op jit(solution)/shard_map/all_to_all | solution.py:29
  146.7 4.6 %all-to-all-done.1 = f32[16,2,128]{2,1,0:T(2,128)S(1)} async-done(((f32[16,2,128]{2,1,0:T(2,128)}), f32[16,2,128]{2,1,0:T(2,128)S(1)}, u32[]{:S(2)}, u32[]{:S(2)}) %all-to-all-start.1) | async-done | bytes 16416 | tf_op jit(solution)/shard_map/all_to_all | solution.py:29
  151.7 2.2 multiply_add_fusion
  153.9 3.4 %rev.8 = f32[1024,128]{1,0:T(8,128)S(1)} reverse(f32[1024,128]{1,0:T(8,128)} %multiply_add_fusion), dimensions={0} | reverse | bytes 1048576 | tf_op jit(solution)/shard_map/jit(_flip)/rev | solution.py:162
  157.4 2.0 fusion.47
  159.3 11.7 %all-to-all-start.2 = ((bf16[16,64,128]{2,1,0:T(8,128)(2,1)}), bf16[16,64,128]{2,1,0:T(8,128)(2,1)S(1)}, u32[]{:S(2)}, u32[]{:S(2)}) async-start(bf16[16,64,128]{2,1,0:T(8,128)(2,1)} %bitcast.24), calls=%async_computation.2 | async-start | bytes 524288 | tf_op jit(solution)/shard_map/all_to_all | solution.py:164
  171.2 11.4 %all-to-all-done.2 = bf16[16,64,128]{2,1,0:T(8,128)(2,1)S(1)} async-done(((bf16[16,64,128]{2,1,0:T(8,128)(2,1)}), bf16[16,64,128]{2,1,0:T(8,128)(2,1)S(1)}, u32[]{:S(2)}, u32[]{:S(2)}) %all-to-all-start.2) | async-done | bytes 262176 | tf_op jit(solution)/shard_map/all_to_all | solution.py:164
  182.6 5.0 %convolution_convert_fusion.2 = bf16[64,2048]{1,0:T(8,128)(2,1)S(1)} fusion(bf16[2048,2048]{1,0:T(8,128)(2,1)} %param.27, bf16[16,64,128]{2,1,0:T(8,128)(2,1)S(1)} %all-to-all-done.2), kind=kOutput, calls=%fused_computation.9 | convolution fusion | flops 537001984 | bytes 8912896 | tf_op jit(solution)/shard_map/dot_general | solution.py:165
  188.6 19.8 %all_to_all.47 = bf16[16,16,2048]{2,1,0:T(8,128)(2,1)S(1)} all-to-all(bf16[16,16,2048]{2,1,0:T(8,128)(2,1)S(1)} %bitcast.114), channel_id=1, replica_groups=mesh['sp'=16,'tp'=16] {'sp'}, dimensions={0} | all-to-all | bytes 2097152 | tf_op jit(solution)/shard_map/all_to_all | solution.py:189
  208.4 3.5 %fusion.1 = f32[256,1024]{1,0:T(8,128)S(1)} fusion(bf16[256,2048]{1,0:T(8,128)(2,1)S(1)} %bitcast.115, bf16[1024,4096]{1,0:T(8,128)(2,1)} %all-gather.3.cloned.1.call-done), kind=kOutput, calls=%fused_computation.3 | convolution fusion | flops 1073741824 | bytes 6291456 | tf_op jit(solution)/shard_map/emd,edf->emf/dot_general | solution.py:197
  212.0 6.9 %fusion.4 = bf16[256,2048]{1,0:T(8,128)(2,1)} fusion(bf16[1,1024,2048]{2,1,0:T(8,128)(2,1)} %all-gather.5.cloned.1.call-done, bf16[256,2048]{1,0:T(8,128)(2,1)S(1)} %bitcast.116, bf16[1024,4096]{1,0:T(8,128)(2,1)} %all-gather.3.cloned.1.call-done, f32[256,1024]{1,0:T(8,128)S(1)} %fusion.1), kind=kOutput, calls=%fused_computation.6 | convolution fusion | flops 2149580800 | bytes 11534336 | tf_op jit(solution)/shard_map/emf,efd->emd/dot_general | solution.py:200
  218.9 3.7 %all-to-all-start.4 = ((bf16[1,16,16,2048]{3,2,0,1:T(8,128)(2,1)}), bf16[1,16,16,2048]{3,2,0,1:T(8,128)(2,1)S(1)}, u32[]{:S(2)}, u32[]{:S(2)}) async-start(bf16[1,16,16,2048]{3,2,0,1:T(8,128)(2,1)} %bitcast.42), calls=%async_computation.4 | async-start | bytes 2097152 | tf_op jit(solution)/shard_map/all_to_all | solution.py:207
  223.4 15.0 %all-to-all-done.4 = bf16[1,16,16,2048]{3,2,0,1:T(8,128)(2,1)S(1)} async-done(((bf16[1,16,16,2048]{3,2,0,1:T(8,128)(2,1)}), bf16[1,16,16,2048]{3,2,0,1:T(8,128)(2,1)S(1)}, u32[]{:S(2)}, u32[]{:S(2)}) %all-to-all-start.4) | async-done | bytes 1048608 | tf_op jit(solution)/shard_map/all_to_all | solution.py:207
  (435 shorter events, 106.9 us)
Async XLA Ops:
  6.5 9.5 %copy-start = (s32[1024,2]{0,1:T(2,128)S(1)}, s32[1024,2]{0,1:T(2,128)}, u32[]{:S(2)}) copy-start(s32[1024,2]{0,1:T(2,128)} %param.29) | copy-start | bytes 24580
  6.5 201.9 %all-gather.3.cloned.1.call-start = ((), (), s32[]{:S(2)}) async-start(), calls=%async_computation.5 | async-start | bytes 8912896 | tf_op jit(solution)/shard_map/all_gather | solution.py:75
  8.4 203.5 %all-gather.5.cloned.1.call-start = ((), (), s32[]{:S(2)}) async-start(), calls=%async_computation.6 | async-start | bytes 4456448 | tf_op jit(solution)/shard_map/all_gather | solution.py:203
  9.2 11.6 %collective-permute-start = (bf16[2,128]{1,0:T(2,128)(2,1)S(1)}, bf16[2,128]{1,0:T(2,128)(2,1)S(1)}, u32[]{:S(2)}, u32[]{:S(2)}) collective-permute-start(bf16[2,128]{1,0:T(2,128)(2,1)S(1)} %get-tuple-element.14), channel_id=1, source_target_pairs={{0,16},{16,32},{32,48},{48,64},{64,80},{80,96},{96,112},{112,128},... | collective-permute-start | bytes 1544 | tf_op jit(solution)/shard_map/ppermute | solution.py:18
  13.1 7.6 %collective-permute-start.1 = (bf16[2,128]{1,0:T(2,128)(2,1)S(1)}, bf16[2,128]{1,0:T(2,128)(2,1)S(1)}, u32[]{:S(2)}, u32[]{:S(2)}) collective-permute-start(bf16[2,128]{1,0:T(2,128)(2,1)S(1)} %get-tuple-element.13), channel_id=1, source_target_pairs={{16,0},{32,16},{48,32},{64,48},{80,64},{96,80},{112,96},{128,112},... | collective-permute-start | bytes 1544 | tf_op jit(solution)/shard_map/ppermute | solution.py:20
  23.7 0.8 copy-start.3
  25.4 29.9 %copy-start.1 = (f32[1024,128]{1,0:T(8,128)}, f32[1024,128]{1,0:T(8,128)S(1)}, u32[]{:S(2)}) copy-start(f32[1024,128]{1,0:T(8,128)S(1)} %fusion.25) | copy-start | bytes 1572868
  55.8 40.9 %copy-start.2 = (f32[511,128]{1,0:T(8,128)S(1)}, f32[511,128]{1,0:T(8,128)}, u32[]{:S(2)}) copy-start(f32[511,128]{1,0:T(8,128)} %slice.817) | copy-start | bytes 784900
  56.2 40.6 %copy-start.8 = (f32[1,128]{1,0:T(1,128)S(1)}, f32[1,128]{1,0:T(1,128)}, u32[]{:S(2)}) copy-start(f32[1,128]{1,0:T(1,128)} %slice.1083) | copy-start | bytes 1540
  56.6 40.5 %slice-start = ((f32[1024,128]{1,0:T(8,128)}), f32[1,128]{1,0:T(1,128)S(1)}, s32[]{:S(2)}) async-start(f32[1024,128]{1,0:T(8,128)} %copy-done.1), calls=%async_computation.7 | async-start | bytes 1024 | tf_op jit(solution)/shard_map/slice | solution.py:155
  97.8 39.9 %all-to-all-start = ((f32[16,2,128]{2,1,0:T(2,128)}), f32[16,2,128]{2,1,0:T(2,128)}, u32[]{:S(2)}, u32[]{:S(2)}) async-start(f32[16,2,128]{2,1,0:T(2,128)} %broadcast_in_dim.59), calls=%async_computation | async-start | bytes 32768 | tf_op jit(solution)/shard_map/all_to_all | solution.py:29
  112.8 38.5 %copy-start.7 = (pred[16]{0:T(512)(128)(4,1)S(1)}, pred[16]{0:T(512)(128)(4,1)}, u32[]{:S(2)}) copy-start(pred[16]{0:T(512)(128)(4,1)} %get-tuple-element.140) | copy-start | bytes 52
  123.1 48.0 %copy-start.6 = (s32[64,2]{0,1:T(2,128)S(1)}, s32[64,2]{0,1:T(2,128)}, u32[]{:S(2)}) copy-start(s32[64,2]{0,1:T(2,128)} %copy.35) | copy-start | bytes 1540
  123.1 48.0 %copy-start.5 = (f32[3,2048]{1,0:T(4,128)S(1)}, f32[3,2048]{1,0:T(4,128)}, u32[]{:S(2)}) copy-start(f32[3,2048]{1,0:T(4,128)} %param.28) | copy-start | bytes 73732
  138.3 13.1 %all-to-all-start.1 = ((f32[16,2,128]{2,1,0:T(2,128)}), f32[16,2,128]{2,1,0:T(2,128)S(1)}, u32[]{:S(2)}, u32[]{:S(2)}) async-start(f32[16,2,128]{2,1,0:T(2,128)} %broadcast_in_dim.63), calls=%async_computation.1 | async-start | bytes 32768 | tf_op jit(solution)/shard_map/all_to_all | solution.py:29
  159.3 23.3 %all-to-all-start.2 = ((bf16[16,64,128]{2,1,0:T(8,128)(2,1)}), bf16[16,64,128]{2,1,0:T(8,128)(2,1)S(1)}, u32[]{:S(2)}, u32[]{:S(2)}) async-start(bf16[16,64,128]{2,1,0:T(8,128)(2,1)} %bitcast.24), calls=%async_computation.2 | async-start | bytes 524288 | tf_op jit(solution)/shard_map/all_to_all | solution.py:164
  171.2 16.6 %copy-start.4 = (bf16[64,2048]{1,0:T(8,128)(2,1)S(1)}, bf16[64,2048]{1,0:T(8,128)(2,1)}, u32[]{:S(2)}) copy-start(bf16[64,2048]{1,0:T(8,128)(2,1)} %param.26) | copy-start | bytes 786436
  218.9 19.5 %all-to-all-start.4 = ((bf16[1,16,16,2048]{3,2,0,1:T(8,128)(2,1)}), bf16[1,16,16,2048]{3,2,0,1:T(8,128)(2,1)S(1)}, u32[]{:S(2)}, u32[]{:S(2)}) async-start(bf16[1,16,16,2048]{3,2,0,1:T(8,128)(2,1)} %bitcast.42), calls=%async_computation.4 | async-start | bytes 2097152 | tf_op jit(solution)/shard_map/all_to_all | solution.py:207
Sparse Core Ops, SparseCore 0:
  9.2 60.0 all-gather.2
  71.1 40.5 all-gather.4
where the time goes:
time: 249 us; the launch traced here: 247 us
  local copies, waits for them, and re-layouts  71.7 us (29%)
  other arithmetic  52.7 us (21%)
  starting transfers between devices  34.9 us (14%)
  waiting for transfers between devices  31.2 us (13%)
  matrix products  21.8 us (9%)
  blocking collectives  19.8 us (8%)
  between operations  14.9 us (6%)
    slice x74, local copies, waits for them, and re-layouts, on_device(): lax.associative_scan(pair_join, (jnp.flip(bwd_decay, 0), jnp.flip(bwd_dri...  26 us
    slice x69, local copies, waits for them, and re-layouts, on_device(): lax.associative_scan(pair_join, (fwd_decay, fwd_drive), axis=0)  21 us
    all_to_all x1, blocking collectives, on_device(): lax.all_to_all(outgoing.reshape(experts, capacity, width_model), 'sp', sp...  19.8 us
    all_to_all x1, waiting for transfers between devices, on_device(): lax.all_to_all(out_rows, 'sp', split_axis=1, concat_axis=0, tiled=True)  15 us
    all_to_all x2, starting transfers between devices, copy_for_each(): return lax.all_to_all(copies, axis, split_axis=0, concat_axis=0, tiled=True)  14.3 us
    concatenate x18, other arithmetic, on_device(): lax.associative_scan(pair_join, (jnp.flip(bwd_decay, 0), jnp.flip(bwd_dri...  12.9 us
    add x36, other arithmetic, pair_join(): later_pair[0] * earlier[1] + later_pair[1]  12.6 us
    all_to_all x1, starting transfers between devices, on_device(): lax.all_to_all(mixed, 'tp', split_axis=0, concat_axis=1, tiled=True)  11.7 us
  transfers between devices with their start and end apart: 8, of which 3 were waited for; matrix products, arithmetic and copies ran while one was open for 55% of the time, Pallas kernels for 0%

commit v1 on v0

v1 whole, which is shorter than its diff:
```python
import jax
import jax.numpy as jnp
from jax import lax
from jax.experimental import pallas as pl
from jax.experimental.pallas import tpu as pltpu
from jax.sharding import PartitionSpec as P

EPSILON = 1e-06
F32 = jnp.float32
BF16 = jnp.bfloat16
SEGS = 8
VMEM = pltpu.MemorySpace.VMEM


def whole():
    return pl.BlockSpec(memory_space=VMEM)


def params(mib):
    return pltpu.CompilerParams(vmem_limit_bytes=mib * 1024 * 1024)


def one_minus_square(log_decay, decay):
    y = 2.0 * log_decay
    series = 1.0 + y * (1.0 / 7.0)
    for k in (6.0, 5.0, 4.0, 3.0, 2.0):
        series = 1.0 + y * (1.0 / k) * series
    return jnp.where(y > -0.5, -y * series, 1.0 - decay * decay)


def softplus_of(x):
    u = jnp.exp(-jnp.abs(x))
    z = u / (2.0 + u)
    z2 = z * z
    series = jnp.full_like(z, 1.0 / 17.0)
    for k in (15.0, 13.0, 11.0, 9.0, 7.0, 5.0, 3.0, 1.0):
        series = 1.0 / k + z2 * series
    return jnp.maximum(x, 0.0) + 2.0 * z * series


def scan_kernel(
    mix, before, after, conv_w, conv_b, decay_param, recur_gate, recur_bias, input_gate, input_bias,
    h_f, p_f, h_b, p_b, seg, total,
    padded, conv, split, wide, wlow, pre, a_f, b_f, a_b, b_b,
):
    length = mix.shape[0]
    step = length // SEGS
    stride = step + 8
    padded[0:8, :] = jnp.zeros((8, 128), F32)
    padded[6:8, :] = before[...].astype(F32)
    padded[8 : 8 + length, :] = mix[...].astype(F32)
    padded[8 + length : 16 + length, :] = jnp.zeros((8, 128), F32)
    padded[8 + length : 10 + length, :] = after[...].astype(F32)
    zero = jnp.zeros((64, 64), F32)
    columns = []
    for sense in range(2):
        for gate in (recur_gate, input_gate):
            columns.append(
                jnp.concatenate(
                    [
                        jnp.concatenate([gate[sense, 0], zero], axis=1),
                        jnp.concatenate([zero, gate[sense, 1]], axis=1),
                    ],
                    axis=0,
                )
            )
    maps = jnp.concatenate(columns, axis=1)
    high = maps.astype(BF16)
    wide[0:128, :] = high
    wide[128:256, :] = high
    wlow[...] = (maps - high.astype(F32)).astype(BF16)

    rows = 64

    def convolve(k, carry):
        at = pl.multiple_of(k * rows, rows)
        out = conv_b[...] + padded[pl.ds(at + 6, rows), :] * conv_w[0:1, :]
        for tap in range(1, 4):
            out = out + padded[pl.ds(at + 6 + tap, rows), :] * conv_w[tap : tap + 1, :]
        conv[pl.ds(at, rows), :] = out
        top = out.astype(BF16)
        split[pl.ds(at, rows), 0:128] = top
        split[pl.ds(at, rows), 128:256] = (out - top.astype(F32)).astype(BF16)
        return carry

    lax.fori_loop(0, length // rows, convolve, 0)
    pre[...] = jnp.dot(split[...], wide[...], preferred_element_type=F32) + jnp.dot(
        split[:, 0:128], wlow[...], preferred_element_type=F32
    )
    rate = -8.0 * softplus_of(-decay_param[...])

    per = step // rows

    def gates(k, carry):
        at = pl.multiple_of(k * rows, rows)
        to = pl.multiple_of((k // per) * stride + (k % per) * rows, 8)
        signal = conv[pl.ds(at, rows), :]
        for sense, (a_ref, b_ref) in enumerate(((a_f, b_f), (a_b, b_b))):
            base = sense * 256
            recur = jax.nn.sigmoid(pre[pl.ds(at, rows), base : base + 128] + recur_bias[sense : sense + 1, :])
            inner = jax.nn.sigmoid(pre[pl.ds(at, rows), base + 128 : base + 256] + input_bias[sense : sense + 1, :])
            log_decay = recur * rate[sense : sense + 1, :]
            decay = jnp.exp(log_decay)
            a_ref[pl.ds(to, rows), :] = decay
            b_ref[pl.ds(to, rows), :] = jnp.sqrt(one_minus_square(log_decay, decay)) * (inner * signal)
        return carry

    lax.fori_loop(0, length // rows, gates, 0)

    def advance(t, carry):
        hf, pf, hb, pb = carry
        back = step - 1 - t
        af = a_f[pl.ds(t, SEGS, stride=stride), :]
        bf = b_f[pl.ds(t, SEGS, stride=stride), :]
        ab = a_b[pl.ds(back, SEGS, stride=stride), :]
        bb = b_b[pl.ds(back, SEGS, stride=stride), :]
        hf = af * hf + bf
        pf = pf * af
        hb = ab * hb + bb
        pb = pb * ab
        here = pl.multiple_of(t * SEGS, SEGS)
        there = pl.multiple_of(back * SEGS, SEGS)
        h_f[pl.ds(here, SEGS), :] = hf
        p_f[pl.ds(here, SEGS), :] = pf
        h_b[pl.ds(there, SEGS), :] = hb
        p_b[pl.ds(there, SEGS), :] = pb
        return hf, pf, hb, pb

    none = jnp.zeros((SEGS, 128), F32)
    ones = jnp.ones((SEGS, 128), F32)
    hf, pf, hb, pb = lax.fori_loop(0, step, advance, (none, ones, none, ones), unroll=8)

    sums = []
    for base, h, p, order in ((0, hf, pf, range(SEGS)), (16, hb, pb, reversed(range(SEGS)))):
        enter = jnp.zeros((1, 128), F32)
        factor = jnp.ones((1, 128), F32)
        for s in order:
            seg[base + s : base + s + 1, :] = enter
            seg[base + 8 + s : base + 9 + s, :] = factor
            enter = p[s : s + 1, :] * enter + h[s : s + 1, :]
            factor = p[s : s + 1, :] * factor
        sums += [factor, enter]
    both = jnp.concatenate(sums + [jnp.zeros((4, 128), F32)], axis=0)
    total[...] = jnp.broadcast_to(both[None], total.shape)


def mix_kernel(h_f, p_f, h_b, p_b, seg, totals, gate_in, out, natural):
    length = out.shape[0]
    step = length // SEGS
    stride = step + 8
    count = totals.shape[0]
    here = lax.axis_index("sp")
    enter_f = jnp.zeros((1, 128), F32)
    enter_b = jnp.zeros((1, 128), F32)
    for j in range(count):
        enter_f = jnp.where(j < here, totals[j, 0:1, :] * enter_f + totals[j, 1:2, :], enter_f)
        k = count - 1 - j
        enter_b = jnp.where(k > here, totals[k, 2:3, :] * enter_b + totals[k, 3:4, :], enter_b)
    into_f = seg[0:8, :] + seg[8:16, :] * enter_f
    into_b = seg[16:24, :] + seg[24:32, :] * enter_b

    def place(t, carry):
        at = pl.multiple_of(t * SEGS, SEGS)
        rows = pl.ds(at, SEGS)
        natural[pl.ds(t, SEGS, stride=stride), :] = (
            h_f[rows, :] + p_f[rows, :] * into_f + (h_b[rows, :] + p_b[rows, :] * into_b)
        )
        return carry

    lax.fori_loop(0, step, place, 0, unroll=8)
    for s in range(SEGS):
        gate = gate_in[s * step : (s + 1) * step, :].astype(F32)
        out[s * step : (s + 1) * step, :] = (
            natural[s * stride : s * stride + step, :] * jax.nn.gelu(gate)
        ).astype(BF16)


def scaled(values, gain):
    return values * lax.rsqrt(jnp.mean(values * values, axis=-1, keepdims=True) + EPSILON) * gain


def proj_kernel(mixed, weights, residual, gain, routes, stream_out, outgoing, acc):
    k = pl.program_id(0)

    @pl.when(k == 0)
    def _():
        acc[...] = jnp.zeros_like(acc)

    lanes = jnp.concatenate([mixed[j] for j in range(mixed.shape[0])], axis=1)
    acc[...] += jnp.dot(lanes, weights[...], preferred_element_type=F32)

    @pl.when(k == pl.num_programs(0) - 1)
    def _():
        proj = acc[...].astype(BF16).astype(F32)
        stream = (residual[...].astype(F32) + scaled(proj, gain[0:1, :])).astype(BF16)
        stream_out[...] = stream
        normed = scaled(stream.astype(F32), gain[1:2, :]).astype(BF16)
        rows = normed.shape[0]
        slots = outgoing.shape[0]
        experts = 16
        capacity = slots // experts
        first, second = routes[0:1, :], routes[1:2, :]
        ids = lax.broadcasted_iota(jnp.int32, (experts, rows), 0)
        hit0 = (ids == first).astype(F32)
        hit1 = (ids == second).astype(F32)
        r = lax.broadcasted_iota(jnp.int32, (rows, rows), 0)
        c = lax.broadcasted_iota(jnp.int32, (rows, rows), 1)
        earlier = jnp.dot((hit0 + hit1).astype(BF16), (r < c).astype(BF16), preferred_element_type=F32)
        slot0 = first * capacity + jnp.sum(hit0 * earlier, axis=0, keepdims=True).astype(jnp.int32)
        slot1 = second * capacity + jnp.sum(hit1 * earlier, axis=0, keepdims=True).astype(jnp.int32)
        places = lax.broadcasted_iota(jnp.int32, (slots, rows), 0)
        pick = jnp.where(jnp.logical_or(places == slot0, places == slot1), 1.0, 0.0).astype(BF16)
        outgoing[...] = jnp.dot(pick, normed, preferred_element_type=F32).astype(BF16)


def pack_kernel(gate, up, down, out):
    d = gate.shape[1]
    ff = down.shape[1]
    out[0:d, :] = jnp.concatenate([gate[0], up[0]], axis=1)
    for c in range(down.shape[2] // 128):
        out[d + c * ff : d + (c + 1) * ff, :] = down[0, :, c * 128 : (c + 1) * 128]


def expert_kernel(tokens, packed, out, acc):
    k = pl.program_id(0)
    width = tokens.shape[1]

    @pl.when(k == 0)
    def _():
        acc[...] = jnp.zeros_like(acc)

    x = tokens[...]
    rows = x.shape[0]
    low = lax.broadcasted_iota(jnp.int32, (rows, 128), 1) < 64
    hidden = []
    for pair in range(2):
        both = jnp.concatenate([packed[2 * pair, 0:width, :], packed[2 * pair + 1, 0:width, :]], axis=1)
        z = jnp.dot(x, both, preferred_element_type=F32)
        even, odd = z[:, 0:128], z[:, 128:256]
        gate = jnp.where(low, even, pltpu.roll(odd, 64, 1))
        up = jnp.where(low, pltpu.roll(even, 64, 1), odd)
        hidden.append((jax.nn.silu(gate) * up).astype(BF16))
    hid = jnp.concatenate(hidden, axis=1)
    for c in range(width // 256):
        cols = []
        for half in range(2):
            at = width + (2 * c + half) * 64
            cols.append(jnp.concatenate([packed[p, at : at + 64, :] for p in range(4)], axis=0))
        acc[:, c * 256 : (c + 1) * 256] += jnp.dot(
            hid, jnp.concatenate(cols, axis=1), preferred_element_type=F32
        )

    @pl.when(k == pl.num_programs(0) - 1)
    def _():
        out[...] = acc[...].astype(BF16)


def combine_kernel(values, stream, gain, routes, weights, out):
    rows = stream.shape[0]
    slots = values.shape[0]
    experts = 16
    capacity = slots // experts
    first, second = routes[:, 0:1], routes[:, 1:2]
    ids = lax.broadcasted_iota(jnp.int32, (rows, experts), 1)
    hit0 = (ids == first).astype(F32)
    hit1 = (ids == second).astype(F32)
    r = lax.broadcasted_iota(jnp.int32, (rows, rows), 0)
    c = lax.broadcasted_iota(jnp.int32, (rows, rows), 1)
    earlier = jnp.dot((c < r).astype(BF16), (hit0 + hit1).astype(BF16), preferred_element_type=F32)
    slot0 = first * capacity + jnp.sum(hit0 * earlier, axis=1, keepdims=True).astype(jnp.int32)
    slot1 = second * capacity + jnp.sum(hit1 * earlier, axis=1, keepdims=True).astype(jnp.int32)
    places = lax.broadcasted_iota(jnp.int32, (rows, slots), 1)
    table = jnp.where(places == slot0, weights[:, 0:1], 0.0) + jnp.where(
        places == slot1, weights[:, 1:2], 0.0
    )
    high = table.astype(BF16)
    rest = table - high.astype(F32)
    mid = rest.astype(BF16)
    low = (rest - mid.astype(F32)).astype(BF16)
    parts = jnp.dot(jnp.concatenate([high, mid, low], axis=0), values[...], preferred_element_type=F32)
    mixture = parts[0:rows] + (parts[rows : 2 * rows] + parts[2 * rows : 3 * rows])
    mixture = mixture.astype(BF16).astype(F32)
    out[...] = (stream[...].astype(F32) + scaled(mixture, gain[2:3, :])).astype(BF16)


def shape(dims, dtype):
    return jax.ShapeDtypeStruct(dims, dtype)


def on_device(
    mix_in,
    gate_in,
    conv_w,
    conv_b,
    decay_param,
    recur_gate,
    recur_bias,
    input_gate,
    input_bias,
    residual,
    out_proj,
    norm_gain,
    routes,
    route_wt,
    exp_gate,
    exp_up,
    exp_down,
):
    length, channels = mix_in.shape
    rows, width = residual.shape
    sp = lax.axis_size("sp")
    tp = lax.axis_size("tp")
    ff_own = exp_down.shape[1]
    packed_rows = width + ff_own * width // 128
    packed = pl.pallas_call(
        pack_kernel,
        out_shape=shape((packed_rows, 128), BF16),
        in_specs=[whole()] * 3,
        out_specs=whole(),
        compiler_params=params(8),
        name="pack",
    )(exp_gate, exp_up, exp_down)
    gathered = lax.all_gather(packed, "tp", axis=0, tiled=False)

    ends = sp - 1
    before = lax.ppermute(mix_in[length - 2 :], "sp", [(i, i + 1) for i in range(ends)])
    after = lax.ppermute(mix_in[:2], "sp", [(i + 1, i) for i in range(ends)])
    step = length // SEGS
    lines = SEGS * (step + 8)
    state = shape((length, channels), F32)
    h_f, p_f, h_b, p_b, seg, total = pl.pallas_call(
        scan_kernel,
        out_shape=(state, state, state, state, shape((32, 128), F32), shape((sp, 8, 128), F32)),
        in_specs=[whole()] * 10,
        out_specs=(whole(),) * 6,
        scratch_shapes=[
            pltpu.VMEM((length + 16, 128), F32),
            pltpu.VMEM((length, 128), F32),
            pltpu.VMEM((length, 256), BF16),
            pltpu.VMEM((256, 512), BF16),
            pltpu.VMEM((128, 512), BF16),
            pltpu.VMEM((length, 512), F32),
            pltpu.VMEM((lines, 128), F32),
            pltpu.VMEM((lines, 128), F32),
            pltpu.VMEM((lines, 128), F32),
            pltpu.VMEM((lines, 128), F32),
        ],
        compiler_params=params(20),
        name="scan",
    )(mix_in, before, after, conv_w, conv_b[None], decay_param, recur_gate, recur_bias, input_gate, input_bias)
    totals = lax.all_to_all(total, "sp", split_axis=0, concat_axis=0, tiled=True)
    mixed = pl.pallas_call(
        mix_kernel,
        out_shape=shape((length, channels), BF16),
        in_specs=[whole()] * 7,
        out_specs=whole(),
        scratch_shapes=[pltpu.VMEM((lines, 128), F32)],
        compiler_params=params(12),
        name="mix",
    )(h_f, p_f, h_b, p_b, seg, totals, gate_in)
    token_rows = lax.all_to_all(
        mixed.reshape(tp, rows, channels), "tp", split_axis=0, concat_axis=0, tiled=True
    )
    own = lax.axis_index("tp") * rows
    own_routes = lax.dynamic_slice_in_dim(routes, own, rows, 0)
    own_weights = lax.dynamic_slice_in_dim(route_wt, own, rows, 0)
    slots = 2 * rows * routes.shape[1]
    block = 256
    fixed = lambda *dims: pl.BlockSpec(dims, lambda k: (0,) * len(dims))
    stream, outgoing = pl.pallas_call(
        proj_kernel,
        grid=(width // block,),
        out_shape=(shape((rows, width), BF16), shape((slots, width), BF16)),
        in_specs=[
            pl.BlockSpec((block // channels, rows, channels), lambda k: (k, 0, 0)),
            pl.BlockSpec((block, width), lambda k: (k, 0)),
            fixed(rows, width),
            fixed(*norm_gain.shape),
            fixed(routes.shape[1], rows),
        ],
        out_specs=(fixed(rows, width), fixed(slots, width)),
        scratch_shapes=[pltpu.VMEM((rows, width), F32)],
        compiler_params=params(16),
        name="proj",
    )(token_rows, out_proj, residual, norm_gain, own_routes.T)
    arrived = lax.all_to_all(
        outgoing.reshape(sp, slots // sp, width), "sp", split_axis=0, concat_axis=0, tiled=True
    )
    done = pl.pallas_call(
        expert_kernel,
        grid=(tp // 4,),
        out_shape=shape((slots, width), BF16),
        in_specs=[
            fixed(slots, width),
            pl.BlockSpec((4, packed_rows, 128), lambda k: (k, 0, 0)),
        ],
        out_specs=fixed(slots, width),
        scratch_shapes=[pltpu.VMEM((slots, width), F32)],
        compiler_params=params(32),
        name="experts",
    )(arrived.reshape(slots, width), gathered)
    returned = lax.all_to_all(
        done.reshape(sp, slots // sp, width), "sp", split_axis=0, concat_axis=0, tiled=True
    )
    return pl.pallas_call(
        combine_kernel,
        out_shape=shape((rows, width), BF16),
        in_specs=[whole()] * 5,
        out_specs=whole(),
        compiler_params=params(16),
        name="combine",
    )(returned.reshape(slots, width), stream, norm_gain, own_routes, own_weights)


def solution(mesh):
    return jax.shard_map(
        on_device,
        mesh=mesh,
        in_specs=(
            P("sp", "tp"),
            P("sp", "tp"),
            P(None, "tp"),
            P("tp"),
            P(None, "tp"),
            P(None, "tp", None, None),
            P(None, "tp"),
            P(None, "tp", None, None),
            P(None, "tp"),
            P(("sp", "tp"), None),
            P(),
            P(),
            P("sp", None),
            P("sp", None),
            P("sp", None, "tp"),
            P("sp", None, "tp"),
            P("sp", "tp", None),
        ),
        out_specs=P(("sp", "tp"), None),
        check_vma=False,
    )
```

time: 249 us -> 140 us (0.56)
  other arithmetic: 52.7 us -> 0 us
  local copies, waits for them, and re-layouts: 71.7 us -> 22.1 us
  matrix products: 21.8 us -> 0 us
  Pallas kernels: 0 us -> 16.6 us
  blocking collectives: 19.8 us -> 34.4 us
  starting transfers between devices: 34.9 us -> 20.9 us
    slice x175 -> x1, local copies, waits for them, and re-layouts: 49.1 us -> 0.71 us  [on_device(): after = lax.ppermute(mix_in[:2], 'sp', [(i + 1, i) for i in range(ends)])]
    concatenate x39 -> x0, other arithmetic: 25.4 us -> none  [the longest x18 12.9 us: on_device(): lax.associative_scan(pair_join, (jnp.flip(bwd_decay, 0), jnp.flip(bwd_dri...]
    dot_general x9 -> x0, matrix products: 21.8 us -> none  [the longest x1 6.93 us: on_device(): jnp.einsum('emf,efd->emd', hidden, lax.all_gather(exp_down, 'tp', axis=1,...]
    unnamed x19 -> x36, local copies, waits for them, and re-layouts: 0.29 us -> 20.5 us
    add x79 -> x0, other arithmetic: 19.5 us -> none  [the longest x36 12.6 us: pair_join(): later_pair[0] * earlier[1] + later_pair[1]]
    pallas_call x0 -> x6, Pallas kernels: none -> 16.6 us  [the longest x1 6.07 us: on_device(): pl.pallas_call(expert_kernel, grid=(tp // 4,), out_shape=shape((slots, wi...]
    all_to_all x1 -> x2, blocking collectives: 19.8 us -> 34.4 us  [the longest x1 19.7 us: on_device(): lax.all_to_all(outgoing.reshape(sp, slots // sp, width), 'sp', split_axis...]
    all_to_all x4 -> x2, starting transfers between devices: 29.6 us -> 15.7 us  [the longest x1 12 us: on_device(): lax.all_to_all(mixed.reshape(tp, rows, channels), 'tp', split_axis=0, con...]
  transfers between devices with their start and end apart: 8 -> 5, of which waited for: 3 -> 3; matrix products, arithmetic and copies ran while one was open for 55% -> 1% of each run, Pallas kernels for 0% -> 6%
where the time goes in v1:
time: 140 us
  blocking collectives  34.4 us (25%)
  waiting for transfers between devices  32.1 us (23%)
  local copies, waits for them, and re-layouts  22.1 us (16%)
  starting transfers between devices  20.9 us (15%)
  Pallas kernels  16.6 us (12%)
  between operations  13.5 us (10%)
    unnamed x36, local copies, waits for them, and re-layouts  20.5 us
    all_to_all x1, blocking collectives, on_device(): lax.all_to_all(outgoing.reshape(sp, slots // sp, width), 'sp', split_axis...  19.7 us
    all_to_all x1, waiting for transfers between devices, on_device(): lax.all_to_all(done.reshape(sp, slots // sp, width), 'sp', split_axis=0,...  14.7 us
    all_to_all x1, blocking collectives, on_device(): lax.all_to_all(total, 'sp', split_axis=0, concat_axis=0, tiled=True)  14.6 us
    all_to_all x1, waiting for transfers between devices, on_device(): lax.all_to_all(mixed.reshape(tp, rows, channels), 'tp', split_axis=0, con...  14.3 us
    all_to_all x1, starting transfers between devices, on_device(): lax.all_to_all(mixed.reshape(tp, rows, channels), 'tp', split_axis=0, con...  12 us
    pallas_call x1, Pallas kernels, on_device(): pl.pallas_call(expert_kernel, grid=(tp // 4,), out_shape=shape((slots, wi...  6.07 us
    ppermute x1, starting transfers between devices, on_device(): lax.ppermute(mix_in[length - 2:], 'sp', [(i, i + 1) for i in range(ends)])  3.92 us
  transfers between devices with their start and end apart: 5, of which 3 were waited for; matrix products, arithmetic and copies ran while one was open for 1% of the time, Pallas kernels for 6%

profile of v1, /device:TPU:1, one launch (start us, length us, event | category | flops | bytes accessed | tf_op | source)
XLA Modules:
  0.0 139.5 jit_solution(11413074216715186306)
XLA Ops:
  6.5 1.2 copy.20.gate
  7.8 1.2 copy.21.up
  9.0 0.9 copy-done.5
  10.0 1.2 pack.1
  11.9 3.9 %collective-permute-start = (bf16[2,128]{1,0:T(2,128)(2,1)S(1)}, bf16[2,128]{1,0:T(2,128)(2,1)S(1)}, u32[]{:S(2)}, u32[]{:S(2)}) collective-permute-start(bf16[2,128]{1,0:T(2,128)(2,1)S(1)} %get-tuple-element.22), channel_id=1, source_target_pairs={{0,16},{16,32},{32,48},{48,64},{64,80},{80,96},{96,112},{112,128},... | collective-permute-start | bytes 1544 | tf_op jit(solution)/shard_map/ppermute | solution.py:326
  15.8 1.3 collective-permute-start.1
  17.1 3.0 %collective-permute-done.1.after = bf16[2,128]{1,0:T(2,128)(2,1)S(1)} collective-permute-done((bf16[2,128]{1,0:T(2,128)(2,1)S(1)}, bf16[2,128]{1,0:T(2,128)(2,1)S(1)}, u32[]{:S(2)}, u32[]{:S(2)}) %collective-permute-start.1) | collective-permute-done | bytes 544 | tf_op jit(solution)/shard_map/ppermute | solution.py:327
  20.1 0.9 copy-done.3
  21.1 0.9 copy-done.9
  26.3 3.3 %scan.1 = (f32[1024,128]{1,0:T(8,128)S(1)}, f32[1024,128]{1,0:T(8,128)S(1)}, f32[1024,128]{1,0:T(8,128)S(1)}, f32[1024,128]{1,0:T(8,128)S(1)}, f32[32,128]{1,0:T(8,128)S(1)}, /*index=5*/f32[16,8,128]{2,1,0:T(8,128)S(1)}) custom-call(bf16[1024,128]{1,0:T(8,128)(2,1)S(1)} %copy-done.3, bf16[2,128]{1,0:T(2,128)(2,1)S(1)} %collective-permute-done.before, ...), custom_call_target="tpu_custom_call" | custom-call | tf_op jit(solution)/shard_map/scan/pallas_call | solution.py:331
  29.6 14.6 %all_to_all.20.totals = f32[16,8,128]{2,1,0:T(8,128)S(1)} all-to-all(f32[16,8,128]{2,1,0:T(8,128)S(1)} %get-tuple-element.18), channel_id=1, replica_groups=mesh['sp'=16,'tp'=16] {'sp'}, dimensions={0} | all-to-all | bytes 131072 | tf_op jit(solution)/shard_map/all_to_all | solution.py:351
  44.2 0.9 copy-done.6
  45.1 1.2 mix.3
  46.3 12.0 %all-to-all-start.1 = ((bf16[16,64,128]{2,1,0:T(8,128)(2,1)}), bf16[16,64,128]{2,1,0:T(8,128)(2,1)S(1)}, u32[]{:S(2)}, u32[]{:S(2)}) async-start(bf16[16,64,128]{2,1,0:T(8,128)(2,1)} %bitcast.1), calls=%async_computation.1 | async-start | bytes 524288 | tf_op jit(solution)/shard_map/all_to_all | solution.py:361
  58.6 14.3 %all-to-all-done.1.mixed = bf16[16,64,128]{2,1,0:T(8,128)(2,1)S(1)} async-done(((bf16[16,64,128]{2,1,0:T(8,128)(2,1)}), bf16[16,64,128]{2,1,0:T(8,128)(2,1)S(1)}, u32[]{:S(2)}, u32[]{:S(2)}) %all-to-all-start.1) | async-done | bytes 262176 | tf_op jit(solution)/shard_map/all_to_all | solution.py:361
  72.9 3.5 %copy-done.2 = bf16[2048,2048]{1,0:T(8,128)(2,1)S(1)} copy-done((bf16[2048,2048]{1,0:T(8,128)(2,1)S(1)}, bf16[2048,2048]{1,0:T(8,128)(2,1)}, u32[]{:S(2)}) %copy-start.2) | copy-done | bytes 8388632
  76.4 1.0 copy-done.4
  78.2 3.3 %proj.1 = (bf16[64,2048]{1,0:T(8,128)(2,1)S(1)}, bf16[256,2048]{1,0:T(8,128)(2,1)S(1)}) custom-call(bf16[16,64,128]{2,1,0:T(8,128)(2,1)S(1)} %all-to-all-done.1.mixed, bf16[2048,2048]{1,0:T(8,128)(2,1)S(1)} %copy-done.2, bf16[64,2048]{1,0:T(8,128)(2,1)S(1)} %copy-done.4, f32[3,2048]{1,0:T(4,128)S(1)} %copy-done.7, s32[2,64]{1,0:T(2,128)S(1)} %copy.19.routes), custom_call_target="tpu_custom_call" | custom-call | tf_op jit(solution)/shard_map/proj/pallas_call | solution.py:370
  81.4 19.7 %all_to_all.21 = bf16[16,16,2048]{2,1,0:T(8,128)(2,1)S(1)} all-to-all(bf16[16,16,2048]{2,1,0:T(8,128)(2,1)S(1)} %bitcast.11), channel_id=1, replica_groups=mesh['sp'=16,'tp'=16] {'sp'}, dimensions={0} | all-to-all | bytes 2097152 | tf_op jit(solution)/shard_map/all_to_all | solution.py:386
  101.2 4.6 %copy-done.1 = bf16[49152,128]{1,0:T(8,128)(2,1)S(1)} copy-done((bf16[49152,128]{1,0:T(8,128)(2,1)S(1)}, bf16[49152,128]{1,0:T(8,128)(2,1)}, u32[]{:S(2)}) %copy-start.1) | copy-done | bytes 12582936
  105.7 6.1 %experts.1 = bf16[256,2048]{1,0:T(8,128)(2,1)} custom-call(bf16[256,2048]{1,0:T(8,128)(2,1)S(1)} %bitcast.9, bf16[16,3072,128]{2,1,0:T(8,128)(2,1)S(1)} %bitcast.8), custom_call_target="tpu_custom_call" | custom-call | tf_op jit(solution)/shard_map/experts/pallas_call | solution.py:389
  111.8 3.7 %all-to-all-start.3 = ((bf16[16,16,2048]{2,1,0:T(8,128)(2,1)}), bf16[16,16,2048]{2,1,0:T(8,128)(2,1)S(1)}, u32[]{:S(2)}, u32[]{:S(2)}) async-start(bf16[16,16,2048]{2,1,0:T(8,128)(2,1)} %bitcast.6), calls=%async_computation.3 | async-start | bytes 2097152 | tf_op jit(solution)/shard_map/all_to_all | solution.py:402
  116.3 14.7 %all-to-all-done.3 = bf16[16,16,2048]{2,1,0:T(8,128)(2,1)S(1)} async-done(((bf16[16,16,2048]{2,1,0:T(8,128)(2,1)}), bf16[16,16,2048]{2,1,0:T(8,128)(2,1)S(1)}, u32[]{:S(2)}, u32[]{:S(2)}) %all-to-all-start.3) | async-done | bytes 1048608 | tf_op jit(solution)/shard_map/all_to_all | solution.py:402
  131.1 1.6 %combine.1 = bf16[64,2048]{1,0:T(8,128)(2,1)} custom-call(bf16[256,2048]{1,0:T(8,128)(2,1)S(1)} %bitcast.10, bf16[64,2048]{1,0:T(8,128)(2,1)S(1)} %get-tuple-element.20.stream, f32[3,2048]{1,0:T(4,128)S(1)} %copy-done.8, s32[64,2]{1,0:T(8,128)S(1)} %copy.23.routes, f32[64,2]{1,0:T(8,128)S(1)} %copy.24.weights), custom_call_target="tpu_custom_call" | custom-call | tf_op jit(solution)/shard_map/combine/pallas_call | solution.py:405
  (35 shorter events, 6.9 us)
Async XLA Ops:
  6.5 51.8 %copy-start = (s32[1024,2]{0,1:T(2,128)S(1)}, s32[1024,2]{0,1:T(2,128)}, u32[]{:S(2)}) copy-start(s32[1024,2]{0,1:T(2,128)} %param.29) | copy-start | bytes 24580
  6.5 94.6 %all-gather.3.cloned.1.call-start = ((), (), s32[]{:S(2)}) async-start(), calls=%async_computation.4 | async-start | bytes 13369344 | tf_op jit(solution)/shard_map/all_gather | solution.py:323
  9.0 1.0 copy-start.5
  11.9 5.2 %collective-permute-start = (bf16[2,128]{1,0:T(2,128)(2,1)S(1)}, bf16[2,128]{1,0:T(2,128)(2,1)S(1)}, u32[]{:S(2)}, u32[]{:S(2)}) collective-permute-start(bf16[2,128]{1,0:T(2,128)(2,1)S(1)} %get-tuple-element.22), channel_id=1, source_target_pairs={{0,16},{16,32},{32,48},{48,64},{64,80},{80,96},{96,112},{112,128},... | collective-permute-start | bytes 1544 | tf_op jit(solution)/shard_map/ppermute | solution.py:326
  15.8 4.3 %collective-permute-start.1 = (bf16[2,128]{1,0:T(2,128)(2,1)S(1)}, bf16[2,128]{1,0:T(2,128)(2,1)S(1)}, u32[]{:S(2)}, u32[]{:S(2)}) collective-permute-start(bf16[2,128]{1,0:T(2,128)(2,1)S(1)} %get-tuple-element.21), channel_id=1, source_target_pairs={{16,0},{32,16},{48,32},{64,48},{80,64},{96,80},{112,96},{128,112},... | collective-permute-start | bytes 1544 | tf_op jit(solution)/shard_map/ppermute | solution.py:327
  20.1 1.0 copy-start.3
  21.1 0.9 copy-start.9
  22.0 0.9 copy-start.10
  22.9 0.7 copy-start.11
  23.6 0.7 copy-start.12
  24.2 0.7 copy-start.13
  24.9 0.7 copy-start.14
  25.6 0.7 copy-start.15
  44.2 1.0 copy-start.6
  46.3 26.6 %all-to-all-start.1 = ((bf16[16,64,128]{2,1,0:T(8,128)(2,1)}), bf16[16,64,128]{2,1,0:T(8,128)(2,1)S(1)}, u32[]{:S(2)}, u32[]{:S(2)}) async-start(bf16[16,64,128]{2,1,0:T(8,128)(2,1)} %bitcast.1), calls=%async_computation.1 | async-start | bytes 524288 | tf_op jit(solution)/shard_map/all_to_all | solution.py:361
  72.9 3.5 %copy-start.2 = (bf16[2048,2048]{1,0:T(8,128)(2,1)S(1)}, bf16[2048,2048]{1,0:T(8,128)(2,1)}, u32[]{:S(2)}) copy-start(bf16[2048,2048]{1,0:T(8,128)(2,1)} %weights.1) | copy-start | bytes 25165828
  76.4 1.0 copy-start.4
  77.4 0.8 copy-start.7
  78.2 52.9 %copy-start.8 = (f32[3,2048]{1,0:T(4,128)S(1)}, f32[3,2048]{1,0:T(4,128)}, u32[]{:S(2)}) copy-start(f32[3,2048]{1,0:T(4,128)} %gain.3) | copy-start | bytes 73732
  101.2 4.6 %copy-start.1 = (bf16[49152,128]{1,0:T(8,128)(2,1)S(1)}, bf16[49152,128]{1,0:T(8,128)(2,1)}, u32[]{:S(2)}) copy-start(bf16[49152,128]{1,0:T(8,128)(2,1)} %all-gather.3.cloned.1.call-done) | copy-start | bytes 37748740
  111.8 19.3 %all-to-all-start.3 = ((bf16[16,16,2048]{2,1,0:T(8,128)(2,1)}), bf16[16,16,2048]{2,1,0:T(8,128)(2,1)S(1)}, u32[]{:S(2)}, u32[]{:S(2)}) async-start(bf16[16,16,2048]{2,1,0:T(8,128)(2,1)} %bitcast.6), calls=%async_computation.3 | async-start | bytes 2097152 | tf_op jit(solution)/shard_map/all_to_all | solution.py:402
Sparse Core Ops, SparseCore 0:
  11.3 85.3 all-gather.2

commit v2 on v1

--- a/solution.py
+++ b/solution.py
@@ -18,6 +18,17 @@
 
 def params(mib):
     return pltpu.CompilerParams(vmem_limit_bytes=mib * 1024 * 1024)
+
+
+def anywhere():
+    return pl.BlockSpec(memory_space=pl.ANY)
+
+
+def fetched(sources, buffers, sems, first=0):
+    copies = [pltpu.make_async_copy(src, dst, sems.at[first + k]) for k, (src, dst) in enumerate(zip(sources, buffers))]
+    for copy in copies:
+        copy.start()
+    return copies
 
 
 def one_minus_square(log_decay, decay):
@@ -39,10 +50,17 @@
 
 
 def scan_kernel(
-    mix, before, after, conv_w, conv_b, decay_param, recur_gate, recur_bias, input_gate, input_bias,
+    mix_h, before, after, conv_w_h, conv_b_h, decay_param_h, recur_gate_h, recur_bias_h, input_gate_h, input_bias_h,
     h_f, p_f, h_b, p_b, seg, total,
     padded, conv, split, wide, wlow, pre, a_f, b_f, a_b, b_b,
+    mix, conv_w, conv_b, decay_param, recur_gate, recur_bias, input_gate, input_bias, sems,
 ):
+    for copy in fetched(
+        (mix_h, conv_w_h, conv_b_h, decay_param_h, recur_gate_h, recur_bias_h, input_gate_h, input_bias_h),
+        (mix, conv_w, conv_b, decay_param, recur_gate, recur_bias, input_gate, input_bias),
+        sems,
+    ):
+        copy.wait()
     length = mix.shape[0]
     step = length // SEGS
     stride = step + 8
@@ -144,7 +162,8 @@
     total[...] = jnp.broadcast_to(both[None], total.shape)
 
 
-def mix_kernel(h_f, p_f, h_b, p_b, seg, totals, gate_in, out, natural):
+def mix_kernel(h_f, p_f, h_b, p_b, seg, totals, gate_h, out, natural, gate_in, sems):
+    (copy,) = fetched((gate_h,), (gate_in,), sems)
     length = out.shape[0]
     step = length // SEGS
     stride = step + 8
@@ -168,6 +187,7 @@
         return carry
 
     lax.fori_loop(0, step, place, 0, unroll=8)
+    copy.wait()
     for s in range(SEGS):
         gate = gate_in[s * step : (s + 1) * step, :].astype(F32)
         out[s * step : (s + 1) * step, :] = (
@@ -179,19 +199,23 @@
     return values * lax.rsqrt(jnp.mean(values * values, axis=-1, keepdims=True) + EPSILON) * gain
 
 
-def proj_kernel(mixed, weights, residual, gain, routes, stream_out, outgoing, acc):
-    k = pl.program_id(0)
-
-    @pl.when(k == 0)
-    def _():
-        acc[...] = jnp.zeros_like(acc)
-
-    lanes = jnp.concatenate([mixed[j] for j in range(mixed.shape[0])], axis=1)
-    acc[...] += jnp.dot(lanes, weights[...], preferred_element_type=F32)
-
-    @pl.when(k == pl.num_programs(0) - 1)
-    def _():
-        proj = acc[...].astype(BF16).astype(F32)
+def proj_kernel(mixed, weights_h, residual_h, gain_h, routes, stream_out, outgoing, weights, residual, gain, sems):
+    width = weights.shape[0]
+    blocks = 8
+    block = width // blocks
+    parts = [(weights_h.at[pl.ds(k * block, block)], weights.at[pl.ds(k * block, block)]) for k in range(blocks)]
+    loads = fetched(*zip(*parts), sems)
+    others = fetched((residual_h, gain_h), (residual, gain), sems, blocks)
+    acc = jnp.zeros(residual.shape, F32)
+    per = mixed.shape[0] // blocks
+    for k in range(blocks):
+        lanes = jnp.concatenate([mixed[k * per + j] for j in range(per)], axis=1)
+        loads[k].wait()
+        acc = acc + jnp.dot(lanes, weights[k * block : (k + 1) * block, :], preferred_element_type=F32)
+    for copy in others:
+        copy.wait()
+    if True:
+        proj = acc.astype(BF16).astype(F32)
         stream = (residual[...].astype(F32) + scaled(proj, gain[0:1, :])).astype(BF16)
         stream_out[...] = stream
         normed = scaled(stream.astype(F32), gain[1:2, :]).astype(BF16)
@@ -213,46 +237,51 @@
         outgoing[...] = jnp.dot(pick, normed, preferred_element_type=F32).astype(BF16)
 
 
-def pack_kernel(gate, up, down, out):
-    d = gate.shape[1]
-    ff = down.shape[1]
-    out[0:d, :] = jnp.concatenate([gate[0], up[0]], axis=1)
-    for c in range(down.shape[2] // 128):
-        out[d + c * ff : d + (c + 1) * ff, :] = down[0, :, c * 128 : (c + 1) * 128]
-
-
-def expert_kernel(tokens, packed, out, acc):
-    k = pl.program_id(0)
-    width = tokens.shape[1]
-
-    @pl.when(k == 0)
-    def _():
-        acc[...] = jnp.zeros_like(acc)
-
+def pack_kernel(*refs):
+    own, other, out, sems = refs[0:3], refs[3:6], refs[6], refs[7]
+    ff = own[0].shape[0]
+    core = lax.rem(lax.axis_index("tp"), 2)
+    copies = []
+    for side, group in enumerate((own, other)):
+        first = (core if side == 0 else 1 - core) * 3 * ff
+        for j, ref in enumerate(group):
+            copy = pltpu.make_async_copy(ref, out.at[pl.ds(first + j * ff, ff)], sems.at[3 * side + j])
+            copy.start()
+            copies.append(copy)
+    for copy in copies:
+        copy.wait()
+
+
+def expert_kernel(*refs):
+    tokens, shares, (out, gate_w, up_w, down_w, sems) = refs[0], refs[1:-5], refs[-5:]
+    ff = 64
+    copies = []
+    at = 0
+    for share in shares:
+        for piece in range(share.shape[0] // (3 * ff)):
+            copies.append(
+                fetched(
+                    [share.at[pl.ds((3 * piece + j) * ff, ff)] for j in range(3)],
+                    [w.at[pl.ds(at * ff, ff)] for w in (gate_w, up_w, down_w)],
+                    sems,
+                    3 * at,
+                )
+            )
+            at += 1
     x = tokens[...]
-    rows = x.shape[0]
-    low = lax.broadcasted_iota(jnp.int32, (rows, 128), 1) < 64
-    hidden = []
-    for pair in range(2):
-        both = jnp.concatenate([packed[2 * pair, 0:width, :], packed[2 * pair + 1, 0:width, :]], axis=1)
-        z = jnp.dot(x, both, preferred_element_type=F32)
-        even, odd = z[:, 0:128], z[:, 128:256]
-        gate = jnp.where(low, even, pltpu.roll(odd, 64, 1))
-        up = jnp.where(low, pltpu.roll(even, 64, 1), odd)
-        hidden.append((jax.nn.silu(gate) * up).astype(BF16))
-    hid = jnp.concatenate(hidden, axis=1)
-    for c in range(width // 256):
-        cols = []
-        for half in range(2):
-            at = width + (2 * c + half) * 64
-            cols.append(jnp.concatenate([packed[p, at : at + 64, :] for p in range(4)], axis=0))
-        acc[:, c * 256 : (c + 1) * 256] += jnp.dot(
-            hid, jnp.concatenate(cols, axis=1), preferred_element_type=F32
-        )
-
-    @pl.when(k == pl.num_programs(0) - 1)
-    def _():
-        out[...] = acc[...].astype(BF16)
+    acc = jnp.zeros(out.shape, F32)
+    block = 256
+    last = (((1,), (1,)), ((), ()))
+    for k in range(at * ff // block):
+        for piece in range(k * block // ff, (k + 1) * block // ff):
+            for copy in copies[piece]:
+                copy.wait()
+        rows = slice(k * block, (k + 1) * block)
+        gate = lax.dot_general(x, gate_w[rows, :], last, preferred_element_type=F32)
+        up = lax.dot_general(x, up_w[rows, :], last, preferred_element_type=F32)
+        hidden = (jax.nn.silu(gate) * up).astype(BF16)
+        acc = acc + jnp.dot(hidden, down_w[rows, :], preferred_element_type=F32)
+    out[...] = acc.astype(BF16)
 
 
 def combine_kernel(values, stream, gain, routes, weights, out):
@@ -310,17 +339,20 @@
     rows, width = residual.shape
     sp = lax.axis_size("sp")
     tp = lax.axis_size("tp")
+    own_share = (jnp.swapaxes(exp_gate, 1, 2)[0], jnp.swapaxes(exp_up, 1, 2)[0], exp_down[0])
+    partner = [(i, i ^ 1) for i in range(tp)]
+    around = [(i, (i + 2) % tp if i % 2 == 0 else (i - 2) % tp) for i in range(tp)]
+    other_share = [lax.ppermute(part, "tp", partner) for part in own_share]
     ff_own = exp_down.shape[1]
-    packed_rows = width + ff_own * width // 128
-    packed = pl.pallas_call(
+    share0 = pl.pallas_call(
         pack_kernel,
-        out_shape=shape((packed_rows, 128), BF16),
-        in_specs=[whole()] * 3,
-        out_specs=whole(),
-        compiler_params=params(8),
+        out_shape=shape((6 * ff_own, width), BF16),
+        in_specs=[anywhere()] * 6,
+        out_specs=anywhere(),
+        scratch_shapes=[pltpu.SemaphoreType.DMA((6,))],
         name="pack",
-    )(exp_gate, exp_up, exp_down)
-    gathered = lax.all_gather(packed, "tp", axis=0, tiled=False)
+    )(*own_share, *other_share)
+    share1 = lax.ppermute(share0, "tp", around)
 
     ends = sp - 1
     before = lax.ppermute(mix_in[length - 2 :], "sp", [(i, i + 1) for i in range(ends)])
@@ -331,7 +363,7 @@
     h_f, p_f, h_b, p_b, seg, total = pl.pallas_call(
         scan_kernel,
         out_shape=(state, state, state, state, shape((32, 128), F32), shape((sp, 8, 128), F32)),
-        in_specs=[whole()] * 10,
+        in_specs=[anywhere(), whole(), whole()] + [anywhere()] * 7,
         out_specs=(whole(),) * 6,
         scratch_shapes=[
             pltpu.VMEM((length + 16, 128), F32),
@@ -344,61 +376,80 @@
             pltpu.VMEM((lines, 128), F32),
             pltpu.VMEM((lines, 128), F32),
             pltpu.VMEM((lines, 128), F32),
+            pltpu.VMEM(mix_in.shape, BF16),
+            pltpu.VMEM(conv_w.shape, F32),
+            pltpu.VMEM((1, 128), F32),
+            pltpu.VMEM(decay_param.shape, F32),
+            pltpu.VMEM(recur_gate.shape, F32),
+            pltpu.VMEM(recur_bias.shape, F32),
+            pltpu.VMEM(input_gate.shape, F32),
+            pltpu.VMEM(input_bias.shape, F32),
+            pltpu.SemaphoreType.DMA((8,)),
         ],
         compiler_params=params(20),
         name="scan",
     )(mix_in, before, after, conv_w, conv_b[None], decay_param, recur_gate, recur_bias, input_gate, input_bias)
     totals = lax.all_to_all(total, "sp", split_axis=0, concat_axis=0, tiled=True)
+    totals, share1 = lax.optimization_barrier((totals, share1))
+    share2 = lax.ppermute(share1, "tp", around)
+    other1 = lax.ppermute(share1, "tp", partner)
     mixed = pl.pallas_call(
         mix_kernel,
         out_shape=shape((length, channels), BF16),
-        in_specs=[whole()] * 7,
+        in_specs=[whole()] * 6 + [anywhere()],
         out_specs=whole(),
-        scratch_shapes=[pltpu.VMEM((lines, 128), F32)],
+        scratch_shapes=[
+            pltpu.VMEM((lines, 128), F32),
+            pltpu.VMEM((length, channels), BF16),
+            pltpu.SemaphoreType.DMA((1,)),
+        ],
         compiler_params=params(12),
         name="mix",
     )(h_f, p_f, h_b, p_b, seg, totals, gate_in)
     token_rows = lax.all_to_all(
         mixed.reshape(tp, rows, channels), "tp", split_axis=0, concat_axis=0, tiled=True
     )
+    token_rows, share2 = lax.optimization_barrier((token_rows, share2))
+    share3 = lax.ppermute(share2, "tp", around)
+    other2 = lax.ppermute(share2, "tp", partner)
     own = lax.axis_index("tp") * rows
     own_routes = lax.dynamic_slice_in_dim(routes, own, rows, 0)
     own_weights = lax.dynamic_slice_in_dim(route_wt, own, rows, 0)
     slots = 2 * rows * routes.shape[1]
-    block = 256
-    fixed = lambda *dims: pl.BlockSpec(dims, lambda k: (0,) * len(dims))
     stream, outgoing = pl.pallas_call(
         proj_kernel,
-        grid=(width // block,),
         out_shape=(shape((rows, width), BF16), shape((slots, width), BF16)),
-        in_specs=[
-            pl.BlockSpec((block // channels, rows, channels), lambda k: (k, 0, 0)),
-            pl.BlockSpec((block, width), lambda k: (k, 0)),
-            fixed(rows, width),
-            fixed(*norm_gain.shape),
-            fixed(routes.shape[1], rows),
+        in_specs=[whole(), anywhere(), anywhere(), anywhere(), whole()],
+        out_specs=(whole(), whole()),
+        scratch_shapes=[
+            pltpu.VMEM(out_proj.shape, BF16),
+            pltpu.VMEM(residual.shape, BF16),
+            pltpu.VMEM(norm_gain.shape, F32),
+            pltpu.SemaphoreType.DMA((10,)),
         ],
-        out_specs=(fixed(rows, width), fixed(slots, width)),
-        scratch_shapes=[pltpu.VMEM((rows, width), F32)],
         compiler_params=params(16),
         name="proj",
     )(token_rows, out_proj, residual, norm_gain, own_routes.T)
     arrived = lax.all_to_all(
         outgoing.reshape(sp, slots // sp, width), "sp", split_axis=0, concat_axis=0, tiled=True
     )
+    arrived, share3 = lax.optimization_barrier((arrived, share3))
+    half = 3 * ff_own
+    core = lax.rem(lax.axis_index("tp"), 2)
+    share4 = lax.ppermute(lax.dynamic_slice_in_dim(share3, core * half, half, 0), "tp", around)
+    other3 = lax.ppermute(share3, "tp", partner)
+    other4 = lax.ppermute(share4, "tp", partner)
+    shares = (share0, share1, other1, share2, other2, share3, other3, share4, other4)
+    hidden_units = tp * ff_own
     done = pl.pallas_call(
         expert_kernel,
-        grid=(tp // 4,),
         out_shape=shape((slots, width), BF16),
-        in_specs=[
-            fixed(slots, width),
-            pl.BlockSpec((4, packed_rows, 128), lambda k: (k, 0, 0)),
-        ],
-        out_specs=fixed(slots, width),
-        scratch_shapes=[pltpu.VMEM((slots, width), F32)],
+        in_specs=[whole()] + [anywhere()] * len(shares),
+        out_specs=whole(),
+        scratch_shapes=[pltpu.VMEM((hidden_units, width), BF16)] * 3 + [pltpu.SemaphoreType.DMA((3 * tp,))],
         compiler_params=params(32),
         name="experts",
-    )(arrived.reshape(slots, width), gathered)
+    )(arrived.reshape(slots, width), *shares)
     returned = lax.all_to_all(
         done.reshape(sp, slots // sp, width), "sp", split_axis=0, concat_axis=0, tiled=True
     )

time: 140 us -> 192 us (1.37)
  Pallas kernels: 16.6 us -> 63.9 us
  waiting for transfers between devices: 32.1 us -> 50.9 us
  local copies, waits for them, and re-layouts: 22.1 us -> 8.85 us
  between operations: 13.5 us -> 0.25 us
  blocking collectives: 34.4 us -> 42 us
  starting transfers between devices: 20.9 us -> 25.8 us
    pallas_call x3, Pallas kernels: 10.5 us -> 58 us  [the longest x1 48.8 us: on_device(): pl.pallas_call(pack_kernel, out_shape=shape((6 * ff_own, width), BF16), i...]
    ppermute x0 -> x11, starting transfers between devices: none -> 14 us  [the longest x1 3.95 us: on_device(): share1 = lax.ppermute(share0, 'tp', around)]
    unnamed x36 -> x44, local copies, waits for them, and re-layouts: 20.5 us -> 6.62 us
    ppermute x0 -> x11, waiting for transfers between devices: none -> 12.4 us  [the longest x1 9.04 us: on_device(): lax.ppermute(lax.dynamic_slice_in_dim(share3, core * half, half, 0), 'tp'...]
    all_to_all x1, starting transfers between devices: 12 us -> 3.78 us  [on_device(): lax.all_to_all(outgoing.reshape(sp, slots // sp, width), 'sp', split_axis...]
    all_to_all x1, blocking collectives: 19.7 us -> 27.6 us  [on_device(): lax.all_to_all(mixed.reshape(tp, rows, channels), 'tp', split_axis=0, con...]
    all_to_all x1, waiting for transfers between devices: 14.3 us -> 19.3 us  [on_device(): lax.all_to_all(outgoing.reshape(sp, slots // sp, width), 'sp', split_axis...]
  transfers between devices with their start and end apart: 5 -> 15, of which waited for: 3 -> 8; matrix products, arithmetic and copies ran while one was open for 1% -> 1% of each run, Pallas kernels for 6% -> 4%
where the time goes in v2:
time: 192 us
  Pallas kernels  63.9 us (33%)
  waiting for transfers between devices  50.9 us (27%)
  blocking collectives  42 us (22%)
  starting transfers between devices  25.8 us (13%)
  local copies, waits for them, and re-layouts  8.85 us (5%)
    pallas_call x1, Pallas kernels, on_device(): pl.pallas_call(pack_kernel, out_shape=shape((6 * ff_own, width), BF16), i...  48.8 us
    all_to_all x1, blocking collectives, on_device(): lax.all_to_all(mixed.reshape(tp, rows, channels), 'tp', split_axis=0, con...  27.6 us
    all_to_all x1, waiting for transfers between devices, on_device(): lax.all_to_all(outgoing.reshape(sp, slots // sp, width), 'sp', split_axis...  19.3 us
    all_to_all x1, waiting for transfers between devices, on_device(): lax.all_to_all(done.reshape(sp, slots // sp, width), 'sp', split_axis=0,...  16 us
    all_to_all x1, blocking collectives, on_device(): lax.all_to_all(total, 'sp', split_axis=0, concat_axis=0, tiled=True)  14.3 us
    ppermute x1, waiting for transfers between devices, on_device(): lax.ppermute(lax.dynamic_slice_in_dim(share3, core * half, half, 0), 'tp'...  9.04 us
    unnamed x44, local copies, waits for them, and re-layouts  6.62 us
    pallas_call x1, Pallas kernels, on_device(): pl.pallas_call(expert_kernel, out_shape=shape((slots, width), BF16), in_s...  5.97 us
  transfers between devices with their start and end apart: 15, of which 8 were waited for; matrix products, arithmetic and copies ran while one was open for 1% of the time, Pallas kernels for 4%

profile of v2, /device:TPU:1, one launch (start us, length us, event | category | flops | bytes accessed | tf_op | source)
XLA Modules:
  0.0 191.7 jit_solution(7871633368400810333)
XLA Ops:
  0.0 3.2 %collective-permute-start.2 = (bf16[64,2048]{1,0:T(8,128)(2,1)}, bf16[64,2048]{1,0:T(8,128)(2,1)S(1)}, u32[]{:S(2)}, u32[]{:S(2)}) collective-permute-start(bf16[64,2048]{1,0:T(8,128)(2,1)} %bitcast.21), channel_id=1, source_target_pairs={{0,1},{1,0},{2,3},{3,2},{4,5},{5,4},{6,7},{7,6},{8,9},{9,8},{10,11... | collective-permute-start | bytes 786440 | tf_op jit(solution)/shard_map/ppermute | solution.py:345
  6.4 48.8 %pack.1.refs_1_ = bf16[384,2048]{1,0:T(8,128)(2,1)} custom-call(bf16[64,2048]{1,0:T(8,128)(2,1)} %bitcast.22, bf16[64,2048]{1,0:T(8,128)(2,1)} %bitcast.24, bf16[64,2048]{1,0:T(8,128)(2,1)} %bitcast.26, bf16[64,2048]{1,0:T(8,128)(2,1)} %copy-done.18, bf16[64,2048]{1,0:T(8,128)(2,1)} %copy-done.19, bf16[64,2048]{1,0:T(8,128)(2,1)} %copy-done.20), custom_call_target="tpu_custom_call" | custom-call | tf_op jit(solution)/shard_map/pack/pallas_call | solution.py:347
  55.2 3.9 %collective-permute-start.5 = (bf16[384,2048]{1,0:T(8,128)(2,1)}, bf16[384,2048]{1,0:T(8,128)(2,1)S(1)}, u32[]{:S(2)}, u32[]{:S(2)}) collective-permute-start(bf16[384,2048]{1,0:T(8,128)(2,1)} %pack.1.refs_1_), channel_id=1, source_target_pairs={{0,2},{1,15},{2,4},{3,1},{4,6},{5,3},{6,8},{7,5},{8,10},{9,7},{10,... | collective-permute-start | bytes 4718600 | tf_op jit(solution)/shard_map/ppermute | solution.py:355
  59.1 3.1 %collective-permute-start = (bf16[2,128]{1,0:T(2,128)(2,1)S(1)}, bf16[2,128]{1,0:T(2,128)(2,1)S(1)}, u32[]{:S(2)}, u32[]{:S(2)}) collective-permute-start(bf16[2,128]{1,0:T(2,128)(2,1)S(1)} %get-tuple-element.34), channel_id=1, source_target_pairs={{0,16},{16,32},{32,48},{48,64},{64,80},{80,96},{96,112},{112,128},... | collective-permute-start | bytes 1544 | tf_op jit(solution)/shard_map/ppermute | solution.py:358
  62.2 1.3 collective-permute-start.1
  63.5 3.3 %collective-permute-done.1.after = bf16[2,128]{1,0:T(2,128)(2,1)S(1)} collective-permute-done((bf16[2,128]{1,0:T(2,128)(2,1)S(1)}, bf16[2,128]{1,0:T(2,128)(2,1)S(1)}, u32[]{:S(2)}, u32[]{:S(2)}) %collective-permute-start.1) | collective-permute-done | bytes 544 | tf_op jit(solution)/shard_map/ppermute | solution.py:359
  66.9 3.8 %scan.1 = (f32[1024,128]{1,0:T(8,128)S(1)}, f32[1024,128]{1,0:T(8,128)S(1)}, f32[1024,128]{1,0:T(8,128)S(1)}, f32[1024,128]{1,0:T(8,128)S(1)}, f32[32,128]{1,0:T(8,128)S(1)}, /*index=5*/f32[16,8,128]{2,1,0:T(8,128)S(1)}) custom-call(bf16[1024,128]{1,0:T(8,128)(2,1)S(1)} %copy-done.7, bf16[2,128]{1,0:T(2,128)(2,1)S(1)} %collective-permute-done.before, ...), custom_call_target="tpu_custom_call" | custom-call | tf_op jit(solution)/shard_map/scan/pallas_call | solution.py:363
  70.7 14.3 %all_to_all.20.totals = f32[16,8,128]{2,1,0:T(8,128)S(1)} all-to-all(f32[16,8,128]{2,1,0:T(8,128)S(1)} %get-tuple-element.24), channel_id=1, replica_groups=mesh['sp'=16,'tp'=16] {'sp'}, dimensions={0} | all-to-all | bytes 131072 | tf_op jit(solution)/shard_map/all_to_all | solution.py:392
  86.3 27.6 %all_to_all.21.mixed = bf16[16,64,128]{2,1,0:T(8,128)(2,1)S(1)} all-to-all(bf16[16,64,128]{2,1,0:T(8,128)(2,1)S(1)} %bitcast.18), channel_id=1, replica_groups=mesh['sp'=16,'tp'=16] {'tp'}, dimensions={0} | all-to-all | bytes 524288 | tf_op jit(solution)/shard_map/all_to_all | solution.py:409
  114.3 3.4 %copy-done.1 = bf16[2048,2048]{1,0:T(8,128)(2,1)S(1)} copy-done((bf16[2048,2048]{1,0:T(8,128)(2,1)S(1)}, bf16[2048,2048]{1,0:T(8,128)(2,1)}, u32[]{:S(2)}) %copy-start.1) | copy-done | bytes 8388632
  117.7 3.2 %proj.1 = (bf16[64,2048]{1,0:T(8,128)(2,1)S(1)}, bf16[256,2048]{1,0:T(8,128)(2,1)S(1)}) custom-call(bf16[16,64,128]{2,1,0:T(8,128)(2,1)S(1)} %all_to_all.21.mixed, bf16[2048,2048]{1,0:T(8,128)(2,1)S(1)} %copy-done.1, bf16[64,2048]{1,0:T(8,128)(2,1)S(1)} %copy-done.8, f32[3,2048]{1,0:T(4,128)S(1)} %copy-done.10, s32[2,64]{1,0:T(2,128)S(1)} %copy.19.routes), custom_call_target="tpu_custom_call" | custom-call | tf_op jit(solution)/shard_map/proj/pallas_call | solution.py:419
  120.9 1.0 copy-done.6
  121.9 3.8 %all-to-all-start.2 = ((bf16[16,16,2048]{2,1,0:T(8,128)(2,1)}), bf16[16,16,2048]{2,1,0:T(8,128)(2,1)S(1)}, u32[]{:S(2)}, u32[]{:S(2)}) async-start(bf16[16,16,2048]{2,1,0:T(8,128)(2,1)} %bitcast.17), calls=%async_computation.2 | async-start | bytes 2097152 | tf_op jit(solution)/shard_map/all_to_all | solution.py:433
  126.3 19.3 %all-to-all-done.2 = bf16[16,16,2048]{2,1,0:T(8,128)(2,1)S(1)} async-done(((bf16[16,16,2048]{2,1,0:T(8,128)(2,1)}), bf16[16,16,2048]{2,1,0:T(8,128)(2,1)S(1)}, u32[]{:S(2)}, u32[]{:S(2)}) %all-to-all-start.2) | async-done | bytes 1048608 | tf_op jit(solution)/shard_map/all_to_all | solution.py:433
  145.5 1.3 constant_dynamic-slice_fusion.1
  146.9 2.1 %collective-permute-start.11 = (bf16[192,2048]{1,0:T(8,128)(2,1)S(1)}, bf16[192,2048]{1,0:T(8,128)(2,1)S(1)}, u32[]{:S(2)}, u32[]{:S(2)}) collective-permute-start(bf16[192,2048]{1,0:T(8,128)(2,1)S(1)} %constant_dynamic-slice_fusion.1), channel_id=1, source_target_pairs={{0,2},{1,15},{2,4},{3,1},{4,6},{5,3},{6,8},{7,5},{8,10},{9,7},{10,... | collective-permute-start | bytes 2359304 | tf_op jit(solution)/shard_map/ppermute | solution.py:439
  149.0 9.0 %collective-permute-done.11.refs_8_ = bf16[192,2048]{1,0:T(8,128)(2,1)S(1)} collective-permute-done((bf16[192,2048]{1,0:T(8,128)(2,1)S(1)}, bf16[192,2048]{1,0:T(8,128)(2,1)S(1)}, u32[]{:S(2)}, u32[]{:S(2)}) %collective-permute-start.11) | collective-permute-done | bytes 786464 | tf_op jit(solution)/shard_map/ppermute | solution.py:439
  158.1 2.7 %collective-permute-start.12 = (bf16[192,2048]{1,0:T(8,128)(2,1)S(1)}, bf16[192,2048]{1,0:T(8,128)(2,1)S(1)}, u32[]{:S(2)}, u32[]{:S(2)}) collective-permute-start(bf16[192,2048]{1,0:T(8,128)(2,1)S(1)} %collective-permute-done.11.refs_8_), channel_id=1, source_target_pairs={{0,1},{1,0},{2,3},{3,2},{4,5},{5,4},{6,7},{7,6},{8,9},{9,8},{10,11... | collective-permute-start | bytes 2359304 | tf_op jit(solution)/shard_map/ppermute | solution.py:441
  160.8 1.9 collective-permute-done.12.refs_9_
  162.7 6.0 %experts.1 = bf16[256,2048]{1,0:T(8,128)(2,1)S(1)} custom-call(bf16[256,2048]{1,0:T(8,128)(2,1)S(1)} %bitcast.14, bf16[384,2048]{1,0:T(8,128)(2,1)S(1)} %copy-done.2, bf16[384,2048]{1,0:T(8,128)(2,1)S(1)} %copy-done.5, bf16[384,2048]{1,0:T(8,128)(2,1)} %collective-permute-done.8.refs_3_, bf16[384,2048]{1,0:T(8,128)(2,1)} %collective-permute-done.6.refs_4_, ...), custom_call_target="tpu_custom_call" | custom-call | tf_op jit(solution)/shard_map/experts/pallas_call | solution.py:444
  168.7 1.0 copy-done.3
  169.6 3.7 %all-to-all-start.3 = ((bf16[16,16,2048]{2,1,0:T(8,128)(2,1)}), bf16[16,16,2048]{2,1,0:T(8,128)(2,1)S(1)}, u32[]{:S(2)}, u32[]{:S(2)}) async-start(bf16[16,16,2048]{2,1,0:T(8,128)(2,1)} %bitcast.15), calls=%async_computation.3 | async-start | bytes 2097152 | tf_op jit(solution)/shard_map/all_to_all | solution.py:453
  174.1 16.0 %all-to-all-done.3 = bf16[16,16,2048]{2,1,0:T(8,128)(2,1)S(1)} async-done(((bf16[16,16,2048]{2,1,0:T(8,128)(2,1)}), bf16[16,16,2048]{2,1,0:T(8,128)(2,1)S(1)}, u32[]{:S(2)}, u32[]{:S(2)}) %all-to-all-start.3) | async-done | bytes 1048608 | tf_op jit(solution)/shard_map/all_to_all | solution.py:453
  190.1 1.6 combine.1
  (63 shorter events, 6.3 us)
Async XLA Ops:
  0.0 114.0 %copy-start = (s32[1024,2]{0,1:T(2,128)S(1)}, s32[1024,2]{0,1:T(2,128)}, u32[]{:S(2)}) copy-start(s32[1024,2]{0,1:T(2,128)} %param.29) | copy-start | bytes 24580
  0.0 4.6 %collective-permute-start.2 = (bf16[64,2048]{1,0:T(8,128)(2,1)}, bf16[64,2048]{1,0:T(8,128)(2,1)S(1)}, u32[]{:S(2)}, u32[]{:S(2)}) collective-permute-start(bf16[64,2048]{1,0:T(8,128)(2,1)} %bitcast.21), channel_id=1, source_target_pairs={{0,1},{1,0},{2,3},{3,2},{4,5},{5,4},{6,7},{7,6},{8,9},{9,8},{10,11... | collective-permute-start | bytes 786440 | tf_op jit(solution)/shard_map/ppermute | solution.py:345
  3.2 1.7 collective-permute-start.3
  3.2 63.6 %copy-start.11 = (f32[2,2,64,64]{3,2,1,0:T(8,128)S(1)}, f32[2,2,64,64]{3,2,1,0:T(8,128)}, u32[]{:S(2)}) copy-start(f32[2,2,64,64]{3,2,1,0:T(8,128)} %recur_gate_h.1) | copy-start | bytes 196612
  3.2 63.6 %copy-start.12 = (f32[2,2,64,64]{3,2,1,0:T(8,128)S(1)}, f32[2,2,64,64]{3,2,1,0:T(8,128)}, u32[]{:S(2)}) copy-start(f32[2,2,64,64]{3,2,1,0:T(8,128)} %input_gate_h.1) | copy-start | bytes 196612
  3.2 63.6 %copy-start.13 = (f32[4,128]{1,0:T(4,128)S(1)}, f32[4,128]{1,0:T(4,128)}, u32[]{:S(2)}) copy-start(f32[4,128]{1,0:T(4,128)} %conv_w_h.1) | copy-start | bytes 6148
  3.2 63.6 %copy-start.14 = (f32[2,128]{1,0:T(2,128)S(1)}, f32[2,128]{1,0:T(2,128)}, u32[]{:S(2)}) copy-start(f32[2,128]{1,0:T(2,128)} %decay_param_h.1) | copy-start | bytes 3076
  3.2 63.6 %copy-start.15 = (f32[2,128]{1,0:T(2,128)S(1)}, f32[2,128]{1,0:T(2,128)}, u32[]{:S(2)}) copy-start(f32[2,128]{1,0:T(2,128)} %recur_bias_h.1) | copy-start | bytes 3076
  3.2 63.6 %copy-start.16 = (f32[2,128]{1,0:T(2,128)S(1)}, f32[2,128]{1,0:T(2,128)}, u32[]{:S(2)}) copy-start(f32[2,128]{1,0:T(2,128)} %input_bias_h.1) | copy-start | bytes 3076
  3.3 63.6 %copy-start.17 = (f32[128]{0:T(128)S(1)}, f32[128]{0:T(128)}, u32[]{:S(2)}) copy-start(f32[128]{0:T(128)} %param.20) | copy-start | bytes 1540
  3.3 82.5 %copy-start.9 = (bf16[1024,128]{1,0:T(8,128)(2,1)S(1)}, bf16[1024,128]{1,0:T(8,128)(2,1)}, u32[]{:S(2)}) copy-start(bf16[1024,128]{1,0:T(8,128)(2,1)} %gate_h.1) | copy-start | bytes 786436
  3.3 2.0 %collective-permute-start.4 = (bf16[64,2048]{1,0:T(8,128)(2,1)}, bf16[64,2048]{1,0:T(8,128)(2,1)S(1)}, u32[]{:S(2)}, u32[]{:S(2)}) collective-permute-start(bf16[64,2048]{1,0:T(8,128)(2,1)} %bitcast.25), channel_id=1, source_target_pairs={{0,1},{1,0},{2,3},{3,2},{4,5},{5,4},{6,7},{7,6},{8,9},{9,8},{10,11... | collective-permute-start | bytes 786440 | tf_op jit(solution)/shard_map/ppermute | solution.py:345
  55.2 29.9 %collective-permute-start.5 = (bf16[384,2048]{1,0:T(8,128)(2,1)}, bf16[384,2048]{1,0:T(8,128)(2,1)S(1)}, u32[]{:S(2)}, u32[]{:S(2)}) collective-permute-start(bf16[384,2048]{1,0:T(8,128)(2,1)} %pack.1.refs_1_), channel_id=1, source_target_pairs={{0,2},{1,15},{2,4},{3,1},{4,6},{5,3},{6,8},{7,5},{8,10},{9,7},{10,... | collective-permute-start | bytes 4718600 | tf_op jit(solution)/shard_map/ppermute | solution.py:355
  59.1 4.4 %collective-permute-start = (bf16[2,128]{1,0:T(2,128)(2,1)S(1)}, bf16[2,128]{1,0:T(2,128)(2,1)S(1)}, u32[]{:S(2)}, u32[]{:S(2)}) collective-permute-start(bf16[2,128]{1,0:T(2,128)(2,1)S(1)} %get-tuple-element.34), channel_id=1, source_target_pairs={{0,16},{16,32},{32,48},{48,64},{64,80},{80,96},{96,112},{112,128},... | collective-permute-start | bytes 1544 | tf_op jit(solution)/shard_map/ppermute | solution.py:358
  62.2 4.6 %collective-permute-start.1 = (bf16[2,128]{1,0:T(2,128)(2,1)S(1)}, bf16[2,128]{1,0:T(2,128)(2,1)S(1)}, u32[]{:S(2)}, u32[]{:S(2)}) collective-permute-start(bf16[2,128]{1,0:T(2,128)(2,1)S(1)} %get-tuple-element.33), channel_id=1, source_target_pairs={{16,0},{32,16},{48,32},{64,48},{80,64},{96,80},{112,96},{128,112},... | collective-permute-start | bytes 1544 | tf_op jit(solution)/shard_map/ppermute | solution.py:359
  85.0 28.9 %collective-permute-start.6 = (bf16[384,2048]{1,0:T(8,128)(2,1)S(1)}, bf16[384,2048]{1,0:T(8,128)(2,1)}, u32[]{:S(2)}, u32[]{:S(2)}) collective-permute-start(bf16[384,2048]{1,0:T(8,128)(2,1)S(1)} %collective-permute-done.5.refs_2_), channel_id=1, source_target_pairs={{0,2},{1,15},{2,4},{3,1},{4,6},{5,3},{6,8},{7,5},{8,10},{9,7},{10,... | collective-permute-start | bytes 4718600 | tf_op jit(solution)/shard_map/ppermute | solution.py:394
  113.9 31.6 %collective-permute-start.7 = (bf16[384,2048]{1,0:T(8,128)(2,1)}, bf16[384,2048]{1,0:T(8,128)(2,1)}, u32[]{:S(2)}, u32[]{:S(2)}) collective-permute-start(bf16[384,2048]{1,0:T(8,128)(2,1)} %collective-permute-done.6.refs_4_), channel_id=1, source_target_pairs={{0,2},{1,15},{2,4},{3,1},{4,6},{5,3},{6,8},{7,5},{8,10},{9,7},{10,... | collective-permute-start | bytes 4718600 | tf_op jit(solution)/shard_map/ppermute | solution.py:413
  121.9 23.7 %all-to-all-start.2 = ((bf16[16,16,2048]{2,1,0:T(8,128)(2,1)}), bf16[16,16,2048]{2,1,0:T(8,128)(2,1)S(1)}, u32[]{:S(2)}, u32[]{:S(2)}) async-start(bf16[16,16,2048]{2,1,0:T(8,128)(2,1)} %bitcast.17), calls=%async_computation.2 | async-start | bytes 2097152 | tf_op jit(solution)/shard_map/all_to_all | solution.py:433
  125.7 35.1 %collective-permute-start.8 = (bf16[384,2048]{1,0:T(8,128)(2,1)}, bf16[384,2048]{1,0:T(8,128)(2,1)}, u32[]{:S(2)}, u32[]{:S(2)}) collective-permute-start(bf16[384,2048]{1,0:T(8,128)(2,1)} %copy-done.4), channel_id=1, source_target_pairs={{0,1},{1,0},{2,3},{3,2},{4,5},{5,4},{6,7},{7,6},{8,9},{9,8},{10,11... | collective-permute-start | bytes 4718600 | tf_op jit(solution)/shard_map/ppermute | solution.py:395
  125.8 35.0 %collective-permute-start.9 = (bf16[384,2048]{1,0:T(8,128)(2,1)}, bf16[384,2048]{1,0:T(8,128)(2,1)}, u32[]{:S(2)}, u32[]{:S(2)}) collective-permute-start(bf16[384,2048]{1,0:T(8,128)(2,1)} %collective-permute-done.6.refs_4_), channel_id=1, source_target_pairs={{0,1},{1,0},{2,3},{3,2},{4,5},{5,4},{6,7},{7,6},{8,9},{9,8},{10,11... | collective-permute-start | bytes 4718600 | tf_op jit(solution)/shard_map/ppermute | solution.py:414
  146.9 11.2 %collective-permute-start.11 = (bf16[192,2048]{1,0:T(8,128)(2,1)S(1)}, bf16[192,2048]{1,0:T(8,128)(2,1)S(1)}, u32[]{:S(2)}, u32[]{:S(2)}) collective-permute-start(bf16[192,2048]{1,0:T(8,128)(2,1)S(1)} %constant_dynamic-slice_fusion.1), channel_id=1, source_target_pairs={{0,2},{1,15},{2,4},{3,1},{4,6},{5,3},{6,8},{7,5},{8,10},{9,7},{10,... | collective-permute-start | bytes 2359304 | tf_op jit(solution)/shard_map/ppermute | solution.py:439
  148.9 13.7 %collective-permute-start.10 = (bf16[384,2048]{1,0:T(8,128)(2,1)}, bf16[384,2048]{1,0:T(8,128)(2,1)S(1)}, u32[]{:S(2)}, u32[]{:S(2)}) collective-permute-start(bf16[384,2048]{1,0:T(8,128)(2,1)} %collective-permute-done.7.refs_6_), channel_id=1, source_target_pairs={{0,1},{1,0},{2,3},{3,2},{4,5},{5,4},{6,7},{7,6},{8,9},{9,8},{10,11... | collective-permute-start | bytes 4718600 | tf_op jit(solution)/shard_map/ppermute | solution.py:440
  158.1 4.6 %collective-permute-start.12 = (bf16[192,2048]{1,0:T(8,128)(2,1)S(1)}, bf16[192,2048]{1,0:T(8,128)(2,1)S(1)}, u32[]{:S(2)}, u32[]{:S(2)}) collective-permute-start(bf16[192,2048]{1,0:T(8,128)(2,1)S(1)} %collective-permute-done.11.refs_8_), channel_id=1, source_target_pairs={{0,1},{1,0},{2,3},{3,2},{4,5},{5,4},{6,7},{7,6},{8,9},{9,8},{10,11... | collective-permute-start | bytes 2359304 | tf_op jit(solution)/shard_map/ppermute | solution.py:441
  169.6 20.5 %all-to-all-start.3 = ((bf16[16,16,2048]{2,1,0:T(8,128)(2,1)}), bf16[16,16,2048]{2,1,0:T(8,128)(2,1)S(1)}, u32[]{:S(2)}, u32[]{:S(2)}) async-start(bf16[16,16,2048]{2,1,0:T(8,128)(2,1)} %bitcast.15), calls=%async_computation.3 | async-start | bytes 2097152 | tf_op jit(solution)/shard_map/all_to_all | solution.py:453
  (12 other events, 207.3 us)

commit v3 on v2

--- a/solution.py
+++ b/solution.py
@@ -1,3 +1,5 @@
+import functools
+
 import jax
 import jax.numpy as jnp
 from jax import lax
@@ -5,6 +7,7 @@
 from jax.experimental.pallas import tpu as pltpu
 from jax.sharding import PartitionSpec as P
 
+
 EPSILON = 1e-06
 F32 = jnp.float32
 BF16 = jnp.bfloat16
@@ -22,6 +25,10 @@
 
 def anywhere():
     return pl.BlockSpec(memory_space=pl.ANY)
+
+
+def in_hbm():
+    return pl.BlockSpec(memory_space=pltpu.MemorySpace.HBM)
 
 
 def fetched(sources, buffers, sems, first=0):
@@ -199,7 +206,7 @@
     return values * lax.rsqrt(jnp.mean(values * values, axis=-1, keepdims=True) + EPSILON) * gain
 
 
-def proj_kernel(mixed, weights_h, residual_h, gain_h, routes, stream_out, outgoing, weights, residual, gain, sems):
+def proj_kernel(mixed, weights_h, residual_h, gain_h, routes, stream_out, outgoing_h, weights, residual, gain, outgoing, sems):
     width = weights.shape[0]
     blocks = 8
     block = width // blocks
@@ -214,65 +221,68 @@
         acc = acc + jnp.dot(lanes, weights[k * block : (k + 1) * block, :], preferred_element_type=F32)
     for copy in others:
         copy.wait()
-    if True:
-        proj = acc.astype(BF16).astype(F32)
-        stream = (residual[...].astype(F32) + scaled(proj, gain[0:1, :])).astype(BF16)
-        stream_out[...] = stream
-        normed = scaled(stream.astype(F32), gain[1:2, :]).astype(BF16)
-        rows = normed.shape[0]
-        slots = outgoing.shape[0]
-        experts = 16
-        capacity = slots // experts
-        first, second = routes[0:1, :], routes[1:2, :]
-        ids = lax.broadcasted_iota(jnp.int32, (experts, rows), 0)
-        hit0 = (ids == first).astype(F32)
-        hit1 = (ids == second).astype(F32)
-        r = lax.broadcasted_iota(jnp.int32, (rows, rows), 0)
-        c = lax.broadcasted_iota(jnp.int32, (rows, rows), 1)
-        earlier = jnp.dot((hit0 + hit1).astype(BF16), (r < c).astype(BF16), preferred_element_type=F32)
-        slot0 = first * capacity + jnp.sum(hit0 * earlier, axis=0, keepdims=True).astype(jnp.int32)
-        slot1 = second * capacity + jnp.sum(hit1 * earlier, axis=0, keepdims=True).astype(jnp.int32)
-        places = lax.broadcasted_iota(jnp.int32, (slots, rows), 0)
-        pick = jnp.where(jnp.logical_or(places == slot0, places == slot1), 1.0, 0.0).astype(BF16)
-        outgoing[...] = jnp.dot(pick, normed, preferred_element_type=F32).astype(BF16)
-
-
-def pack_kernel(*refs):
-    own, other, out, sems = refs[0:3], refs[3:6], refs[6], refs[7]
-    ff = own[0].shape[0]
-    core = lax.rem(lax.axis_index("tp"), 2)
-    copies = []
-    for side, group in enumerate((own, other)):
-        first = (core if side == 0 else 1 - core) * 3 * ff
-        for j, ref in enumerate(group):
-            copy = pltpu.make_async_copy(ref, out.at[pl.ds(first + j * ff, ff)], sems.at[3 * side + j])
-            copy.start()
-            copies.append(copy)
-    for copy in copies:
+    proj = acc.astype(BF16).astype(F32)
+    stream = (residual[...].astype(F32) + scaled(proj, gain[0:1, :])).astype(BF16)
+    stream_out[...] = stream
+    normed = scaled(stream.astype(F32), gain[1:2, :]).astype(BF16)
+    rows = normed.shape[0]
+    slots = outgoing.shape[0]
+    experts = 16
+    capacity = slots // experts
+    first, second = routes[0:1, :], routes[1:2, :]
+    ids = lax.broadcasted_iota(jnp.int32, (experts, rows), 0)
+    hit0 = (ids == first).astype(F32)
+    hit1 = (ids == second).astype(F32)
+    r = lax.broadcasted_iota(jnp.int32, (rows, rows), 0)
+    c = lax.broadcasted_iota(jnp.int32, (rows, rows), 1)
+    earlier = jnp.dot((hit0 + hit1).astype(BF16), (r < c).astype(BF16), preferred_element_type=F32)
+    slot0 = first * capacity + jnp.sum(hit0 * earlier, axis=0, keepdims=True).astype(jnp.int32)
+    slot1 = second * capacity + jnp.sum(hit1 * earlier, axis=0, keepdims=True).astype(jnp.int32)
+    places = lax.broadcasted_iota(jnp.int32, (slots, rows), 0)
+    pick = jnp.where(jnp.logical_or(places == slot0, places == slot1), 1.0, 0.0).astype(BF16)
+    sent = []
+    for k in range(4):
+        part = slice(k * 512, (k + 1) * 512)
+        outgoing[:, part] = jnp.dot(pick, normed[:, part], preferred_element_type=F32).astype(BF16)
+        sent += fetched([outgoing.at[:, part]], [outgoing_h.at[:, part]], sems, 10 + k)
+    for copy in sent:
         copy.wait()
 
 
-def expert_kernel(*refs):
-    tokens, shares, (out, gate_w, up_w, down_w, sems) = refs[0], refs[1:-5], refs[-5:]
-    ff = 64
-    copies = []
-    at = 0
-    for share in shares:
-        for piece in range(share.shape[0] // (3 * ff)):
-            copies.append(
-                fetched(
-                    [share.at[pl.ds((3 * piece + j) * ff, ff)] for j in range(3)],
-                    [w.at[pl.ds(at * ff, ff)] for w in (gate_w, up_w, down_w)],
-                    sems,
-                    3 * at,
-                )
-            )
-            at += 1
+def pack_kernel(gate, up, down, out, buffer, sems):
+    ff = gate.shape[0]
+    refs = (gate, up, down)
+    parts = [pl.ds(j * ff, ff) for j in range(3)]
+    inward = fetched(refs, [buffer.at[part] for part in parts], sems)
+    outward = []
+    for copy, part in zip(inward, parts):
+        copy.wait()
+        outward += fetched([buffer.at[part]], [out.at[part]], sems, 3 + len(outward))
+    for copy in outward:
+        copy.wait()
+
+
+def expert_kernel(*refs, pieces, head, tail):
+    tokens, shares = refs[0], refs[1 : 1 + pieces]
+    rest = refs[1 + pieces :]
+    if not head:
+        before, rest = rest[0], rest[1:]
+    out, gate_w, up_w, down_w, sems = rest[:5]
+    ff = shares[0].shape[0] // 3
+    copies = [
+        fetched(
+            [share.at[pl.ds(j * ff, ff)] for j in range(3)],
+            [w.at[pl.ds(at * ff, ff)] for w in (gate_w, up_w, down_w)],
+            sems,
+            3 * at,
+        )
+        for at, share in enumerate(shares)
+    ]
     x = tokens[...]
-    acc = jnp.zeros(out.shape, F32)
+    acc = jnp.zeros(x.shape, F32) if head else before[...]
     block = 256
     last = (((1,), (1,)), ((), ()))
-    for k in range(at * ff // block):
+    for k in range(pieces * ff // block):
         for piece in range(k * block // ff, (k + 1) * block // ff):
             for copy in copies[piece]:
                 copy.wait()
@@ -281,7 +291,14 @@
         up = lax.dot_general(x, up_w[rows, :], last, preferred_element_type=F32)
         hidden = (jax.nn.silu(gate) * up).astype(BF16)
         acc = acc + jnp.dot(hidden, down_w[rows, :], preferred_element_type=F32)
-    out[...] = acc.astype(BF16)
+    if tail:
+        result, done = rest[5:]
+        result[...] = acc.astype(BF16)
+        copy = pltpu.make_async_copy(result, out, done.at[0])
+        copy.start()
+        copy.wait()
+    else:
+        out[...] = acc
 
 
 def combine_kernel(values, stream, gain, routes, weights, out):
@@ -316,7 +333,7 @@
     return jax.ShapeDtypeStruct(dims, dtype)
 
 
-def on_device(
+def layer(
     mix_in,
     gate_in,
     conv_w,
@@ -339,24 +356,29 @@
     rows, width = residual.shape
     sp = lax.axis_size("sp")
     tp = lax.axis_size("tp")
-    own_share = (jnp.swapaxes(exp_gate, 1, 2)[0], jnp.swapaxes(exp_up, 1, 2)[0], exp_down[0])
-    partner = [(i, i ^ 1) for i in range(tp)]
-    around = [(i, (i + 2) % tp if i % 2 == 0 else (i - 2) % tp) for i in range(tp)]
-    other_share = [lax.ppermute(part, "tp", partner) for part in own_share]
-    ff_own = exp_down.shape[1]
-    share0 = pl.pallas_call(
-        pack_kernel,
-        out_shape=shape((6 * ff_own, width), BF16),
-        in_specs=[anywhere()] * 6,
-        out_specs=anywhere(),
-        scratch_shapes=[pltpu.SemaphoreType.DMA((6,))],
-        name="pack",
-    )(*own_share, *other_share)
-    share1 = lax.ppermute(share0, "tp", around)
-
     ends = sp - 1
     before = lax.ppermute(mix_in[length - 2 :], "sp", [(i, i + 1) for i in range(ends)])
     after = lax.ppermute(mix_in[:2], "sp", [(i + 1, i) for i in range(ends)])
+    ff_own = exp_down.shape[1]
+    piece = shape((3 * ff_own, width), BF16)
+    own = pl.pallas_call(
+        pack_kernel,
+        out_shape=piece,
+        in_specs=[in_hbm()] * 3,
+        out_specs=in_hbm(),
+        scratch_shapes=[pltpu.VMEM(piece.shape, BF16), pltpu.SemaphoreType.DMA((6,))],
+        name="pack",
+    )(jnp.swapaxes(exp_gate, 1, 2)[0], jnp.swapaxes(exp_up, 1, 2)[0], exp_down[0])
+
+    def around(part):
+        return lax.ppermute(part, "tp", [(i, (i + 2 - 4 * (i % 2)) % tp) for i in range(tp)])
+
+    def across(part):
+        return lax.ppermute(part, "tp", [(i, i ^ 1) for i in range(tp)])
+
+    other = across(own)
+    r1a = around(own)
+    r1b = around(other)
     step = length // SEGS
     lines = SEGS * (step + 8)
     state = shape((length, channels), F32)
@@ -389,10 +411,11 @@
         compiler_params=params(20),
         name="scan",
     )(mix_in, before, after, conv_w, conv_b[None], decay_param, recur_gate, recur_bias, input_gate, input_bias)
+    total, r1a = lax.optimization_barrier((total, r1a))
+    r2a, e1a = around(r1a), across(r1a)
     totals = lax.all_to_all(total, "sp", split_axis=0, concat_axis=0, tiled=True)
-    totals, share1 = lax.optimization_barrier((totals, share1))
-    share2 = lax.ppermute(share1, "tp", around)
-    other1 = lax.ppermute(share1, "tp", partner)
+    totals, r1b = lax.optimization_barrier((totals, r1b))
+    r2b, e1b = around(r1b), across(r1b)
     mixed = pl.pallas_call(
         mix_kernel,
         out_shape=shape((length, channels), BF16),
@@ -409,47 +432,52 @@
     token_rows = lax.all_to_all(
         mixed.reshape(tp, rows, channels), "tp", split_axis=0, concat_axis=0, tiled=True
     )
-    token_rows, share2 = lax.optimization_barrier((token_rows, share2))
-    share3 = lax.ppermute(share2, "tp", around)
-    other2 = lax.ppermute(share2, "tp", partner)
-    own = lax.axis_index("tp") * rows
-    own_routes = lax.dynamic_slice_in_dim(routes, own, rows, 0)
-    own_weights = lax.dynamic_slice_in_dim(route_wt, own, rows, 0)
+    r3a, e2a = around(r2a), across(r2a)
+    first_row = lax.axis_index("tp") * rows
+    own_routes = lax.dynamic_slice_in_dim(routes, first_row, rows, 0)
+    own_weights = lax.dynamic_slice_in_dim(route_wt, first_row, rows, 0)
     slots = 2 * rows * routes.shape[1]
-    stream, outgoing = pl.pallas_call(
+    project = pl.pallas_call(
         proj_kernel,
         out_shape=(shape((rows, width), BF16), shape((slots, width), BF16)),
-        in_specs=[whole(), anywhere(), anywhere(), anywhere(), whole()],
-        out_specs=(whole(), whole()),
+        in_specs=[whole(), in_hbm(), anywhere(), anywhere(), whole()],
+        out_specs=(whole(), in_hbm()),
         scratch_shapes=[
             pltpu.VMEM(out_proj.shape, BF16),
             pltpu.VMEM(residual.shape, BF16),
             pltpu.VMEM(norm_gain.shape, F32),
-            pltpu.SemaphoreType.DMA((10,)),
+            pltpu.VMEM((slots, width), BF16),
+            pltpu.SemaphoreType.DMA((14,)),
         ],
         compiler_params=params(16),
         name="proj",
-    )(token_rows, out_proj, residual, norm_gain, own_routes.T)
-    arrived = lax.all_to_all(
-        outgoing.reshape(sp, slots // sp, width), "sp", split_axis=0, concat_axis=0, tiled=True
     )
-    arrived, share3 = lax.optimization_barrier((arrived, share3))
-    half = 3 * ff_own
-    core = lax.rem(lax.axis_index("tp"), 2)
-    share4 = lax.ppermute(lax.dynamic_slice_in_dim(share3, core * half, half, 0), "tp", around)
-    other3 = lax.ppermute(share3, "tp", partner)
-    other4 = lax.ppermute(share4, "tp", partner)
-    shares = (share0, share1, other1, share2, other2, share3, other3, share4, other4)
-    hidden_units = tp * ff_own
-    done = pl.pallas_call(
-        expert_kernel,
-        out_shape=shape((slots, width), BF16),
-        in_specs=[whole()] + [anywhere()] * len(shares),
-        out_specs=whole(),
-        scratch_shapes=[pltpu.VMEM((hidden_units, width), BF16)] * 3 + [pltpu.SemaphoreType.DMA((3 * tp,))],
-        compiler_params=params(32),
-        name="experts",
-    )(arrived.reshape(slots, width), *shares)
+    stream, outgoing = project(token_rows, out_proj, residual, norm_gain, own_routes.T)
+    r3b, e2b = around(r2b), across(r2b)
+    r4, e3a = around(r3a), across(r3a)
+    e3b, e4 = across(r3b), across(r4)
+    arrived = lax.all_to_all(outgoing.reshape(sp, slots // sp, width), "sp", split_axis=0, concat_axis=0, tiled=True)
+    arrived = arrived.reshape(slots, width)
+
+    def experts(shares, before, tail):
+        count = len(shares)
+        tall = count * ff_own
+        scratch = [pltpu.VMEM((tall, width), BF16)] * 3 + [pltpu.SemaphoreType.DMA((3 * count,))]
+        if tail:
+            scratch += [pltpu.VMEM((slots, width), BF16), pltpu.SemaphoreType.DMA((1,))]
+        head = before is None
+        return pl.pallas_call(
+            functools.partial(expert_kernel, pieces=count, head=head, tail=tail),
+            out_shape=shape((slots, width), BF16 if tail else F32),
+            in_specs=[whole()] + [in_hbm()] * count + [whole()] * (not head),
+            out_specs=in_hbm() if tail else whole(),
+            scratch_shapes=scratch,
+            compiler_params=params(24),
+            name="experts_tail" if tail else "experts_head",
+        )(arrived, *shares, *([] if head else [before]))
+
+    first = experts((own, other, r1a, e1a, r1b, e1b, r2a, e2a, r2b, e2b, r3a, e3a), None, False)
+    done = experts((r3b, e3b, r4, e4), first, True)
     returned = lax.all_to_all(
         done.reshape(sp, slots // sp, width), "sp", split_axis=0, concat_axis=0, tiled=True
     )
@@ -465,7 +493,7 @@
 
 def solution(mesh):
     return jax.shard_map(
-        on_device,
+        layer,
         mesh=mesh,
         in_specs=(
             P("sp", "tp"),

time: 192 us -> 158 us (0.82)
  Pallas kernels: 63.9 us -> 21.6 us
  blocking collectives: 42 us -> 14.3 us
  starting transfers between devices: 25.8 us -> 39.9 us
  waiting for transfers between devices: 50.9 us -> 62.5 us
  local copies, waits for them, and re-layouts: 8.85 us -> 18.8 us
    pallas_call x6 -> x7, Pallas kernels: 63.9 us -> 21.6 us  [the longest x2 8.95 us: experts(): pl.pallas_call(functools.partial(expert_kernel, pieces=count, head=head,...]
    all_to_all x2 -> x1, blocking collectives: 42 us -> 14.3 us  [layer(): lax.all_to_all(total, 'sp', split_axis=0, concat_axis=0, tiled=True)]
    all_to_all x2 -> x3, starting transfers between devices: 7.44 us -> 19.3 us  [the longest x1 8.04 us: layer(): lax.all_to_all(outgoing.reshape(sp, slots // sp, width), 'sp', split_axis...]
    unnamed x44, local copies, waits for them, and re-layouts: 6.62 us -> 17.1 us
    all_to_all x2 -> x3, waiting for transfers between devices: 35.2 us -> 42.7 us  [the longest x1 15.1 us: layer(): lax.all_to_all(done.reshape(sp, slots // sp, width), 'sp', split_axis=0,...]
    ppermute x13 -> x17, waiting for transfers between devices: 15.7 us -> 19.8 us  [the longest x7 15.3 us: around(): lax.ppermute(part, 'tp', [(i, (i + 2 - 4 * (i % 2)) % tp) for i in range(...]
    ppermute x13 -> x17, starting transfers between devices: 18.4 us -> 20.6 us  [the longest x7 11.1 us: around(): lax.ppermute(part, 'tp', [(i, (i + 2 - 4 * (i % 2)) % tp) for i in range(...]
  transfers between devices with their start and end apart: 15 -> 20, of which waited for: 8 -> 8; matrix products, arithmetic and copies ran while one was open for 1% -> 1% of each run, Pallas kernels for 4% -> 9%
where the time goes in v3:
time: 158 us; the launch traced here: 157 us
  waiting for transfers between devices  62.5 us (40%)
  starting transfers between devices  39.9 us (25%)
  Pallas kernels  21.6 us (14%)
  local copies, waits for them, and re-layouts  18.8 us (12%)
  blocking collectives  14.3 us (9%)
    unnamed x44, local copies, waits for them, and re-layouts  17.1 us
    ppermute x7, waiting for transfers between devices, around(): lax.ppermute(part, 'tp', [(i, (i + 2 - 4 * (i % 2)) % tp) for i in range(...  15.3 us
    all_to_all x1, waiting for transfers between devices, layer(): lax.all_to_all(done.reshape(sp, slots // sp, width), 'sp', split_axis=0,...  15.1 us
    all_to_all x1, waiting for transfers between devices, layer(): lax.all_to_all(outgoing.reshape(sp, slots // sp, width), 'sp', split_axis...  14.9 us
    all_to_all x1, blocking collectives, layer(): lax.all_to_all(total, 'sp', split_axis=0, concat_axis=0, tiled=True)  14.3 us
    all_to_all x1, waiting for transfers between devices, layer(): lax.all_to_all(mixed.reshape(tp, rows, channels), 'tp', split_axis=0, con...  12.7 us
    ppermute x7, starting transfers between devices, around(): lax.ppermute(part, 'tp', [(i, (i + 2 - 4 * (i % 2)) % tp) for i in range(...  11.1 us
    pallas_call x2, Pallas kernels, experts(): pl.pallas_call(functools.partial(expert_kernel, pieces=count, head=head,...  8.95 us
  transfers between devices with their start and end apart: 20, of which 8 were waited for; matrix products, arithmetic and copies ran while one was open for 1% of the time, Pallas kernels for 9%

profile of v3, /device:TPU:1, one launch (start us, length us, event | category | flops | bytes accessed | tf_op | source)
XLA Modules:
  0.0 157.3 jit_solution(9920243120211011146)
XLA Ops:
  0.0 2.0 %pack.1.refs_1_ = bf16[192,2048]{1,0:T(8,128)(2,1)} custom-call(bf16[64,2048]{1,0:T(8,128)(2,1)} %bitcast.19, bf16[64,2048]{1,0:T(8,128)(2,1)} %bitcast.20, bf16[64,2048]{1,0:T(8,128)(2,1)} %bitcast.21), custom_call_target="tpu_custom_call" | custom-call | tf_op jit(solution)/shard_map/pack/pallas_call | solution.py:364
  2.0 3.3 %collective-permute-start.3 = (bf16[192,2048]{1,0:T(8,128)(2,1)}, bf16[192,2048]{1,0:T(8,128)(2,1)S(1)}, u32[]{:S(2)}, u32[]{:S(2)}) collective-permute-start(bf16[192,2048]{1,0:T(8,128)(2,1)} %pack.1.refs_1_), channel_id=1, source_target_pairs={{0,1},{1,0},{2,3},{3,2},{4,5},{5,4},{6,7},{7,6},{8,9},{9,8},{10,11... | collective-permute-start | bytes 2359304 | tf_op jit(solution)/shard_map/ppermute | solution.py:377
  5.3 3.9 %collective-permute-start.2 = (bf16[192,2048]{1,0:T(8,128)(2,1)}, bf16[192,2048]{1,0:T(8,128)(2,1)S(1)}, u32[]{:S(2)}, u32[]{:S(2)}) collective-permute-start(bf16[192,2048]{1,0:T(8,128)(2,1)} %pack.1.refs_1_), channel_id=1, source_target_pairs={{0,2},{1,15},{2,4},{3,1},{4,6},{5,3},{6,8},{7,5},{8,10},{9,7},{10,... | collective-permute-start | bytes 2359304 | tf_op jit(solution)/shard_map/ppermute | solution.py:374
  9.9 3.1 %collective-permute-start = (bf16[2,128]{1,0:T(2,128)(2,1)S(1)}, bf16[2,128]{1,0:T(2,128)(2,1)S(1)}, u32[]{:S(2)}, u32[]{:S(2)}) collective-permute-start(bf16[2,128]{1,0:T(2,128)(2,1)S(1)} %get-tuple-element.30), channel_id=1, source_target_pairs={{0,16},{16,32},{32,48},{48,64},{64,80},{80,96},{96,112},{112,128},... | collective-permute-start | bytes 1544 | tf_op jit(solution)/shard_map/ppermute | solution.py:360
  14.3 3.3 %collective-permute-done.1.after = bf16[2,128]{1,0:T(2,128)(2,1)S(1)} collective-permute-done((bf16[2,128]{1,0:T(2,128)(2,1)S(1)}, bf16[2,128]{1,0:T(2,128)(2,1)S(1)}, u32[]{:S(2)}, u32[]{:S(2)}) %collective-permute-start.1) | collective-permute-done | bytes 544 | tf_op jit(solution)/shard_map/ppermute | solution.py:361
  23.7 3.8 %scan.1 = (f32[1024,128]{1,0:T(8,128)S(1)}, f32[1024,128]{1,0:T(8,128)S(1)}, f32[1024,128]{1,0:T(8,128)S(1)}, f32[1024,128]{1,0:T(8,128)S(1)}, f32[32,128]{1,0:T(8,128)S(1)}, /*index=5*/f32[16,8,128]{2,1,0:T(8,128)S(1)}) custom-call(bf16[1024,128]{1,0:T(8,128)(2,1)S(1)} %copy-done.7, bf16[2,128]{1,0:T(2,128)(2,1)S(1)} %collective-permute-done.before, ...), custom_call_target="tpu_custom_call" | custom-call | tf_op jit(solution)/shard_map/scan/pallas_call | solution.py:385
  29.1 14.3 %all_to_all.20.totals = f32[16,8,128]{2,1,0:T(8,128)S(1)} all-to-all(f32[16,8,128]{2,1,0:T(8,128)S(1)} %get-tuple-element.23), channel_id=1, replica_groups=mesh['sp'=16,'tp'=16] {'sp'}, dimensions={0} | all-to-all | bytes 131072 | tf_op jit(solution)/shard_map/all_to_all | solution.py:416
  44.1 3.0 %collective-permute-done.8.refs_7_ = bf16[192,2048]{1,0:T(8,128)(2,1)S(1)} collective-permute-done((bf16[192,2048]{1,0:T(8,128)(2,1)S(1)}, bf16[192,2048]{1,0:T(8,128)(2,1)S(1)}, u32[]{:S(2)}, u32[]{:S(2)}) %collective-permute-start.8) | collective-permute-done | bytes 786464 | tf_op jit(solution)/shard_map/ppermute | solution.py:374
  48.1 1.6 %collective-permute-start.9 = (bf16[192,2048]{1,0:T(8,128)(2,1)S(1)}, bf16[192,2048]{1,0:T(8,128)(2,1)}, u32[]{:S(2)}, u32[]{:S(2)}) collective-permute-start(bf16[192,2048]{1,0:T(8,128)(2,1)S(1)} %collective-permute-done.8.refs_7_), channel_id=1, source_target_pairs={{0,2},{1,15},{2,4},{3,1},{4,6},{5,3},{6,8},{7,5},{8,10},{9,7},{10,... | collective-permute-start | bytes 2359304 | tf_op jit(solution)/shard_map/ppermute | solution.py:374
  50.2 5.5 %collective-permute-done.5.refs_9_ = bf16[192,2048]{1,0:T(8,128)(2,1)} collective-permute-done((bf16[192,2048]{1,0:T(8,128)(2,1)}, bf16[192,2048]{1,0:T(8,128)(2,1)}, u32[]{:S(2)}, u32[]{:S(2)}) %collective-permute-start.5) | collective-permute-done | bytes 786464 | tf_op jit(solution)/shard_map/ppermute | solution.py:374
  55.7 1.6 %collective-permute-start.6 = (bf16[192,2048]{1,0:T(8,128)(2,1)}, bf16[192,2048]{1,0:T(8,128)(2,1)}, u32[]{:S(2)}, u32[]{:S(2)}) collective-permute-start(bf16[192,2048]{1,0:T(8,128)(2,1)} %collective-permute-done.5.refs_9_), channel_id=1, source_target_pairs={{0,2},{1,15},{2,4},{3,1},{4,6},{5,3},{6,8},{7,5},{8,10},{9,7},{10,... | collective-permute-start | bytes 2359304 | tf_op jit(solution)/shard_map/ppermute | solution.py:374
  57.3 6.8 %collective-permute-done.9.refs_11_ = bf16[192,2048]{1,0:T(8,128)(2,1)} collective-permute-done((bf16[192,2048]{1,0:T(8,128)(2,1)S(1)}, bf16[192,2048]{1,0:T(8,128)(2,1)}, u32[]{:S(2)}, u32[]{:S(2)}) %collective-permute-start.9) | collective-permute-done | bytes 786464 | tf_op jit(solution)/shard_map/ppermute | solution.py:374
  64.1 1.6 %collective-permute-start.10 = (bf16[192,2048]{1,0:T(8,128)(2,1)}, bf16[192,2048]{1,0:T(8,128)(2,1)}, u32[]{:S(2)}, u32[]{:S(2)}) collective-permute-start(bf16[192,2048]{1,0:T(8,128)(2,1)} %collective-permute-done.9.refs_11_), channel_id=1, source_target_pairs={{0,2},{1,15},{2,4},{3,1},{4,6},{5,3},{6,8},{7,5},{8,10},{9,7},{10,... | collective-permute-start | bytes 2359304 | tf_op jit(solution)/shard_map/ppermute | solution.py:374
  67.9 7.6 %all-to-all-start.1 = ((bf16[16,64,128]{2,1,0:T(8,128)(2,1)}), bf16[16,64,128]{2,1,0:T(8,128)(2,1)S(1)}, u32[]{:S(2)}, u32[]{:S(2)}) async-start(bf16[16,64,128]{2,1,0:T(8,128)(2,1)} %bitcast.6), calls=%async_computation.1 | async-start | bytes 524288 | tf_op jit(solution)/shard_map/all_to_all | solution.py:432
  75.8 12.7 %all-to-all-done.1.mixed = bf16[16,64,128]{2,1,0:T(8,128)(2,1)S(1)} async-done(((bf16[16,64,128]{2,1,0:T(8,128)(2,1)}), bf16[16,64,128]{2,1,0:T(8,128)(2,1)S(1)}, u32[]{:S(2)}, u32[]{:S(2)}) %all-to-all-start.1) | async-done | bytes 262176 | tf_op jit(solution)/shard_map/all_to_all | solution.py:432
  88.4 3.4 %copy-done.1 = bf16[2048,2048]{1,0:T(8,128)(2,1)S(1)} copy-done((bf16[2048,2048]{1,0:T(8,128)(2,1)S(1)}, bf16[2048,2048]{1,0:T(8,128)(2,1)}, u32[]{:S(2)}) %copy-start.1) | copy-done | bytes 8388632
  93.5 4.0 %proj.1 = (bf16[64,2048]{1,0:T(8,128)(2,1)S(1)}, bf16[256,2048]{1,0:T(8,128)(2,1)}) custom-call(bf16[16,64,128]{2,1,0:T(8,128)(2,1)S(1)} %all-to-all-done.1.mixed, bf16[2048,2048]{1,0:T(8,128)(2,1)S(1)} %copy-done.1, bf16[64,2048]{1,0:T(8,128)(2,1)S(1)} %copy-done.8, f32[3,2048]{1,0:T(4,128)S(1)} %copy-done.12, s32[2,64]{1,0:T(2,128)S(1)} %copy.19.routes), custom_call_target="tpu_custom_call" | custom-call | tf_op jit(solution)/shard_map/proj/pallas_call | solution.py:455
  98.3 8.0 %all-to-all-start.2 = ((bf16[16,16,2048]{2,1,0:T(8,128)(2,1)}), bf16[16,16,2048]{2,1,0:T(8,128)(2,1)S(1)}, u32[]{:S(2)}, u32[]{:S(2)}) async-start(bf16[16,16,2048]{2,1,0:T(8,128)(2,1)} %bitcast.8), calls=%async_computation.2 | async-start | bytes 2097152 | tf_op jit(solution)/shard_map/all_to_all | solution.py:459
  109.8 14.9 %all-to-all-done.2 = bf16[16,16,2048]{2,1,0:T(8,128)(2,1)S(1)} async-done(((bf16[16,16,2048]{2,1,0:T(8,128)(2,1)}), bf16[16,16,2048]{2,1,0:T(8,128)(2,1)S(1)}, u32[]{:S(2)}, u32[]{:S(2)}) %all-to-all-start.2) | async-done | bytes 1048608 | tf_op jit(solution)/shard_map/all_to_all | solution.py:459
  127.0 4.9 %experts_head.1.refs_5_ = f32[256,2048]{1,0:T(8,128)S(1)} custom-call(bf16[256,2048]{1,0:T(8,128)(2,1)S(1)} %bitcast.14, bf16[192,2048]{1,0:T(8,128)(2,1)S(1)} %copy-done.2, bf16[192,2048]{1,0:T(8,128)(2,1)S(1)} %collective-permute-done.3.refs_2_, bf16[192,2048]{1,0:T(8,128)(2,1)S(1)} %collective-permute-done.2.refs_3_, ...), custom_call_target="tpu_custom_call" | custom-call | tf_op jit(solution)/shard_map/experts_head/pallas_call | solution.py:469
  131.9 4.1 %experts_tail.1 = bf16[256,2048]{1,0:T(8,128)(2,1)} custom-call(bf16[256,2048]{1,0:T(8,128)(2,1)S(1)} %bitcast.15, bf16[192,2048]{1,0:T(8,128)(2,1)} %collective-permute-done.6.refs_1_, bf16[192,2048]{1,0:T(8,128)(2,1)} %collective-permute-done.7.refs_2_, bf16[192,2048]{1,0:T(8,128)(2,1)} %collective-permute-done.10.refs_3_, ...), custom_call_target="tpu_custom_call" | custom-call | tf_op jit(solution)/shard_map/experts_tail/pallas_call | solution.py:469
  136.0 3.7 %all-to-all-start.3 = ((bf16[16,16,2048]{2,1,0:T(8,128)(2,1)}), bf16[16,16,2048]{2,1,0:T(8,128)(2,1)S(1)}, u32[]{:S(2)}, u32[]{:S(2)}) async-start(bf16[16,16,2048]{2,1,0:T(8,128)(2,1)} %bitcast.10), calls=%async_computation.3 | async-start | bytes 2097152 | tf_op jit(solution)/shard_map/all_to_all | solution.py:481
  140.5 15.1 %all-to-all-done.3 = bf16[16,16,2048]{2,1,0:T(8,128)(2,1)S(1)} async-done(((bf16[16,16,2048]{2,1,0:T(8,128)(2,1)}), bf16[16,16,2048]{2,1,0:T(8,128)(2,1)S(1)}, u32[]{:S(2)}, u32[]{:S(2)}) %all-to-all-start.3) | async-done | bytes 1048608 | tf_op jit(solution)/shard_map/all_to_all | solution.py:481
  155.7 1.6 %combine.1 = bf16[64,2048]{1,0:T(8,128)(2,1)} custom-call(bf16[256,2048]{1,0:T(8,128)(2,1)S(1)} %bitcast.16, bf16[64,2048]{1,0:T(8,128)(2,1)S(1)} %copy-done.10, f32[3,2048]{1,0:T(4,128)S(1)} %copy-done.13, s32[64,2]{1,0:T(8,128)S(1)} %copy.21.routes, f32[64,2]{1,0:T(8,128)S(1)} %copy.22.weights), custom_call_target="tpu_custom_call" | custom-call | tf_op jit(solution)/shard_map/combine/pallas_call | solution.py:484
  (72 shorter events, 23.2 us)
Async XLA Ops:
  0.0 75.5 %copy-start = (s32[1024,2]{0,1:T(2,128)S(1)}, s32[1024,2]{0,1:T(2,128)}, u32[]{:S(2)}) copy-start(s32[1024,2]{0,1:T(2,128)} %param.29) | copy-start | bytes 24580
  2.0 122.7 %copy-start.2 = (bf16[192,2048]{1,0:T(8,128)(2,1)S(1)}, bf16[192,2048]{1,0:T(8,128)(2,1)}, u32[]{:S(2)}) copy-start(bf16[192,2048]{1,0:T(8,128)(2,1)} %pack.1.refs_1_) | copy-start | bytes 2359300
  2.0 25.5 %collective-permute-start.3 = (bf16[192,2048]{1,0:T(8,128)(2,1)}, bf16[192,2048]{1,0:T(8,128)(2,1)S(1)}, u32[]{:S(2)}, u32[]{:S(2)}) collective-permute-start(bf16[192,2048]{1,0:T(8,128)(2,1)} %pack.1.refs_1_), channel_id=1, source_target_pairs={{0,1},{1,0},{2,3},{3,2},{4,5},{5,4},{6,7},{7,6},{8,9},{9,8},{10,11... | collective-permute-start | bytes 2359304 | tf_op jit(solution)/shard_map/ppermute | solution.py:377
  5.3 23.0 %collective-permute-start.2 = (bf16[192,2048]{1,0:T(8,128)(2,1)}, bf16[192,2048]{1,0:T(8,128)(2,1)S(1)}, u32[]{:S(2)}, u32[]{:S(2)}) collective-permute-start(bf16[192,2048]{1,0:T(8,128)(2,1)} %pack.1.refs_1_), channel_id=1, source_target_pairs={{0,2},{1,15},{2,4},{3,1},{4,6},{5,3},{6,8},{7,5},{8,10},{9,7},{10,... | collective-permute-start | bytes 2359304 | tf_op jit(solution)/shard_map/ppermute | solution.py:374
  9.9 4.4 %collective-permute-start = (bf16[2,128]{1,0:T(2,128)(2,1)S(1)}, bf16[2,128]{1,0:T(2,128)(2,1)S(1)}, u32[]{:S(2)}, u32[]{:S(2)}) collective-permute-start(bf16[2,128]{1,0:T(2,128)(2,1)S(1)} %get-tuple-element.30), channel_id=1, source_target_pairs={{0,16},{16,32},{32,48},{48,64},{64,80},{80,96},{96,112},{112,128},... | collective-permute-start | bytes 1544 | tf_op jit(solution)/shard_map/ppermute | solution.py:360
  13.0 4.6 %collective-permute-start.1 = (bf16[2,128]{1,0:T(2,128)(2,1)S(1)}, bf16[2,128]{1,0:T(2,128)(2,1)S(1)}, u32[]{:S(2)}, u32[]{:S(2)}) collective-permute-start(bf16[2,128]{1,0:T(2,128)(2,1)S(1)} %get-tuple-element.29), channel_id=1, source_target_pairs={{16,0},{32,16},{48,32},{64,48},{80,64},{96,80},{112,96},{128,112},... | collective-permute-start | bytes 1544 | tf_op jit(solution)/shard_map/ppermute | solution.py:361
  27.5 15.9 %collective-permute-start.4 = (bf16[192,2048]{1,0:T(8,128)(2,1)S(1)}, bf16[192,2048]{1,0:T(8,128)(2,1)}, u32[]{:S(2)}, u32[]{:S(2)}) collective-permute-start(bf16[192,2048]{1,0:T(8,128)(2,1)S(1)} %collective-permute-done.3.refs_2_), channel_id=1, source_target_pairs={{0,2},{1,15},{2,4},{3,1},{4,6},{5,3},{6,8},{7,5},{8,10},{9,7},{10,... | collective-permute-start | bytes 2359304 | tf_op jit(solution)/shard_map/ppermute | solution.py:374
  28.3 18.8 %collective-permute-start.8 = (bf16[192,2048]{1,0:T(8,128)(2,1)S(1)}, bf16[192,2048]{1,0:T(8,128)(2,1)S(1)}, u32[]{:S(2)}, u32[]{:S(2)}) collective-permute-start(bf16[192,2048]{1,0:T(8,128)(2,1)S(1)} %collective-permute-done.2.refs_3_), channel_id=1, source_target_pairs={{0,2},{1,15},{2,4},{3,1},{4,6},{5,3},{6,8},{7,5},{8,10},{9,7},{10,... | collective-permute-start | bytes 2359304 | tf_op jit(solution)/shard_map/ppermute | solution.py:374
  43.4 12.3 %collective-permute-start.5 = (bf16[192,2048]{1,0:T(8,128)(2,1)}, bf16[192,2048]{1,0:T(8,128)(2,1)}, u32[]{:S(2)}, u32[]{:S(2)}) collective-permute-start(bf16[192,2048]{1,0:T(8,128)(2,1)} %collective-permute-done.4.refs_5_), channel_id=1, source_target_pairs={{0,2},{1,15},{2,4},{3,1},{4,6},{5,3},{6,8},{7,5},{8,10},{9,7},{10,... | collective-permute-start | bytes 2359304 | tf_op jit(solution)/shard_map/ppermute | solution.py:374
  48.1 16.1 %collective-permute-start.9 = (bf16[192,2048]{1,0:T(8,128)(2,1)S(1)}, bf16[192,2048]{1,0:T(8,128)(2,1)}, u32[]{:S(2)}, u32[]{:S(2)}) collective-permute-start(bf16[192,2048]{1,0:T(8,128)(2,1)S(1)} %collective-permute-done.8.refs_7_), channel_id=1, source_target_pairs={{0,2},{1,15},{2,4},{3,1},{4,6},{5,3},{6,8},{7,5},{8,10},{9,7},{10,... | collective-permute-start | bytes 2359304 | tf_op jit(solution)/shard_map/ppermute | solution.py:374
  49.7 56.9 %collective-permute-start.12 = (bf16[192,2048]{1,0:T(8,128)(2,1)S(1)}, bf16[192,2048]{1,0:T(8,128)(2,1)}, u32[]{:S(2)}, u32[]{:S(2)}) collective-permute-start(bf16[192,2048]{1,0:T(8,128)(2,1)S(1)} %collective-permute-done.2.refs_3_), channel_id=1, source_target_pairs={{0,1},{1,0},{2,3},{3,2},{4,5},{5,4},{6,7},{7,6},{8,9},{9,8},{10,11... | collective-permute-start | bytes 2359304 | tf_op jit(solution)/shard_map/ppermute | solution.py:377
  50.1 56.8 %collective-permute-start.13 = (bf16[192,2048]{1,0:T(8,128)(2,1)}, bf16[192,2048]{1,0:T(8,128)(2,1)}, u32[]{:S(2)}, u32[]{:S(2)}) collective-permute-start(bf16[192,2048]{1,0:T(8,128)(2,1)} %collective-permute-done.4.refs_5_), channel_id=1, source_target_pairs={{0,1},{1,0},{2,3},{3,2},{4,5},{5,4},{6,7},{7,6},{8,9},{9,8},{10,11... | collective-permute-start | bytes 2359304 | tf_op jit(solution)/shard_map/ppermute | solution.py:377
  55.7 51.5 %collective-permute-start.6 = (bf16[192,2048]{1,0:T(8,128)(2,1)}, bf16[192,2048]{1,0:T(8,128)(2,1)}, u32[]{:S(2)}, u32[]{:S(2)}) collective-permute-start(bf16[192,2048]{1,0:T(8,128)(2,1)} %collective-permute-done.5.refs_9_), channel_id=1, source_target_pairs={{0,2},{1,15},{2,4},{3,1},{4,6},{5,3},{6,8},{7,5},{8,10},{9,7},{10,... | collective-permute-start | bytes 2359304 | tf_op jit(solution)/shard_map/ppermute | solution.py:374
  64.1 43.3 %collective-permute-start.10 = (bf16[192,2048]{1,0:T(8,128)(2,1)}, bf16[192,2048]{1,0:T(8,128)(2,1)}, u32[]{:S(2)}, u32[]{:S(2)}) collective-permute-start(bf16[192,2048]{1,0:T(8,128)(2,1)} %collective-permute-done.9.refs_11_), channel_id=1, source_target_pairs={{0,2},{1,15},{2,4},{3,1},{4,6},{5,3},{6,8},{7,5},{8,10},{9,7},{10,... | collective-permute-start | bytes 2359304 | tf_op jit(solution)/shard_map/ppermute | solution.py:374
  67.9 20.5 %all-to-all-start.1 = ((bf16[16,64,128]{2,1,0:T(8,128)(2,1)}), bf16[16,64,128]{2,1,0:T(8,128)(2,1)S(1)}, u32[]{:S(2)}, u32[]{:S(2)}) async-start(bf16[16,64,128]{2,1,0:T(8,128)(2,1)} %bitcast.6), calls=%async_computation.1 | async-start | bytes 524288 | tf_op jit(solution)/shard_map/all_to_all | solution.py:432
  98.3 26.4 %all-to-all-start.2 = ((bf16[16,16,2048]{2,1,0:T(8,128)(2,1)}), bf16[16,16,2048]{2,1,0:T(8,128)(2,1)S(1)}, u32[]{:S(2)}, u32[]{:S(2)}) async-start(bf16[16,16,2048]{2,1,0:T(8,128)(2,1)} %bitcast.8), calls=%async_computation.2 | async-start | bytes 2097152 | tf_op jit(solution)/shard_map/all_to_all | solution.py:459
  106.3 2.6 %collective-permute-start.14 = (bf16[192,2048]{1,0:T(8,128)(2,1)}, bf16[192,2048]{1,0:T(8,128)(2,1)S(1)}, u32[]{:S(2)}, u32[]{:S(2)}) collective-permute-start(bf16[192,2048]{1,0:T(8,128)(2,1)} %copy-done.3), channel_id=1, source_target_pairs={{0,1},{1,0},{2,3},{3,2},{4,5},{5,4},{6,7},{7,6},{8,9},{9,8},{10,11... | collective-permute-start | bytes 2359304 | tf_op jit(solution)/shard_map/ppermute | solution.py:377
  106.6 18.2 %collective-permute-start.15 = (bf16[192,2048]{1,0:T(8,128)(2,1)}, bf16[192,2048]{1,0:T(8,128)(2,1)}, u32[]{:S(2)}, u32[]{:S(2)}) collective-permute-start(bf16[192,2048]{1,0:T(8,128)(2,1)} %collective-permute-done.5.refs_9_), channel_id=1, source_target_pairs={{0,1},{1,0},{2,3},{3,2},{4,5},{5,4},{6,7},{7,6},{8,9},{9,8},{10,11... | collective-permute-start | bytes 2359304 | tf_op jit(solution)/shard_map/ppermute | solution.py:377
  106.9 17.8 %collective-permute-start.16 = (bf16[192,2048]{1,0:T(8,128)(2,1)}, bf16[192,2048]{1,0:T(8,128)(2,1)}, u32[]{:S(2)}, u32[]{:S(2)}) collective-permute-start(bf16[192,2048]{1,0:T(8,128)(2,1)} %collective-permute-done.9.refs_11_), channel_id=1, source_target_pairs={{0,1},{1,0},{2,3},{3,2},{4,5},{5,4},{6,7},{7,6},{8,9},{9,8},{10,11... | collective-permute-start | bytes 2359304 | tf_op jit(solution)/shard_map/ppermute | solution.py:377
  107.2 24.6 %collective-permute-start.7 = (bf16[192,2048]{1,0:T(8,128)(2,1)}, bf16[192,2048]{1,0:T(8,128)(2,1)}, u32[]{:S(2)}, u32[]{:S(2)}) collective-permute-start(bf16[192,2048]{1,0:T(8,128)(2,1)} %collective-permute-done.6.refs_1_), channel_id=1, source_target_pairs={{0,1},{1,0},{2,3},{3,2},{4,5},{5,4},{6,7},{7,6},{8,9},{9,8},{10,11... | collective-permute-start | bytes 2359304 | tf_op jit(solution)/shard_map/ppermute | solution.py:377
  107.5 24.4 %collective-permute-start.11 = (bf16[192,2048]{1,0:T(8,128)(2,1)}, bf16[192,2048]{1,0:T(8,128)(2,1)}, u32[]{:S(2)}, u32[]{:S(2)}) collective-permute-start(bf16[192,2048]{1,0:T(8,128)(2,1)} %collective-permute-done.10.refs_3_), channel_id=1, source_target_pairs={{0,1},{1,0},{2,3},{3,2},{4,5},{5,4},{6,7},{7,6},{8,9},{9,8},{10,11... | collective-permute-start | bytes 2359304 | tf_op jit(solution)/shard_map/ppermute | solution.py:377
  127.0 28.7 %copy-start.13 = (f32[3,2048]{1,0:T(4,128)S(1)}, f32[3,2048]{1,0:T(4,128)}, u32[]{:S(2)}) copy-start(f32[3,2048]{1,0:T(4,128)} %gain.1) | copy-start | bytes 73732
  131.9 23.8 %copy-start.10 = (bf16[64,2048]{1,0:T(8,128)(2,1)S(1)}, bf16[64,2048]{1,0:T(8,128)(2,1)}, u32[]{:S(2)}) copy-start(bf16[64,2048]{1,0:T(8,128)(2,1)} %copy-done.9) | copy-start | bytes 786436
  136.0 19.7 %all-to-all-start.3 = ((bf16[16,16,2048]{2,1,0:T(8,128)(2,1)}), bf16[16,16,2048]{2,1,0:T(8,128)(2,1)S(1)}, u32[]{:S(2)}, u32[]{:S(2)}) async-start(bf16[16,16,2048]{2,1,0:T(8,128)(2,1)} %bitcast.10), calls=%async_computation.3 | async-start | bytes 2097152 | tf_op jit(solution)/shard_map/all_to_all | solution.py:481
  (17 other events, 17.0 us)

commit v4 on v3

--- a/solution.py
+++ b/solution.py
@@ -12,15 +12,9 @@
 F32 = jnp.float32
 BF16 = jnp.bfloat16
 SEGS = 8
-VMEM = pltpu.MemorySpace.VMEM
-
-
-def whole():
-    return pl.BlockSpec(memory_space=VMEM)
-
-
-def params(mib):
-    return pltpu.CompilerParams(vmem_limit_bytes=mib * 1024 * 1024)
+
+
+FULL = pltpu.CompilerParams(vmem_limit_bytes=67043328)
 
 
 def anywhere():
@@ -57,14 +51,18 @@
 
 
 def scan_kernel(
-    mix_h, before, after, conv_w_h, conv_b_h, decay_param_h, recur_gate_h, recur_bias_h, input_gate_h, input_bias_h,
-    h_f, p_f, h_b, p_b, seg, total,
+    mix_h, before_h, after_h, conv_w_h, conv_b_h, decay_param_h, recur_gate_h, recur_bias_h, input_gate_h, input_bias_h,
+    h_f_h, p_f_h, h_b_h, p_b_h, seg_h, total_h,
     padded, conv, split, wide, wlow, pre, a_f, b_f, a_b, b_b,
-    mix, conv_w, conv_b, decay_param, recur_gate, recur_bias, input_gate, input_bias, sems,
+    mix, before, after, conv_w, conv_b, decay_param, recur_gate, recur_bias, input_gate, input_bias,
+    h_f, p_f, h_b, p_b, seg, total, sems,
 ):
     for copy in fetched(
-        (mix_h, conv_w_h, conv_b_h, decay_param_h, recur_gate_h, recur_bias_h, input_gate_h, input_bias_h),
-        (mix, conv_w, conv_b, decay_param, recur_gate, recur_bias, input_gate, input_bias),
+        (
+            mix_h, before_h, after_h, conv_w_h, conv_b_h, decay_param_h,
+            recur_gate_h, recur_bias_h, input_gate_h, input_bias_h,
+        ),
+        (mix, before, after, conv_w, conv_b, decay_param, recur_gate, recur_bias, input_gate, input_bias),
         sems,
     ):
         copy.wait()
@@ -167,10 +165,15 @@
         sums += [factor, enter]
     both = jnp.concatenate(sums + [jnp.zeros((4, 128), F32)], axis=0)
     total[...] = jnp.broadcast_to(both[None], total.shape)
-
-
-def mix_kernel(h_f, p_f, h_b, p_b, seg, totals, gate_h, out, natural, gate_in, sems):
-    (copy,) = fetched((gate_h,), (gate_in,), sems)
+    for copy in fetched((h_f, p_f, h_b, p_b, seg, total), (h_f_h, p_f_h, h_b_h, p_b_h, seg_h, total_h), sems, 10):
+        copy.wait()
+
+
+def mix_kernel(*refs):
+    sources, out_h, natural, buffers, out, sems = refs[:7], refs[7], refs[8], refs[9:16], refs[16], refs[17]
+    h_f, p_f, h_b, p_b, seg, totals, gate_in = buffers
+    for copy in fetched(sources, buffers, sems):
+        copy.wait()
     length = out.shape[0]
     step = length // SEGS
     stride = step + 8
@@ -194,25 +197,31 @@
         return carry
 
     lax.fori_loop(0, step, place, 0, unroll=8)
-    copy.wait()
     for s in range(SEGS):
         gate = gate_in[s * step : (s + 1) * step, :].astype(F32)
         out[s * step : (s + 1) * step, :] = (
             natural[s * stride : s * stride + step, :] * jax.nn.gelu(gate)
         ).astype(BF16)
+    (copy,) = fetched((out,), (out_h,), sems, 7)
+    copy.wait()
 
 
 def scaled(values, gain):
     return values * lax.rsqrt(jnp.mean(values * values, axis=-1, keepdims=True) + EPSILON) * gain
 
 
-def proj_kernel(mixed, weights_h, residual_h, gain_h, routes, stream_out, outgoing_h, weights, residual, gain, outgoing, sems):
+def proj_kernel(
+    mixed_h, weights_h, residual_h, gain_h, routes_h, stream_h, outgoing_h,
+    mixed, weights, residual, gain, routes, stream_out, outgoing, sems,
+):
+    (mixed_copy,) = fetched((mixed_h,), (mixed,), sems, 15)
     width = weights.shape[0]
     blocks = 8
     block = width // blocks
     parts = [(weights_h.at[pl.ds(k * block, block)], weights.at[pl.ds(k * block, block)]) for k in range(blocks)]
     loads = fetched(*zip(*parts), sems)
-    others = fetched((residual_h, gain_h), (residual, gain), sems, blocks)
+    others = fetched((residual_h, gain_h, routes_h), (residual, gain, routes), sems, blocks)
+    mixed_copy.wait()
     acc = jnp.zeros(residual.shape, F32)
     per = mixed.shape[0] // blocks
     for k in range(blocks):
@@ -224,6 +233,7 @@
     proj = acc.astype(BF16).astype(F32)
     stream = (residual[...].astype(F32) + scaled(proj, gain[0:1, :])).astype(BF16)
     stream_out[...] = stream
+    sent = fetched((stream_out,), (stream_h,), sems, 16)
     normed = scaled(stream.astype(F32), gain[1:2, :]).astype(BF16)
     rows = normed.shape[0]
     slots = outgoing.shape[0]
@@ -240,11 +250,10 @@
     slot1 = second * capacity + jnp.sum(hit1 * earlier, axis=0, keepdims=True).astype(jnp.int32)
     places = lax.broadcasted_iota(jnp.int32, (slots, rows), 0)
     pick = jnp.where(jnp.logical_or(places == slot0, places == slot1), 1.0, 0.0).astype(BF16)
-    sent = []
     for k in range(4):
         part = slice(k * 512, (k + 1) * 512)
         outgoing[:, part] = jnp.dot(pick, normed[:, part], preferred_element_type=F32).astype(BF16)
-        sent += fetched([outgoing.at[:, part]], [outgoing_h.at[:, part]], sems, 10 + k)
+        sent += fetched([outgoing.at[:, part]], [outgoing_h.at[:, part]], sems, 11 + k)
     for copy in sent:
         copy.wait()
 
@@ -267,7 +276,8 @@
     rest = refs[1 + pieces :]
     if not head:
         before, rest = rest[0], rest[1:]
-    out, gate_w, up_w, down_w, sems = rest[:5]
+    out, gate_w, up_w, down_w, held, acc_held, sems, extra = rest
+    starts = fetched((tokens,), (held,), extra) + ([] if head else fetched((before,), (acc_held,), extra, 1))
     ff = shares[0].shape[0] // 3
     copies = [
         fetched(
@@ -278,8 +288,10 @@
         )
         for at, share in enumerate(shares)
     ]
-    x = tokens[...]
-    acc = jnp.zeros(x.shape, F32) if head else before[...]
+    for copy in starts:
+        copy.wait()
+    x = held[...]
+    acc = jnp.zeros(x.shape, F32) if head else acc_held[...]
     block = 256
     last = (((1,), (1,)), ((), ()))
     for k in range(pieces * ff // block):
@@ -291,17 +303,17 @@
         up = lax.dot_general(x, up_w[rows, :], last, preferred_element_type=F32)
         hidden = (jax.nn.silu(gate) * up).astype(BF16)
         acc = acc + jnp.dot(hidden, down_w[rows, :], preferred_element_type=F32)
-    if tail:
-        result, done = rest[5:]
-        result[...] = acc.astype(BF16)
-        copy = pltpu.make_async_copy(result, out, done.at[0])
-        copy.start()
-        copy.wait()
-    else:
-        out[...] = acc
-
-
-def combine_kernel(values, stream, gain, routes, weights, out):
+    result = held if tail else acc_held
+    result[...] = acc.astype(result.dtype)
+    (copy,) = fetched((result,), (out,), extra, 2)
+    copy.wait()
+
+
+def combine_kernel(*refs):
+    sources, out_h, buffers, out, sems = refs[:5], refs[5], refs[6:11], refs[11], refs[12]
+    values, stream, gain, routes, weights = buffers
+    for copy in fetched(sources, buffers, sems):
+        copy.wait()
     rows = stream.shape[0]
     slots = values.shape[0]
     experts = 16
@@ -327,6 +339,8 @@
     mixture = parts[0:rows] + (parts[rows : 2 * rows] + parts[2 * rows : 3 * rows])
     mixture = mixture.astype(BF16).astype(F32)
     out[...] = (stream[...].astype(F32) + scaled(mixture, gain[2:3, :])).astype(BF16)
+    (copy,) = fetched((out,), (out_h,), sems, 5)
+    copy.wait()
 
 
 def shape(dims, dtype):
@@ -367,6 +381,7 @@
         in_specs=[in_hbm()] * 3,
         out_specs=in_hbm(),
         scratch_shapes=[pltpu.VMEM(piece.shape, BF16), pltpu.SemaphoreType.DMA((6,))],
+        compiler_params=FULL,
         name="pack",
     )(jnp.swapaxes(exp_gate, 1, 2)[0], jnp.swapaxes(exp_up, 1, 2)[0], exp_down[0])
 
@@ -385,8 +400,8 @@
     h_f, p_f, h_b, p_b, seg, total = pl.pallas_call(
         scan_kernel,
         out_shape=(state, state, state, state, shape((32, 128), F32), shape((sp, 8, 128), F32)),
-        in_specs=[anywhere(), whole(), whole()] + [anywhere()] * 7,
-        out_specs=(whole(),) * 6,
+        in_specs=[anywhere()] * 10,
+        out_specs=(anywhere(),) * 6,
         scratch_shapes=[
             pltpu.VMEM((length + 16, 128), F32),
             pltpu.VMEM((length, 128), F32),
@@ -399,6 +414,8 @@
             pltpu.VMEM((lines, 128), F32),
             pltpu.VMEM((lines, 128), F32),
             pltpu.VMEM(mix_in.shape, BF16),
+            pltpu.VMEM(before.shape, BF16),
+            pltpu.VMEM(after.shape, BF16),
             pltpu.VMEM(conv_w.shape, F32),
             pltpu.VMEM((1, 128), F32),
             pltpu.VMEM(decay_param.shape, F32),
@@ -406,9 +423,15 @@
             pltpu.VMEM(recur_bias.shape, F32),
             pltpu.VMEM(input_gate.shape, F32),
             pltpu.VMEM(input_bias.shape, F32),
-            pltpu.SemaphoreType.DMA((8,)),
+            pltpu.VMEM(state.shape, F32),
+            pltpu.VMEM(state.shape, F32),
+            pltpu.VMEM(state.shape, F32),
+            pltpu.VMEM(state.shape, F32),
+            pltpu.VMEM((32, 128), F32),
+            pltpu.VMEM((sp, 8, 128), F32),
+            pltpu.SemaphoreType.DMA((16,)),
         ],
-        compiler_params=params(20),
+        compiler_params=FULL,
         name="scan",
     )(mix_in, before, after, conv_w, conv_b[None], decay_param, recur_gate, recur_bias, input_gate, input_bias)
     total, r1a = lax.optimization_barrier((total, r1a))
@@ -419,14 +442,18 @@
     mixed = pl.pallas_call(
         mix_kernel,
         out_shape=shape((length, channels), BF16),
-        in_specs=[whole()] * 6 + [anywhere()],
-        out_specs=whole(),
-        scratch_shapes=[
-            pltpu.VMEM((lines, 128), F32),
+        in_specs=[anywhere()] * 7,
+        out_specs=anywhere(),
+        scratch_shapes=[pltpu.VMEM((lines, 128), F32)]
+        + [pltpu.VMEM(state.shape, F32)] * 4
+        + [
+            pltpu.VMEM((32, 128), F32),
+            pltpu.VMEM((sp, 8, 128), F32),
             pltpu.VMEM((length, channels), BF16),
-            pltpu.SemaphoreType.DMA((1,)),
+            pltpu.VMEM((length, channels), BF16),
+            pltpu.SemaphoreType.DMA((8,)),
         ],
-        compiler_params=params(12),
+        compiler_params=FULL,
         name="mix",
     )(h_f, p_f, h_b, p_b, seg, totals, gate_in)
     token_rows = lax.all_to_all(
@@ -440,16 +467,19 @@
     project = pl.pallas_call(
         proj_kernel,
         out_shape=(shape((rows, width), BF16), shape((slots, width), BF16)),
-        in_specs=[whole(), in_hbm(), anywhere(), anywhere(), whole()],
-        out_specs=(whole(), in_hbm()),
+        in_specs=[anywhere()] * 5,
+        out_specs=(anywhere(), anywhere()),
         scratch_shapes=[
+            pltpu.VMEM(token_rows.shape, BF16),
             pltpu.VMEM(out_proj.shape, BF16),
             pltpu.VMEM(residual.shape, BF16),
             pltpu.VMEM(norm_gain.shape, F32),
+            pltpu.VMEM((routes.shape[1], rows), jnp.int32),
+            pltpu.VMEM(residual.shape, BF16),
             pltpu.VMEM((slots, width), BF16),
-            pltpu.SemaphoreType.DMA((14,)),
+            pltpu.SemaphoreType.DMA((17,)),
         ],
-        compiler_params=params(16),
+        compiler_params=FULL,
         name="proj",
     )
     stream, outgoing = project(token_rows, out_proj, residual, norm_gain, own_routes.T)
@@ -462,17 +492,20 @@
     def experts(shares, before, tail):
         count = len(shares)
         tall = count * ff_own
-        scratch = [pltpu.VMEM((tall, width), BF16)] * 3 + [pltpu.SemaphoreType.DMA((3 * count,))]
-        if tail:
-            scratch += [pltpu.VMEM((slots, width), BF16), pltpu.SemaphoreType.DMA((1,))]
+        scratch = [pltpu.VMEM((tall, width), BF16)] * 3 + [
+            pltpu.VMEM((slots, width), BF16),
+            pltpu.VMEM((slots, width), F32),
+            pltpu.SemaphoreType.DMA((3 * count,)),
+            pltpu.SemaphoreType.DMA((3,)),
+        ]
         head = before is None
         return pl.pallas_call(
             functools.partial(expert_kernel, pieces=count, head=head, tail=tail),
             out_shape=shape((slots, width), BF16 if tail else F32),
-            in_specs=[whole()] + [in_hbm()] * count + [whole()] * (not head),
-            out_specs=in_hbm() if tail else whole(),
+            in_specs=[anywhere()] * (1 + count + (not head)),
+            out_specs=anywhere(),
             scratch_shapes=scratch,
-            compiler_params=params(24),
+            compiler_params=FULL,
             name="experts_tail" if tail else "experts_head",
         )(arrived, *shares, *([] if head else [before]))
 
@@ -484,9 +517,18 @@
     return pl.pallas_call(
         combine_kernel,
         out_shape=shape((rows, width), BF16),
-        in_specs=[whole()] * 5,
-        out_specs=whole(),
-        compiler_params=params(16),
+        in_specs=[anywhere()] * 5,
+        out_specs=anywhere(),
+        scratch_shapes=[
+            pltpu.VMEM((slots, width), BF16),
+            pltpu.VMEM((rows, width), BF16),
+            pltpu.VMEM(norm_gain.shape, F32),
+            pltpu.VMEM(own_routes.shape, jnp.int32),
+            pltpu.VMEM(own_weights.shape, F32),
+            pltpu.VMEM((rows, width), BF16),
+            pltpu.SemaphoreType.DMA((6,)),
+        ],
+        compiler_params=FULL,
         name="combine",
     )(returned.reshape(slots, width), stream, norm_gain, own_routes, own_weights)
 

time: 158 us -> 155 us (0.981)
  local copies, waits for them, and re-layouts: 18.8 us -> 5.13 us
  Pallas kernels: 21.6 us -> 33.3 us
    unnamed x44 -> x6, local copies, waits for them, and re-layouts: 17.1 us -> 2.27 us
    pallas_call x2, Pallas kernels: 8.95 us -> 14.2 us  [experts(): pl.pallas_call(functools.partial(expert_kernel, pieces=count, head=head,...]
    all_to_all x1, waiting for transfers between devices: 12.7 us -> 10.4 us  [layer(): lax.all_to_all(mixed.reshape(tp, rows, channels), 'tp', split_axis=0, con...]
    pallas_call x1, Pallas kernels: 3.77 us -> 5.92 us  [layer(): pl.pallas_call(scan_kernel, out_shape=(state, state, state, state, shape(...]
    pallas_call x1, Pallas kernels: 1.2 us -> 2.86 us  [layer(): pl.pallas_call(mix_kernel, out_shape=shape((length, channels), BF16), in_...]
  transfers between devices with their start and end apart: 20 -> 20, of which waited for: 8 -> 8; matrix products, arithmetic and copies ran while one was open for 1% -> 2% of each run, Pallas kernels for 9% -> 15%
where the time goes in v4:
time: 155 us
  waiting for transfers between devices  61.4 us (40%)
  starting transfers between devices  40.6 us (26%)
  Pallas kernels  33.3 us (21%)
  blocking collectives  14 us (9%)
  local copies, waits for them, and re-layouts  5.13 us (3%)
    ppermute x7, waiting for transfers between devices, around(): lax.ppermute(part, 'tp', [(i, (i + 2 - 4 * (i % 2)) % tp) for i in range(...  15.9 us
    all_to_all x1, waiting for transfers between devices, layer(): lax.all_to_all(outgoing.reshape(sp, slots // sp, width), 'sp', split_axis...  15.8 us
    all_to_all x1, waiting for transfers between devices, layer(): lax.all_to_all(done.reshape(sp, slots // sp, width), 'sp', split_axis=0,...  14.6 us
    pallas_call x2, Pallas kernels, experts(): pl.pallas_call(functools.partial(expert_kernel, pieces=count, head=head,...  14.2 us
    all_to_all x1, blocking collectives, layer(): lax.all_to_all(total, 'sp', split_axis=0, concat_axis=0, tiled=True)  14 us
    ppermute x7, starting transfers between devices, around(): lax.ppermute(part, 'tp', [(i, (i + 2 - 4 * (i % 2)) % tp) for i in range(...  11.1 us
    all_to_all x1, waiting for transfers between devices, layer(): lax.all_to_all(mixed.reshape(tp, rows, channels), 'tp', split_axis=0, con...  10.4 us
    all_to_all x1, starting transfers between devices, layer(): lax.all_to_all(outgoing.reshape(sp, slots // sp, width), 'sp', split_axis...  7.84 us
  transfers between devices with their start and end apart: 20, of which 8 were waited for; matrix products, arithmetic and copies ran while one was open for 2% of the time, Pallas kernels for 15%

profile of v4, /device:TPU:1, one launch (start us, length us, event | category | flops | bytes accessed | tf_op | source)
XLA Modules:
  0.0 154.6 jit_solution(3803888950725153319)
XLA Ops:
  0.0 1.9 %pack.1.refs_1_ = bf16[192,2048]{1,0:T(8,128)(2,1)} custom-call(bf16[64,2048]{1,0:T(8,128)(2,1)} %bitcast.18, bf16[64,2048]{1,0:T(8,128)(2,1)} %bitcast.19, bf16[64,2048]{1,0:T(8,128)(2,1)} %bitcast.20), custom_call_target="tpu_custom_call" | custom-call | tf_op jit(solution)/shard_map/pack/pallas_call | solution.py:378
  1.9 3.3 %collective-permute-start.3 = (bf16[192,2048]{1,0:T(8,128)(2,1)}, bf16[192,2048]{1,0:T(8,128)(2,1)}, u32[]{:S(2)}, u32[]{:S(2)}) collective-permute-start(bf16[192,2048]{1,0:T(8,128)(2,1)} %pack.1.refs_1_), channel_id=1, source_target_pairs={{0,1},{1,0},{2,3},{3,2},{4,5},{5,4},{6,7},{7,6},{8,9},{9,8},{10,11... | collective-permute-start | bytes 2359304 | tf_op jit(solution)/shard_map/ppermute | solution.py:392
  5.2 3.9 %collective-permute-start.2 = (bf16[192,2048]{1,0:T(8,128)(2,1)}, bf16[192,2048]{1,0:T(8,128)(2,1)}, u32[]{:S(2)}, u32[]{:S(2)}) collective-permute-start(bf16[192,2048]{1,0:T(8,128)(2,1)} %pack.1.refs_1_), channel_id=1, source_target_pairs={{0,2},{1,15},{2,4},{3,1},{4,6},{5,3},{6,8},{7,5},{8,10},{9,7},{10,... | collective-permute-start | bytes 2359304 | tf_op jit(solution)/shard_map/ppermute | solution.py:389
  9.8 3.6 %collective-permute-start = (bf16[2,128]{1,0:T(2,128)(2,1)S(1)}, bf16[2,128]{1,0:T(2,128)(2,1)}, u32[]{:S(2)}, u32[]{:S(2)}) collective-permute-start(bf16[2,128]{1,0:T(2,128)(2,1)S(1)} %get-tuple-element.30), channel_id=1, source_target_pairs={{0,16},{16,32},{32,48},{48,64},{64,80},{80,96},{96,112},{112,128},... | collective-permute-start | bytes 1544 | tf_op jit(solution)/shard_map/ppermute | solution.py:374
  14.7 3.4 %collective-permute-done.1.after_h = bf16[2,128]{1,0:T(2,128)(2,1)} collective-permute-done((bf16[2,128]{1,0:T(2,128)(2,1)S(1)}, bf16[2,128]{1,0:T(2,128)(2,1)}, u32[]{:S(2)}, u32[]{:S(2)}) %collective-permute-start.1) | collective-permute-done | bytes 544 | tf_op jit(solution)/shard_map/ppermute | solution.py:375
  18.1 5.9 %scan.1 = (f32[1024,128]{1,0:T(8,128)}, f32[1024,128]{1,0:T(8,128)}, f32[1024,128]{1,0:T(8,128)}, f32[1024,128]{1,0:T(8,128)}, f32[32,128]{1,0:T(8,128)}, /*index=5*/f32[16,8,128]{2,1,0:T(8,128)}) custom-call(bf16[1024,128]{1,0:T(8,128)(2,1)} %mix_h.1, bf16[2,128]{1,0:T(2,128)(2,1)} %collective-permute-done.before_h, ...), custom_call_target="tpu_custom_call" | custom-call | tf_op jit(solution)/shard_map/scan/pallas_call | solution.py:400
  25.6 14.0 %all_to_all.20.refs_5_ = f32[16,8,128]{2,1,0:T(8,128)} all-to-all(f32[16,8,128]{2,1,0:T(8,128)} %get-tuple-element.23), channel_id=1, replica_groups=mesh['sp'=16,'tp'=16] {'sp'}, dimensions={0} | all-to-all | bytes 131072 | tf_op jit(solution)/shard_map/all_to_all | solution.py:439
  40.3 3.6 %collective-permute-done.8.refs_7_ = bf16[192,2048]{1,0:T(8,128)(2,1)S(1)} collective-permute-done((bf16[192,2048]{1,0:T(8,128)(2,1)}, bf16[192,2048]{1,0:T(8,128)(2,1)S(1)}, u32[]{:S(2)}, u32[]{:S(2)}) %collective-permute-start.8) | collective-permute-done | bytes 786464 | tf_op jit(solution)/shard_map/ppermute | solution.py:389
  44.8 1.7 %collective-permute-start.9 = (bf16[192,2048]{1,0:T(8,128)(2,1)S(1)}, bf16[192,2048]{1,0:T(8,128)(2,1)}, u32[]{:S(2)}, u32[]{:S(2)}) collective-permute-start(bf16[192,2048]{1,0:T(8,128)(2,1)S(1)} %collective-permute-done.8.refs_7_), channel_id=1, source_target_pairs={{0,2},{1,15},{2,4},{3,1},{4,6},{5,3},{6,8},{7,5},{8,10},{9,7},{10,... | collective-permute-start | bytes 2359304 | tf_op jit(solution)/shard_map/ppermute | solution.py:389
  46.9 5.5 %collective-permute-done.5.refs_9_ = bf16[192,2048]{1,0:T(8,128)(2,1)} collective-permute-done((bf16[192,2048]{1,0:T(8,128)(2,1)}, bf16[192,2048]{1,0:T(8,128)(2,1)}, u32[]{:S(2)}, u32[]{:S(2)}) %collective-permute-start.5) | collective-permute-done | bytes 786464 | tf_op jit(solution)/shard_map/ppermute | solution.py:389
  52.4 1.6 %collective-permute-start.6 = (bf16[192,2048]{1,0:T(8,128)(2,1)}, bf16[192,2048]{1,0:T(8,128)(2,1)}, u32[]{:S(2)}, u32[]{:S(2)}) collective-permute-start(bf16[192,2048]{1,0:T(8,128)(2,1)} %collective-permute-done.5.refs_9_), channel_id=1, source_target_pairs={{0,2},{1,15},{2,4},{3,1},{4,6},{5,3},{6,8},{7,5},{8,10},{9,7},{10,... | collective-permute-start | bytes 2359304 | tf_op jit(solution)/shard_map/ppermute | solution.py:389
  54.1 6.8 %collective-permute-done.9.refs_11_ = bf16[192,2048]{1,0:T(8,128)(2,1)} collective-permute-done((bf16[192,2048]{1,0:T(8,128)(2,1)S(1)}, bf16[192,2048]{1,0:T(8,128)(2,1)}, u32[]{:S(2)}, u32[]{:S(2)}) %collective-permute-start.9) | collective-permute-done | bytes 786464 | tf_op jit(solution)/shard_map/ppermute | solution.py:389
  60.9 1.6 %collective-permute-start.10 = (bf16[192,2048]{1,0:T(8,128)(2,1)}, bf16[192,2048]{1,0:T(8,128)(2,1)}, u32[]{:S(2)}, u32[]{:S(2)}) collective-permute-start(bf16[192,2048]{1,0:T(8,128)(2,1)} %collective-permute-done.9.refs_11_), channel_id=1, source_target_pairs={{0,2},{1,15},{2,4},{3,1},{4,6},{5,3},{6,8},{7,5},{8,10},{9,7},{10,... | collective-permute-start | bytes 2359304 | tf_op jit(solution)/shard_map/ppermute | solution.py:389
  62.5 2.9 %mix.1 = bf16[1024,128]{1,0:T(8,128)(2,1)} custom-call(f32[1024,128]{1,0:T(8,128)} %get-tuple-element.17.refs_0_, f32[1024,128]{1,0:T(8,128)} %get-tuple-element.18.refs_1_, f32[1024,128]{1,0:T(8,128)} %get-tuple-element.19.refs_2_, f32[1024,128]{1,0:T(8,128)} %get-tuple-element.20.refs_3_, f32[32,128]{1,0:T(8,128)} %get-tuple-element.21.refs_4_, ...), custom_call_target="tpu_custom_call" | custom-call | tf_op jit(solution)/shard_map/mix/pallas_call | solution.py:442
  65.4 7.2 %all-to-all-start.1 = ((bf16[16,64,128]{2,1,0:T(8,128)(2,1)}), bf16[16,64,128]{2,1,0:T(8,128)(2,1)}, u32[]{:S(2)}, u32[]{:S(2)}) async-start(bf16[16,64,128]{2,1,0:T(8,128)(2,1)} %bitcast.16), calls=%async_computation.1 | async-start | bytes 524288 | tf_op jit(solution)/shard_map/all_to_all | solution.py:459
  74.6 10.4 %all-to-all-done.1.mixed_h = bf16[16,64,128]{2,1,0:T(8,128)(2,1)} async-done(((bf16[16,64,128]{2,1,0:T(8,128)(2,1)}), bf16[16,64,128]{2,1,0:T(8,128)(2,1)}, u32[]{:S(2)}, u32[]{:S(2)}) %all-to-all-start.1) | async-done | bytes 262176 | tf_op jit(solution)/shard_map/all_to_all | solution.py:459
  85.0 5.5 %proj.1 = (bf16[64,2048]{1,0:T(8,128)(2,1)}, bf16[256,2048]{1,0:T(8,128)(2,1)}) custom-call(bf16[16,64,128]{2,1,0:T(8,128)(2,1)} %all-to-all-done.1.mixed_h, bf16[2048,2048]{1,0:T(8,128)(2,1)} %weights_h.1, bf16[64,2048]{1,0:T(8,128)(2,1)} %residual_h.1, f32[3,2048]{1,0:T(4,128)} %refs_2_.1, s32[2,64]{1,0:T(2,128)} %copy.19.routes_h), custom_call_target="tpu_custom_call" | custom-call | tf_op jit(solution)/shard_map/proj/pallas_call | solution.py:485
  90.5 7.8 %all-to-all-start.2 = ((bf16[16,16,2048]{2,1,0:T(8,128)(2,1)}), bf16[16,16,2048]{2,1,0:T(8,128)(2,1)}, u32[]{:S(2)}, u32[]{:S(2)}) async-start(bf16[16,16,2048]{2,1,0:T(8,128)(2,1)} %bitcast.15), calls=%async_computation.2 | async-start | bytes 2097152 | tf_op jit(solution)/shard_map/all_to_all | solution.py:489
  101.1 15.8 %all-to-all-done.2 = bf16[16,16,2048]{2,1,0:T(8,128)(2,1)} async-done(((bf16[16,16,2048]{2,1,0:T(8,128)(2,1)}), bf16[16,16,2048]{2,1,0:T(8,128)(2,1)}, u32[]{:S(2)}, u32[]{:S(2)}) %all-to-all-start.2) | async-done | bytes 1048608 | tf_op jit(solution)/shard_map/all_to_all | solution.py:489
  116.9 9.0 %experts_head.1.refs_5_ = f32[256,2048]{1,0:T(8,128)} custom-call(bf16[256,2048]{1,0:T(8,128)(2,1)} %bitcast.9.refs_0_, bf16[192,2048]{1,0:T(8,128)(2,1)} %pack.1.refs_1_, bf16[192,2048]{1,0:T(8,128)(2,1)} %collective-permute-done.3.refs_2_, bf16[192,2048]{1,0:T(8,128)(2,1)} %collective-permute-done.2.refs_3_, ...), custom_call_target="tpu_custom_call" | custom-call | tf_op jit(solution)/shard_map/experts_head/pallas_call | solution.py:502
  125.9 5.2 %experts_tail.1 = bf16[256,2048]{1,0:T(8,128)(2,1)} custom-call(bf16[256,2048]{1,0:T(8,128)(2,1)} %bitcast.9.refs_0_, bf16[192,2048]{1,0:T(8,128)(2,1)} %collective-permute-done.6.refs_1_, bf16[192,2048]{1,0:T(8,128)(2,1)} %collective-permute-done.7.refs_2_, bf16[192,2048]{1,0:T(8,128)(2,1)} %collective-permute-done.10.refs_3_, ...), custom_call_target="tpu_custom_call" | custom-call | tf_op jit(solution)/shard_map/experts_tail/pallas_call | solution.py:502
  131.1 4.3 %all-to-all-start.3 = ((bf16[16,16,2048]{2,1,0:T(8,128)(2,1)}), bf16[16,16,2048]{2,1,0:T(8,128)(2,1)}, u32[]{:S(2)}, u32[]{:S(2)}) async-start(bf16[16,16,2048]{2,1,0:T(8,128)(2,1)} %bitcast.14), calls=%async_computation.3 | async-start | bytes 2097152 | tf_op jit(solution)/shard_map/all_to_all | solution.py:514
  136.9 14.6 %all-to-all-done.3 = bf16[16,16,2048]{2,1,0:T(8,128)(2,1)} async-done(((bf16[16,16,2048]{2,1,0:T(8,128)(2,1)}), bf16[16,16,2048]{2,1,0:T(8,128)(2,1)}, u32[]{:S(2)}, u32[]{:S(2)}) %all-to-all-start.3) | async-done | bytes 1048608 | tf_op jit(solution)/shard_map/all_to_all | solution.py:514
  151.5 2.9 %combine.1 = bf16[64,2048]{1,0:T(8,128)(2,1)} custom-call(bf16[256,2048]{1,0:T(8,128)(2,1)} %bitcast.11.refs_0_, bf16[64,2048]{1,0:T(8,128)(2,1)} %get-tuple-element.28.refs_1_, f32[3,2048]{1,0:T(4,128)} %refs_2_.1, s32[64,2]{1,0:T(8,128)} %copy-done.1, f32[64,2]{1,0:T(8,128)} %copy.22.refs_4_), custom_call_target="tpu_custom_call" | custom-call | tf_op jit(solution)/shard_map/combine/pallas_call | solution.py:517
  (34 shorter events, 11.9 us)
Async XLA Ops:
  1.9 22.1 %collective-permute-start.3 = (bf16[192,2048]{1,0:T(8,128)(2,1)}, bf16[192,2048]{1,0:T(8,128)(2,1)}, u32[]{:S(2)}, u32[]{:S(2)}) collective-permute-start(bf16[192,2048]{1,0:T(8,128)(2,1)} %pack.1.refs_1_), channel_id=1, source_target_pairs={{0,1},{1,0},{2,3},{3,2},{4,5},{5,4},{6,7},{7,6},{8,9},{9,8},{10,11... | collective-permute-start | bytes 2359304 | tf_op jit(solution)/shard_map/ppermute | solution.py:392
  5.2 19.7 %collective-permute-start.2 = (bf16[192,2048]{1,0:T(8,128)(2,1)}, bf16[192,2048]{1,0:T(8,128)(2,1)}, u32[]{:S(2)}, u32[]{:S(2)}) collective-permute-start(bf16[192,2048]{1,0:T(8,128)(2,1)} %pack.1.refs_1_), channel_id=1, source_target_pairs={{0,2},{1,15},{2,4},{3,1},{4,6},{5,3},{6,8},{7,5},{8,10},{9,7},{10,... | collective-permute-start | bytes 2359304 | tf_op jit(solution)/shard_map/ppermute | solution.py:389
  9.8 4.9 %collective-permute-start = (bf16[2,128]{1,0:T(2,128)(2,1)S(1)}, bf16[2,128]{1,0:T(2,128)(2,1)}, u32[]{:S(2)}, u32[]{:S(2)}) collective-permute-start(bf16[2,128]{1,0:T(2,128)(2,1)S(1)} %get-tuple-element.30), channel_id=1, source_target_pairs={{0,16},{16,32},{32,48},{48,64},{64,80},{80,96},{96,112},{112,128},... | collective-permute-start | bytes 1544 | tf_op jit(solution)/shard_map/ppermute | solution.py:374
  13.4 4.7 %collective-permute-start.1 = (bf16[2,128]{1,0:T(2,128)(2,1)S(1)}, bf16[2,128]{1,0:T(2,128)(2,1)}, u32[]{:S(2)}, u32[]{:S(2)}) collective-permute-start(bf16[2,128]{1,0:T(2,128)(2,1)S(1)} %get-tuple-element.29), channel_id=1, source_target_pairs={{16,0},{32,16},{48,32},{64,48},{80,64},{96,80},{112,96},{128,112},... | collective-permute-start | bytes 1544 | tf_op jit(solution)/shard_map/ppermute | solution.py:375
  24.1 15.5 %collective-permute-start.4 = (bf16[192,2048]{1,0:T(8,128)(2,1)}, bf16[192,2048]{1,0:T(8,128)(2,1)}, u32[]{:S(2)}, u32[]{:S(2)}) collective-permute-start(bf16[192,2048]{1,0:T(8,128)(2,1)} %collective-permute-done.3.refs_2_), channel_id=1, source_target_pairs={{0,2},{1,15},{2,4},{3,1},{4,6},{5,3},{6,8},{7,5},{8,10},{9,7},{10,... | collective-permute-start | bytes 2359304 | tf_op jit(solution)/shard_map/ppermute | solution.py:389
  24.9 19.0 %collective-permute-start.8 = (bf16[192,2048]{1,0:T(8,128)(2,1)}, bf16[192,2048]{1,0:T(8,128)(2,1)S(1)}, u32[]{:S(2)}, u32[]{:S(2)}) collective-permute-start(bf16[192,2048]{1,0:T(8,128)(2,1)} %collective-permute-done.2.refs_3_), channel_id=1, source_target_pairs={{0,2},{1,15},{2,4},{3,1},{4,6},{5,3},{6,8},{7,5},{8,10},{9,7},{10,... | collective-permute-start | bytes 2359304 | tf_op jit(solution)/shard_map/ppermute | solution.py:389
  39.6 12.9 %collective-permute-start.5 = (bf16[192,2048]{1,0:T(8,128)(2,1)}, bf16[192,2048]{1,0:T(8,128)(2,1)}, u32[]{:S(2)}, u32[]{:S(2)}) collective-permute-start(bf16[192,2048]{1,0:T(8,128)(2,1)} %collective-permute-done.4.refs_5_), channel_id=1, source_target_pairs={{0,2},{1,15},{2,4},{3,1},{4,6},{5,3},{6,8},{7,5},{8,10},{9,7},{10,... | collective-permute-start | bytes 2359304 | tf_op jit(solution)/shard_map/ppermute | solution.py:389
  43.9 0.9 copy-start
  44.8 16.1 %collective-permute-start.9 = (bf16[192,2048]{1,0:T(8,128)(2,1)S(1)}, bf16[192,2048]{1,0:T(8,128)(2,1)}, u32[]{:S(2)}, u32[]{:S(2)}) collective-permute-start(bf16[192,2048]{1,0:T(8,128)(2,1)S(1)} %collective-permute-done.8.refs_7_), channel_id=1, source_target_pairs={{0,2},{1,15},{2,4},{3,1},{4,6},{5,3},{6,8},{7,5},{8,10},{9,7},{10,... | collective-permute-start | bytes 2359304 | tf_op jit(solution)/shard_map/ppermute | solution.py:389
  46.4 52.2 %collective-permute-start.12 = (bf16[192,2048]{1,0:T(8,128)(2,1)}, bf16[192,2048]{1,0:T(8,128)(2,1)}, u32[]{:S(2)}, u32[]{:S(2)}) collective-permute-start(bf16[192,2048]{1,0:T(8,128)(2,1)} %collective-permute-done.2.refs_3_), channel_id=1, source_target_pairs={{0,1},{1,0},{2,3},{3,2},{4,5},{5,4},{6,7},{7,6},{8,9},{9,8},{10,11... | collective-permute-start | bytes 2359304 | tf_op jit(solution)/shard_map/ppermute | solution.py:392
  46.4 52.6 %collective-permute-start.13 = (bf16[192,2048]{1,0:T(8,128)(2,1)}, bf16[192,2048]{1,0:T(8,128)(2,1)}, u32[]{:S(2)}, u32[]{:S(2)}) collective-permute-start(bf16[192,2048]{1,0:T(8,128)(2,1)} %collective-permute-done.4.refs_5_), channel_id=1, source_target_pairs={{0,1},{1,0},{2,3},{3,2},{4,5},{5,4},{6,7},{7,6},{8,9},{9,8},{10,11... | collective-permute-start | bytes 2359304 | tf_op jit(solution)/shard_map/ppermute | solution.py:392
  52.4 46.8 %collective-permute-start.6 = (bf16[192,2048]{1,0:T(8,128)(2,1)}, bf16[192,2048]{1,0:T(8,128)(2,1)}, u32[]{:S(2)}, u32[]{:S(2)}) collective-permute-start(bf16[192,2048]{1,0:T(8,128)(2,1)} %collective-permute-done.5.refs_9_), channel_id=1, source_target_pairs={{0,2},{1,15},{2,4},{3,1},{4,6},{5,3},{6,8},{7,5},{8,10},{9,7},{10,... | collective-permute-start | bytes 2359304 | tf_op jit(solution)/shard_map/ppermute | solution.py:389
  60.9 38.6 %collective-permute-start.10 = (bf16[192,2048]{1,0:T(8,128)(2,1)}, bf16[192,2048]{1,0:T(8,128)(2,1)}, u32[]{:S(2)}, u32[]{:S(2)}) collective-permute-start(bf16[192,2048]{1,0:T(8,128)(2,1)} %collective-permute-done.9.refs_11_), channel_id=1, source_target_pairs={{0,2},{1,15},{2,4},{3,1},{4,6},{5,3},{6,8},{7,5},{8,10},{9,7},{10,... | collective-permute-start | bytes 2359304 | tf_op jit(solution)/shard_map/ppermute | solution.py:389
  65.4 19.7 %all-to-all-start.1 = ((bf16[16,64,128]{2,1,0:T(8,128)(2,1)}), bf16[16,64,128]{2,1,0:T(8,128)(2,1)}, u32[]{:S(2)}, u32[]{:S(2)}) async-start(bf16[16,64,128]{2,1,0:T(8,128)(2,1)} %bitcast.16), calls=%async_computation.1 | async-start | bytes 524288 | tf_op jit(solution)/shard_map/all_to_all | solution.py:459
  73.4 0.6 copy-start.1
  90.5 26.3 %all-to-all-start.2 = ((bf16[16,16,2048]{2,1,0:T(8,128)(2,1)}), bf16[16,16,2048]{2,1,0:T(8,128)(2,1)}, u32[]{:S(2)}, u32[]{:S(2)}) async-start(bf16[16,16,2048]{2,1,0:T(8,128)(2,1)} %bitcast.15), calls=%async_computation.2 | async-start | bytes 2097152 | tf_op jit(solution)/shard_map/all_to_all | solution.py:489
  98.4 2.7 %collective-permute-start.14 = (bf16[192,2048]{1,0:T(8,128)(2,1)}, bf16[192,2048]{1,0:T(8,128)(2,1)}, u32[]{:S(2)}, u32[]{:S(2)}) collective-permute-start(bf16[192,2048]{1,0:T(8,128)(2,1)} %copy-done), channel_id=1, source_target_pairs={{0,1},{1,0},{2,3},{3,2},{4,5},{5,4},{6,7},{7,6},{8,9},{9,8},{10,11... | collective-permute-start | bytes 2359304 | tf_op jit(solution)/shard_map/ppermute | solution.py:392
  98.6 18.3 %collective-permute-start.15 = (bf16[192,2048]{1,0:T(8,128)(2,1)}, bf16[192,2048]{1,0:T(8,128)(2,1)}, u32[]{:S(2)}, u32[]{:S(2)}) collective-permute-start(bf16[192,2048]{1,0:T(8,128)(2,1)} %collective-permute-done.5.refs_9_), channel_id=1, source_target_pairs={{0,1},{1,0},{2,3},{3,2},{4,5},{5,4},{6,7},{7,6},{8,9},{9,8},{10,11... | collective-permute-start | bytes 2359304 | tf_op jit(solution)/shard_map/ppermute | solution.py:392
  99.0 17.9 %collective-permute-start.16 = (bf16[192,2048]{1,0:T(8,128)(2,1)}, bf16[192,2048]{1,0:T(8,128)(2,1)}, u32[]{:S(2)}, u32[]{:S(2)}) collective-permute-start(bf16[192,2048]{1,0:T(8,128)(2,1)} %collective-permute-done.9.refs_11_), channel_id=1, source_target_pairs={{0,1},{1,0},{2,3},{3,2},{4,5},{5,4},{6,7},{7,6},{8,9},{9,8},{10,11... | collective-permute-start | bytes 2359304 | tf_op jit(solution)/shard_map/ppermute | solution.py:392
  99.3 26.6 %collective-permute-start.7 = (bf16[192,2048]{1,0:T(8,128)(2,1)}, bf16[192,2048]{1,0:T(8,128)(2,1)}, u32[]{:S(2)}, u32[]{:S(2)}) collective-permute-start(bf16[192,2048]{1,0:T(8,128)(2,1)} %collective-permute-done.6.refs_1_), channel_id=1, source_target_pairs={{0,1},{1,0},{2,3},{3,2},{4,5},{5,4},{6,7},{7,6},{8,9},{9,8},{10,11... | collective-permute-start | bytes 2359304 | tf_op jit(solution)/shard_map/ppermute | solution.py:392
  99.5 26.3 %collective-permute-start.11 = (bf16[192,2048]{1,0:T(8,128)(2,1)}, bf16[192,2048]{1,0:T(8,128)(2,1)}, u32[]{:S(2)}, u32[]{:S(2)}) collective-permute-start(bf16[192,2048]{1,0:T(8,128)(2,1)} %collective-permute-done.10.refs_3_), channel_id=1, source_target_pairs={{0,1},{1,0},{2,3},{3,2},{4,5},{5,4},{6,7},{7,6},{8,9},{9,8},{10,11... | collective-permute-start | bytes 2359304 | tf_op jit(solution)/shard_map/ppermute | solution.py:392
  131.1 20.4 %all-to-all-start.3 = ((bf16[16,16,2048]{2,1,0:T(8,128)(2,1)}), bf16[16,16,2048]{2,1,0:T(8,128)(2,1)}, u32[]{:S(2)}, u32[]{:S(2)}) async-start(bf16[16,16,2048]{2,1,0:T(8,128)(2,1)} %bitcast.14), calls=%async_computation.3 | async-start | bytes 2097152 | tf_op jit(solution)/shard_map/all_to_all | solution.py:514

commit v5 on v4

--- a/solution.py
+++ b/solution.py
@@ -15,6 +15,7 @@
 
 
 FULL = pltpu.CompilerParams(vmem_limit_bytes=67043328)
+ROOMY = pltpu.CompilerParams(vmem_limit_bytes=30 * 1024 * 1024)
 
 
 def anywhere():
@@ -52,10 +53,10 @@
 
 def scan_kernel(
     mix_h, before_h, after_h, conv_w_h, conv_b_h, decay_param_h, recur_gate_h, recur_bias_h, input_gate_h, input_bias_h,
-    h_f_h, p_f_h, h_b_h, p_b_h, seg_h, total_h,
+    h_h, p_f_h, p_b_h, seg_h, total_h,
     padded, conv, split, wide, wlow, pre, a_f, b_f, a_b, b_b,
     mix, before, after, conv_w, conv_b, decay_param, recur_gate, recur_bias, input_gate, input_bias,
-    h_f, p_f, h_b, p_b, seg, total, sems,
+    h, p_f, p_b, seg, total, sems,
 ):
     for copy in fetched(
         (
@@ -130,7 +131,7 @@
 
     lax.fori_loop(0, length // rows, gates, 0)
 
-    def advance(t, carry):
+    def advance(t, carry, meet):
         hf, pf, hb, pb = carry
         back = step - 1 - t
         af = a_f[pl.ds(t, SEGS, stride=stride), :]
@@ -141,37 +142,44 @@
         pf = pf * af
         hb = ab * hb + bb
         pb = pb * ab
-        here = pl.multiple_of(t * SEGS, SEGS)
-        there = pl.multiple_of(back * SEGS, SEGS)
-        h_f[pl.ds(here, SEGS), :] = hf
-        p_f[pl.ds(here, SEGS), :] = pf
-        h_b[pl.ds(there, SEGS), :] = hb
-        p_b[pl.ds(there, SEGS), :] = pb
+        here = pl.ds(pl.multiple_of(t * SEGS, SEGS), SEGS)
+        there = pl.ds(pl.multiple_of(back * SEGS, SEGS), SEGS)
+        h[here, :] = hf + h[here, :] if meet else hf
+        h[there, :] = hb + h[there, :] if meet else hb
+        p_f[here, :] = pf
+        p_b[there, :] = pb
         return hf, pf, hb, pb
 
     none = jnp.zeros((SEGS, 128), F32)
     ones = jnp.ones((SEGS, 128), F32)
-    hf, pf, hb, pb = lax.fori_loop(0, step, advance, (none, ones, none, ones), unroll=8)
+    half = step // 2
+    state = (none, ones, none, ones)
+    state = lax.fori_loop(0, half, functools.partial(advance, meet=False), state, unroll=8)
+    low, high = pl.ds(0, length // 2), pl.ds(length // 2, length // 2)
+    sent = fetched((p_f.at[low], p_b.at[high]), (p_f_h.at[low], p_b_h.at[high]), sems, 10)
+    hf, pf, hb, pb = lax.fori_loop(half, step, functools.partial(advance, meet=True), state, unroll=8)
+    sent += fetched((h, p_f.at[high], p_b.at[low]), (h_h, p_f_h.at[high], p_b_h.at[low]), sems, 12)
 
     sums = []
-    for base, h, p, order in ((0, hf, pf, range(SEGS)), (16, hb, pb, reversed(range(SEGS)))):
+    for base, last, p, order in ((0, hf, pf, range(SEGS)), (16, hb, pb, reversed(range(SEGS)))):
         enter = jnp.zeros((1, 128), F32)
         factor = jnp.ones((1, 128), F32)
         for s in order:
             seg[base + s : base + s + 1, :] = enter
             seg[base + 8 + s : base + 9 + s, :] = factor
-            enter = p[s : s + 1, :] * enter + h[s : s + 1, :]
+            enter = p[s : s + 1, :] * enter + last[s : s + 1, :]
             factor = p[s : s + 1, :] * factor
         sums += [factor, enter]
     both = jnp.concatenate(sums + [jnp.zeros((4, 128), F32)], axis=0)
     total[...] = jnp.broadcast_to(both[None], total.shape)
-    for copy in fetched((h_f, p_f, h_b, p_b, seg, total), (h_f_h, p_f_h, h_b_h, p_b_h, seg_h, total_h), sems, 10):
+    sent += fetched((seg, total), (seg_h, total_h), sems, 15)
+    for copy in sent:
         copy.wait()
 
 
 def mix_kernel(*refs):
-    sources, out_h, natural, buffers, out, sems = refs[:7], refs[7], refs[8], refs[9:16], refs[16], refs[17]
-    h_f, p_f, h_b, p_b, seg, totals, gate_in = buffers
+    sources, out_h, natural, buffers, out, sems = refs[:6], refs[6], refs[7], refs[8:14], refs[14], refs[15]
+    h, p_f, p_b, seg, totals, gate_in = buffers
     for copy in fetched(sources, buffers, sems):
         copy.wait()
     length = out.shape[0]
@@ -192,7 +200,7 @@
         at = pl.multiple_of(t * SEGS, SEGS)
         rows = pl.ds(at, SEGS)
         natural[pl.ds(t, SEGS, stride=stride), :] = (
-            h_f[rows, :] + p_f[rows, :] * into_f + (h_b[rows, :] + p_b[rows, :] * into_b)
+            h[rows, :] + p_f[rows, :] * into_f + p_b[rows, :] * into_b
         )
         return carry
 
@@ -202,7 +210,7 @@
         out[s * step : (s + 1) * step, :] = (
             natural[s * stride : s * stride + step, :] * jax.nn.gelu(gate)
         ).astype(BF16)
-    (copy,) = fetched((out,), (out_h,), sems, 7)
+    (copy,) = fetched((out,), (out_h,), sems, 6)
     copy.wait()
 
 
@@ -271,13 +279,10 @@
         copy.wait()
 
 
-def expert_kernel(*refs, pieces, head, tail):
-    tokens, shares = refs[0], refs[1 : 1 + pieces]
-    rest = refs[1 + pieces :]
-    if not head:
-        before, rest = rest[0], rest[1:]
-    out, gate_w, up_w, down_w, held, acc_held, sems, extra = rest
-    starts = fetched((tokens,), (held,), extra) + ([] if head else fetched((before,), (acc_held,), extra, 1))
+def expert_kernel(*refs):
+    tokens, shares = refs[0], refs[1:-7]
+    out, gate_w, up_w, down_w, held, sems, extra = refs[-7:]
+    (tokens_copy,) = fetched((tokens,), (held,), extra)
     ff = shares[0].shape[0] // 3
     copies = [
         fetched(
@@ -288,13 +293,12 @@
         )
         for at, share in enumerate(shares)
     ]
-    for copy in starts:
-        copy.wait()
+    tokens_copy.wait()
     x = held[...]
-    acc = jnp.zeros(x.shape, F32) if head else acc_held[...]
+    acc = jnp.zeros(x.shape, F32)
     block = 256
     last = (((1,), (1,)), ((), ()))
-    for k in range(pieces * ff // block):
+    for k in range(len(shares) * ff // block):
         for piece in range(k * block // ff, (k + 1) * block // ff):
             for copy in copies[piece]:
                 copy.wait()
@@ -303,9 +307,8 @@
         up = lax.dot_general(x, up_w[rows, :], last, preferred_element_type=F32)
         hidden = (jax.nn.silu(gate) * up).astype(BF16)
         acc = acc + jnp.dot(hidden, down_w[rows, :], preferred_element_type=F32)
-    result = held if tail else acc_held
-    result[...] = acc.astype(result.dtype)
-    (copy,) = fetched((result,), (out,), extra, 2)
+    held[...] = acc.astype(BF16)
+    (copy,) = fetched((held,), (out,), extra, 1)
     copy.wait()
 
 
@@ -397,11 +400,11 @@
     step = length // SEGS
     lines = SEGS * (step + 8)
     state = shape((length, channels), F32)
-    h_f, p_f, h_b, p_b, seg, total = pl.pallas_call(
+    h, p_f, p_b, seg, total = pl.pallas_call(
         scan_kernel,
-        out_shape=(state, state, state, state, shape((32, 128), F32), shape((sp, 8, 128), F32)),
+        out_shape=(state, state, state, shape((32, 128), F32), shape((sp, 8, 128), F32)),
         in_specs=[anywhere()] * 10,
-        out_specs=(anywhere(),) * 6,
+        out_specs=(anywhere(),) * 5,
         scratch_shapes=[
             pltpu.VMEM((length + 16, 128), F32),
             pltpu.VMEM((length, 128), F32),
@@ -426,26 +429,24 @@
             pltpu.VMEM(state.shape, F32),
             pltpu.VMEM(state.shape, F32),
             pltpu.VMEM(state.shape, F32),
-            pltpu.VMEM(state.shape, F32),
             pltpu.VMEM((32, 128), F32),
             pltpu.VMEM((sp, 8, 128), F32),
-            pltpu.SemaphoreType.DMA((16,)),
+            pltpu.SemaphoreType.DMA((17,)),
         ],
         compiler_params=FULL,
         name="scan",
     )(mix_in, before, after, conv_w, conv_b[None], decay_param, recur_gate, recur_bias, input_gate, input_bias)
-    total, r1a = lax.optimization_barrier((total, r1a))
+    total, r1a, r1b = lax.optimization_barrier((total, r1a, r1b))
     r2a, e1a = around(r1a), across(r1a)
+    r2b, e1b = around(r1b), across(r1b)
     totals = lax.all_to_all(total, "sp", split_axis=0, concat_axis=0, tiled=True)
-    totals, r1b = lax.optimization_barrier((totals, r1b))
-    r2b, e1b = around(r1b), across(r1b)
     mixed = pl.pallas_call(
         mix_kernel,
         out_shape=shape((length, channels), BF16),
-        in_specs=[anywhere()] * 7,
+        in_specs=[anywhere()] * 6,
         out_specs=anywhere(),
         scratch_shapes=[pltpu.VMEM((lines, 128), F32)]
-        + [pltpu.VMEM(state.shape, F32)] * 4
+        + [pltpu.VMEM(state.shape, F32)] * 3
         + [
             pltpu.VMEM((32, 128), F32),
             pltpu.VMEM((sp, 8, 128), F32),
@@ -455,11 +456,12 @@
         ],
         compiler_params=FULL,
         name="mix",
-    )(h_f, p_f, h_b, p_b, seg, totals, gate_in)
+    )(h, p_f, p_b, seg, totals, gate_in)
     token_rows = lax.all_to_all(
         mixed.reshape(tp, rows, channels), "tp", split_axis=0, concat_axis=0, tiled=True
     )
     r3a, e2a = around(r2a), across(r2a)
+    r3b, e2b = around(r2b), across(r2b)
     first_row = lax.axis_index("tp") * rows
     own_routes = lax.dynamic_slice_in_dim(routes, first_row, rows, 0)
     own_weights = lax.dynamic_slice_in_dim(route_wt, first_row, rows, 0)
@@ -483,34 +485,27 @@
         name="proj",
     )
     stream, outgoing = project(token_rows, out_proj, residual, norm_gain, own_routes.T)
-    r3b, e2b = around(r2b), across(r2b)
     r4, e3a = around(r3a), across(r3a)
     e3b, e4 = across(r3b), across(r4)
     arrived = lax.all_to_all(outgoing.reshape(sp, slots // sp, width), "sp", split_axis=0, concat_axis=0, tiled=True)
     arrived = arrived.reshape(slots, width)
 
-    def experts(shares, before, tail):
-        count = len(shares)
-        tall = count * ff_own
-        scratch = [pltpu.VMEM((tall, width), BF16)] * 3 + [
+    shares = (own, other, r1a, e1a, r1b, e1b, r2a, e2a, r2b, e2b, r3a, e3a, r3b, e3b, r4, e4)
+    experts = pl.pallas_call(
+        expert_kernel,
+        out_shape=shape((slots, width), BF16),
+        in_specs=[anywhere()] * (1 + len(shares)),
+        out_specs=anywhere(),
+        scratch_shapes=[pltpu.VMEM((len(shares) * ff_own, width), BF16)] * 3
+        + [
             pltpu.VMEM((slots, width), BF16),
-            pltpu.VMEM((slots, width), F32),
-            pltpu.SemaphoreType.DMA((3 * count,)),
-            pltpu.SemaphoreType.DMA((3,)),
-        ]
-        head = before is None
-        return pl.pallas_call(
-            functools.partial(expert_kernel, pieces=count, head=head, tail=tail),
-            out_shape=shape((slots, width), BF16 if tail else F32),
-            in_specs=[anywhere()] * (1 + count + (not head)),
-            out_specs=anywhere(),
-            scratch_shapes=scratch,
-            compiler_params=FULL,
-            name="experts_tail" if tail else "experts_head",
-        )(arrived, *shares, *([] if head else [before]))
-
-    first = experts((own, other, r1a, e1a, r1b, e1b, r2a, e2a, r2b, e2b, r3a, e3a), None, False)
-    done = experts((r3b, e3b, r4, e4), first, True)
+            pltpu.SemaphoreType.DMA((3 * len(shares),)),
+            pltpu.SemaphoreType.DMA((2,)),
+        ],
+        compiler_params=ROOMY,
+        name="experts",
+    )
+    done = experts(arrived, *shares)
     returned = lax.all_to_all(
         done.reshape(sp, slots // sp, width), "sp", split_axis=0, concat_axis=0, tiled=True
     )

time: 155 us -> 158 us (1.019)
  Pallas kernels: 33.3 us -> 26.3 us
  waiting for transfers between devices: 61.4 us -> 65.6 us
  starting transfers between devices: 40.6 us -> 43.5 us
  local copies, waits for them, and re-layouts: 5.13 us -> 7.42 us
    ppermute x7, starting transfers between devices: 11.1 us -> 18.6 us  [around(): lax.ppermute(part, 'tp', [(i, (i + 2 - 4 * (i % 2)) % tp) for i in range(...]
    pallas_call x3 -> x2, Pallas kernels: 20.1 us -> 13.3 us  [the longest x1 7.48 us: layer(): done = experts(arrived, *shares)]
    all_to_all x1, starting transfers between devices: 7.84 us -> 3.66 us  [layer(): lax.all_to_all(outgoing.reshape(sp, slots // sp, width), 'sp', split_axis...]
    ppermute x7, waiting for transfers between devices: 15.9 us -> 19 us  [around(): lax.ppermute(part, 'tp', [(i, (i + 2 - 4 * (i % 2)) % tp) for i in range(...]
    all_to_all x1, waiting for transfers between devices: 15.8 us -> 18.6 us  [layer(): lax.all_to_all(outgoing.reshape(sp, slots // sp, width), 'sp', split_axis...]
    unnamed x6 -> x10, local copies, waits for them, and re-layouts: 2.27 us -> 4.55 us
  transfers between devices with their start and end apart: 20 -> 20, of which waited for: 8 -> 8; matrix products, arithmetic and copies ran while one was open for 2% -> 2% of each run, Pallas kernels for 15% -> 9%
where the time goes in v5:
time: 158 us; the launch traced here: 157 us
  waiting for transfers between devices  65.6 us (42%)
  starting transfers between devices  43.5 us (28%)
  Pallas kernels  26.3 us (17%)
  blocking collectives  13.8 us (9%)
  local copies, waits for them, and re-layouts  7.42 us (5%)
    ppermute x7, waiting for transfers between devices, around(): lax.ppermute(part, 'tp', [(i, (i + 2 - 4 * (i % 2)) % tp) for i in range(...  19 us
    ppermute x7, starting transfers between devices, around(): lax.ppermute(part, 'tp', [(i, (i + 2 - 4 * (i % 2)) % tp) for i in range(...  18.6 us
    all_to_all x1, waiting for transfers between devices, layer(): lax.all_to_all(outgoing.reshape(sp, slots // sp, width), 'sp', split_axis...  18.6 us
    all_to_all x1, waiting for transfers between devices, layer(): lax.all_to_all(done.reshape(sp, slots // sp, width), 'sp', split_axis=0,...  15 us
    all_to_all x1, blocking collectives, layer(): lax.all_to_all(total, 'sp', split_axis=0, concat_axis=0, tiled=True)  13.8 us
    all_to_all x1, waiting for transfers between devices, layer(): lax.all_to_all(mixed.reshape(tp, rows, channels), 'tp', split_axis=0, con...  9.58 us
    pallas_call x1, Pallas kernels, layer(): done = experts(arrived, *shares)  7.48 us
    all_to_all x1, starting transfers between devices, layer(): lax.all_to_all(mixed.reshape(tp, rows, channels), 'tp', split_axis=0, con...  6.87 us
  transfers between devices with their start and end apart: 20, of which 8 were waited for; matrix products, arithmetic and copies ran while one was open for 2% of the time, Pallas kernels for 9%

profile of v5, /device:TPU:1, one launch (start us, length us, event | category | flops | bytes accessed | tf_op | source)
XLA Modules:
  0.0 157.0 jit_solution(3864048394398802282)
XLA Ops:
  1.9 3.3 %collective-permute-start.3 = (bf16[192,2048]{1,0:T(8,128)(2,1)}, bf16[192,2048]{1,0:T(8,128)(2,1)}, u32[]{:S(2)}, u32[]{:S(2)}) collective-permute-start(bf16[192,2048]{1,0:T(8,128)(2,1)} %pack.1.refs_1_), channel_id=1, source_target_pairs={{0,1},{1,0},{2,3},{3,2},{4,5},{5,4},{6,7},{7,6},{8,9},{9,8},{10,11... | collective-permute-start | bytes 2359304 | tf_op jit(solution)/shard_map/ppermute | solution.py:395
  5.2 3.9 %collective-permute-start.2 = (bf16[192,2048]{1,0:T(8,128)(2,1)}, bf16[192,2048]{1,0:T(8,128)(2,1)}, u32[]{:S(2)}, u32[]{:S(2)}) collective-permute-start(bf16[192,2048]{1,0:T(8,128)(2,1)} %pack.1.refs_1_), channel_id=1, source_target_pairs={{0,2},{1,15},{2,4},{3,1},{4,6},{5,3},{6,8},{7,5},{8,10},{9,7},{10,... | collective-permute-start | bytes 2359304 | tf_op jit(solution)/shard_map/ppermute | solution.py:392
  9.0 2.3 %collective-permute-start.4 = (bf16[192,2048]{1,0:T(8,128)(2,1)}, bf16[192,2048]{1,0:T(8,128)(2,1)}, u32[]{:S(2)}, u32[]{:S(2)}) collective-permute-start(bf16[192,2048]{1,0:T(8,128)(2,1)} %collective-permute-done.3.refs_2_), channel_id=1, source_target_pairs={{0,2},{1,15},{2,4},{3,1},{4,6},{5,3},{6,8},{7,5},{8,10},{9,7},{10,... | collective-permute-start | bytes 2359304 | tf_op jit(solution)/shard_map/ppermute | solution.py:392
  12.0 3.6 %collective-permute-start = (bf16[2,128]{1,0:T(2,128)(2,1)S(1)}, bf16[2,128]{1,0:T(2,128)(2,1)}, u32[]{:S(2)}, u32[]{:S(2)}) collective-permute-start(bf16[2,128]{1,0:T(2,128)(2,1)S(1)} %get-tuple-element.26), channel_id=1, source_target_pairs={{0,16},{16,32},{32,48},{48,64},{64,80},{80,96},{96,112},{112,128},... | collective-permute-start | bytes 1544 | tf_op jit(solution)/shard_map/ppermute | solution.py:377
  16.9 3.4 %collective-permute-done.1.after_h = bf16[2,128]{1,0:T(2,128)(2,1)} collective-permute-done((bf16[2,128]{1,0:T(2,128)(2,1)S(1)}, bf16[2,128]{1,0:T(2,128)(2,1)}, u32[]{:S(2)}, u32[]{:S(2)}) %collective-permute-start.1) | collective-permute-done | bytes 544 | tf_op jit(solution)/shard_map/ppermute | solution.py:378
  20.3 5.8 %scan.1 = (f32[1024,128]{1,0:T(8,128)}, f32[1024,128]{1,0:T(8,128)}, f32[1024,128]{1,0:T(8,128)}, f32[32,128]{1,0:T(8,128)}, f32[16,8,128]{2,1,0:T(8,128)}) custom-call(bf16[1024,128]{1,0:T(8,128)(2,1)} %mix_h.1, bf16[2,128]{1,0:T(2,128)(2,1)} %collective-permute-done.before_h, bf16[2,128]{1,0:T(2,128)(2,1)} %collective-permute-done.1.after_h, ...), custom_call_target="tpu_custom_call" | custom-call | tf_op jit(solution)/shard_map/scan/pallas_call | solution.py:403
  26.7 3.1 %collective-permute-start.7 = (bf16[192,2048]{1,0:T(8,128)(2,1)}, bf16[192,2048]{1,0:T(8,128)(2,1)S(1)}, u32[]{:S(2)}, u32[]{:S(2)}) collective-permute-start(bf16[192,2048]{1,0:T(8,128)(2,1)} %collective-permute-done.2.refs_3_), channel_id=1, source_target_pairs={{0,2},{1,15},{2,4},{3,1},{4,6},{5,3},{6,8},{7,5},{8,10},{9,7},{10,... | collective-permute-start | bytes 2359304 | tf_op jit(solution)/shard_map/ppermute | solution.py:392
  29.9 9.2 %collective-permute-done.7.refs_7_ = bf16[192,2048]{1,0:T(8,128)(2,1)S(1)} collective-permute-done((bf16[192,2048]{1,0:T(8,128)(2,1)}, bf16[192,2048]{1,0:T(8,128)(2,1)S(1)}, u32[]{:S(2)}, u32[]{:S(2)}) %collective-permute-start.7) | collective-permute-done | bytes 786464 | tf_op jit(solution)/shard_map/ppermute | solution.py:392
  40.0 3.0 %collective-permute-start.11 = (bf16[192,2048]{1,0:T(8,128)(2,1)S(1)}, bf16[192,2048]{1,0:T(8,128)(2,1)}, u32[]{:S(2)}, u32[]{:S(2)}) collective-permute-start(bf16[192,2048]{1,0:T(8,128)(2,1)S(1)} %collective-permute-done.7.refs_7_), channel_id=1, source_target_pairs={{0,2},{1,15},{2,4},{3,1},{4,6},{5,3},{6,8},{7,5},{8,10},{9,7},{10,... | collective-permute-start | bytes 2359304 | tf_op jit(solution)/shard_map/ppermute | solution.py:392
  43.5 4.0 %collective-permute-done.9.refs_9_ = bf16[192,2048]{1,0:T(8,128)(2,1)} collective-permute-done((bf16[192,2048]{1,0:T(8,128)(2,1)}, bf16[192,2048]{1,0:T(8,128)(2,1)}, u32[]{:S(2)}, u32[]{:S(2)}) %collective-permute-start.9) | collective-permute-done | bytes 786464 | tf_op jit(solution)/shard_map/ppermute | solution.py:392
  47.5 3.1 %collective-permute-start.13 = (bf16[192,2048]{1,0:T(8,128)(2,1)}, bf16[192,2048]{1,0:T(8,128)(2,1)}, u32[]{:S(2)}, u32[]{:S(2)}) collective-permute-start(bf16[192,2048]{1,0:T(8,128)(2,1)} %collective-permute-done.9.refs_9_), channel_id=1, source_target_pairs={{0,2},{1,15},{2,4},{3,1},{4,6},{5,3},{6,8},{7,5},{8,10},{9,7},{10,... | collective-permute-start | bytes 2359304 | tf_op jit(solution)/shard_map/ppermute | solution.py:392
  50.6 5.2 %collective-permute-done.11.refs_11_ = bf16[192,2048]{1,0:T(8,128)(2,1)} collective-permute-done((bf16[192,2048]{1,0:T(8,128)(2,1)S(1)}, bf16[192,2048]{1,0:T(8,128)(2,1)}, u32[]{:S(2)}, u32[]{:S(2)}) %collective-permute-start.11) | collective-permute-done | bytes 786464 | tf_op jit(solution)/shard_map/ppermute | solution.py:392
  55.8 3.2 %collective-permute-start.15 = (bf16[192,2048]{1,0:T(8,128)(2,1)}, bf16[192,2048]{1,0:T(8,128)(2,1)}, u32[]{:S(2)}, u32[]{:S(2)}) collective-permute-start(bf16[192,2048]{1,0:T(8,128)(2,1)} %collective-permute-done.11.refs_11_), channel_id=1, source_target_pairs={{0,2},{1,15},{2,4},{3,1},{4,6},{5,3},{6,8},{7,5},{8,10},{9,7},{10,... | collective-permute-start | bytes 2359304 | tf_op jit(solution)/shard_map/ppermute | solution.py:392
  59.1 13.8 %all_to_all.20.refs_4_ = f32[16,8,128]{2,1,0:T(8,128)} all-to-all(f32[16,8,128]{2,1,0:T(8,128)} %get-tuple-element.20), channel_id=1, replica_groups=mesh['sp'=16,'tp'=16] {'sp'}, dimensions={0} | all-to-all | bytes 131072 | tf_op jit(solution)/shard_map/all_to_all | solution.py:442
  72.9 2.7 %mix.1 = bf16[1024,128]{1,0:T(8,128)(2,1)} custom-call(f32[1024,128]{1,0:T(8,128)} %get-tuple-element.15.refs_0_, f32[1024,128]{1,0:T(8,128)} %get-tuple-element.16.refs_1_, f32[1024,128]{1,0:T(8,128)} %get-tuple-element.17.refs_2_, f32[32,128]{1,0:T(8,128)} %get-tuple-element.18.refs_3_, f32[16,8,128]{2,1,0:T(8,128)} %all_to_all.20.refs_4_, ...), custom_call_target="tpu_custom_call" | custom-call | tf_op jit(solution)/shard_map/mix/pallas_call | solution.py:443
  75.6 6.9 %all-to-all-start.1 = ((bf16[16,64,128]{2,1,0:T(8,128)(2,1)}), bf16[16,64,128]{2,1,0:T(8,128)(2,1)}, u32[]{:S(2)}, u32[]{:S(2)}) async-start(bf16[16,64,128]{2,1,0:T(8,128)(2,1)} %bitcast.15), calls=%async_computation.1 | async-start | bytes 524288 | tf_op jit(solution)/shard_map/all_to_all | solution.py:460
  84.5 9.6 %all-to-all-done.1.mixed_h = bf16[16,64,128]{2,1,0:T(8,128)(2,1)} async-done(((bf16[16,64,128]{2,1,0:T(8,128)(2,1)}), bf16[16,64,128]{2,1,0:T(8,128)(2,1)}, u32[]{:S(2)}, u32[]{:S(2)}) %all-to-all-start.1) | async-done | bytes 262176 | tf_op jit(solution)/shard_map/all_to_all | solution.py:460
  94.1 5.5 %proj.1 = (bf16[64,2048]{1,0:T(8,128)(2,1)}, bf16[256,2048]{1,0:T(8,128)(2,1)}) custom-call(bf16[16,64,128]{2,1,0:T(8,128)(2,1)} %all-to-all-done.1.mixed_h, bf16[2048,2048]{1,0:T(8,128)(2,1)} %weights_h.1, bf16[64,2048]{1,0:T(8,128)(2,1)} %residual_h.1, f32[3,2048]{1,0:T(4,128)} %refs_2_.1, s32[2,64]{1,0:T(2,128)} %copy.19.routes_h), custom_call_target="tpu_custom_call" | custom-call | tf_op jit(solution)/shard_map/proj/pallas_call | solution.py:487
  99.6 3.7 %all-to-all-start.2 = ((bf16[16,16,2048]{2,1,0:T(8,128)(2,1)}), bf16[16,16,2048]{2,1,0:T(8,128)(2,1)S(1)}, u32[]{:S(2)}, u32[]{:S(2)}) async-start(bf16[16,16,2048]{2,1,0:T(8,128)(2,1)} %bitcast.16), calls=%async_computation.2 | async-start | bytes 2097152 | tf_op jit(solution)/shard_map/all_to_all | solution.py:490
  104.7 18.6 %all-to-all-done.2 = bf16[16,16,2048]{2,1,0:T(8,128)(2,1)S(1)} async-done(((bf16[16,16,2048]{2,1,0:T(8,128)(2,1)}), bf16[16,16,2048]{2,1,0:T(8,128)(2,1)S(1)}, u32[]{:S(2)}, u32[]{:S(2)}) %all-to-all-start.2) | async-done | bytes 1048608 | tf_op jit(solution)/shard_map/all_to_all | solution.py:490
  125.5 7.5 %experts.1 = bf16[256,2048]{1,0:T(8,128)(2,1)} custom-call(bf16[256,2048]{1,0:T(8,128)(2,1)S(1)} %bitcast.14, bf16[192,2048]{1,0:T(8,128)(2,1)S(1)} %copy-done, bf16[192,2048]{1,0:T(8,128)(2,1)} %collective-permute-done.3.refs_2_, bf16[192,2048]{1,0:T(8,128)(2,1)} %collective-permute-done.2.refs_3_, bf16[192,2048]{1,0:T(8,128)(2,1)} %collective-permute-done.5.refs_4_, ...), custom_call_target="tpu_custom_call" | custom-call | tf_op jit(solution)/shard_map/experts/pallas_call | solution.py:508
  133.0 4.4 %all-to-all-start.3 = ((bf16[16,16,2048]{2,1,0:T(8,128)(2,1)}), bf16[16,16,2048]{2,1,0:T(8,128)(2,1)}, u32[]{:S(2)}, u32[]{:S(2)}) async-start(bf16[16,16,2048]{2,1,0:T(8,128)(2,1)} %bitcast.10), calls=%async_computation.3 | async-start | bytes 2097152 | tf_op jit(solution)/shard_map/all_to_all | solution.py:509
  138.8 15.0 %all-to-all-done.3 = bf16[16,16,2048]{2,1,0:T(8,128)(2,1)} async-done(((bf16[16,16,2048]{2,1,0:T(8,128)(2,1)}), bf16[16,16,2048]{2,1,0:T(8,128)(2,1)}, u32[]{:S(2)}, u32[]{:S(2)}) %all-to-all-start.3) | async-done | bytes 1048608 | tf_op jit(solution)/shard_map/all_to_all | solution.py:509
  153.9 2.9 %combine.1 = bf16[64,2048]{1,0:T(8,128)(2,1)} custom-call(bf16[256,2048]{1,0:T(8,128)(2,1)} %bitcast.11.refs_0_, bf16[64,2048]{1,0:T(8,128)(2,1)} %get-tuple-element.24.refs_1_, f32[3,2048]{1,0:T(4,128)} %refs_2_.1, s32[64,2]{1,0:T(8,128)} %copy-done.3, f32[64,2]{1,0:T(8,128)} %copy.22.refs_4_), custom_call_target="tpu_custom_call" | custom-call | tf_op jit(solution)/shard_map/combine/pallas_call | solution.py:512
  (37 shorter events, 13.1 us)
Async XLA Ops:
  1.9 7.2 %collective-permute-start.3 = (bf16[192,2048]{1,0:T(8,128)(2,1)}, bf16[192,2048]{1,0:T(8,128)(2,1)}, u32[]{:S(2)}, u32[]{:S(2)}) collective-permute-start(bf16[192,2048]{1,0:T(8,128)(2,1)} %pack.1.refs_1_), channel_id=1, source_target_pairs={{0,1},{1,0},{2,3},{3,2},{4,5},{5,4},{6,7},{7,6},{8,9},{9,8},{10,11... | collective-permute-start | bytes 2359304 | tf_op jit(solution)/shard_map/ppermute | solution.py:395
  5.2 21.0 %collective-permute-start.2 = (bf16[192,2048]{1,0:T(8,128)(2,1)}, bf16[192,2048]{1,0:T(8,128)(2,1)}, u32[]{:S(2)}, u32[]{:S(2)}) collective-permute-start(bf16[192,2048]{1,0:T(8,128)(2,1)} %pack.1.refs_1_), channel_id=1, source_target_pairs={{0,2},{1,15},{2,4},{3,1},{4,6},{5,3},{6,8},{7,5},{8,10},{9,7},{10,... | collective-permute-start | bytes 2359304 | tf_op jit(solution)/shard_map/ppermute | solution.py:392
  9.0 17.7 %collective-permute-start.4 = (bf16[192,2048]{1,0:T(8,128)(2,1)}, bf16[192,2048]{1,0:T(8,128)(2,1)}, u32[]{:S(2)}, u32[]{:S(2)}) collective-permute-start(bf16[192,2048]{1,0:T(8,128)(2,1)} %collective-permute-done.3.refs_2_), channel_id=1, source_target_pairs={{0,2},{1,15},{2,4},{3,1},{4,6},{5,3},{6,8},{7,5},{8,10},{9,7},{10,... | collective-permute-start | bytes 2359304 | tf_op jit(solution)/shard_map/ppermute | solution.py:392
  12.0 4.9 %collective-permute-start = (bf16[2,128]{1,0:T(2,128)(2,1)S(1)}, bf16[2,128]{1,0:T(2,128)(2,1)}, u32[]{:S(2)}, u32[]{:S(2)}) collective-permute-start(bf16[2,128]{1,0:T(2,128)(2,1)S(1)} %get-tuple-element.26), channel_id=1, source_target_pairs={{0,16},{16,32},{32,48},{48,64},{64,80},{80,96},{96,112},{112,128},... | collective-permute-start | bytes 1544 | tf_op jit(solution)/shard_map/ppermute | solution.py:377
  15.6 4.7 %collective-permute-start.1 = (bf16[2,128]{1,0:T(2,128)(2,1)S(1)}, bf16[2,128]{1,0:T(2,128)(2,1)}, u32[]{:S(2)}, u32[]{:S(2)}) collective-permute-start(bf16[2,128]{1,0:T(2,128)(2,1)S(1)} %get-tuple-element.25), channel_id=1, source_target_pairs={{16,0},{32,16},{48,32},{64,48},{80,64},{96,80},{112,96},{128,112},... | collective-permute-start | bytes 1544 | tf_op jit(solution)/shard_map/ppermute | solution.py:378
  26.7 12.4 %collective-permute-start.7 = (bf16[192,2048]{1,0:T(8,128)(2,1)}, bf16[192,2048]{1,0:T(8,128)(2,1)S(1)}, u32[]{:S(2)}, u32[]{:S(2)}) collective-permute-start(bf16[192,2048]{1,0:T(8,128)(2,1)} %collective-permute-done.2.refs_3_), channel_id=1, source_target_pairs={{0,2},{1,15},{2,4},{3,1},{4,6},{5,3},{6,8},{7,5},{8,10},{9,7},{10,... | collective-permute-start | bytes 2359304 | tf_op jit(solution)/shard_map/ppermute | solution.py:392
  29.8 17.7 %collective-permute-start.9 = (bf16[192,2048]{1,0:T(8,128)(2,1)}, bf16[192,2048]{1,0:T(8,128)(2,1)}, u32[]{:S(2)}, u32[]{:S(2)}) collective-permute-start(bf16[192,2048]{1,0:T(8,128)(2,1)} %collective-permute-done.4.refs_5_), channel_id=1, source_target_pairs={{0,2},{1,15},{2,4},{3,1},{4,6},{5,3},{6,8},{7,5},{8,10},{9,7},{10,... | collective-permute-start | bytes 2359304 | tf_op jit(solution)/shard_map/ppermute | solution.py:392
  39.1 0.9 copy-start.1
  40.0 15.9 %collective-permute-start.11 = (bf16[192,2048]{1,0:T(8,128)(2,1)S(1)}, bf16[192,2048]{1,0:T(8,128)(2,1)}, u32[]{:S(2)}, u32[]{:S(2)}) collective-permute-start(bf16[192,2048]{1,0:T(8,128)(2,1)S(1)} %collective-permute-done.7.refs_7_), channel_id=1, source_target_pairs={{0,2},{1,15},{2,4},{3,1},{4,6},{5,3},{6,8},{7,5},{8,10},{9,7},{10,... | collective-permute-start | bytes 2359304 | tf_op jit(solution)/shard_map/ppermute | solution.py:392
  43.0 60.4 %collective-permute-start.5 = (bf16[192,2048]{1,0:T(8,128)(2,1)}, bf16[192,2048]{1,0:T(8,128)(2,1)}, u32[]{:S(2)}, u32[]{:S(2)}) collective-permute-start(bf16[192,2048]{1,0:T(8,128)(2,1)} %collective-permute-done.2.refs_3_), channel_id=1, source_target_pairs={{0,1},{1,0},{2,3},{3,2},{4,5},{5,4},{6,7},{7,6},{8,9},{9,8},{10,11... | collective-permute-start | bytes 2359304 | tf_op jit(solution)/shard_map/ppermute | solution.py:395
  43.0 60.9 %collective-permute-start.6 = (bf16[192,2048]{1,0:T(8,128)(2,1)}, bf16[192,2048]{1,0:T(8,128)(2,1)}, u32[]{:S(2)}, u32[]{:S(2)}) collective-permute-start(bf16[192,2048]{1,0:T(8,128)(2,1)} %collective-permute-done.4.refs_5_), channel_id=1, source_target_pairs={{0,1},{1,0},{2,3},{3,2},{4,5},{5,4},{6,7},{7,6},{8,9},{9,8},{10,11... | collective-permute-start | bytes 2359304 | tf_op jit(solution)/shard_map/ppermute | solution.py:395
  47.5 56.7 %collective-permute-start.13 = (bf16[192,2048]{1,0:T(8,128)(2,1)}, bf16[192,2048]{1,0:T(8,128)(2,1)}, u32[]{:S(2)}, u32[]{:S(2)}) collective-permute-start(bf16[192,2048]{1,0:T(8,128)(2,1)} %collective-permute-done.9.refs_9_), channel_id=1, source_target_pairs={{0,2},{1,15},{2,4},{3,1},{4,6},{5,3},{6,8},{7,5},{8,10},{9,7},{10,... | collective-permute-start | bytes 2359304 | tf_op jit(solution)/shard_map/ppermute | solution.py:392
  55.8 48.6 %collective-permute-start.15 = (bf16[192,2048]{1,0:T(8,128)(2,1)}, bf16[192,2048]{1,0:T(8,128)(2,1)}, u32[]{:S(2)}, u32[]{:S(2)}) collective-permute-start(bf16[192,2048]{1,0:T(8,128)(2,1)} %collective-permute-done.11.refs_11_), channel_id=1, source_target_pairs={{0,2},{1,15},{2,4},{3,1},{4,6},{5,3},{6,8},{7,5},{8,10},{9,7},{10,... | collective-permute-start | bytes 2359304 | tf_op jit(solution)/shard_map/ppermute | solution.py:392
  75.6 18.6 %all-to-all-start.1 = ((bf16[16,64,128]{2,1,0:T(8,128)(2,1)}), bf16[16,64,128]{2,1,0:T(8,128)(2,1)}, u32[]{:S(2)}, u32[]{:S(2)}) async-start(bf16[16,64,128]{2,1,0:T(8,128)(2,1)} %bitcast.15), calls=%async_computation.1 | async-start | bytes 524288 | tf_op jit(solution)/shard_map/all_to_all | solution.py:460
  83.3 0.6 copy-start.3
  99.6 23.6 %all-to-all-start.2 = ((bf16[16,16,2048]{2,1,0:T(8,128)(2,1)}), bf16[16,16,2048]{2,1,0:T(8,128)(2,1)S(1)}, u32[]{:S(2)}, u32[]{:S(2)}) async-start(bf16[16,16,2048]{2,1,0:T(8,128)(2,1)} %bitcast.16), calls=%async_computation.2 | async-start | bytes 2097152 | tf_op jit(solution)/shard_map/all_to_all | solution.py:490
  103.3 20.0 %collective-permute-start.10 = (bf16[192,2048]{1,0:T(8,128)(2,1)}, bf16[192,2048]{1,0:T(8,128)(2,1)S(1)}, u32[]{:S(2)}, u32[]{:S(2)}) collective-permute-start(bf16[192,2048]{1,0:T(8,128)(2,1)} %collective-permute-done.9.refs_9_), channel_id=1, source_target_pairs={{0,1},{1,0},{2,3},{3,2},{4,5},{5,4},{6,7},{7,6},{8,9},{9,8},{10,11... | collective-permute-start | bytes 2359304 | tf_op jit(solution)/shard_map/ppermute | solution.py:395
  103.4 19.8 %collective-permute-start.8 = (bf16[192,2048]{1,0:T(8,128)(2,1)}, bf16[192,2048]{1,0:T(8,128)(2,1)S(1)}, u32[]{:S(2)}, u32[]{:S(2)}) collective-permute-start(bf16[192,2048]{1,0:T(8,128)(2,1)} %copy-done.1), channel_id=1, source_target_pairs={{0,1},{1,0},{2,3},{3,2},{4,5},{5,4},{6,7},{7,6},{8,9},{9,8},{10,11... | collective-permute-start | bytes 2359304 | tf_op jit(solution)/shard_map/ppermute | solution.py:395
  103.9 19.4 %collective-permute-start.12 = (bf16[192,2048]{1,0:T(8,128)(2,1)}, bf16[192,2048]{1,0:T(8,128)(2,1)S(1)}, u32[]{:S(2)}, u32[]{:S(2)}) collective-permute-start(bf16[192,2048]{1,0:T(8,128)(2,1)} %collective-permute-done.11.refs_11_), channel_id=1, source_target_pairs={{0,1},{1,0},{2,3},{3,2},{4,5},{5,4},{6,7},{7,6},{8,9},{9,8},{10,11... | collective-permute-start | bytes 2359304 | tf_op jit(solution)/shard_map/ppermute | solution.py:395
  104.2 19.1 %collective-permute-start.14 = (bf16[192,2048]{1,0:T(8,128)(2,1)}, bf16[192,2048]{1,0:T(8,128)(2,1)}, u32[]{:S(2)}, u32[]{:S(2)}) collective-permute-start(bf16[192,2048]{1,0:T(8,128)(2,1)} %collective-permute-done.13.refs_13_), channel_id=1, source_target_pairs={{0,1},{1,0},{2,3},{3,2},{4,5},{5,4},{6,7},{7,6},{8,9},{9,8},{10,11... | collective-permute-start | bytes 2359304 | tf_op jit(solution)/shard_map/ppermute | solution.py:395
  104.4 18.9 %collective-permute-start.16 = (bf16[192,2048]{1,0:T(8,128)(2,1)}, bf16[192,2048]{1,0:T(8,128)(2,1)}, u32[]{:S(2)}, u32[]{:S(2)}) collective-permute-start(bf16[192,2048]{1,0:T(8,128)(2,1)} %collective-permute-done.15.refs_15_), channel_id=1, source_target_pairs={{0,1},{1,0},{2,3},{3,2},{4,5},{5,4},{6,7},{7,6},{8,9},{9,8},{10,11... | collective-permute-start | bytes 2359304 | tf_op jit(solution)/shard_map/ppermute | solution.py:395
  123.3 1.1 copy-start
  124.4 1.1 copy-start.2
  133.0 20.9 %all-to-all-start.3 = ((bf16[16,16,2048]{2,1,0:T(8,128)(2,1)}), bf16[16,16,2048]{2,1,0:T(8,128)(2,1)}, u32[]{:S(2)}, u32[]{:S(2)}) async-start(bf16[16,16,2048]{2,1,0:T(8,128)(2,1)} %bitcast.10), calls=%async_computation.3 | async-start | bytes 2097152 | tf_op jit(solution)/shard_map/all_to_all | solution.py:509

commit v6 on v5

--- a/solution.py
+++ b/solution.py
@@ -12,10 +12,17 @@
 F32 = jnp.float32
 BF16 = jnp.bfloat16
 SEGS = 8
+VMEM = pltpu.MemorySpace.VMEM
+
+
+def whole():
+    return pl.BlockSpec(memory_space=VMEM)
 
 
 FULL = pltpu.CompilerParams(vmem_limit_bytes=67043328)
-ROOMY = pltpu.CompilerParams(vmem_limit_bytes=30 * 1024 * 1024)
+SMALL = pltpu.CompilerParams(vmem_limit_bytes=8 * 1024 * 1024)
+PROJ = pltpu.CompilerParams(vmem_limit_bytes=67043328 - (8 * 1024 + 448) * 1024)
+ROOMY = pltpu.CompilerParams(vmem_limit_bytes=48 * 1024 * 1024)
 
 
 def anywhere():
@@ -218,50 +225,68 @@
     return values * lax.rsqrt(jnp.mean(values * values, axis=-1, keepdims=True) + EPSILON) * gain
 
 
-def proj_kernel(
-    mixed_h, weights_h, residual_h, gain_h, routes_h, stream_h, outgoing_h,
-    mixed, weights, residual, gain, routes, stream_out, outgoing, sems,
-):
-    (mixed_copy,) = fetched((mixed_h,), (mixed,), sems, 15)
-    width = weights.shape[0]
-    blocks = 8
-    block = width // blocks
-    parts = [(weights_h.at[pl.ds(k * block, block)], weights.at[pl.ds(k * block, block)]) for k in range(blocks)]
-    loads = fetched(*zip(*parts), sems)
-    others = fetched((residual_h, gain_h, routes_h), (residual, gain, routes), sems, blocks)
-    mixed_copy.wait()
-    acc = jnp.zeros(residual.shape, F32)
-    per = mixed.shape[0] // blocks
-    for k in range(blocks):
-        lanes = jnp.concatenate([mixed[k * per + j] for j in range(per)], axis=1)
-        loads[k].wait()
-        acc = acc + jnp.dot(lanes, weights[k * block : (k + 1) * block, :], preferred_element_type=F32)
-    for copy in others:
-        copy.wait()
-    proj = acc.astype(BF16).astype(F32)
-    stream = (residual[...].astype(F32) + scaled(proj, gain[0:1, :])).astype(BF16)
-    stream_out[...] = stream
-    sent = fetched((stream_out,), (stream_h,), sems, 16)
-    normed = scaled(stream.astype(F32), gain[1:2, :]).astype(BF16)
-    rows = normed.shape[0]
-    slots = outgoing.shape[0]
-    experts = 16
-    capacity = slots // experts
-    first, second = routes[0:1, :], routes[1:2, :]
-    ids = lax.broadcasted_iota(jnp.int32, (experts, rows), 0)
+def preload_kernel(source, target, sem):
+    (copy,) = fetched((source,), (target,), sem)
+    copy.wait()
+
+
+def slots_of(first, second, axis, capacity, experts):
+    rows = first.size
+    ids = lax.broadcasted_iota(jnp.int32, (experts, rows) if axis == 0 else (rows, experts), axis)
     hit0 = (ids == first).astype(F32)
     hit1 = (ids == second).astype(F32)
     r = lax.broadcasted_iota(jnp.int32, (rows, rows), 0)
     c = lax.broadcasted_iota(jnp.int32, (rows, rows), 1)
-    earlier = jnp.dot((hit0 + hit1).astype(BF16), (r < c).astype(BF16), preferred_element_type=F32)
-    slot0 = first * capacity + jnp.sum(hit0 * earlier, axis=0, keepdims=True).astype(jnp.int32)
-    slot1 = second * capacity + jnp.sum(hit1 * earlier, axis=0, keepdims=True).astype(jnp.int32)
+    both = (hit0 + hit1).astype(BF16)
+    if axis == 0:
+        earlier = jnp.dot(both, (r < c).astype(BF16), preferred_element_type=F32)
+    else:
+        earlier = jnp.dot((c < r).astype(BF16), both, preferred_element_type=F32)
+    return tuple(
+        ids0 * capacity + jnp.sum(hit * earlier, axis=axis, keepdims=True).astype(jnp.int32)
+        for ids0, hit in ((first, hit0), (second, hit1))
+    )
+
+
+def proj_kernel(
+    weights, mixed, residual_h, gain_h, routes_h, columns_h, route_wt_h, stream_h, outgoing_h, table_h,
+    residual, gain, routes, columns, route_wt, stream_out, outgoing, table_out, sems,
+):
+    small = fetched((routes_h, columns_h, route_wt_h), (routes, columns, route_wt), sems)
+    small += fetched((residual_h, gain_h), (residual, gain), sems, 9)
+    width = weights.shape[0]
+    rows = residual.shape[0]
+    slots = outgoing.shape[0]
+    experts = 16
+    capacity = slots // experts
+    lanes = jnp.concatenate([mixed[j] for j in range(mixed.shape[0])], axis=1)
+    acc = jnp.dot(lanes, weights[...], preferred_element_type=F32)
+    for copy in small:
+        copy.wait()
+    slot0, slot1 = slots_of(columns[:, 0:1], columns[:, 1:2], 1, capacity, experts)
+    places = lax.broadcasted_iota(jnp.int32, (rows, slots), 1)
+    table = jnp.where(places == slot0, route_wt[:, 0:1], 0.0) + jnp.where(
+        places == slot1, route_wt[:, 1:2], 0.0
+    )
+    high = table.astype(BF16)
+    rest = table - high.astype(F32)
+    mid = rest.astype(BF16)
+    table_out[0:rows, :] = high
+    table_out[rows : 2 * rows, :] = mid
+    table_out[2 * rows : 3 * rows, :] = (rest - mid.astype(F32)).astype(BF16)
+    sent = fetched((table_out,), (table_h,), sems, 3)
+    slot0, slot1 = slots_of(routes[0:1, :], routes[1:2, :], 0, capacity, experts)
     places = lax.broadcasted_iota(jnp.int32, (slots, rows), 0)
     pick = jnp.where(jnp.logical_or(places == slot0, places == slot1), 1.0, 0.0).astype(BF16)
+    proj = acc.astype(BF16).astype(F32)
+    stream = (residual[...].astype(F32) + scaled(proj, gain[0:1, :])).astype(BF16)
+    stream_out[...] = stream
+    sent += fetched((stream_out,), (stream_h,), sems, 4)
+    normed = scaled(stream.astype(F32), gain[1:2, :]).astype(BF16)
     for k in range(4):
-        part = slice(k * 512, (k + 1) * 512)
+        part = slice(k * width // 4, (k + 1) * width // 4)
         outgoing[:, part] = jnp.dot(pick, normed[:, part], preferred_element_type=F32).astype(BF16)
-        sent += fetched([outgoing.at[:, part]], [outgoing_h.at[:, part]], sems, 11 + k)
+        sent += fetched([outgoing.at[:, part]], [outgoing_h.at[:, part]], sems, 5 + k)
     for copy in sent:
         copy.wait()
 
@@ -313,36 +338,16 @@
 
 
 def combine_kernel(*refs):
-    sources, out_h, buffers, out, sems = refs[:5], refs[5], refs[6:11], refs[11], refs[12]
-    values, stream, gain, routes, weights = buffers
+    sources, out_h, buffers, out, sems = refs[:4], refs[4], refs[5:9], refs[9], refs[10]
+    values, stream, gain, table = buffers
     for copy in fetched(sources, buffers, sems):
         copy.wait()
     rows = stream.shape[0]
-    slots = values.shape[0]
-    experts = 16
-    capacity = slots // experts
-    first, second = routes[:, 0:1], routes[:, 1:2]
-    ids = lax.broadcasted_iota(jnp.int32, (rows, experts), 1)
-    hit0 = (ids == first).astype(F32)
-    hit1 = (ids == second).astype(F32)
-    r = lax.broadcasted_iota(jnp.int32, (rows, rows), 0)
-    c = lax.broadcasted_iota(jnp.int32, (rows, rows), 1)
-    earlier = jnp.dot((c < r).astype(BF16), (hit0 + hit1).astype(BF16), preferred_element_type=F32)
-    slot0 = first * capacity + jnp.sum(hit0 * earlier, axis=1, keepdims=True).astype(jnp.int32)
-    slot1 = second * capacity + jnp.sum(hit1 * earlier, axis=1, keepdims=True).astype(jnp.int32)
-    places = lax.broadcasted_iota(jnp.int32, (rows, slots), 1)
-    table = jnp.where(places == slot0, weights[:, 0:1], 0.0) + jnp.where(
-        places == slot1, weights[:, 1:2], 0.0
-    )
-    high = table.astype(BF16)
-    rest = table - high.astype(F32)
-    mid = rest.astype(BF16)
-    low = (rest - mid.astype(F32)).astype(BF16)
-    parts = jnp.dot(jnp.concatenate([high, mid, low], axis=0), values[...], preferred_element_type=F32)
+    parts = jnp.dot(table[...], values[...], preferred_element_type=F32)
     mixture = parts[0:rows] + (parts[rows : 2 * rows] + parts[2 * rows : 3 * rows])
     mixture = mixture.astype(BF16).astype(F32)
     out[...] = (stream[...].astype(F32) + scaled(mixture, gain[2:3, :])).astype(BF16)
-    (copy,) = fetched((out,), (out_h,), sems, 5)
+    (copy,) = fetched((out,), (out_h,), sems, 4)
     copy.wait()
 
 
@@ -466,28 +471,47 @@
     own_routes = lax.dynamic_slice_in_dim(routes, first_row, rows, 0)
     own_weights = lax.dynamic_slice_in_dim(route_wt, first_row, rows, 0)
     slots = 2 * rows * routes.shape[1]
+    preload = pl.pallas_call(
+        preload_kernel,
+        out_shape=shape(out_proj.shape, BF16),
+        in_specs=[anywhere()],
+        out_specs=whole(),
+        scratch_shapes=[pltpu.SemaphoreType.DMA((1,))],
+        compiler_params=PROJ,
+        name="preload",
+    )
+    weights_v = preload(out_proj)
     project = pl.pallas_call(
         proj_kernel,
-        out_shape=(shape((rows, width), BF16), shape((slots, width), BF16)),
-        in_specs=[anywhere()] * 5,
-        out_specs=(anywhere(), anywhere()),
+        out_shape=(
+            shape((rows, width), BF16),
+            shape((slots, width), BF16),
+            shape((3 * rows, slots), BF16),
+        ),
+        in_specs=[whole()] * 2 + [anywhere()] * 5,
+        out_specs=(anywhere(),) * 3,
         scratch_shapes=[
-            pltpu.VMEM(token_rows.shape, BF16),
-            pltpu.VMEM(out_proj.shape, BF16),
             pltpu.VMEM(residual.shape, BF16),
             pltpu.VMEM(norm_gain.shape, F32),
             pltpu.VMEM((routes.shape[1], rows), jnp.int32),
+            pltpu.VMEM(own_routes.shape, jnp.int32),
+            pltpu.VMEM(own_weights.shape, F32),
             pltpu.VMEM(residual.shape, BF16),
             pltpu.VMEM((slots, width), BF16),
-            pltpu.SemaphoreType.DMA((17,)),
+            pltpu.VMEM((3 * rows, slots), BF16),
+            pltpu.SemaphoreType.DMA((11,)),
         ],
-        compiler_params=FULL,
+        compiler_params=PROJ,
         name="proj",
     )
-    stream, outgoing = project(token_rows, out_proj, residual, norm_gain, own_routes.T)
+    stream, outgoing, table = project(
+        weights_v, token_rows, residual, norm_gain, own_routes.T, own_routes, own_weights
+    )
     r4, e3a = around(r3a), across(r3a)
     e3b, e4 = across(r3b), across(r4)
-    arrived = lax.all_to_all(outgoing.reshape(sp, slots // sp, width), "sp", split_axis=0, concat_axis=0, tiled=True)
+    arrived = lax.all_to_all(
+        outgoing.reshape(sp, slots // sp, width), "sp", split_axis=0, concat_axis=0, tiled=True
+    )
     arrived = arrived.reshape(slots, width)
 
     shares = (own, other, r1a, e1a, r1b, e1b, r2a, e2a, r2b, e2b, r3a, e3a, r3b, e3b, r4, e4)
@@ -512,20 +536,19 @@
     return pl.pallas_call(
         combine_kernel,
         out_shape=shape((rows, width), BF16),
-        in_specs=[anywhere()] * 5,
+        in_specs=[anywhere()] * 4,
         out_specs=anywhere(),
         scratch_shapes=[
             pltpu.VMEM((slots, width), BF16),
             pltpu.VMEM((rows, width), BF16),
             pltpu.VMEM(norm_gain.shape, F32),
-            pltpu.VMEM(own_routes.shape, jnp.int32),
-            pltpu.VMEM(own_weights.shape, F32),
+            pltpu.VMEM((3 * rows, slots), BF16),
             pltpu.VMEM((rows, width), BF16),
-            pltpu.SemaphoreType.DMA((6,)),
+            pltpu.SemaphoreType.DMA((5,)),
         ],
         compiler_params=FULL,
         name="combine",
-    )(returned.reshape(slots, width), stream, norm_gain, own_routes, own_weights)
+    )(returned.reshape(slots, width), stream, norm_gain, table)
 
 
 def solution(mesh):

time: 158 us -> 158 us (level)
  waiting for transfers between devices: 65.6 us -> 42.9 us
  blocking collectives: 13.8 us -> 34.6 us
  Pallas kernels: 26.3 us -> 34.3 us
  starting transfers between devices: 43.5 us -> 39.2 us
    all_to_all x0 -> x1, blocking collectives: none -> 20.8 us  [layer(): lax.all_to_all(done.reshape(sp, slots // sp, width), 'sp', split_axis=0,...]
    all_to_all x1 -> x0, waiting for transfers between devices: 15 us -> none  [layer(): lax.all_to_all(done.reshape(sp, slots // sp, width), 'sp', split_axis=0,...]
    pallas_call x1 -> x2, Pallas kernels: 5.48 us -> 13.5 us  [the longest x1 6.88 us: layer(): project(weights_v, token_rows, residual, norm_gain, own_routes.T, own_rou...]
    all_to_all x1, waiting for transfers between devices: 9.58 us -> 1.93 us  [layer(): lax.all_to_all(mixed.reshape(tp, rows, channels), 'tp', split_axis=0, con...]
    all_to_all x1 -> x0, starting transfers between devices: 4.35 us -> none  [layer(): lax.all_to_all(done.reshape(sp, slots // sp, width), 'sp', split_axis=0,...]
    unnamed x10 -> x16, local copies, waits for them, and re-layouts: 4.55 us -> 3.64 us
  transfers between devices with their start and end apart: 20 -> 19, of which waited for: 8 -> 7; matrix products, arithmetic and copies ran while one was open for 2% -> 2% of each run, Pallas kernels for 9% -> 14%
where the time goes in v6:
time: 158 us
  waiting for transfers between devices  42.9 us (27%)
  starting transfers between devices  39.2 us (25%)
  blocking collectives  34.6 us (22%)
  Pallas kernels  34.3 us (22%)
  local copies, waits for them, and re-layouts  6.49 us (4%)
    all_to_all x1, blocking collectives, layer(): lax.all_to_all(done.reshape(sp, slots // sp, width), 'sp', split_axis=0,...  20.8 us
    ppermute x7, waiting for transfers between devices, around(): lax.ppermute(part, 'tp', [(i, (i + 2 - 4 * (i % 2)) % tp) for i in range(...  18.9 us
    ppermute x7, starting transfers between devices, around(): lax.ppermute(part, 'tp', [(i, (i + 2 - 4 * (i % 2)) % tp) for i in range(...  18.6 us
    all_to_all x1, waiting for transfers between devices, layer(): lax.all_to_all(outgoing.reshape(sp, slots // sp, width), 'sp', split_axis...  18.6 us
    all_to_all x1, blocking collectives, layer(): lax.all_to_all(total, 'sp', split_axis=0, concat_axis=0, tiled=True)  13.8 us
    pallas_call x1, Pallas kernels, layer(): done = experts(arrived, *shares)  7.66 us
    pallas_call x1, Pallas kernels, layer(): project(weights_v, token_rows, residual, norm_gain, own_routes.T, own_rou...  6.88 us
    all_to_all x1, starting transfers between devices, layer(): lax.all_to_all(mixed.reshape(tp, rows, channels), 'tp', split_axis=0, con...  6.87 us
  transfers between devices with their start and end apart: 19, of which 7 were waited for; matrix products, arithmetic and copies ran while one was open for 2% of the time, Pallas kernels for 14%

profile of v6, /device:TPU:1, one launch (start us, length us, event | category | flops | bytes accessed | tf_op | source)
XLA Modules:
  0.0 157.7 jit_solution(8814033865518907927)
XLA Ops:
  1.9 3.3 %collective-permute-start.3 = (bf16[192,2048]{1,0:T(8,128)(2,1)}, bf16[192,2048]{1,0:T(8,128)(2,1)}, u32[]{:S(2)}, u32[]{:S(2)}) collective-permute-start(bf16[192,2048]{1,0:T(8,128)(2,1)} %pack.1.refs_1_), channel_id=1, source_target_pairs={{0,1},{1,0},{2,3},{3,2},{4,5},{5,4},{6,7},{7,6},{8,9},{9,8},{10,11... | collective-permute-start | bytes 2359304 | tf_op jit(solution)/shard_map/ppermute | solution.py:400
  5.2 3.9 %collective-permute-start.2 = (bf16[192,2048]{1,0:T(8,128)(2,1)}, bf16[192,2048]{1,0:T(8,128)(2,1)}, u32[]{:S(2)}, u32[]{:S(2)}) collective-permute-start(bf16[192,2048]{1,0:T(8,128)(2,1)} %pack.1.refs_1_), channel_id=1, source_target_pairs={{0,2},{1,15},{2,4},{3,1},{4,6},{5,3},{6,8},{7,5},{8,10},{9,7},{10,... | collective-permute-start | bytes 2359304 | tf_op jit(solution)/shard_map/ppermute | solution.py:397
  9.1 2.3 %collective-permute-start.4 = (bf16[192,2048]{1,0:T(8,128)(2,1)}, bf16[192,2048]{1,0:T(8,128)(2,1)}, u32[]{:S(2)}, u32[]{:S(2)}) collective-permute-start(bf16[192,2048]{1,0:T(8,128)(2,1)} %collective-permute-done.3.refs_2_), channel_id=1, source_target_pairs={{0,2},{1,15},{2,4},{3,1},{4,6},{5,3},{6,8},{7,5},{8,10},{9,7},{10,... | collective-permute-start | bytes 2359304 | tf_op jit(solution)/shard_map/ppermute | solution.py:397
  12.0 3.6 %collective-permute-start = (bf16[2,128]{1,0:T(2,128)(2,1)S(1)}, bf16[2,128]{1,0:T(2,128)(2,1)}, u32[]{:S(2)}, u32[]{:S(2)}) collective-permute-start(bf16[2,128]{1,0:T(2,128)(2,1)S(1)} %get-tuple-element.28), channel_id=1, source_target_pairs={{0,16},{16,32},{32,48},{48,64},{64,80},{80,96},{96,112},{112,128},... | collective-permute-start | bytes 1544 | tf_op jit(solution)/shard_map/ppermute | solution.py:382
  16.9 3.4 %collective-permute-done.1.after_h = bf16[2,128]{1,0:T(2,128)(2,1)} collective-permute-done((bf16[2,128]{1,0:T(2,128)(2,1)S(1)}, bf16[2,128]{1,0:T(2,128)(2,1)}, u32[]{:S(2)}, u32[]{:S(2)}) %collective-permute-start.1) | collective-permute-done | bytes 544 | tf_op jit(solution)/shard_map/ppermute | solution.py:383
  20.3 5.9 %scan.1 = (f32[1024,128]{1,0:T(8,128)}, f32[1024,128]{1,0:T(8,128)}, f32[1024,128]{1,0:T(8,128)}, f32[32,128]{1,0:T(8,128)}, f32[16,8,128]{2,1,0:T(8,128)}) custom-call(bf16[1024,128]{1,0:T(8,128)(2,1)} %mix_h.1, bf16[2,128]{1,0:T(2,128)(2,1)} %collective-permute-done.before_h, bf16[2,128]{1,0:T(2,128)(2,1)} %collective-permute-done.1.after_h, ...), custom_call_target="tpu_custom_call" | custom-call | tf_op jit(solution)/shard_map/scan/pallas_call | solution.py:408
  26.8 3.1 %collective-permute-start.7 = (bf16[192,2048]{1,0:T(8,128)(2,1)}, bf16[192,2048]{1,0:T(8,128)(2,1)S(1)}, u32[]{:S(2)}, u32[]{:S(2)}) collective-permute-start(bf16[192,2048]{1,0:T(8,128)(2,1)} %collective-permute-done.2.refs_3_), channel_id=1, source_target_pairs={{0,2},{1,15},{2,4},{3,1},{4,6},{5,3},{6,8},{7,5},{8,10},{9,7},{10,... | collective-permute-start | bytes 2359304 | tf_op jit(solution)/shard_map/ppermute | solution.py:397
  29.9 9.2 %collective-permute-done.7.refs_7_ = bf16[192,2048]{1,0:T(8,128)(2,1)S(1)} collective-permute-done((bf16[192,2048]{1,0:T(8,128)(2,1)}, bf16[192,2048]{1,0:T(8,128)(2,1)S(1)}, u32[]{:S(2)}, u32[]{:S(2)}) %collective-permute-start.7) | collective-permute-done | bytes 786464 | tf_op jit(solution)/shard_map/ppermute | solution.py:397
  40.0 3.0 %collective-permute-start.11 = (bf16[192,2048]{1,0:T(8,128)(2,1)S(1)}, bf16[192,2048]{1,0:T(8,128)(2,1)}, u32[]{:S(2)}, u32[]{:S(2)}) collective-permute-start(bf16[192,2048]{1,0:T(8,128)(2,1)S(1)} %collective-permute-done.7.refs_7_), channel_id=1, source_target_pairs={{0,2},{1,15},{2,4},{3,1},{4,6},{5,3},{6,8},{7,5},{8,10},{9,7},{10,... | collective-permute-start | bytes 2359304 | tf_op jit(solution)/shard_map/ppermute | solution.py:397
  43.6 4.0 %collective-permute-done.9.refs_9_ = bf16[192,2048]{1,0:T(8,128)(2,1)} collective-permute-done((bf16[192,2048]{1,0:T(8,128)(2,1)}, bf16[192,2048]{1,0:T(8,128)(2,1)}, u32[]{:S(2)}, u32[]{:S(2)}) %collective-permute-start.9) | collective-permute-done | bytes 786464 | tf_op jit(solution)/shard_map/ppermute | solution.py:397
  47.5 3.1 %collective-permute-start.13 = (bf16[192,2048]{1,0:T(8,128)(2,1)}, bf16[192,2048]{1,0:T(8,128)(2,1)}, u32[]{:S(2)}, u32[]{:S(2)}) collective-permute-start(bf16[192,2048]{1,0:T(8,128)(2,1)} %collective-permute-done.9.refs_9_), channel_id=1, source_target_pairs={{0,2},{1,15},{2,4},{3,1},{4,6},{5,3},{6,8},{7,5},{8,10},{9,7},{10,... | collective-permute-start | bytes 2359304 | tf_op jit(solution)/shard_map/ppermute | solution.py:397
  50.7 5.2 %collective-permute-done.11.refs_11_ = bf16[192,2048]{1,0:T(8,128)(2,1)} collective-permute-done((bf16[192,2048]{1,0:T(8,128)(2,1)S(1)}, bf16[192,2048]{1,0:T(8,128)(2,1)}, u32[]{:S(2)}, u32[]{:S(2)}) %collective-permute-start.11) | collective-permute-done | bytes 786464 | tf_op jit(solution)/shard_map/ppermute | solution.py:397
  55.9 3.2 %collective-permute-start.15 = (bf16[192,2048]{1,0:T(8,128)(2,1)}, bf16[192,2048]{1,0:T(8,128)(2,1)}, u32[]{:S(2)}, u32[]{:S(2)}) collective-permute-start(bf16[192,2048]{1,0:T(8,128)(2,1)} %collective-permute-done.11.refs_11_), channel_id=1, source_target_pairs={{0,2},{1,15},{2,4},{3,1},{4,6},{5,3},{6,8},{7,5},{8,10},{9,7},{10,... | collective-permute-start | bytes 2359304 | tf_op jit(solution)/shard_map/ppermute | solution.py:397
  59.1 13.8 %all_to_all.20.refs_4_ = f32[16,8,128]{2,1,0:T(8,128)} all-to-all(f32[16,8,128]{2,1,0:T(8,128)} %get-tuple-element.21), channel_id=1, replica_groups=mesh['sp'=16,'tp'=16] {'sp'}, dimensions={0} | all-to-all | bytes 131072 | tf_op jit(solution)/shard_map/all_to_all | solution.py:447
  72.9 2.7 %mix.1 = bf16[1024,128]{1,0:T(8,128)(2,1)} custom-call(f32[1024,128]{1,0:T(8,128)} %get-tuple-element.16.refs_0_, f32[1024,128]{1,0:T(8,128)} %get-tuple-element.17.refs_1_, f32[1024,128]{1,0:T(8,128)} %get-tuple-element.18.refs_2_, f32[32,128]{1,0:T(8,128)} %get-tuple-element.19.refs_3_, f32[16,8,128]{2,1,0:T(8,128)} %all_to_all.20.refs_4_, ...), custom_call_target="tpu_custom_call" | custom-call | tf_op jit(solution)/shard_map/mix/pallas_call | solution.py:448
  75.6 6.9 %all-to-all-start.1 = ((bf16[16,64,128]{2,1,0:T(8,128)(2,1)}), bf16[16,64,128]{2,1,0:T(8,128)(2,1)S(1)}, u32[]{:S(2)}, u32[]{:S(2)}) async-start(bf16[16,64,128]{2,1,0:T(8,128)(2,1)} %bitcast.17), calls=%async_computation.1 | async-start | bytes 524288 | tf_op jit(solution)/shard_map/all_to_all | solution.py:465
  85.4 6.7 %preload.1.weights = bf16[2048,2048]{1,0:T(8,128)(2,1)} custom-call(bf16[2048,2048]{1,0:T(8,128)(2,1)} %source.1), custom_call_target="tpu_custom_call" | custom-call | tf_op jit(solution)/shard_map/preload/pallas_call | solution.py:483
  92.1 1.9 %all-to-all-done.1.mixed = bf16[16,64,128]{2,1,0:T(8,128)(2,1)S(1)} async-done(((bf16[16,64,128]{2,1,0:T(8,128)(2,1)}), bf16[16,64,128]{2,1,0:T(8,128)(2,1)S(1)}, u32[]{:S(2)}, u32[]{:S(2)}) %all-to-all-start.1) | async-done | bytes 262176 | tf_op jit(solution)/shard_map/all_to_all | solution.py:465
  94.8 6.9 %proj.1 = (bf16[64,2048]{1,0:T(8,128)(2,1)}, bf16[256,2048]{1,0:T(8,128)(2,1)}, bf16[192,256]{1,0:T(8,128)(2,1)}) custom-call(bf16[2048,2048]{1,0:T(8,128)(2,1)} %preload.1.weights, bf16[16,64,128]{2,1,0:T(8,128)(2,1)} %copy-done.4, bf16[64,2048]{1,0:T(8,128)(2,1)} %residual_h.1, f32[3,2048]{1,0:T(4,128)} %refs_2_.1, s32[2,64]{1,0:T(2,128)} %copy.20.routes_h, ...), custom_call_target="tpu_custom_call" | custom-call | tf_op jit(solution)/shard_map/proj/pallas_call | solution.py:507
  101.6 3.7 %all-to-all-start.2 = ((bf16[16,16,2048]{2,1,0:T(8,128)(2,1)}), bf16[16,16,2048]{2,1,0:T(8,128)(2,1)S(1)}, u32[]{:S(2)}, u32[]{:S(2)}) async-start(bf16[16,16,2048]{2,1,0:T(8,128)(2,1)} %bitcast.18), calls=%async_computation.2 | async-start | bytes 2097152 | tf_op jit(solution)/shard_map/all_to_all | solution.py:512
  106.7 18.6 %all-to-all-done.2 = bf16[16,16,2048]{2,1,0:T(8,128)(2,1)S(1)} async-done(((bf16[16,16,2048]{2,1,0:T(8,128)(2,1)}), bf16[16,16,2048]{2,1,0:T(8,128)(2,1)S(1)}, u32[]{:S(2)}, u32[]{:S(2)}) %all-to-all-start.2) | async-done | bytes 1048608 | tf_op jit(solution)/shard_map/all_to_all | solution.py:512
  126.5 7.7 %experts.1 = bf16[256,2048]{1,0:T(8,128)(2,1)} custom-call(bf16[256,2048]{1,0:T(8,128)(2,1)} %bitcast.14, bf16[192,2048]{1,0:T(8,128)(2,1)S(1)} %copy-done, bf16[192,2048]{1,0:T(8,128)(2,1)} %collective-permute-done.3.refs_2_, bf16[192,2048]{1,0:T(8,128)(2,1)} %collective-permute-done.2.refs_3_, bf16[192,2048]{1,0:T(8,128)(2,1)} %collective-permute-done.5.refs_4_, ...), custom_call_target="tpu_custom_call" | custom-call | tf_op jit(solution)/shard_map/experts/pallas_call | solution.py:532
  134.2 20.8 %all_to_all.21 = bf16[16,16,2048]{2,1,0:T(8,128)(2,1)} all-to-all(bf16[16,16,2048]{2,1,0:T(8,128)(2,1)} %bitcast.15), channel_id=1, replica_groups=mesh['sp'=16,'tp'=16] {'sp'}, dimensions={0} | all-to-all | bytes 2097152 | tf_op jit(solution)/shard_map/all_to_all | solution.py:533
  155.0 2.6 %combine.1 = bf16[64,2048]{1,0:T(8,128)(2,1)} custom-call(bf16[256,2048]{1,0:T(8,128)(2,1)} %bitcast.16, bf16[64,2048]{1,0:T(8,128)(2,1)} %get-tuple-element.25.refs_1_, f32[3,2048]{1,0:T(4,128)} %refs_2_.1, bf16[192,256]{1,0:T(8,128)(2,1)} %get-tuple-element.26.refs_3_), custom_call_target="tpu_custom_call" | custom-call | tf_op jit(solution)/shard_map/combine/pallas_call | solution.py:536
  (43 shorter events, 12.1 us)
Async XLA Ops:
  1.9 7.2 %collective-permute-start.3 = (bf16[192,2048]{1,0:T(8,128)(2,1)}, bf16[192,2048]{1,0:T(8,128)(2,1)}, u32[]{:S(2)}, u32[]{:S(2)}) collective-permute-start(bf16[192,2048]{1,0:T(8,128)(2,1)} %pack.1.refs_1_), channel_id=1, source_target_pairs={{0,1},{1,0},{2,3},{3,2},{4,5},{5,4},{6,7},{7,6},{8,9},{9,8},{10,11... | collective-permute-start | bytes 2359304 | tf_op jit(solution)/shard_map/ppermute | solution.py:400
  5.2 21.0 %collective-permute-start.2 = (bf16[192,2048]{1,0:T(8,128)(2,1)}, bf16[192,2048]{1,0:T(8,128)(2,1)}, u32[]{:S(2)}, u32[]{:S(2)}) collective-permute-start(bf16[192,2048]{1,0:T(8,128)(2,1)} %pack.1.refs_1_), channel_id=1, source_target_pairs={{0,2},{1,15},{2,4},{3,1},{4,6},{5,3},{6,8},{7,5},{8,10},{9,7},{10,... | collective-permute-start | bytes 2359304 | tf_op jit(solution)/shard_map/ppermute | solution.py:397
  9.1 17.7 %collective-permute-start.4 = (bf16[192,2048]{1,0:T(8,128)(2,1)}, bf16[192,2048]{1,0:T(8,128)(2,1)}, u32[]{:S(2)}, u32[]{:S(2)}) collective-permute-start(bf16[192,2048]{1,0:T(8,128)(2,1)} %collective-permute-done.3.refs_2_), channel_id=1, source_target_pairs={{0,2},{1,15},{2,4},{3,1},{4,6},{5,3},{6,8},{7,5},{8,10},{9,7},{10,... | collective-permute-start | bytes 2359304 | tf_op jit(solution)/shard_map/ppermute | solution.py:397
  12.0 4.9 %collective-permute-start = (bf16[2,128]{1,0:T(2,128)(2,1)S(1)}, bf16[2,128]{1,0:T(2,128)(2,1)}, u32[]{:S(2)}, u32[]{:S(2)}) collective-permute-start(bf16[2,128]{1,0:T(2,128)(2,1)S(1)} %get-tuple-element.28), channel_id=1, source_target_pairs={{0,16},{16,32},{32,48},{48,64},{64,80},{80,96},{96,112},{112,128},... | collective-permute-start | bytes 1544 | tf_op jit(solution)/shard_map/ppermute | solution.py:382
  15.6 4.7 %collective-permute-start.1 = (bf16[2,128]{1,0:T(2,128)(2,1)S(1)}, bf16[2,128]{1,0:T(2,128)(2,1)}, u32[]{:S(2)}, u32[]{:S(2)}) collective-permute-start(bf16[2,128]{1,0:T(2,128)(2,1)S(1)} %get-tuple-element.27), channel_id=1, source_target_pairs={{16,0},{32,16},{48,32},{64,48},{80,64},{96,80},{112,96},{128,112},... | collective-permute-start | bytes 1544 | tf_op jit(solution)/shard_map/ppermute | solution.py:383
  26.8 12.4 %collective-permute-start.7 = (bf16[192,2048]{1,0:T(8,128)(2,1)}, bf16[192,2048]{1,0:T(8,128)(2,1)S(1)}, u32[]{:S(2)}, u32[]{:S(2)}) collective-permute-start(bf16[192,2048]{1,0:T(8,128)(2,1)} %collective-permute-done.2.refs_3_), channel_id=1, source_target_pairs={{0,2},{1,15},{2,4},{3,1},{4,6},{5,3},{6,8},{7,5},{8,10},{9,7},{10,... | collective-permute-start | bytes 2359304 | tf_op jit(solution)/shard_map/ppermute | solution.py:397
  29.9 17.7 %collective-permute-start.9 = (bf16[192,2048]{1,0:T(8,128)(2,1)}, bf16[192,2048]{1,0:T(8,128)(2,1)}, u32[]{:S(2)}, u32[]{:S(2)}) collective-permute-start(bf16[192,2048]{1,0:T(8,128)(2,1)} %collective-permute-done.4.refs_5_), channel_id=1, source_target_pairs={{0,2},{1,15},{2,4},{3,1},{4,6},{5,3},{6,8},{7,5},{8,10},{9,7},{10,... | collective-permute-start | bytes 2359304 | tf_op jit(solution)/shard_map/ppermute | solution.py:397
  40.0 15.8 %collective-permute-start.11 = (bf16[192,2048]{1,0:T(8,128)(2,1)S(1)}, bf16[192,2048]{1,0:T(8,128)(2,1)}, u32[]{:S(2)}, u32[]{:S(2)}) collective-permute-start(bf16[192,2048]{1,0:T(8,128)(2,1)S(1)} %collective-permute-done.7.refs_7_), channel_id=1, source_target_pairs={{0,2},{1,15},{2,4},{3,1},{4,6},{5,3},{6,8},{7,5},{8,10},{9,7},{10,... | collective-permute-start | bytes 2359304 | tf_op jit(solution)/shard_map/ppermute | solution.py:397
  43.1 62.4 %collective-permute-start.5 = (bf16[192,2048]{1,0:T(8,128)(2,1)}, bf16[192,2048]{1,0:T(8,128)(2,1)}, u32[]{:S(2)}, u32[]{:S(2)}) collective-permute-start(bf16[192,2048]{1,0:T(8,128)(2,1)} %collective-permute-done.2.refs_3_), channel_id=1, source_target_pairs={{0,1},{1,0},{2,3},{3,2},{4,5},{5,4},{6,7},{7,6},{8,9},{9,8},{10,11... | collective-permute-start | bytes 2359304 | tf_op jit(solution)/shard_map/ppermute | solution.py:400
  43.1 62.9 %collective-permute-start.6 = (bf16[192,2048]{1,0:T(8,128)(2,1)}, bf16[192,2048]{1,0:T(8,128)(2,1)}, u32[]{:S(2)}, u32[]{:S(2)}) collective-permute-start(bf16[192,2048]{1,0:T(8,128)(2,1)} %collective-permute-done.4.refs_5_), channel_id=1, source_target_pairs={{0,1},{1,0},{2,3},{3,2},{4,5},{5,4},{6,7},{7,6},{8,9},{9,8},{10,11... | collective-permute-start | bytes 2359304 | tf_op jit(solution)/shard_map/ppermute | solution.py:400
  47.5 58.7 %collective-permute-start.13 = (bf16[192,2048]{1,0:T(8,128)(2,1)}, bf16[192,2048]{1,0:T(8,128)(2,1)}, u32[]{:S(2)}, u32[]{:S(2)}) collective-permute-start(bf16[192,2048]{1,0:T(8,128)(2,1)} %collective-permute-done.9.refs_9_), channel_id=1, source_target_pairs={{0,2},{1,15},{2,4},{3,1},{4,6},{5,3},{6,8},{7,5},{8,10},{9,7},{10,... | collective-permute-start | bytes 2359304 | tf_op jit(solution)/shard_map/ppermute | solution.py:397
  55.9 50.6 %collective-permute-start.15 = (bf16[192,2048]{1,0:T(8,128)(2,1)}, bf16[192,2048]{1,0:T(8,128)(2,1)}, u32[]{:S(2)}, u32[]{:S(2)}) collective-permute-start(bf16[192,2048]{1,0:T(8,128)(2,1)} %collective-permute-done.11.refs_11_), channel_id=1, source_target_pairs={{0,2},{1,15},{2,4},{3,1},{4,6},{5,3},{6,8},{7,5},{8,10},{9,7},{10,... | collective-permute-start | bytes 2359304 | tf_op jit(solution)/shard_map/ppermute | solution.py:397
  75.6 18.5 %all-to-all-start.1 = ((bf16[16,64,128]{2,1,0:T(8,128)(2,1)}), bf16[16,64,128]{2,1,0:T(8,128)(2,1)S(1)}, u32[]{:S(2)}, u32[]{:S(2)}) async-start(bf16[16,64,128]{2,1,0:T(8,128)(2,1)} %bitcast.17), calls=%async_computation.1 | async-start | bytes 524288 | tf_op jit(solution)/shard_map/all_to_all | solution.py:465
  83.3 8.8 %copy-start.6 = (s32[64,2]{1,0:T(8,128)}, s32[64,2]{1,0:T(8,128)S(1)}, u32[]{:S(2)}) copy-start(s32[64,2]{1,0:T(8,128)S(1)} %copy.21.columns_h) | copy-start | bytes 1540
  92.1 13.3 %copy-start.2 = (bf16[192,2048]{1,0:T(8,128)(2,1)S(1)}, bf16[192,2048]{1,0:T(8,128)(2,1)}, u32[]{:S(2)}) copy-start(bf16[192,2048]{1,0:T(8,128)(2,1)} %copy-done.1) | copy-start | bytes 2359300
  92.1 34.4 %copy-start = (bf16[192,2048]{1,0:T(8,128)(2,1)S(1)}, bf16[192,2048]{1,0:T(8,128)(2,1)}, u32[]{:S(2)}) copy-start(bf16[192,2048]{1,0:T(8,128)(2,1)} %pack.1.refs_1_) | copy-start | bytes 2359300
  101.6 23.6 %all-to-all-start.2 = ((bf16[16,16,2048]{2,1,0:T(8,128)(2,1)}), bf16[16,16,2048]{2,1,0:T(8,128)(2,1)S(1)}, u32[]{:S(2)}, u32[]{:S(2)}) async-start(bf16[16,16,2048]{2,1,0:T(8,128)(2,1)} %bitcast.18), calls=%async_computation.2 | async-start | bytes 2097152 | tf_op jit(solution)/shard_map/all_to_all | solution.py:512
  105.3 20.0 %collective-permute-start.10 = (bf16[192,2048]{1,0:T(8,128)(2,1)}, bf16[192,2048]{1,0:T(8,128)(2,1)S(1)}, u32[]{:S(2)}, u32[]{:S(2)}) collective-permute-start(bf16[192,2048]{1,0:T(8,128)(2,1)} %collective-permute-done.9.refs_9_), channel_id=1, source_target_pairs={{0,1},{1,0},{2,3},{3,2},{4,5},{5,4},{6,7},{7,6},{8,9},{9,8},{10,11... | collective-permute-start | bytes 2359304 | tf_op jit(solution)/shard_map/ppermute | solution.py:400
  105.4 19.9 %collective-permute-start.8 = (bf16[192,2048]{1,0:T(8,128)(2,1)S(1)}, bf16[192,2048]{1,0:T(8,128)(2,1)}, u32[]{:S(2)}, u32[]{:S(2)}) collective-permute-start(bf16[192,2048]{1,0:T(8,128)(2,1)S(1)} %copy-done.2), channel_id=1, source_target_pairs={{0,1},{1,0},{2,3},{3,2},{4,5},{5,4},{6,7},{7,6},{8,9},{9,8},{10,11... | collective-permute-start | bytes 2359304 | tf_op jit(solution)/shard_map/ppermute | solution.py:400
  105.9 19.4 %collective-permute-start.12 = (bf16[192,2048]{1,0:T(8,128)(2,1)}, bf16[192,2048]{1,0:T(8,128)(2,1)}, u32[]{:S(2)}, u32[]{:S(2)}) collective-permute-start(bf16[192,2048]{1,0:T(8,128)(2,1)} %collective-permute-done.11.refs_11_), channel_id=1, source_target_pairs={{0,1},{1,0},{2,3},{3,2},{4,5},{5,4},{6,7},{7,6},{8,9},{9,8},{10,11... | collective-permute-start | bytes 2359304 | tf_op jit(solution)/shard_map/ppermute | solution.py:400
  106.2 19.1 %collective-permute-start.14 = (bf16[192,2048]{1,0:T(8,128)(2,1)}, bf16[192,2048]{1,0:T(8,128)(2,1)}, u32[]{:S(2)}, u32[]{:S(2)}) collective-permute-start(bf16[192,2048]{1,0:T(8,128)(2,1)} %collective-permute-done.13.refs_13_), channel_id=1, source_target_pairs={{0,1},{1,0},{2,3},{3,2},{4,5},{5,4},{6,7},{7,6},{8,9},{9,8},{10,11... | collective-permute-start | bytes 2359304 | tf_op jit(solution)/shard_map/ppermute | solution.py:400
  106.4 18.9 %collective-permute-start.16 = (bf16[192,2048]{1,0:T(8,128)(2,1)}, bf16[192,2048]{1,0:T(8,128)(2,1)}, u32[]{:S(2)}, u32[]{:S(2)}) collective-permute-start(bf16[192,2048]{1,0:T(8,128)(2,1)} %collective-permute-done.15.refs_15_), channel_id=1, source_target_pairs={{0,1},{1,0},{2,3},{3,2},{4,5},{5,4},{6,7},{7,6},{8,9},{9,8},{10,11... | collective-permute-start | bytes 2359304 | tf_op jit(solution)/shard_map/ppermute | solution.py:400
  125.3 1.0 copy-start.3
  125.3 1.2 copy-start.5
  (2 other events, 1.6 us)

commit v7 on v6

--- a/solution.py
+++ b/solution.py
@@ -12,17 +12,10 @@
 F32 = jnp.float32
 BF16 = jnp.bfloat16
 SEGS = 8
-VMEM = pltpu.MemorySpace.VMEM
-
-
-def whole():
-    return pl.BlockSpec(memory_space=VMEM)
 
 
 FULL = pltpu.CompilerParams(vmem_limit_bytes=67043328)
-SMALL = pltpu.CompilerParams(vmem_limit_bytes=8 * 1024 * 1024)
-PROJ = pltpu.CompilerParams(vmem_limit_bytes=67043328 - (8 * 1024 + 448) * 1024)
-ROOMY = pltpu.CompilerParams(vmem_limit_bytes=48 * 1024 * 1024)
+ROOMY = pltpu.CompilerParams(vmem_limit_bytes=30 * 1024 * 1024)
 
 
 def anywhere():
@@ -225,11 +218,6 @@
     return values * lax.rsqrt(jnp.mean(values * values, axis=-1, keepdims=True) + EPSILON) * gain
 
 
-def preload_kernel(source, target, sem):
-    (copy,) = fetched((source,), (target,), sem)
-    copy.wait()
-
-
 def slots_of(first, second, axis, capacity, experts):
     rows = first.size
     ids = lax.broadcasted_iota(jnp.int32, (experts, rows) if axis == 0 else (rows, experts), axis)
@@ -249,18 +237,21 @@
 
 
 def proj_kernel(
-    weights, mixed, residual_h, gain_h, routes_h, columns_h, route_wt_h, stream_h, outgoing_h, table_h,
-    residual, gain, routes, columns, route_wt, stream_out, outgoing, table_out, sems,
+    mixed_h, weights_h, residual_h, gain_h, routes_h, columns_h, route_wt_h, stream_h, outgoing_h, table_h,
+    mixed, weights, residual, gain, routes, columns, route_wt, stream_out, outgoing, table_out, sems,
 ):
     small = fetched((routes_h, columns_h, route_wt_h), (routes, columns, route_wt), sems)
-    small += fetched((residual_h, gain_h), (residual, gain), sems, 9)
+    (mixed_copy,) = fetched((mixed_h,), (mixed,), sems, 9)
     width = weights.shape[0]
+    blocks = 8
+    block = width // blocks
+    parts = [(weights_h.at[pl.ds(k * block, block)], weights.at[pl.ds(k * block, block)]) for k in range(blocks)]
+    loads = fetched(*zip(*parts), sems, 12)
+    others = fetched((residual_h, gain_h), (residual, gain), sems, 10)
     rows = residual.shape[0]
     slots = outgoing.shape[0]
     experts = 16
     capacity = slots // experts
-    lanes = jnp.concatenate([mixed[j] for j in range(mixed.shape[0])], axis=1)
-    acc = jnp.dot(lanes, weights[...], preferred_element_type=F32)
     for copy in small:
         copy.wait()
     slot0, slot1 = slots_of(columns[:, 0:1], columns[:, 1:2], 1, capacity, experts)
@@ -278,6 +269,15 @@
     slot0, slot1 = slots_of(routes[0:1, :], routes[1:2, :], 0, capacity, experts)
     places = lax.broadcasted_iota(jnp.int32, (slots, rows), 0)
     pick = jnp.where(jnp.logical_or(places == slot0, places == slot1), 1.0, 0.0).astype(BF16)
+    mixed_copy.wait()
+    acc = jnp.zeros(residual.shape, F32)
+    per = mixed.shape[0] // blocks
+    for k in range(blocks):
+        lanes = jnp.concatenate([mixed[k * per + j] for j in range(per)], axis=1)
+        loads[k].wait()
+        acc = acc + jnp.dot(lanes, weights[k * block : (k + 1) * block, :], preferred_element_type=F32)
+    for copy in others:
+        copy.wait()
     proj = acc.astype(BF16).astype(F32)
     stream = (residual[...].astype(F32) + scaled(proj, gain[0:1, :])).astype(BF16)
     stream_out[...] = stream
@@ -441,11 +441,12 @@
         compiler_params=FULL,
         name="scan",
     )(mix_in, before, after, conv_w, conv_b[None], decay_param, recur_gate, recur_bias, input_gate, input_bias)
-    total, r1a, r1b = lax.optimization_barrier((total, r1a, r1b))
+    total, r1a = lax.optimization_barrier((total, r1a))
     r2a, e1a = around(r1a), across(r1a)
+    totals = lax.all_to_all(total, "sp", split_axis=0, concat_axis=0, tiled=True)
+    totals, r1b = lax.optimization_barrier((totals, r1b))
     r2b, e1b = around(r1b), across(r1b)
-    totals = lax.all_to_all(total, "sp", split_axis=0, concat_axis=0, tiled=True)
-    mixed = pl.pallas_call(
+    mix = pl.pallas_call(
         mix_kernel,
         out_shape=shape((length, channels), BF16),
         in_specs=[anywhere()] * 6,
@@ -461,7 +462,8 @@
         ],
         compiler_params=FULL,
         name="mix",
-    )(h, p_f, p_b, seg, totals, gate_in)
+    )
+    mixed = mix(h, p_f, p_b, seg, totals, gate_in)
     token_rows = lax.all_to_all(
         mixed.reshape(tp, rows, channels), "tp", split_axis=0, concat_axis=0, tiled=True
     )
@@ -471,16 +473,6 @@
     own_routes = lax.dynamic_slice_in_dim(routes, first_row, rows, 0)
     own_weights = lax.dynamic_slice_in_dim(route_wt, first_row, rows, 0)
     slots = 2 * rows * routes.shape[1]
-    preload = pl.pallas_call(
-        preload_kernel,
-        out_shape=shape(out_proj.shape, BF16),
-        in_specs=[anywhere()],
-        out_specs=whole(),
-        scratch_shapes=[pltpu.SemaphoreType.DMA((1,))],
-        compiler_params=PROJ,
-        name="preload",
-    )
-    weights_v = preload(out_proj)
     project = pl.pallas_call(
         proj_kernel,
         out_shape=(
@@ -488,9 +480,11 @@
             shape((slots, width), BF16),
             shape((3 * rows, slots), BF16),
         ),
-        in_specs=[whole()] * 2 + [anywhere()] * 5,
+        in_specs=[anywhere()] * 7,
         out_specs=(anywhere(),) * 3,
         scratch_shapes=[
+            pltpu.VMEM(token_rows.shape, BF16),
+            pltpu.VMEM(out_proj.shape, BF16),
             pltpu.VMEM(residual.shape, BF16),
             pltpu.VMEM(norm_gain.shape, F32),
             pltpu.VMEM((routes.shape[1], rows), jnp.int32),
@@ -499,19 +493,15 @@
             pltpu.VMEM(residual.shape, BF16),
             pltpu.VMEM((slots, width), BF16),
             pltpu.VMEM((3 * rows, slots), BF16),
-            pltpu.SemaphoreType.DMA((11,)),
+            pltpu.SemaphoreType.DMA((20,)),
         ],
-        compiler_params=PROJ,
+        compiler_params=FULL,
         name="proj",
     )
-    stream, outgoing, table = project(
-        weights_v, token_rows, residual, norm_gain, own_routes.T, own_routes, own_weights
-    )
+    stream, outgoing, table = project(token_rows, out_proj, residual, norm_gain, own_routes.T, own_routes, own_weights)
     r4, e3a = around(r3a), across(r3a)
     e3b, e4 = across(r3b), across(r4)
-    arrived = lax.all_to_all(
-        outgoing.reshape(sp, slots // sp, width), "sp", split_axis=0, concat_axis=0, tiled=True
-    )
+    arrived = lax.all_to_all(outgoing.reshape(sp, slots // sp, width), "sp", split_axis=0, concat_axis=0, tiled=True)
     arrived = arrived.reshape(slots, width)
 
     shares = (own, other, r1a, e1a, r1b, e1b, r2a, e2a, r2b, e2b, r3a, e3a, r3b, e3b, r4, e4)

time: 158 us -> 148 us (0.937)
  Pallas kernels: 34.3 us -> 25.2 us
  starting transfers between devices: 39.2 us -> 36.2 us
  waiting for transfers between devices: 42.9 us -> 45.2 us
    pallas_call x3 -> x2, Pallas kernels: 16.2 us -> 8.26 us  [the longest x1 5.57 us: layer(): project(token_rows, out_proj, residual, norm_gain, own_routes.T, own_rout...]
    ppermute x7, starting transfers between devices: 18.6 us -> 11.1 us  [around(): lax.ppermute(part, 'tp', [(i, (i + 2 - 4 * (i % 2)) % tp) for i in range(...]
    all_to_all x1, waiting for transfers between devices: 1.93 us -> 9.04 us  [layer(): lax.all_to_all(mixed.reshape(tp, rows, channels), 'tp', split_axis=0, con...]
    all_to_all x1, starting transfers between devices: 3.66 us -> 7.86 us  [layer(): lax.all_to_all(outgoing.reshape(sp, slots // sp, width), 'sp', split_axis...]
    ppermute x7, waiting for transfers between devices: 18.9 us -> 15.8 us  [around(): lax.ppermute(part, 'tp', [(i, (i + 2 - 4 * (i % 2)) % tp) for i in range(...]
    all_to_all x1, waiting for transfers between devices: 18.6 us -> 15.8 us  [layer(): lax.all_to_all(outgoing.reshape(sp, slots // sp, width), 'sp', split_axis...]
    unnamed x16 -> x10, local copies, waits for them, and re-layouts: 3.64 us -> 4.54 us
  transfers between devices with their start and end apart: 19 -> 19, of which waited for: 7 -> 7; matrix products, arithmetic and copies ran while one was open for 2% -> 2% of each run, Pallas kernels for 14% -> 10%
where the time goes in v7:
time: 148 us
  waiting for transfers between devices  45.2 us (31%)
  starting transfers between devices  36.2 us (24%)
  blocking collectives  33.3 us (22%)
  Pallas kernels  25.2 us (17%)
  local copies, waits for them, and re-layouts  7.39 us (5%)
    all_to_all x1, blocking collectives, layer(): lax.all_to_all(done.reshape(sp, slots // sp, width), 'sp', split_axis=0,...  19.3 us
    all_to_all x1, waiting for transfers between devices, layer(): lax.all_to_all(outgoing.reshape(sp, slots // sp, width), 'sp', split_axis...  15.8 us
    ppermute x7, waiting for transfers between devices, around(): lax.ppermute(part, 'tp', [(i, (i + 2 - 4 * (i % 2)) % tp) for i in range(...  15.8 us
    all_to_all x1, blocking collectives, layer(): lax.all_to_all(total, 'sp', split_axis=0, concat_axis=0, tiled=True)  14 us
    ppermute x7, starting transfers between devices, around(): lax.ppermute(part, 'tp', [(i, (i + 2 - 4 * (i % 2)) % tp) for i in range(...  11.1 us
    all_to_all x1, waiting for transfers between devices, layer(): lax.all_to_all(mixed.reshape(tp, rows, channels), 'tp', split_axis=0, con...  9.04 us
    all_to_all x1, starting transfers between devices, layer(): lax.all_to_all(outgoing.reshape(sp, slots // sp, width), 'sp', split_axis...  7.86 us
    all_to_all x1, starting transfers between devices, layer(): lax.all_to_all(mixed.reshape(tp, rows, channels), 'tp', split_axis=0, con...  7.24 us
  transfers between devices with their start and end apart: 19, of which 7 were waited for; matrix products, arithmetic and copies ran while one was open for 2% of the time, Pallas kernels for 10%

profile of v7, /device:TPU:1, one launch (start us, length us, event | category | flops | bytes accessed | tf_op | source)
XLA Modules:
  0.0 147.7 jit_solution(2616016272170779014)
XLA Ops:
  0.0 1.9 %pack.1.refs_1_ = bf16[192,2048]{1,0:T(8,128)(2,1)} custom-call(bf16[64,2048]{1,0:T(8,128)(2,1)} %bitcast.20, bf16[64,2048]{1,0:T(8,128)(2,1)} %bitcast.21, bf16[64,2048]{1,0:T(8,128)(2,1)} %bitcast.22), custom_call_target="tpu_custom_call" | custom-call | tf_op jit(solution)/shard_map/pack/pallas_call | solution.py:386
  1.9 3.3 %collective-permute-start.3 = (bf16[192,2048]{1,0:T(8,128)(2,1)}, bf16[192,2048]{1,0:T(8,128)(2,1)}, u32[]{:S(2)}, u32[]{:S(2)}) collective-permute-start(bf16[192,2048]{1,0:T(8,128)(2,1)} %pack.1.refs_1_), channel_id=1, source_target_pairs={{0,1},{1,0},{2,3},{3,2},{4,5},{5,4},{6,7},{7,6},{8,9},{9,8},{10,11... | collective-permute-start | bytes 2359304 | tf_op jit(solution)/shard_map/ppermute | solution.py:400
  5.2 3.9 %collective-permute-start.2 = (bf16[192,2048]{1,0:T(8,128)(2,1)}, bf16[192,2048]{1,0:T(8,128)(2,1)}, u32[]{:S(2)}, u32[]{:S(2)}) collective-permute-start(bf16[192,2048]{1,0:T(8,128)(2,1)} %pack.1.refs_1_), channel_id=1, source_target_pairs={{0,2},{1,15},{2,4},{3,1},{4,6},{5,3},{6,8},{7,5},{8,10},{9,7},{10,... | collective-permute-start | bytes 2359304 | tf_op jit(solution)/shard_map/ppermute | solution.py:397
  9.8 3.6 %collective-permute-start = (bf16[2,128]{1,0:T(2,128)(2,1)S(1)}, bf16[2,128]{1,0:T(2,128)(2,1)}, u32[]{:S(2)}, u32[]{:S(2)}) collective-permute-start(bf16[2,128]{1,0:T(2,128)(2,1)S(1)} %get-tuple-element.30), channel_id=1, source_target_pairs={{0,16},{16,32},{32,48},{48,64},{64,80},{80,96},{96,112},{112,128},... | collective-permute-start | bytes 1544 | tf_op jit(solution)/shard_map/ppermute | solution.py:382
  13.4 1.3 collective-permute-start.1
  14.6 3.4 %collective-permute-done.1.after_h = bf16[2,128]{1,0:T(2,128)(2,1)} collective-permute-done((bf16[2,128]{1,0:T(2,128)(2,1)S(1)}, bf16[2,128]{1,0:T(2,128)(2,1)}, u32[]{:S(2)}, u32[]{:S(2)}) %collective-permute-start.1) | collective-permute-done | bytes 544 | tf_op jit(solution)/shard_map/ppermute | solution.py:383
  18.1 5.9 %scan.1 = (f32[1024,128]{1,0:T(8,128)}, f32[1024,128]{1,0:T(8,128)}, f32[1024,128]{1,0:T(8,128)}, f32[32,128]{1,0:T(8,128)}, f32[16,8,128]{2,1,0:T(8,128)}) custom-call(bf16[1024,128]{1,0:T(8,128)(2,1)} %mix_h.1, bf16[2,128]{1,0:T(2,128)(2,1)} %collective-permute-done.before_h, bf16[2,128]{1,0:T(2,128)(2,1)} %collective-permute-done.1.after_h, ...), custom_call_target="tpu_custom_call" | custom-call | tf_op jit(solution)/shard_map/scan/pallas_call | solution.py:408
  25.5 14.0 %all_to_all.20.refs_4_ = f32[16,8,128]{2,1,0:T(8,128)} all-to-all(f32[16,8,128]{2,1,0:T(8,128)} %get-tuple-element.22), channel_id=1, replica_groups=mesh['sp'=16,'tp'=16] {'sp'}, dimensions={0} | all-to-all | bytes 131072 | tf_op jit(solution)/shard_map/all_to_all | solution.py:446
  40.2 3.5 %collective-permute-done.7.refs_7_ = bf16[192,2048]{1,0:T(8,128)(2,1)S(1)} collective-permute-done((bf16[192,2048]{1,0:T(8,128)(2,1)}, bf16[192,2048]{1,0:T(8,128)(2,1)S(1)}, u32[]{:S(2)}, u32[]{:S(2)}) %collective-permute-start.7) | collective-permute-done | bytes 786464 | tf_op jit(solution)/shard_map/ppermute | solution.py:397
  44.6 1.7 %collective-permute-start.11 = (bf16[192,2048]{1,0:T(8,128)(2,1)S(1)}, bf16[192,2048]{1,0:T(8,128)(2,1)}, u32[]{:S(2)}, u32[]{:S(2)}) collective-permute-start(bf16[192,2048]{1,0:T(8,128)(2,1)S(1)} %collective-permute-done.7.refs_7_), channel_id=1, source_target_pairs={{0,2},{1,15},{2,4},{3,1},{4,6},{5,3},{6,8},{7,5},{8,10},{9,7},{10,... | collective-permute-start | bytes 2359304 | tf_op jit(solution)/shard_map/ppermute | solution.py:397
  46.8 5.5 %collective-permute-done.9.refs_9_ = bf16[192,2048]{1,0:T(8,128)(2,1)} collective-permute-done((bf16[192,2048]{1,0:T(8,128)(2,1)}, bf16[192,2048]{1,0:T(8,128)(2,1)}, u32[]{:S(2)}, u32[]{:S(2)}) %collective-permute-start.9) | collective-permute-done | bytes 786464 | tf_op jit(solution)/shard_map/ppermute | solution.py:397
  52.3 1.6 %collective-permute-start.13 = (bf16[192,2048]{1,0:T(8,128)(2,1)}, bf16[192,2048]{1,0:T(8,128)(2,1)}, u32[]{:S(2)}, u32[]{:S(2)}) collective-permute-start(bf16[192,2048]{1,0:T(8,128)(2,1)} %collective-permute-done.9.refs_9_), channel_id=1, source_target_pairs={{0,2},{1,15},{2,4},{3,1},{4,6},{5,3},{6,8},{7,5},{8,10},{9,7},{10,... | collective-permute-start | bytes 2359304 | tf_op jit(solution)/shard_map/ppermute | solution.py:397
  54.0 6.8 %collective-permute-done.11.refs_11_ = bf16[192,2048]{1,0:T(8,128)(2,1)} collective-permute-done((bf16[192,2048]{1,0:T(8,128)(2,1)S(1)}, bf16[192,2048]{1,0:T(8,128)(2,1)}, u32[]{:S(2)}, u32[]{:S(2)}) %collective-permute-start.11) | collective-permute-done | bytes 786464 | tf_op jit(solution)/shard_map/ppermute | solution.py:397
  60.7 1.6 %collective-permute-start.15 = (bf16[192,2048]{1,0:T(8,128)(2,1)}, bf16[192,2048]{1,0:T(8,128)(2,1)}, u32[]{:S(2)}, u32[]{:S(2)}) collective-permute-start(bf16[192,2048]{1,0:T(8,128)(2,1)} %collective-permute-done.11.refs_11_), channel_id=1, source_target_pairs={{0,2},{1,15},{2,4},{3,1},{4,6},{5,3},{6,8},{7,5},{8,10},{9,7},{10,... | collective-permute-start | bytes 2359304 | tf_op jit(solution)/shard_map/ppermute | solution.py:397
  62.4 2.7 %mix.1 = bf16[1024,128]{1,0:T(8,128)(2,1)} custom-call(f32[1024,128]{1,0:T(8,128)} %get-tuple-element.17.refs_0_, f32[1024,128]{1,0:T(8,128)} %get-tuple-element.18.refs_1_, f32[1024,128]{1,0:T(8,128)} %get-tuple-element.19.refs_2_, f32[32,128]{1,0:T(8,128)} %get-tuple-element.20.refs_3_, f32[16,8,128]{2,1,0:T(8,128)} %all_to_all.20.refs_4_, ...), custom_call_target="tpu_custom_call" | custom-call | tf_op jit(solution)/shard_map/mix/pallas_call | solution.py:466
  65.1 7.2 %all-to-all-start.1 = ((bf16[16,64,128]{2,1,0:T(8,128)(2,1)}), bf16[16,64,128]{2,1,0:T(8,128)(2,1)}, u32[]{:S(2)}, u32[]{:S(2)}) async-start(bf16[16,64,128]{2,1,0:T(8,128)(2,1)} %bitcast.17), calls=%async_computation.1 | async-start | bytes 524288 | tf_op jit(solution)/shard_map/all_to_all | solution.py:467
  75.9 9.0 %all-to-all-done.1.mixed_h = bf16[16,64,128]{2,1,0:T(8,128)(2,1)} async-done(((bf16[16,64,128]{2,1,0:T(8,128)(2,1)}), bf16[16,64,128]{2,1,0:T(8,128)(2,1)}, u32[]{:S(2)}, u32[]{:S(2)}) %all-to-all-start.1) | async-done | bytes 262176 | tf_op jit(solution)/shard_map/all_to_all | solution.py:467
  84.9 5.6 %proj.1 = (bf16[64,2048]{1,0:T(8,128)(2,1)}, bf16[256,2048]{1,0:T(8,128)(2,1)}, bf16[192,256]{1,0:T(8,128)(2,1)}) custom-call(bf16[16,64,128]{2,1,0:T(8,128)(2,1)} %all-to-all-done.1.mixed_h, bf16[2048,2048]{1,0:T(8,128)(2,1)} %weights_h.1, bf16[64,2048]{1,0:T(8,128)(2,1)} %residual_h.1, f32[3,2048]{1,0:T(4,128)} %refs_2_.1, s32[2,64]{1,0:T(2,128)} %copy.20.routes_h, ...), custom_call_target="tpu_custom_call" | custom-call | tf_op jit(solution)/shard_map/proj/pallas_call | solution.py:501
  90.5 7.9 %all-to-all-start.2 = ((bf16[16,16,2048]{2,1,0:T(8,128)(2,1)}), bf16[16,16,2048]{2,1,0:T(8,128)(2,1)S(1)}, u32[]{:S(2)}, u32[]{:S(2)}) async-start(bf16[16,16,2048]{2,1,0:T(8,128)(2,1)} %bitcast.18), calls=%async_computation.2 | async-start | bytes 2097152 | tf_op jit(solution)/shard_map/all_to_all | solution.py:504
  99.8 1.2 collective-permute-done.8.refs_8_
  100.9 15.8 %all-to-all-done.2 = bf16[16,16,2048]{2,1,0:T(8,128)(2,1)S(1)} async-done(((bf16[16,16,2048]{2,1,0:T(8,128)(2,1)}), bf16[16,16,2048]{2,1,0:T(8,128)(2,1)S(1)}, u32[]{:S(2)}, u32[]{:S(2)}) %all-to-all-start.2) | async-done | bytes 1048608 | tf_op jit(solution)/shard_map/all_to_all | solution.py:504
  119.0 6.6 %experts.1 = bf16[256,2048]{1,0:T(8,128)(2,1)S(1)} custom-call(bf16[256,2048]{1,0:T(8,128)(2,1)S(1)} %bitcast.14, bf16[192,2048]{1,0:T(8,128)(2,1)S(1)} %copy-done, bf16[192,2048]{1,0:T(8,128)(2,1)} %collective-permute-done.3.refs_2_, bf16[192,2048]{1,0:T(8,128)(2,1)} %collective-permute-done.2.refs_3_, bf16[192,2048]{1,0:T(8,128)(2,1)} %collective-permute-done.5.refs_4_, ...), custom_call_target="tpu_custom_call" | custom-call | tf_op jit(solution)/shard_map/experts/pallas_call | solution.py:522
  125.6 19.3 %all_to_all.21 = bf16[16,16,2048]{2,1,0:T(8,128)(2,1)} all-to-all(bf16[16,16,2048]{2,1,0:T(8,128)(2,1)S(1)} %bitcast.15), channel_id=1, replica_groups=mesh['sp'=16,'tp'=16] {'sp'}, dimensions={0} | all-to-all | bytes 2097152 | tf_op jit(solution)/shard_map/all_to_all | solution.py:523
  144.9 2.6 %combine.1 = bf16[64,2048]{1,0:T(8,128)(2,1)} custom-call(bf16[256,2048]{1,0:T(8,128)(2,1)} %bitcast.16, bf16[64,2048]{1,0:T(8,128)(2,1)} %get-tuple-element.27.refs_1_, f32[3,2048]{1,0:T(4,128)} %refs_2_.1, bf16[192,256]{1,0:T(8,128)(2,1)} %get-tuple-element.28.refs_3_), custom_call_target="tpu_custom_call" | custom-call | tf_op jit(solution)/shard_map/combine/pallas_call | solution.py:526
  (36 shorter events, 11.6 us)
Async XLA Ops:
  1.9 22.0 %collective-permute-start.3 = (bf16[192,2048]{1,0:T(8,128)(2,1)}, bf16[192,2048]{1,0:T(8,128)(2,1)}, u32[]{:S(2)}, u32[]{:S(2)}) collective-permute-start(bf16[192,2048]{1,0:T(8,128)(2,1)} %pack.1.refs_1_), channel_id=1, source_target_pairs={{0,1},{1,0},{2,3},{3,2},{4,5},{5,4},{6,7},{7,6},{8,9},{9,8},{10,11... | collective-permute-start | bytes 2359304 | tf_op jit(solution)/shard_map/ppermute | solution.py:400
  5.2 19.5 %collective-permute-start.2 = (bf16[192,2048]{1,0:T(8,128)(2,1)}, bf16[192,2048]{1,0:T(8,128)(2,1)}, u32[]{:S(2)}, u32[]{:S(2)}) collective-permute-start(bf16[192,2048]{1,0:T(8,128)(2,1)} %pack.1.refs_1_), channel_id=1, source_target_pairs={{0,2},{1,15},{2,4},{3,1},{4,6},{5,3},{6,8},{7,5},{8,10},{9,7},{10,... | collective-permute-start | bytes 2359304 | tf_op jit(solution)/shard_map/ppermute | solution.py:397
  9.8 4.9 %collective-permute-start = (bf16[2,128]{1,0:T(2,128)(2,1)S(1)}, bf16[2,128]{1,0:T(2,128)(2,1)}, u32[]{:S(2)}, u32[]{:S(2)}) collective-permute-start(bf16[2,128]{1,0:T(2,128)(2,1)S(1)} %get-tuple-element.30), channel_id=1, source_target_pairs={{0,16},{16,32},{32,48},{48,64},{64,80},{80,96},{96,112},{112,128},... | collective-permute-start | bytes 1544 | tf_op jit(solution)/shard_map/ppermute | solution.py:382
  13.4 4.7 %collective-permute-start.1 = (bf16[2,128]{1,0:T(2,128)(2,1)S(1)}, bf16[2,128]{1,0:T(2,128)(2,1)}, u32[]{:S(2)}, u32[]{:S(2)}) collective-permute-start(bf16[2,128]{1,0:T(2,128)(2,1)S(1)} %get-tuple-element.29), channel_id=1, source_target_pairs={{16,0},{32,16},{48,32},{64,48},{80,64},{96,80},{112,96},{128,112},... | collective-permute-start | bytes 1544 | tf_op jit(solution)/shard_map/ppermute | solution.py:383
  23.9 15.6 %collective-permute-start.4 = (bf16[192,2048]{1,0:T(8,128)(2,1)}, bf16[192,2048]{1,0:T(8,128)(2,1)}, u32[]{:S(2)}, u32[]{:S(2)}) collective-permute-start(bf16[192,2048]{1,0:T(8,128)(2,1)} %collective-permute-done.3.refs_2_), channel_id=1, source_target_pairs={{0,2},{1,15},{2,4},{3,1},{4,6},{5,3},{6,8},{7,5},{8,10},{9,7},{10,... | collective-permute-start | bytes 2359304 | tf_op jit(solution)/shard_map/ppermute | solution.py:397
  24.7 19.0 %collective-permute-start.7 = (bf16[192,2048]{1,0:T(8,128)(2,1)}, bf16[192,2048]{1,0:T(8,128)(2,1)S(1)}, u32[]{:S(2)}, u32[]{:S(2)}) collective-permute-start(bf16[192,2048]{1,0:T(8,128)(2,1)} %collective-permute-done.2.refs_3_), channel_id=1, source_target_pairs={{0,2},{1,15},{2,4},{3,1},{4,6},{5,3},{6,8},{7,5},{8,10},{9,7},{10,... | collective-permute-start | bytes 2359304 | tf_op jit(solution)/shard_map/ppermute | solution.py:397
  39.5 12.8 %collective-permute-start.9 = (bf16[192,2048]{1,0:T(8,128)(2,1)}, bf16[192,2048]{1,0:T(8,128)(2,1)}, u32[]{:S(2)}, u32[]{:S(2)}) collective-permute-start(bf16[192,2048]{1,0:T(8,128)(2,1)} %collective-permute-done.4.refs_5_), channel_id=1, source_target_pairs={{0,2},{1,15},{2,4},{3,1},{4,6},{5,3},{6,8},{7,5},{8,10},{9,7},{10,... | collective-permute-start | bytes 2359304 | tf_op jit(solution)/shard_map/ppermute | solution.py:397
  43.8 0.9 copy-start.1
  44.6 16.1 %collective-permute-start.11 = (bf16[192,2048]{1,0:T(8,128)(2,1)S(1)}, bf16[192,2048]{1,0:T(8,128)(2,1)}, u32[]{:S(2)}, u32[]{:S(2)}) collective-permute-start(bf16[192,2048]{1,0:T(8,128)(2,1)S(1)} %collective-permute-done.7.refs_7_), channel_id=1, source_target_pairs={{0,2},{1,15},{2,4},{3,1},{4,6},{5,3},{6,8},{7,5},{8,10},{9,7},{10,... | collective-permute-start | bytes 2359304 | tf_op jit(solution)/shard_map/ppermute | solution.py:397
  46.3 52.2 %collective-permute-start.5 = (bf16[192,2048]{1,0:T(8,128)(2,1)}, bf16[192,2048]{1,0:T(8,128)(2,1)}, u32[]{:S(2)}, u32[]{:S(2)}) collective-permute-start(bf16[192,2048]{1,0:T(8,128)(2,1)} %collective-permute-done.2.refs_3_), channel_id=1, source_target_pairs={{0,1},{1,0},{2,3},{3,2},{4,5},{5,4},{6,7},{7,6},{8,9},{9,8},{10,11... | collective-permute-start | bytes 2359304 | tf_op jit(solution)/shard_map/ppermute | solution.py:400
  46.4 52.6 %collective-permute-start.6 = (bf16[192,2048]{1,0:T(8,128)(2,1)}, bf16[192,2048]{1,0:T(8,128)(2,1)}, u32[]{:S(2)}, u32[]{:S(2)}) collective-permute-start(bf16[192,2048]{1,0:T(8,128)(2,1)} %collective-permute-done.4.refs_5_), channel_id=1, source_target_pairs={{0,1},{1,0},{2,3},{3,2},{4,5},{5,4},{6,7},{7,6},{8,9},{9,8},{10,11... | collective-permute-start | bytes 2359304 | tf_op jit(solution)/shard_map/ppermute | solution.py:400
  52.3 46.9 %collective-permute-start.13 = (bf16[192,2048]{1,0:T(8,128)(2,1)}, bf16[192,2048]{1,0:T(8,128)(2,1)}, u32[]{:S(2)}, u32[]{:S(2)}) collective-permute-start(bf16[192,2048]{1,0:T(8,128)(2,1)} %collective-permute-done.9.refs_9_), channel_id=1, source_target_pairs={{0,2},{1,15},{2,4},{3,1},{4,6},{5,3},{6,8},{7,5},{8,10},{9,7},{10,... | collective-permute-start | bytes 2359304 | tf_op jit(solution)/shard_map/ppermute | solution.py:397
  60.7 38.7 %collective-permute-start.15 = (bf16[192,2048]{1,0:T(8,128)(2,1)}, bf16[192,2048]{1,0:T(8,128)(2,1)}, u32[]{:S(2)}, u32[]{:S(2)}) collective-permute-start(bf16[192,2048]{1,0:T(8,128)(2,1)} %collective-permute-done.11.refs_11_), channel_id=1, source_target_pairs={{0,2},{1,15},{2,4},{3,1},{4,6},{5,3},{6,8},{7,5},{8,10},{9,7},{10,... | collective-permute-start | bytes 2359304 | tf_op jit(solution)/shard_map/ppermute | solution.py:397
  65.1 19.8 %all-to-all-start.1 = ((bf16[16,64,128]{2,1,0:T(8,128)(2,1)}), bf16[16,64,128]{2,1,0:T(8,128)(2,1)}, u32[]{:S(2)}, u32[]{:S(2)}) async-start(bf16[16,64,128]{2,1,0:T(8,128)(2,1)} %bitcast.17), calls=%async_computation.1 | async-start | bytes 524288 | tf_op jit(solution)/shard_map/all_to_all | solution.py:467
  73.2 0.6 copy-start.3
  90.5 26.3 %all-to-all-start.2 = ((bf16[16,16,2048]{2,1,0:T(8,128)(2,1)}), bf16[16,16,2048]{2,1,0:T(8,128)(2,1)S(1)}, u32[]{:S(2)}, u32[]{:S(2)}) async-start(bf16[16,16,2048]{2,1,0:T(8,128)(2,1)} %bitcast.18), calls=%async_computation.2 | async-start | bytes 2097152 | tf_op jit(solution)/shard_map/all_to_all | solution.py:504
  98.4 2.6 %collective-permute-start.8 = (bf16[192,2048]{1,0:T(8,128)(2,1)}, bf16[192,2048]{1,0:T(8,128)(2,1)S(1)}, u32[]{:S(2)}, u32[]{:S(2)}) collective-permute-start(bf16[192,2048]{1,0:T(8,128)(2,1)} %copy-done.1), channel_id=1, source_target_pairs={{0,1},{1,0},{2,3},{3,2},{4,5},{5,4},{6,7},{7,6},{8,9},{9,8},{10,11... | collective-permute-start | bytes 2359304 | tf_op jit(solution)/shard_map/ppermute | solution.py:400
  98.6 18.2 %collective-permute-start.10 = (bf16[192,2048]{1,0:T(8,128)(2,1)}, bf16[192,2048]{1,0:T(8,128)(2,1)S(1)}, u32[]{:S(2)}, u32[]{:S(2)}) collective-permute-start(bf16[192,2048]{1,0:T(8,128)(2,1)} %collective-permute-done.9.refs_9_), channel_id=1, source_target_pairs={{0,1},{1,0},{2,3},{3,2},{4,5},{5,4},{6,7},{7,6},{8,9},{9,8},{10,11... | collective-permute-start | bytes 2359304 | tf_op jit(solution)/shard_map/ppermute | solution.py:400
  99.0 17.8 %collective-permute-start.12 = (bf16[192,2048]{1,0:T(8,128)(2,1)}, bf16[192,2048]{1,0:T(8,128)(2,1)S(1)}, u32[]{:S(2)}, u32[]{:S(2)}) collective-permute-start(bf16[192,2048]{1,0:T(8,128)(2,1)} %collective-permute-done.11.refs_11_), channel_id=1, source_target_pairs={{0,1},{1,0},{2,3},{3,2},{4,5},{5,4},{6,7},{7,6},{8,9},{9,8},{10,11... | collective-permute-start | bytes 2359304 | tf_op jit(solution)/shard_map/ppermute | solution.py:400
  99.3 17.5 %collective-permute-start.14 = (bf16[192,2048]{1,0:T(8,128)(2,1)}, bf16[192,2048]{1,0:T(8,128)(2,1)}, u32[]{:S(2)}, u32[]{:S(2)}) collective-permute-start(bf16[192,2048]{1,0:T(8,128)(2,1)} %collective-permute-done.13.refs_13_), channel_id=1, source_target_pairs={{0,1},{1,0},{2,3},{3,2},{4,5},{5,4},{6,7},{7,6},{8,9},{9,8},{10,11... | collective-permute-start | bytes 2359304 | tf_op jit(solution)/shard_map/ppermute | solution.py:400
  99.5 17.3 %collective-permute-start.16 = (bf16[192,2048]{1,0:T(8,128)(2,1)}, bf16[192,2048]{1,0:T(8,128)(2,1)}, u32[]{:S(2)}, u32[]{:S(2)}) collective-permute-start(bf16[192,2048]{1,0:T(8,128)(2,1)} %collective-permute-done.15.refs_15_), channel_id=1, source_target_pairs={{0,1},{1,0},{2,3},{3,2},{4,5},{5,4},{6,7},{7,6},{8,9},{9,8},{10,11... | collective-permute-start | bytes 2359304 | tf_op jit(solution)/shard_map/ppermute | solution.py:400
  116.8 1.1 copy-start
  117.9 1.1 copy-start.2

commit v8 on v7

--- a/solution.py
+++ b/solution.py
@@ -12,6 +12,11 @@
 F32 = jnp.float32
 BF16 = jnp.bfloat16
 SEGS = 8
+VMEM = pltpu.MemorySpace.VMEM
+
+
+def whole():
+    return pl.BlockSpec(memory_space=VMEM)
 
 
 FULL = pltpu.CompilerParams(vmem_limit_bytes=67043328)
@@ -337,18 +342,12 @@
     copy.wait()
 
 
-def combine_kernel(*refs):
-    sources, out_h, buffers, out, sems = refs[:4], refs[4], refs[5:9], refs[9], refs[10]
-    values, stream, gain, table = buffers
-    for copy in fetched(sources, buffers, sems):
-        copy.wait()
+def combine_kernel(values, stream, gain, table, out):
     rows = stream.shape[0]
     parts = jnp.dot(table[...], values[...], preferred_element_type=F32)
     mixture = parts[0:rows] + (parts[rows : 2 * rows] + parts[2 * rows : 3 * rows])
     mixture = mixture.astype(BF16).astype(F32)
     out[...] = (stream[...].astype(F32) + scaled(mixture, gain[2:3, :])).astype(BF16)
-    (copy,) = fetched((out,), (out_h,), sems, 4)
-    copy.wait()
 
 
 def shape(dims, dtype):
@@ -526,17 +525,9 @@
     return pl.pallas_call(
         combine_kernel,
         out_shape=shape((rows, width), BF16),
-        in_specs=[anywhere()] * 4,
-        out_specs=anywhere(),
-        scratch_shapes=[
-            pltpu.VMEM((slots, width), BF16),
-            pltpu.VMEM((rows, width), BF16),
-            pltpu.VMEM(norm_gain.shape, F32),
-            pltpu.VMEM((3 * rows, slots), BF16),
-            pltpu.VMEM((rows, width), BF16),
-            pltpu.SemaphoreType.DMA((5,)),
-        ],
-        compiler_params=FULL,
+        in_specs=[whole()] * 4,
+        out_specs=whole(),
+        compiler_params=pltpu.CompilerParams(vmem_limit_bytes=16 * 1024 * 1024),
         name="combine",
     )(returned.reshape(slots, width), stream, norm_gain, table)
 

time: 148 us -> 146 us (0.986)
    unnamed x10 -> x16, local copies, waits for them, and re-layouts: 4.54 us -> 4.57 us
  transfers between devices with their start and end apart: 19 -> 19, of which waited for: 7 -> 7; matrix products, arithmetic and copies ran while one was open for 2% -> 3% of each run, Pallas kernels for 10% -> 10%
where the time goes in v8:
time: 146 us
  waiting for transfers between devices  45 us (31%)
  starting transfers between devices  36.2 us (25%)
  blocking collectives  33.3 us (23%)
  Pallas kernels  23.8 us (16%)
  local copies, waits for them, and re-layouts  7.42 us (5%)
    all_to_all x1, blocking collectives, layer(): lax.all_to_all(done.reshape(sp, slots // sp, width), 'sp', split_axis=0,...  19.2 us
    all_to_all x1, waiting for transfers between devices, layer(): lax.all_to_all(outgoing.reshape(sp, slots // sp, width), 'sp', split_axis...  15.8 us
    ppermute x7, waiting for transfers between devices, around(): lax.ppermute(part, 'tp', [(i, (i + 2 - 4 * (i % 2)) % tp) for i in range(...  15.5 us
    all_to_all x1, blocking collectives, layer(): lax.all_to_all(total, 'sp', split_axis=0, concat_axis=0, tiled=True)  14.1 us
    ppermute x7, starting transfers between devices, around(): lax.ppermute(part, 'tp', [(i, (i + 2 - 4 * (i % 2)) % tp) for i in range(...  11.3 us
    all_to_all x1, waiting for transfers between devices, layer(): lax.all_to_all(mixed.reshape(tp, rows, channels), 'tp', split_axis=0, con...  9.08 us
    all_to_all x1, starting transfers between devices, layer(): lax.all_to_all(outgoing.reshape(sp, slots // sp, width), 'sp', split_axis...  7.81 us
    all_to_all x1, starting transfers between devices, layer(): lax.all_to_all(mixed.reshape(tp, rows, channels), 'tp', split_axis=0, con...  7.04 us
  transfers between devices with their start and end apart: 19, of which 7 were waited for; matrix products, arithmetic and copies ran while one was open for 3% of the time, Pallas kernels for 10%

profile of v8, /device:TPU:1, one launch (start us, length us, event | category | flops | bytes accessed | tf_op | source)
XLA Modules:
  0.0 145.9 jit_solution(2263783477980951183)
XLA Ops:
  0.0 1.9 %pack.1.refs_1_ = bf16[192,2048]{1,0:T(8,128)(2,1)} custom-call(bf16[64,2048]{1,0:T(8,128)(2,1)} %bitcast.20, bf16[64,2048]{1,0:T(8,128)(2,1)} %bitcast.21, bf16[64,2048]{1,0:T(8,128)(2,1)} %bitcast.22), custom_call_target="tpu_custom_call" | custom-call | tf_op jit(solution)/shard_map/pack/pallas_call | solution.py:385
  1.9 3.3 %collective-permute-start.3 = (bf16[192,2048]{1,0:T(8,128)(2,1)}, bf16[192,2048]{1,0:T(8,128)(2,1)}, u32[]{:S(2)}, u32[]{:S(2)}) collective-permute-start(bf16[192,2048]{1,0:T(8,128)(2,1)} %pack.1.refs_1_), channel_id=1, source_target_pairs={{0,1},{1,0},{2,3},{3,2},{4,5},{5,4},{6,7},{7,6},{8,9},{9,8},{10,11... | collective-permute-start | bytes 2359304 | tf_op jit(solution)/shard_map/ppermute | solution.py:399
  5.2 3.9 %collective-permute-start.2 = (bf16[192,2048]{1,0:T(8,128)(2,1)}, bf16[192,2048]{1,0:T(8,128)(2,1)}, u32[]{:S(2)}, u32[]{:S(2)}) collective-permute-start(bf16[192,2048]{1,0:T(8,128)(2,1)} %pack.1.refs_1_), channel_id=1, source_target_pairs={{0,2},{1,15},{2,4},{3,1},{4,6},{5,3},{6,8},{7,5},{8,10},{9,7},{10,... | collective-permute-start | bytes 2359304 | tf_op jit(solution)/shard_map/ppermute | solution.py:396
  9.8 3.6 %collective-permute-start = (bf16[2,128]{1,0:T(2,128)(2,1)S(1)}, bf16[2,128]{1,0:T(2,128)(2,1)}, u32[]{:S(2)}, u32[]{:S(2)}) collective-permute-start(bf16[2,128]{1,0:T(2,128)(2,1)S(1)} %get-tuple-element.30), channel_id=1, source_target_pairs={{0,16},{16,32},{32,48},{48,64},{64,80},{80,96},{96,112},{112,128},... | collective-permute-start | bytes 1544 | tf_op jit(solution)/shard_map/ppermute | solution.py:381
  13.4 1.3 collective-permute-start.1
  14.7 3.4 %collective-permute-done.1.after_h = bf16[2,128]{1,0:T(2,128)(2,1)} collective-permute-done((bf16[2,128]{1,0:T(2,128)(2,1)S(1)}, bf16[2,128]{1,0:T(2,128)(2,1)}, u32[]{:S(2)}, u32[]{:S(2)}) %collective-permute-start.1) | collective-permute-done | bytes 544 | tf_op jit(solution)/shard_map/ppermute | solution.py:382
  18.1 5.8 %scan.1 = (f32[1024,128]{1,0:T(8,128)}, f32[1024,128]{1,0:T(8,128)}, f32[1024,128]{1,0:T(8,128)}, f32[32,128]{1,0:T(8,128)}, f32[16,8,128]{2,1,0:T(8,128)}) custom-call(bf16[1024,128]{1,0:T(8,128)(2,1)} %mix_h.1, bf16[2,128]{1,0:T(2,128)(2,1)} %collective-permute-done.before_h, bf16[2,128]{1,0:T(2,128)(2,1)} %collective-permute-done.1.after_h, ...), custom_call_target="tpu_custom_call" | custom-call | tf_op jit(solution)/shard_map/scan/pallas_call | solution.py:407
  25.5 14.1 %all_to_all.20.refs_4_ = f32[16,8,128]{2,1,0:T(8,128)} all-to-all(f32[16,8,128]{2,1,0:T(8,128)} %get-tuple-element.22), channel_id=1, replica_groups=mesh['sp'=16,'tp'=16] {'sp'}, dimensions={0} | all-to-all | bytes 131072 | tf_op jit(solution)/shard_map/all_to_all | solution.py:445
  40.3 3.3 %collective-permute-done.7.refs_7_ = bf16[192,2048]{1,0:T(8,128)(2,1)S(1)} collective-permute-done((bf16[192,2048]{1,0:T(8,128)(2,1)}, bf16[192,2048]{1,0:T(8,128)(2,1)S(1)}, u32[]{:S(2)}, u32[]{:S(2)}) %collective-permute-start.7) | collective-permute-done | bytes 786464 | tf_op jit(solution)/shard_map/ppermute | solution.py:396
  44.5 1.8 %collective-permute-start.11 = (bf16[192,2048]{1,0:T(8,128)(2,1)S(1)}, bf16[192,2048]{1,0:T(8,128)(2,1)}, u32[]{:S(2)}, u32[]{:S(2)}) collective-permute-start(bf16[192,2048]{1,0:T(8,128)(2,1)S(1)} %collective-permute-done.7.refs_7_), channel_id=1, source_target_pairs={{0,2},{1,15},{2,4},{3,1},{4,6},{5,3},{6,8},{7,5},{8,10},{9,7},{10,... | collective-permute-start | bytes 2359304 | tf_op jit(solution)/shard_map/ppermute | solution.py:396
  46.8 5.5 %collective-permute-done.9.refs_9_ = bf16[192,2048]{1,0:T(8,128)(2,1)} collective-permute-done((bf16[192,2048]{1,0:T(8,128)(2,1)}, bf16[192,2048]{1,0:T(8,128)(2,1)}, u32[]{:S(2)}, u32[]{:S(2)}) %collective-permute-start.9) | collective-permute-done | bytes 786464 | tf_op jit(solution)/shard_map/ppermute | solution.py:396
  52.3 1.6 %collective-permute-start.13 = (bf16[192,2048]{1,0:T(8,128)(2,1)}, bf16[192,2048]{1,0:T(8,128)(2,1)}, u32[]{:S(2)}, u32[]{:S(2)}) collective-permute-start(bf16[192,2048]{1,0:T(8,128)(2,1)} %collective-permute-done.9.refs_9_), channel_id=1, source_target_pairs={{0,2},{1,15},{2,4},{3,1},{4,6},{5,3},{6,8},{7,5},{8,10},{9,7},{10,... | collective-permute-start | bytes 2359304 | tf_op jit(solution)/shard_map/ppermute | solution.py:396
  54.0 6.8 %collective-permute-done.11.refs_11_ = bf16[192,2048]{1,0:T(8,128)(2,1)} collective-permute-done((bf16[192,2048]{1,0:T(8,128)(2,1)S(1)}, bf16[192,2048]{1,0:T(8,128)(2,1)}, u32[]{:S(2)}, u32[]{:S(2)}) %collective-permute-start.11) | collective-permute-done | bytes 786464 | tf_op jit(solution)/shard_map/ppermute | solution.py:396
  60.7 1.6 %collective-permute-start.15 = (bf16[192,2048]{1,0:T(8,128)(2,1)}, bf16[192,2048]{1,0:T(8,128)(2,1)}, u32[]{:S(2)}, u32[]{:S(2)}) collective-permute-start(bf16[192,2048]{1,0:T(8,128)(2,1)} %collective-permute-done.11.refs_11_), channel_id=1, source_target_pairs={{0,2},{1,15},{2,4},{3,1},{4,6},{5,3},{6,8},{7,5},{8,10},{9,7},{10,... | collective-permute-start | bytes 2359304 | tf_op jit(solution)/shard_map/ppermute | solution.py:396
  62.4 2.7 %mix.1 = bf16[1024,128]{1,0:T(8,128)(2,1)} custom-call(f32[1024,128]{1,0:T(8,128)} %get-tuple-element.17.refs_0_, f32[1024,128]{1,0:T(8,128)} %get-tuple-element.18.refs_1_, f32[1024,128]{1,0:T(8,128)} %get-tuple-element.19.refs_2_, f32[32,128]{1,0:T(8,128)} %get-tuple-element.20.refs_3_, f32[16,8,128]{2,1,0:T(8,128)} %all_to_all.20.refs_4_, ...), custom_call_target="tpu_custom_call" | custom-call | tf_op jit(solution)/shard_map/mix/pallas_call | solution.py:465
  65.1 7.0 %all-to-all-start.1 = ((bf16[16,64,128]{2,1,0:T(8,128)(2,1)}), bf16[16,64,128]{2,1,0:T(8,128)(2,1)}, u32[]{:S(2)}, u32[]{:S(2)}) async-start(bf16[16,64,128]{2,1,0:T(8,128)(2,1)} %bitcast.17), calls=%async_computation.1 | async-start | bytes 524288 | tf_op jit(solution)/shard_map/all_to_all | solution.py:466
  75.7 9.1 %all-to-all-done.1.mixed_h = bf16[16,64,128]{2,1,0:T(8,128)(2,1)} async-done(((bf16[16,64,128]{2,1,0:T(8,128)(2,1)}), bf16[16,64,128]{2,1,0:T(8,128)(2,1)}, u32[]{:S(2)}, u32[]{:S(2)}) %all-to-all-start.1) | async-done | bytes 262176 | tf_op jit(solution)/shard_map/all_to_all | solution.py:466
  84.8 5.5 %proj.1 = (bf16[64,2048]{1,0:T(8,128)(2,1)}, bf16[256,2048]{1,0:T(8,128)(2,1)}, bf16[192,256]{1,0:T(8,128)(2,1)}) custom-call(bf16[16,64,128]{2,1,0:T(8,128)(2,1)} %all-to-all-done.1.mixed_h, bf16[2048,2048]{1,0:T(8,128)(2,1)} %weights_h.1, bf16[64,2048]{1,0:T(8,128)(2,1)} %residual_h.1, f32[3,2048]{1,0:T(4,128)} %gain.1, s32[2,64]{1,0:T(2,128)} %copy.20.routes_h, ...), custom_call_target="tpu_custom_call" | custom-call | tf_op jit(solution)/shard_map/proj/pallas_call | solution.py:500
  90.3 7.8 %all-to-all-start.2 = ((bf16[16,16,2048]{2,1,0:T(8,128)(2,1)}), bf16[16,16,2048]{2,1,0:T(8,128)(2,1)S(1)}, u32[]{:S(2)}, u32[]{:S(2)}) async-start(bf16[16,16,2048]{2,1,0:T(8,128)(2,1)} %bitcast.18), calls=%async_computation.2 | async-start | bytes 2097152 | tf_op jit(solution)/shard_map/all_to_all | solution.py:503
  99.5 1.2 collective-permute-done.8.refs_8_
  100.7 15.8 %all-to-all-done.2 = bf16[16,16,2048]{2,1,0:T(8,128)(2,1)S(1)} async-done(((bf16[16,16,2048]{2,1,0:T(8,128)(2,1)}), bf16[16,16,2048]{2,1,0:T(8,128)(2,1)S(1)}, u32[]{:S(2)}, u32[]{:S(2)}) %all-to-all-start.2) | async-done | bytes 1048608 | tf_op jit(solution)/shard_map/all_to_all | solution.py:503
  118.8 6.6 %experts.1 = bf16[256,2048]{1,0:T(8,128)(2,1)S(1)} custom-call(bf16[256,2048]{1,0:T(8,128)(2,1)S(1)} %bitcast.14, bf16[192,2048]{1,0:T(8,128)(2,1)S(1)} %copy-done, bf16[192,2048]{1,0:T(8,128)(2,1)} %collective-permute-done.3.refs_2_, bf16[192,2048]{1,0:T(8,128)(2,1)} %collective-permute-done.2.refs_3_, bf16[192,2048]{1,0:T(8,128)(2,1)} %collective-permute-done.5.refs_4_, ...), custom_call_target="tpu_custom_call" | custom-call | tf_op jit(solution)/shard_map/experts/pallas_call | solution.py:521
  125.4 19.2 %all_to_all.21 = bf16[16,16,2048]{2,1,0:T(8,128)(2,1)S(1)} all-to-all(bf16[16,16,2048]{2,1,0:T(8,128)(2,1)S(1)} %bitcast.15), channel_id=1, replica_groups=mesh['sp'=16,'tp'=16] {'sp'}, dimensions={0} | all-to-all | bytes 2097152 | tf_op jit(solution)/shard_map/all_to_all | solution.py:522
  144.6 1.3 combine.1
  (42 shorter events, 11.6 us)
Async XLA Ops:
  1.9 22.0 %collective-permute-start.3 = (bf16[192,2048]{1,0:T(8,128)(2,1)}, bf16[192,2048]{1,0:T(8,128)(2,1)}, u32[]{:S(2)}, u32[]{:S(2)}) collective-permute-start(bf16[192,2048]{1,0:T(8,128)(2,1)} %pack.1.refs_1_), channel_id=1, source_target_pairs={{0,1},{1,0},{2,3},{3,2},{4,5},{5,4},{6,7},{7,6},{8,9},{9,8},{10,11... | collective-permute-start | bytes 2359304 | tf_op jit(solution)/shard_map/ppermute | solution.py:399
  5.2 19.6 %collective-permute-start.2 = (bf16[192,2048]{1,0:T(8,128)(2,1)}, bf16[192,2048]{1,0:T(8,128)(2,1)}, u32[]{:S(2)}, u32[]{:S(2)}) collective-permute-start(bf16[192,2048]{1,0:T(8,128)(2,1)} %pack.1.refs_1_), channel_id=1, source_target_pairs={{0,2},{1,15},{2,4},{3,1},{4,6},{5,3},{6,8},{7,5},{8,10},{9,7},{10,... | collective-permute-start | bytes 2359304 | tf_op jit(solution)/shard_map/ppermute | solution.py:396
  9.8 4.9 %collective-permute-start = (bf16[2,128]{1,0:T(2,128)(2,1)S(1)}, bf16[2,128]{1,0:T(2,128)(2,1)}, u32[]{:S(2)}, u32[]{:S(2)}) collective-permute-start(bf16[2,128]{1,0:T(2,128)(2,1)S(1)} %get-tuple-element.30), channel_id=1, source_target_pairs={{0,16},{16,32},{32,48},{48,64},{64,80},{80,96},{96,112},{112,128},... | collective-permute-start | bytes 1544 | tf_op jit(solution)/shard_map/ppermute | solution.py:381
  13.4 4.7 %collective-permute-start.1 = (bf16[2,128]{1,0:T(2,128)(2,1)S(1)}, bf16[2,128]{1,0:T(2,128)(2,1)}, u32[]{:S(2)}, u32[]{:S(2)}) collective-permute-start(bf16[2,128]{1,0:T(2,128)(2,1)S(1)} %get-tuple-element.29), channel_id=1, source_target_pairs={{16,0},{32,16},{48,32},{64,48},{80,64},{96,80},{112,96},{128,112},... | collective-permute-start | bytes 1544 | tf_op jit(solution)/shard_map/ppermute | solution.py:382
  23.9 15.7 %collective-permute-start.4 = (bf16[192,2048]{1,0:T(8,128)(2,1)}, bf16[192,2048]{1,0:T(8,128)(2,1)}, u32[]{:S(2)}, u32[]{:S(2)}) collective-permute-start(bf16[192,2048]{1,0:T(8,128)(2,1)} %collective-permute-done.3.refs_2_), channel_id=1, source_target_pairs={{0,2},{1,15},{2,4},{3,1},{4,6},{5,3},{6,8},{7,5},{8,10},{9,7},{10,... | collective-permute-start | bytes 2359304 | tf_op jit(solution)/shard_map/ppermute | solution.py:396
  24.7 18.9 %collective-permute-start.7 = (bf16[192,2048]{1,0:T(8,128)(2,1)}, bf16[192,2048]{1,0:T(8,128)(2,1)S(1)}, u32[]{:S(2)}, u32[]{:S(2)}) collective-permute-start(bf16[192,2048]{1,0:T(8,128)(2,1)} %collective-permute-done.2.refs_3_), channel_id=1, source_target_pairs={{0,2},{1,15},{2,4},{3,1},{4,6},{5,3},{6,8},{7,5},{8,10},{9,7},{10,... | collective-permute-start | bytes 2359304 | tf_op jit(solution)/shard_map/ppermute | solution.py:396
  39.6 12.7 %collective-permute-start.9 = (bf16[192,2048]{1,0:T(8,128)(2,1)}, bf16[192,2048]{1,0:T(8,128)(2,1)}, u32[]{:S(2)}, u32[]{:S(2)}) collective-permute-start(bf16[192,2048]{1,0:T(8,128)(2,1)} %collective-permute-done.4.refs_5_), channel_id=1, source_target_pairs={{0,2},{1,15},{2,4},{3,1},{4,6},{5,3},{6,8},{7,5},{8,10},{9,7},{10,... | collective-permute-start | bytes 2359304 | tf_op jit(solution)/shard_map/ppermute | solution.py:396
  44.5 16.3 %collective-permute-start.11 = (bf16[192,2048]{1,0:T(8,128)(2,1)S(1)}, bf16[192,2048]{1,0:T(8,128)(2,1)}, u32[]{:S(2)}, u32[]{:S(2)}) collective-permute-start(bf16[192,2048]{1,0:T(8,128)(2,1)S(1)} %collective-permute-done.7.refs_7_), channel_id=1, source_target_pairs={{0,2},{1,15},{2,4},{3,1},{4,6},{5,3},{6,8},{7,5},{8,10},{9,7},{10,... | collective-permute-start | bytes 2359304 | tf_op jit(solution)/shard_map/ppermute | solution.py:396
  46.3 52.0 %collective-permute-start.5 = (bf16[192,2048]{1,0:T(8,128)(2,1)}, bf16[192,2048]{1,0:T(8,128)(2,1)}, u32[]{:S(2)}, u32[]{:S(2)}) collective-permute-start(bf16[192,2048]{1,0:T(8,128)(2,1)} %collective-permute-done.2.refs_3_), channel_id=1, source_target_pairs={{0,1},{1,0},{2,3},{3,2},{4,5},{5,4},{6,7},{7,6},{8,9},{9,8},{10,11... | collective-permute-start | bytes 2359304 | tf_op jit(solution)/shard_map/ppermute | solution.py:399
  46.3 52.4 %collective-permute-start.6 = (bf16[192,2048]{1,0:T(8,128)(2,1)}, bf16[192,2048]{1,0:T(8,128)(2,1)}, u32[]{:S(2)}, u32[]{:S(2)}) collective-permute-start(bf16[192,2048]{1,0:T(8,128)(2,1)} %collective-permute-done.4.refs_5_), channel_id=1, source_target_pairs={{0,1},{1,0},{2,3},{3,2},{4,5},{5,4},{6,7},{7,6},{8,9},{9,8},{10,11... | collective-permute-start | bytes 2359304 | tf_op jit(solution)/shard_map/ppermute | solution.py:399
  52.3 46.7 %collective-permute-start.13 = (bf16[192,2048]{1,0:T(8,128)(2,1)}, bf16[192,2048]{1,0:T(8,128)(2,1)}, u32[]{:S(2)}, u32[]{:S(2)}) collective-permute-start(bf16[192,2048]{1,0:T(8,128)(2,1)} %collective-permute-done.9.refs_9_), channel_id=1, source_target_pairs={{0,2},{1,15},{2,4},{3,1},{4,6},{5,3},{6,8},{7,5},{8,10},{9,7},{10,... | collective-permute-start | bytes 2359304 | tf_op jit(solution)/shard_map/ppermute | solution.py:396
  60.7 38.5 %collective-permute-start.15 = (bf16[192,2048]{1,0:T(8,128)(2,1)}, bf16[192,2048]{1,0:T(8,128)(2,1)}, u32[]{:S(2)}, u32[]{:S(2)}) collective-permute-start(bf16[192,2048]{1,0:T(8,128)(2,1)} %collective-permute-done.11.refs_11_), channel_id=1, source_target_pairs={{0,2},{1,15},{2,4},{3,1},{4,6},{5,3},{6,8},{7,5},{8,10},{9,7},{10,... | collective-permute-start | bytes 2359304 | tf_op jit(solution)/shard_map/ppermute | solution.py:396
  65.1 19.7 %all-to-all-start.1 = ((bf16[16,64,128]{2,1,0:T(8,128)(2,1)}), bf16[16,64,128]{2,1,0:T(8,128)(2,1)}, u32[]{:S(2)}, u32[]{:S(2)}) async-start(bf16[16,64,128]{2,1,0:T(8,128)(2,1)} %bitcast.17), calls=%async_computation.1 | async-start | bytes 524288 | tf_op jit(solution)/shard_map/all_to_all | solution.py:466
  90.3 26.2 %all-to-all-start.2 = ((bf16[16,16,2048]{2,1,0:T(8,128)(2,1)}), bf16[16,16,2048]{2,1,0:T(8,128)(2,1)S(1)}, u32[]{:S(2)}, u32[]{:S(2)}) async-start(bf16[16,16,2048]{2,1,0:T(8,128)(2,1)} %bitcast.18), calls=%async_computation.2 | async-start | bytes 2097152 | tf_op jit(solution)/shard_map/all_to_all | solution.py:503
  98.1 2.6 %collective-permute-start.8 = (bf16[192,2048]{1,0:T(8,128)(2,1)}, bf16[192,2048]{1,0:T(8,128)(2,1)S(1)}, u32[]{:S(2)}, u32[]{:S(2)}) collective-permute-start(bf16[192,2048]{1,0:T(8,128)(2,1)} %copy-done.1), channel_id=1, source_target_pairs={{0,1},{1,0},{2,3},{3,2},{4,5},{5,4},{6,7},{7,6},{8,9},{9,8},{10,11... | collective-permute-start | bytes 2359304 | tf_op jit(solution)/shard_map/ppermute | solution.py:399
  98.3 18.2 %collective-permute-start.10 = (bf16[192,2048]{1,0:T(8,128)(2,1)}, bf16[192,2048]{1,0:T(8,128)(2,1)S(1)}, u32[]{:S(2)}, u32[]{:S(2)}) collective-permute-start(bf16[192,2048]{1,0:T(8,128)(2,1)} %collective-permute-done.9.refs_9_), channel_id=1, source_target_pairs={{0,1},{1,0},{2,3},{3,2},{4,5},{5,4},{6,7},{7,6},{8,9},{9,8},{10,11... | collective-permute-start | bytes 2359304 | tf_op jit(solution)/shard_map/ppermute | solution.py:399
  98.7 17.8 %collective-permute-start.12 = (bf16[192,2048]{1,0:T(8,128)(2,1)}, bf16[192,2048]{1,0:T(8,128)(2,1)S(1)}, u32[]{:S(2)}, u32[]{:S(2)}) collective-permute-start(bf16[192,2048]{1,0:T(8,128)(2,1)} %collective-permute-done.11.refs_11_), channel_id=1, source_target_pairs={{0,1},{1,0},{2,3},{3,2},{4,5},{5,4},{6,7},{7,6},{8,9},{9,8},{10,11... | collective-permute-start | bytes 2359304 | tf_op jit(solution)/shard_map/ppermute | solution.py:399
  99.0 17.5 %collective-permute-start.14 = (bf16[192,2048]{1,0:T(8,128)(2,1)}, bf16[192,2048]{1,0:T(8,128)(2,1)}, u32[]{:S(2)}, u32[]{:S(2)}) collective-permute-start(bf16[192,2048]{1,0:T(8,128)(2,1)} %collective-permute-done.13.refs_13_), channel_id=1, source_target_pairs={{0,1},{1,0},{2,3},{3,2},{4,5},{5,4},{6,7},{7,6},{8,9},{9,8},{10,11... | collective-permute-start | bytes 2359304 | tf_op jit(solution)/shard_map/ppermute | solution.py:399
  99.2 17.3 %collective-permute-start.16 = (bf16[192,2048]{1,0:T(8,128)(2,1)}, bf16[192,2048]{1,0:T(8,128)(2,1)}, u32[]{:S(2)}, u32[]{:S(2)}) collective-permute-start(bf16[192,2048]{1,0:T(8,128)(2,1)} %collective-permute-done.15.refs_15_), channel_id=1, source_target_pairs={{0,1},{1,0},{2,3},{3,2},{4,5},{5,4},{6,7},{7,6},{8,9},{9,8},{10,11... | collective-permute-start | bytes 2359304 | tf_op jit(solution)/shard_map/ppermute | solution.py:399
  116.5 1.1 copy-start
  117.7 1.1 copy-start.2
  118.8 25.8 %copy-start.3 = (bf16[64,2048]{1,0:T(8,128)(2,1)S(1)}, bf16[64,2048]{1,0:T(8,128)(2,1)}, u32[]{:S(2)}) copy-start(bf16[64,2048]{1,0:T(8,128)(2,1)} %get-tuple-element.27.stream) | copy-start | bytes 786436
  118.8 25.8 %copy-start.4 = (f32[3,2048]{1,0:T(4,128)S(1)}, f32[3,2048]{1,0:T(4,128)}, u32[]{:S(2)}) copy-start(f32[3,2048]{1,0:T(4,128)} %gain.1) | copy-start | bytes 73732
  118.8 25.8 %copy-start.5 = (bf16[192,256]{1,0:T(8,128)(2,1)S(1)}, bf16[192,256]{1,0:T(8,128)(2,1)}, u32[]{:S(2)}) copy-start(bf16[192,256]{1,0:T(8,128)(2,1)} %get-tuple-element.28.table) | copy-start | bytes 294916
  (2 other events, 1.5 us)

commit v9 on v8

--- a/solution.py
+++ b/solution.py
@@ -20,7 +20,7 @@
 
 
 FULL = pltpu.CompilerParams(vmem_limit_bytes=67043328)
-ROOMY = pltpu.CompilerParams(vmem_limit_bytes=30 * 1024 * 1024)
+ROOMY = pltpu.CompilerParams(vmem_limit_bytes=40 * 1024 * 1024)
 
 
 def anywhere():
@@ -59,27 +59,23 @@
 def scan_kernel(
     mix_h, before_h, after_h, conv_w_h, conv_b_h, decay_param_h, recur_gate_h, recur_bias_h, input_gate_h, input_bias_h,
     h_h, p_f_h, p_b_h, seg_h, total_h,
-    padded, conv, split, wide, wlow, pre, a_f, b_f, a_b, b_b,
+    padded, conv, split, wide, pre, a_f, b_f, a_b, b_b,
     mix, before, after, conv_w, conv_b, decay_param, recur_gate, recur_bias, input_gate, input_bias,
     h, p_f, p_b, seg, total, sems,
 ):
-    for copy in fetched(
+    loads = fetched(
         (
             mix_h, before_h, after_h, conv_w_h, conv_b_h, decay_param_h,
             recur_gate_h, recur_bias_h, input_gate_h, input_bias_h,
         ),
         (mix, before, after, conv_w, conv_b, decay_param, recur_gate, recur_bias, input_gate, input_bias),
         sems,
-    ):
+    )
+    for copy in loads[3:]:
         copy.wait()
     length = mix.shape[0]
     step = length // SEGS
     stride = step + 8
-    padded[0:8, :] = jnp.zeros((8, 128), F32)
-    padded[6:8, :] = before[...].astype(F32)
-    padded[8 : 8 + length, :] = mix[...].astype(F32)
-    padded[8 + length : 16 + length, :] = jnp.zeros((8, 128), F32)
-    padded[8 + length : 10 + length, :] = after[...].astype(F32)
     zero = jnp.zeros((64, 64), F32)
     columns = []
     for sense in range(2):
@@ -97,7 +93,14 @@
     high = maps.astype(BF16)
     wide[0:128, :] = high
     wide[128:256, :] = high
-    wlow[...] = (maps - high.astype(F32)).astype(BF16)
+    wide[256:384, :] = (maps - high.astype(F32)).astype(BF16)
+    for copy in loads[:3]:
+        copy.wait()
+    padded[0:8, :] = jnp.zeros((8, 128), F32)
+    padded[6:8, :] = before[...].astype(F32)
+    padded[8 : 8 + length, :] = mix[...].astype(F32)
+    padded[8 + length : 16 + length, :] = jnp.zeros((8, 128), F32)
+    padded[8 + length : 10 + length, :] = after[...].astype(F32)
 
     rows = 64
 
@@ -110,12 +113,11 @@
         top = out.astype(BF16)
         split[pl.ds(at, rows), 0:128] = top
         split[pl.ds(at, rows), 128:256] = (out - top.astype(F32)).astype(BF16)
+        split[pl.ds(at, rows), 256:384] = top
         return carry
 
     lax.fori_loop(0, length // rows, convolve, 0)
-    pre[...] = jnp.dot(split[...], wide[...], preferred_element_type=F32) + jnp.dot(
-        split[:, 0:128], wlow[...], preferred_element_type=F32
-    )
+    pre[...] = jnp.dot(split[...], wide[...], preferred_element_type=F32)
     rate = -8.0 * softplus_of(-decay_param[...])
 
     per = step // rows
@@ -210,13 +212,16 @@
         return carry
 
     lax.fori_loop(0, step, place, 0, unroll=8)
+    sent = []
     for s in range(SEGS):
         gate = gate_in[s * step : (s + 1) * step, :].astype(F32)
         out[s * step : (s + 1) * step, :] = (
             natural[s * stride : s * stride + step, :] * jax.nn.gelu(gate)
         ).astype(BF16)
-    (copy,) = fetched((out,), (out_h,), sems, 6)
-    copy.wait()
+        part = pl.ds(s * step, step)
+        sent += fetched((out.at[part],), (out_h.at[part],), sems, 6 + s)
+    for copy in sent:
+        copy.wait()
 
 
 def scaled(values, gain):
@@ -310,9 +315,8 @@
 
 
 def expert_kernel(*refs):
-    tokens, shares = refs[0], refs[1:-7]
-    out, gate_w, up_w, down_w, held, sems, extra = refs[-7:]
-    (tokens_copy,) = fetched((tokens,), (held,), extra)
+    tokens, ready, shares = refs[0], refs[1:5], refs[5:-5]
+    out, gate_w, up_w, down_w, sems = refs[-5:]
     ff = shares[0].shape[0] // 3
     copies = [
         fetched(
@@ -323,23 +327,24 @@
         )
         for at, share in enumerate(shares)
     ]
-    tokens_copy.wait()
-    x = held[...]
-    acc = jnp.zeros(x.shape, F32)
-    block = 256
+    x = tokens[...]
+    block = len(ready) * ff
     last = (((1,), (1,)), ((), ()))
+
+    def part(gate_rows, up_rows, down_rows):
+        gate = lax.dot_general(x, gate_rows, last, preferred_element_type=F32)
+        up = lax.dot_general(x, up_rows, last, preferred_element_type=F32)
+        hidden = (jax.nn.silu(gate) * up).astype(BF16)
+        return jnp.dot(hidden, down_rows, preferred_element_type=F32)
+
+    acc = part(*(jnp.concatenate([p[j * ff : (j + 1) * ff, :] for p in ready], axis=0) for j in range(3)))
     for k in range(len(shares) * ff // block):
         for piece in range(k * block // ff, (k + 1) * block // ff):
             for copy in copies[piece]:
                 copy.wait()
         rows = slice(k * block, (k + 1) * block)
-        gate = lax.dot_general(x, gate_w[rows, :], last, preferred_element_type=F32)
-        up = lax.dot_general(x, up_w[rows, :], last, preferred_element_type=F32)
-        hidden = (jax.nn.silu(gate) * up).astype(BF16)
-        acc = acc + jnp.dot(hidden, down_w[rows, :], preferred_element_type=F32)
-    held[...] = acc.astype(BF16)
-    (copy,) = fetched((held,), (out,), extra, 1)
-    copy.wait()
+        acc = acc + part(gate_w[rows, :], up_w[rows, :], down_w[rows, :])
+    out[...] = acc.astype(BF16)
 
 
 def combine_kernel(values, stream, gain, table, out):
@@ -412,9 +417,8 @@
         scratch_shapes=[
             pltpu.VMEM((length + 16, 128), F32),
             pltpu.VMEM((length, 128), F32),
-            pltpu.VMEM((length, 256), BF16),
-            pltpu.VMEM((256, 512), BF16),
-            pltpu.VMEM((128, 512), BF16),
+            pltpu.VMEM((length, 384), BF16),
+            pltpu.VMEM((384, 512), BF16),
             pltpu.VMEM((length, 512), F32),
             pltpu.VMEM((lines, 128), F32),
             pltpu.VMEM((lines, 128), F32),
@@ -457,7 +461,7 @@
             pltpu.VMEM((sp, 8, 128), F32),
             pltpu.VMEM((length, channels), BF16),
             pltpu.VMEM((length, channels), BF16),
-            pltpu.SemaphoreType.DMA((8,)),
+            pltpu.SemaphoreType.DMA((14,)),
         ],
         compiler_params=FULL,
         name="mix",
@@ -503,22 +507,19 @@
     arrived = lax.all_to_all(outgoing.reshape(sp, slots // sp, width), "sp", split_axis=0, concat_axis=0, tiled=True)
     arrived = arrived.reshape(slots, width)
 
-    shares = (own, other, r1a, e1a, r1b, e1b, r2a, e2a, r2b, e2b, r3a, e3a, r3b, e3b, r4, e4)
+    ready = (e3a, e3b, r4, e4)
+    shares = (own, other, r1a, e1a, r1b, e1b, r2a, e2a, r2b, e2b, r3a, r3b)
     experts = pl.pallas_call(
         expert_kernel,
         out_shape=shape((slots, width), BF16),
-        in_specs=[anywhere()] * (1 + len(shares)),
-        out_specs=anywhere(),
+        in_specs=[whole()] * (1 + len(ready)) + [anywhere()] * len(shares),
+        out_specs=whole(),
         scratch_shapes=[pltpu.VMEM((len(shares) * ff_own, width), BF16)] * 3
-        + [
-            pltpu.VMEM((slots, width), BF16),
-            pltpu.SemaphoreType.DMA((3 * len(shares),)),
-            pltpu.SemaphoreType.DMA((2,)),
-        ],
+        + [pltpu.SemaphoreType.DMA((3 * len(shares),))],
         compiler_params=ROOMY,
         name="experts",
     )
-    done = experts(arrived, *shares)
+    done = experts(arrived, *ready, *shares)
     returned = lax.all_to_all(
         done.reshape(sp, slots // sp, width), "sp", split_axis=0, concat_axis=0, tiled=True
     )

time: 146 us -> 148 us (1.014)
  transfers between devices with their start and end apart: 19 -> 19, of which waited for: 7 -> 7; matrix products, arithmetic and copies ran while one was open for 3% -> 2% of each run, Pallas kernels for 10% -> 10%
where the time goes in v9:
time: 148 us; the launch traced here: 147 us
  waiting for transfers between devices  45.4 us (31%)
  starting transfers between devices  36.3 us (25%)
  blocking collectives  33.2 us (22%)
  Pallas kernels  24.5 us (17%)
  local copies, waits for them, and re-layouts  7.42 us (5%)
    all_to_all x1, blocking collectives, layer(): lax.all_to_all(done.reshape(sp, slots // sp, width), 'sp', split_axis=0,...  19.2 us
    all_to_all x1, waiting for transfers between devices, layer(): lax.all_to_all(outgoing.reshape(sp, slots // sp, width), 'sp', split_axis...  15.9 us
    ppermute x7, waiting for transfers between devices, around(): lax.ppermute(part, 'tp', [(i, (i + 2 - 4 * (i % 2)) % tp) for i in range(...  15.8 us
    all_to_all x1, blocking collectives, layer(): lax.all_to_all(total, 'sp', split_axis=0, concat_axis=0, tiled=True)  14 us
    ppermute x7, starting transfers between devices, around(): lax.ppermute(part, 'tp', [(i, (i + 2 - 4 * (i % 2)) % tp) for i in range(...  11.1 us
    all_to_all x1, waiting for transfers between devices, layer(): lax.all_to_all(mixed.reshape(tp, rows, channels), 'tp', split_axis=0, con...  9.09 us
    all_to_all x1, starting transfers between devices, layer(): lax.all_to_all(outgoing.reshape(sp, slots // sp, width), 'sp', split_axis...  7.89 us
    all_to_all x1, starting transfers between devices, layer(): lax.all_to_all(mixed.reshape(tp, rows, channels), 'tp', split_axis=0, con...  7.21 us
  transfers between devices with their start and end apart: 19, of which 7 were waited for; matrix products, arithmetic and copies ran while one was open for 2% of the time, Pallas kernels for 10%

profile of v9, /device:TPU:1, one launch (start us, length us, event | category | flops | bytes accessed | tf_op | source)
XLA Modules:
  0.0 146.9 jit_solution(18099395089946047191)
XLA Ops:
  0.0 1.9 %pack.1.refs_5_ = bf16[192,2048]{1,0:T(8,128)(2,1)} custom-call(bf16[64,2048]{1,0:T(8,128)(2,1)} %bitcast.19, bf16[64,2048]{1,0:T(8,128)(2,1)} %bitcast.20, bf16[64,2048]{1,0:T(8,128)(2,1)} %bitcast.21), custom_call_target="tpu_custom_call" | custom-call | tf_op jit(solution)/shard_map/pack/pallas_call | solution.py:390
  1.9 3.3 %collective-permute-start.3 = (bf16[192,2048]{1,0:T(8,128)(2,1)}, bf16[192,2048]{1,0:T(8,128)(2,1)}, u32[]{:S(2)}, u32[]{:S(2)}) collective-permute-start(bf16[192,2048]{1,0:T(8,128)(2,1)} %pack.1.refs_5_), channel_id=1, source_target_pairs={{0,1},{1,0},{2,3},{3,2},{4,5},{5,4},{6,7},{7,6},{8,9},{9,8},{10,11... | collective-permute-start | bytes 2359304 | tf_op jit(solution)/shard_map/ppermute | solution.py:404
  5.2 3.9 %collective-permute-start.2 = (bf16[192,2048]{1,0:T(8,128)(2,1)}, bf16[192,2048]{1,0:T(8,128)(2,1)}, u32[]{:S(2)}, u32[]{:S(2)}) collective-permute-start(bf16[192,2048]{1,0:T(8,128)(2,1)} %pack.1.refs_5_), channel_id=1, source_target_pairs={{0,2},{1,15},{2,4},{3,1},{4,6},{5,3},{6,8},{7,5},{8,10},{9,7},{10,... | collective-permute-start | bytes 2359304 | tf_op jit(solution)/shard_map/ppermute | solution.py:401
  9.8 3.6 %collective-permute-start = (bf16[2,128]{1,0:T(2,128)(2,1)S(1)}, bf16[2,128]{1,0:T(2,128)(2,1)}, u32[]{:S(2)}, u32[]{:S(2)}) collective-permute-start(bf16[2,128]{1,0:T(2,128)(2,1)S(1)} %get-tuple-element.30), channel_id=1, source_target_pairs={{0,16},{16,32},{32,48},{48,64},{64,80},{80,96},{96,112},{112,128},... | collective-permute-start | bytes 1544 | tf_op jit(solution)/shard_map/ppermute | solution.py:386
  13.4 1.3 collective-permute-start.1
  14.7 3.4 %collective-permute-done.1.after_h = bf16[2,128]{1,0:T(2,128)(2,1)} collective-permute-done((bf16[2,128]{1,0:T(2,128)(2,1)S(1)}, bf16[2,128]{1,0:T(2,128)(2,1)}, u32[]{:S(2)}, u32[]{:S(2)}) %collective-permute-start.1) | collective-permute-done | bytes 544 | tf_op jit(solution)/shard_map/ppermute | solution.py:387
  18.1 5.9 %scan.1 = (f32[1024,128]{1,0:T(8,128)}, f32[1024,128]{1,0:T(8,128)}, f32[1024,128]{1,0:T(8,128)}, f32[32,128]{1,0:T(8,128)}, f32[16,8,128]{2,1,0:T(8,128)}) custom-call(bf16[1024,128]{1,0:T(8,128)(2,1)} %mix_h.1, bf16[2,128]{1,0:T(2,128)(2,1)} %collective-permute-done.before_h, bf16[2,128]{1,0:T(2,128)(2,1)} %collective-permute-done.1.after_h, ...), custom_call_target="tpu_custom_call" | custom-call | tf_op jit(solution)/shard_map/scan/pallas_call | solution.py:412
  25.6 14.0 %all_to_all.20.refs_4_ = f32[16,8,128]{2,1,0:T(8,128)} all-to-all(f32[16,8,128]{2,1,0:T(8,128)} %get-tuple-element.22), channel_id=1, replica_groups=mesh['sp'=16,'tp'=16] {'sp'}, dimensions={0} | all-to-all | bytes 131072 | tf_op jit(solution)/shard_map/all_to_all | solution.py:449
  40.3 3.5 %collective-permute-done.5.refs_11_ = bf16[192,2048]{1,0:T(8,128)(2,1)S(1)} collective-permute-done((bf16[192,2048]{1,0:T(8,128)(2,1)}, bf16[192,2048]{1,0:T(8,128)(2,1)S(1)}, u32[]{:S(2)}, u32[]{:S(2)}) %collective-permute-start.5) | collective-permute-done | bytes 786464 | tf_op jit(solution)/shard_map/ppermute | solution.py:401
  44.7 1.7 %collective-permute-start.6 = (bf16[192,2048]{1,0:T(8,128)(2,1)S(1)}, bf16[192,2048]{1,0:T(8,128)(2,1)}, u32[]{:S(2)}, u32[]{:S(2)}) collective-permute-start(bf16[192,2048]{1,0:T(8,128)(2,1)S(1)} %collective-permute-done.5.refs_11_), channel_id=1, source_target_pairs={{0,2},{1,15},{2,4},{3,1},{4,6},{5,3},{6,8},{7,5},{8,10},{9,7},{10,... | collective-permute-start | bytes 2359304 | tf_op jit(solution)/shard_map/ppermute | solution.py:401
  46.9 5.5 %collective-permute-done.8.refs_13_ = bf16[192,2048]{1,0:T(8,128)(2,1)} collective-permute-done((bf16[192,2048]{1,0:T(8,128)(2,1)}, bf16[192,2048]{1,0:T(8,128)(2,1)}, u32[]{:S(2)}, u32[]{:S(2)}) %collective-permute-start.8) | collective-permute-done | bytes 786464 | tf_op jit(solution)/shard_map/ppermute | solution.py:401
  52.4 1.6 %collective-permute-start.9 = (bf16[192,2048]{1,0:T(8,128)(2,1)}, bf16[192,2048]{1,0:T(8,128)(2,1)}, u32[]{:S(2)}, u32[]{:S(2)}) collective-permute-start(bf16[192,2048]{1,0:T(8,128)(2,1)} %collective-permute-done.8.refs_13_), channel_id=1, source_target_pairs={{0,2},{1,15},{2,4},{3,1},{4,6},{5,3},{6,8},{7,5},{8,10},{9,7},{10,... | collective-permute-start | bytes 2359304 | tf_op jit(solution)/shard_map/ppermute | solution.py:401
  54.0 6.8 %collective-permute-done.6.refs_15_ = bf16[192,2048]{1,0:T(8,128)(2,1)} collective-permute-done((bf16[192,2048]{1,0:T(8,128)(2,1)S(1)}, bf16[192,2048]{1,0:T(8,128)(2,1)}, u32[]{:S(2)}, u32[]{:S(2)}) %collective-permute-start.6) | collective-permute-done | bytes 786464 | tf_op jit(solution)/shard_map/ppermute | solution.py:401
  60.8 1.6 %collective-permute-start.11 = (bf16[192,2048]{1,0:T(8,128)(2,1)}, bf16[192,2048]{1,0:T(8,128)(2,1)}, u32[]{:S(2)}, u32[]{:S(2)}) collective-permute-start(bf16[192,2048]{1,0:T(8,128)(2,1)} %collective-permute-done.6.refs_15_), channel_id=1, source_target_pairs={{0,2},{1,15},{2,4},{3,1},{4,6},{5,3},{6,8},{7,5},{8,10},{9,7},{10,... | collective-permute-start | bytes 2359304 | tf_op jit(solution)/shard_map/ppermute | solution.py:401
  62.5 2.7 %mix.1 = bf16[1024,128]{1,0:T(8,128)(2,1)} custom-call(f32[1024,128]{1,0:T(8,128)} %get-tuple-element.17.refs_0_, f32[1024,128]{1,0:T(8,128)} %get-tuple-element.18.refs_1_, f32[1024,128]{1,0:T(8,128)} %get-tuple-element.19.refs_2_, f32[32,128]{1,0:T(8,128)} %get-tuple-element.20.refs_3_, f32[16,8,128]{2,1,0:T(8,128)} %all_to_all.20.refs_4_, ...), custom_call_target="tpu_custom_call" | custom-call | tf_op jit(solution)/shard_map/mix/pallas_call | solution.py:469
  65.1 7.2 %all-to-all-start.1 = ((bf16[16,64,128]{2,1,0:T(8,128)(2,1)}), bf16[16,64,128]{2,1,0:T(8,128)(2,1)}, u32[]{:S(2)}, u32[]{:S(2)}) async-start(bf16[16,64,128]{2,1,0:T(8,128)(2,1)} %bitcast.16), calls=%async_computation.1 | async-start | bytes 524288 | tf_op jit(solution)/shard_map/all_to_all | solution.py:470
  75.9 9.1 %all-to-all-done.1.mixed_h = bf16[16,64,128]{2,1,0:T(8,128)(2,1)} async-done(((bf16[16,64,128]{2,1,0:T(8,128)(2,1)}), bf16[16,64,128]{2,1,0:T(8,128)(2,1)}, u32[]{:S(2)}, u32[]{:S(2)}) %all-to-all-start.1) | async-done | bytes 262176 | tf_op jit(solution)/shard_map/all_to_all | solution.py:470
  85.0 5.5 %proj.1 = (bf16[64,2048]{1,0:T(8,128)(2,1)}, bf16[256,2048]{1,0:T(8,128)(2,1)}, bf16[192,256]{1,0:T(8,128)(2,1)}) custom-call(bf16[16,64,128]{2,1,0:T(8,128)(2,1)} %all-to-all-done.1.mixed_h, bf16[2048,2048]{1,0:T(8,128)(2,1)} %weights_h.1, bf16[64,2048]{1,0:T(8,128)(2,1)} %residual_h.1, f32[3,2048]{1,0:T(4,128)} %gain.1, s32[2,64]{1,0:T(2,128)} %copy.20.routes_h, ...), custom_call_target="tpu_custom_call" | custom-call | tf_op jit(solution)/shard_map/proj/pallas_call | solution.py:504
  90.5 7.9 %all-to-all-start.2 = ((bf16[16,16,2048]{2,1,0:T(8,128)(2,1)}), bf16[16,16,2048]{2,1,0:T(8,128)(2,1)}, u32[]{:S(2)}, u32[]{:S(2)}) async-start(bf16[16,16,2048]{2,1,0:T(8,128)(2,1)} %bitcast.17), calls=%async_computation.2 | async-start | bytes 2097152 | tf_op jit(solution)/shard_map/all_to_all | solution.py:507
  99.9 1.2 collective-permute-done.15.refs_12_
  101.0 15.9 %all-to-all-done.2 = bf16[16,16,2048]{2,1,0:T(8,128)(2,1)} async-done(((bf16[16,16,2048]{2,1,0:T(8,128)(2,1)}), bf16[16,16,2048]{2,1,0:T(8,128)(2,1)}, u32[]{:S(2)}, u32[]{:S(2)}) %all-to-all-start.2) | async-done | bytes 1048608 | tf_op jit(solution)/shard_map/all_to_all | solution.py:507
  119.2 7.2 %experts.1 = bf16[256,2048]{1,0:T(8,128)(2,1)S(1)} custom-call(bf16[256,2048]{1,0:T(8,128)(2,1)} %bitcast.9.refs_0_, bf16[192,2048]{1,0:T(8,128)(2,1)S(1)} %collective-permute-done.7.refs_1_, bf16[192,2048]{1,0:T(8,128)(2,1)S(1)} %collective-permute-done.10.refs_2_, bf16[192,2048]{1,0:T(8,128)(2,1)} %collective-permute-done.11.refs_3_, ...), custom_call_target="tpu_custom_call" | custom-call | tf_op jit(solution)/shard_map/experts/pallas_call | solution.py:522
  126.4 19.2 %all_to_all.21 = bf16[16,16,2048]{2,1,0:T(8,128)(2,1)S(1)} all-to-all(bf16[16,16,2048]{2,1,0:T(8,128)(2,1)S(1)} %bitcast.14), channel_id=1, replica_groups=mesh['sp'=16,'tp'=16] {'sp'}, dimensions={0} | all-to-all | bytes 2097152 | tf_op jit(solution)/shard_map/all_to_all | solution.py:523
  145.6 1.3 combine.1
  (42 shorter events, 11.6 us)
Async XLA Ops:
  1.9 22.1 %collective-permute-start.3 = (bf16[192,2048]{1,0:T(8,128)(2,1)}, bf16[192,2048]{1,0:T(8,128)(2,1)}, u32[]{:S(2)}, u32[]{:S(2)}) collective-permute-start(bf16[192,2048]{1,0:T(8,128)(2,1)} %pack.1.refs_5_), channel_id=1, source_target_pairs={{0,1},{1,0},{2,3},{3,2},{4,5},{5,4},{6,7},{7,6},{8,9},{9,8},{10,11... | collective-permute-start | bytes 2359304 | tf_op jit(solution)/shard_map/ppermute | solution.py:404
  5.2 19.6 %collective-permute-start.2 = (bf16[192,2048]{1,0:T(8,128)(2,1)}, bf16[192,2048]{1,0:T(8,128)(2,1)}, u32[]{:S(2)}, u32[]{:S(2)}) collective-permute-start(bf16[192,2048]{1,0:T(8,128)(2,1)} %pack.1.refs_5_), channel_id=1, source_target_pairs={{0,2},{1,15},{2,4},{3,1},{4,6},{5,3},{6,8},{7,5},{8,10},{9,7},{10,... | collective-permute-start | bytes 2359304 | tf_op jit(solution)/shard_map/ppermute | solution.py:401
  9.8 4.9 %collective-permute-start = (bf16[2,128]{1,0:T(2,128)(2,1)S(1)}, bf16[2,128]{1,0:T(2,128)(2,1)}, u32[]{:S(2)}, u32[]{:S(2)}) collective-permute-start(bf16[2,128]{1,0:T(2,128)(2,1)S(1)} %get-tuple-element.30), channel_id=1, source_target_pairs={{0,16},{16,32},{32,48},{48,64},{64,80},{80,96},{96,112},{112,128},... | collective-permute-start | bytes 1544 | tf_op jit(solution)/shard_map/ppermute | solution.py:386
  13.4 4.7 %collective-permute-start.1 = (bf16[2,128]{1,0:T(2,128)(2,1)S(1)}, bf16[2,128]{1,0:T(2,128)(2,1)}, u32[]{:S(2)}, u32[]{:S(2)}) collective-permute-start(bf16[2,128]{1,0:T(2,128)(2,1)S(1)} %get-tuple-element.29), channel_id=1, source_target_pairs={{16,0},{32,16},{48,32},{64,48},{80,64},{96,80},{112,96},{128,112},... | collective-permute-start | bytes 1544 | tf_op jit(solution)/shard_map/ppermute | solution.py:387
  24.0 15.5 %collective-permute-start.4 = (bf16[192,2048]{1,0:T(8,128)(2,1)}, bf16[192,2048]{1,0:T(8,128)(2,1)}, u32[]{:S(2)}, u32[]{:S(2)}) collective-permute-start(bf16[192,2048]{1,0:T(8,128)(2,1)} %collective-permute-done.3.refs_6_), channel_id=1, source_target_pairs={{0,2},{1,15},{2,4},{3,1},{4,6},{5,3},{6,8},{7,5},{8,10},{9,7},{10,... | collective-permute-start | bytes 2359304 | tf_op jit(solution)/shard_map/ppermute | solution.py:401
  24.8 19.0 %collective-permute-start.5 = (bf16[192,2048]{1,0:T(8,128)(2,1)}, bf16[192,2048]{1,0:T(8,128)(2,1)S(1)}, u32[]{:S(2)}, u32[]{:S(2)}) collective-permute-start(bf16[192,2048]{1,0:T(8,128)(2,1)} %collective-permute-done.2.refs_7_), channel_id=1, source_target_pairs={{0,2},{1,15},{2,4},{3,1},{4,6},{5,3},{6,8},{7,5},{8,10},{9,7},{10,... | collective-permute-start | bytes 2359304 | tf_op jit(solution)/shard_map/ppermute | solution.py:401
  39.6 12.8 %collective-permute-start.8 = (bf16[192,2048]{1,0:T(8,128)(2,1)}, bf16[192,2048]{1,0:T(8,128)(2,1)}, u32[]{:S(2)}, u32[]{:S(2)}) collective-permute-start(bf16[192,2048]{1,0:T(8,128)(2,1)} %collective-permute-done.4.refs_9_), channel_id=1, source_target_pairs={{0,2},{1,15},{2,4},{3,1},{4,6},{5,3},{6,8},{7,5},{8,10},{9,7},{10,... | collective-permute-start | bytes 2359304 | tf_op jit(solution)/shard_map/ppermute | solution.py:401
  44.7 16.1 %collective-permute-start.6 = (bf16[192,2048]{1,0:T(8,128)(2,1)S(1)}, bf16[192,2048]{1,0:T(8,128)(2,1)}, u32[]{:S(2)}, u32[]{:S(2)}) collective-permute-start(bf16[192,2048]{1,0:T(8,128)(2,1)S(1)} %collective-permute-done.5.refs_11_), channel_id=1, source_target_pairs={{0,2},{1,15},{2,4},{3,1},{4,6},{5,3},{6,8},{7,5},{8,10},{9,7},{10,... | collective-permute-start | bytes 2359304 | tf_op jit(solution)/shard_map/ppermute | solution.py:401
  46.4 52.2 %collective-permute-start.13 = (bf16[192,2048]{1,0:T(8,128)(2,1)}, bf16[192,2048]{1,0:T(8,128)(2,1)}, u32[]{:S(2)}, u32[]{:S(2)}) collective-permute-start(bf16[192,2048]{1,0:T(8,128)(2,1)} %collective-permute-done.2.refs_7_), channel_id=1, source_target_pairs={{0,1},{1,0},{2,3},{3,2},{4,5},{5,4},{6,7},{7,6},{8,9},{9,8},{10,11... | collective-permute-start | bytes 2359304 | tf_op jit(solution)/shard_map/ppermute | solution.py:404
  46.4 52.6 %collective-permute-start.14 = (bf16[192,2048]{1,0:T(8,128)(2,1)}, bf16[192,2048]{1,0:T(8,128)(2,1)}, u32[]{:S(2)}, u32[]{:S(2)}) collective-permute-start(bf16[192,2048]{1,0:T(8,128)(2,1)} %collective-permute-done.4.refs_9_), channel_id=1, source_target_pairs={{0,1},{1,0},{2,3},{3,2},{4,5},{5,4},{6,7},{7,6},{8,9},{9,8},{10,11... | collective-permute-start | bytes 2359304 | tf_op jit(solution)/shard_map/ppermute | solution.py:404
  52.4 46.9 %collective-permute-start.9 = (bf16[192,2048]{1,0:T(8,128)(2,1)}, bf16[192,2048]{1,0:T(8,128)(2,1)}, u32[]{:S(2)}, u32[]{:S(2)}) collective-permute-start(bf16[192,2048]{1,0:T(8,128)(2,1)} %collective-permute-done.8.refs_13_), channel_id=1, source_target_pairs={{0,2},{1,15},{2,4},{3,1},{4,6},{5,3},{6,8},{7,5},{8,10},{9,7},{10,... | collective-permute-start | bytes 2359304 | tf_op jit(solution)/shard_map/ppermute | solution.py:401
  60.8 38.7 %collective-permute-start.11 = (bf16[192,2048]{1,0:T(8,128)(2,1)}, bf16[192,2048]{1,0:T(8,128)(2,1)}, u32[]{:S(2)}, u32[]{:S(2)}) collective-permute-start(bf16[192,2048]{1,0:T(8,128)(2,1)} %collective-permute-done.6.refs_15_), channel_id=1, source_target_pairs={{0,2},{1,15},{2,4},{3,1},{4,6},{5,3},{6,8},{7,5},{8,10},{9,7},{10,... | collective-permute-start | bytes 2359304 | tf_op jit(solution)/shard_map/ppermute | solution.py:401
  65.1 19.9 %all-to-all-start.1 = ((bf16[16,64,128]{2,1,0:T(8,128)(2,1)}), bf16[16,64,128]{2,1,0:T(8,128)(2,1)}, u32[]{:S(2)}, u32[]{:S(2)}) async-start(bf16[16,64,128]{2,1,0:T(8,128)(2,1)} %bitcast.16), calls=%async_computation.1 | async-start | bytes 524288 | tf_op jit(solution)/shard_map/all_to_all | solution.py:470
  90.5 26.3 %all-to-all-start.2 = ((bf16[16,16,2048]{2,1,0:T(8,128)(2,1)}), bf16[16,16,2048]{2,1,0:T(8,128)(2,1)}, u32[]{:S(2)}, u32[]{:S(2)}) async-start(bf16[16,16,2048]{2,1,0:T(8,128)(2,1)} %bitcast.17), calls=%async_computation.2 | async-start | bytes 2097152 | tf_op jit(solution)/shard_map/all_to_all | solution.py:507
  98.4 2.6 %collective-permute-start.15 = (bf16[192,2048]{1,0:T(8,128)(2,1)}, bf16[192,2048]{1,0:T(8,128)(2,1)S(1)}, u32[]{:S(2)}, u32[]{:S(2)}) collective-permute-start(bf16[192,2048]{1,0:T(8,128)(2,1)} %copy-done.1), channel_id=1, source_target_pairs={{0,1},{1,0},{2,3},{3,2},{4,5},{5,4},{6,7},{7,6},{8,9},{9,8},{10,11... | collective-permute-start | bytes 2359304 | tf_op jit(solution)/shard_map/ppermute | solution.py:404
  98.6 18.2 %collective-permute-start.16 = (bf16[192,2048]{1,0:T(8,128)(2,1)}, bf16[192,2048]{1,0:T(8,128)(2,1)S(1)}, u32[]{:S(2)}, u32[]{:S(2)}) collective-permute-start(bf16[192,2048]{1,0:T(8,128)(2,1)} %collective-permute-done.8.refs_13_), channel_id=1, source_target_pairs={{0,1},{1,0},{2,3},{3,2},{4,5},{5,4},{6,7},{7,6},{8,9},{9,8},{10,11... | collective-permute-start | bytes 2359304 | tf_op jit(solution)/shard_map/ppermute | solution.py:404
  99.0 17.8 %collective-permute-start.7 = (bf16[192,2048]{1,0:T(8,128)(2,1)}, bf16[192,2048]{1,0:T(8,128)(2,1)S(1)}, u32[]{:S(2)}, u32[]{:S(2)}) collective-permute-start(bf16[192,2048]{1,0:T(8,128)(2,1)} %collective-permute-done.6.refs_15_), channel_id=1, source_target_pairs={{0,1},{1,0},{2,3},{3,2},{4,5},{5,4},{6,7},{7,6},{8,9},{9,8},{10,11... | collective-permute-start | bytes 2359304 | tf_op jit(solution)/shard_map/ppermute | solution.py:404
  99.3 17.6 %collective-permute-start.10 = (bf16[192,2048]{1,0:T(8,128)(2,1)}, bf16[192,2048]{1,0:T(8,128)(2,1)S(1)}, u32[]{:S(2)}, u32[]{:S(2)}) collective-permute-start(bf16[192,2048]{1,0:T(8,128)(2,1)} %collective-permute-done.9.refs_16_), channel_id=1, source_target_pairs={{0,1},{1,0},{2,3},{3,2},{4,5},{5,4},{6,7},{7,6},{8,9},{9,8},{10,11... | collective-permute-start | bytes 2359304 | tf_op jit(solution)/shard_map/ppermute | solution.py:404
  99.6 17.3 %collective-permute-start.12 = (bf16[192,2048]{1,0:T(8,128)(2,1)}, bf16[192,2048]{1,0:T(8,128)(2,1)}, u32[]{:S(2)}, u32[]{:S(2)}) collective-permute-start(bf16[192,2048]{1,0:T(8,128)(2,1)} %collective-permute-done.11.refs_3_), channel_id=1, source_target_pairs={{0,1},{1,0},{2,3},{3,2},{4,5},{5,4},{6,7},{7,6},{8,9},{9,8},{10,11... | collective-permute-start | bytes 2359304 | tf_op jit(solution)/shard_map/ppermute | solution.py:404
  116.9 1.1 copy-start
  118.0 1.1 copy-start.2
  119.2 26.4 %copy-start.3 = (bf16[64,2048]{1,0:T(8,128)(2,1)S(1)}, bf16[64,2048]{1,0:T(8,128)(2,1)}, u32[]{:S(2)}) copy-start(bf16[64,2048]{1,0:T(8,128)(2,1)} %get-tuple-element.27.stream) | copy-start | bytes 786436
  119.2 26.4 %copy-start.4 = (f32[3,2048]{1,0:T(4,128)S(1)}, f32[3,2048]{1,0:T(4,128)}, u32[]{:S(2)}) copy-start(f32[3,2048]{1,0:T(4,128)} %gain.1) | copy-start | bytes 73732
  119.2 26.4 %copy-start.5 = (bf16[192,256]{1,0:T(8,128)(2,1)S(1)}, bf16[192,256]{1,0:T(8,128)(2,1)}, u32[]{:S(2)}) copy-start(bf16[192,256]{1,0:T(8,128)(2,1)} %get-tuple-element.28.table) | copy-start | bytes 294916
  (2 other events, 1.5 us)

commit v10 on v9

--- a/solution.py
+++ b/solution.py
@@ -20,7 +20,7 @@
 
 
 FULL = pltpu.CompilerParams(vmem_limit_bytes=67043328)
-ROOMY = pltpu.CompilerParams(vmem_limit_bytes=40 * 1024 * 1024)
+ROOMY = pltpu.CompilerParams(vmem_limit_bytes=30 * 1024 * 1024)
 
 
 def anywhere():
@@ -315,7 +315,7 @@
 
 
 def expert_kernel(*refs):
-    tokens, ready, shares = refs[0], refs[1:5], refs[5:-5]
+    tokens, shares = refs[0], refs[1:-5]
     out, gate_w, up_w, down_w, sems = refs[-5:]
     ff = shares[0].shape[0] // 3
     copies = [
@@ -328,22 +328,18 @@
         for at, share in enumerate(shares)
     ]
     x = tokens[...]
-    block = len(ready) * ff
+    acc = jnp.zeros(x.shape, F32)
+    block = 256
     last = (((1,), (1,)), ((), ()))
-
-    def part(gate_rows, up_rows, down_rows):
-        gate = lax.dot_general(x, gate_rows, last, preferred_element_type=F32)
-        up = lax.dot_general(x, up_rows, last, preferred_element_type=F32)
-        hidden = (jax.nn.silu(gate) * up).astype(BF16)
-        return jnp.dot(hidden, down_rows, preferred_element_type=F32)
-
-    acc = part(*(jnp.concatenate([p[j * ff : (j + 1) * ff, :] for p in ready], axis=0) for j in range(3)))
     for k in range(len(shares) * ff // block):
         for piece in range(k * block // ff, (k + 1) * block // ff):
             for copy in copies[piece]:
                 copy.wait()
         rows = slice(k * block, (k + 1) * block)
-        acc = acc + part(gate_w[rows, :], up_w[rows, :], down_w[rows, :])
+        gate = lax.dot_general(x, gate_w[rows, :], last, preferred_element_type=F32)
+        up = lax.dot_general(x, up_w[rows, :], last, preferred_element_type=F32)
+        hidden = (jax.nn.silu(gate) * up).astype(BF16)
+        acc = acc + jnp.dot(hidden, down_w[rows, :], preferred_element_type=F32)
     out[...] = acc.astype(BF16)
 
 
@@ -507,19 +503,18 @@
     arrived = lax.all_to_all(outgoing.reshape(sp, slots // sp, width), "sp", split_axis=0, concat_axis=0, tiled=True)
     arrived = arrived.reshape(slots, width)
 
-    ready = (e3a, e3b, r4, e4)
-    shares = (own, other, r1a, e1a, r1b, e1b, r2a, e2a, r2b, e2b, r3a, r3b)
+    shares = (own, other, r1a, e1a, r1b, e1b, r2a, e2a, r2b, e2b, r3a, r3b, e3a, e3b, r4, e4)
     experts = pl.pallas_call(
         expert_kernel,
         out_shape=shape((slots, width), BF16),
-        in_specs=[whole()] * (1 + len(ready)) + [anywhere()] * len(shares),
+        in_specs=[whole()] + [anywhere()] * len(shares),
         out_specs=whole(),
         scratch_shapes=[pltpu.VMEM((len(shares) * ff_own, width), BF16)] * 3
         + [pltpu.SemaphoreType.DMA((3 * len(shares),))],
         compiler_params=ROOMY,
         name="experts",
     )
-    done = experts(arrived, *ready, *shares)
+    done = experts(arrived, *shares)
     returned = lax.all_to_all(
         done.reshape(sp, slots // sp, width), "sp", split_axis=0, concat_axis=0, tiled=True
     )

time: 148 us -> 146 us (0.986)
  transfers between devices with their start and end apart: 19 -> 19, of which waited for: 7 -> 7; matrix products, arithmetic and copies ran while one was open for 2% -> 3% of each run, Pallas kernels for 10% -> 10%
where the time goes in v10:
time: 146 us
  waiting for transfers between devices  45.1 us (31%)
  starting transfers between devices  36.2 us (25%)
  blocking collectives  33.3 us (23%)
  Pallas kernels  23.7 us (16%)
  local copies, waits for them, and re-layouts  7.42 us (5%)
    all_to_all x1, blocking collectives, layer(): lax.all_to_all(done.reshape(sp, slots // sp, width), 'sp', split_axis=0,...  19.2 us
    all_to_all x1, waiting for transfers between devices, layer(): lax.all_to_all(outgoing.reshape(sp, slots // sp, width), 'sp', split_axis...  15.8 us
    ppermute x7, waiting for transfers between devices, around(): lax.ppermute(part, 'tp', [(i, (i + 2 - 4 * (i % 2)) % tp) for i in range(...  15.5 us
    all_to_all x1, blocking collectives, layer(): lax.all_to_all(total, 'sp', split_axis=0, concat_axis=0, tiled=True)  14.1 us
    ppermute x7, starting transfers between devices, around(): lax.ppermute(part, 'tp', [(i, (i + 2 - 4 * (i % 2)) % tp) for i in range(...  11.3 us
    all_to_all x1, waiting for transfers between devices, layer(): lax.all_to_all(mixed.reshape(tp, rows, channels), 'tp', split_axis=0, con...  9.11 us
    all_to_all x1, starting transfers between devices, layer(): lax.all_to_all(outgoing.reshape(sp, slots // sp, width), 'sp', split_axis...  7.81 us
    all_to_all x1, starting transfers between devices, layer(): lax.all_to_all(mixed.reshape(tp, rows, channels), 'tp', split_axis=0, con...  7.04 us
  transfers between devices with their start and end apart: 19, of which 7 were waited for; matrix products, arithmetic and copies ran while one was open for 3% of the time, Pallas kernels for 10%

profile of v10, /device:TPU:1, one launch (start us, length us, event | category | flops | bytes accessed | tf_op | source)
XLA Modules:
  0.0 145.8 jit_solution(11712593724607458114)
XLA Ops:
  0.0 1.9 %pack.1.refs_1_ = bf16[192,2048]{1,0:T(8,128)(2,1)} custom-call(bf16[64,2048]{1,0:T(8,128)(2,1)} %bitcast.20, bf16[64,2048]{1,0:T(8,128)(2,1)} %bitcast.21, bf16[64,2048]{1,0:T(8,128)(2,1)} %bitcast.22), custom_call_target="tpu_custom_call" | custom-call | tf_op jit(solution)/shard_map/pack/pallas_call | solution.py:386
  1.9 3.3 %collective-permute-start.3 = (bf16[192,2048]{1,0:T(8,128)(2,1)}, bf16[192,2048]{1,0:T(8,128)(2,1)}, u32[]{:S(2)}, u32[]{:S(2)}) collective-permute-start(bf16[192,2048]{1,0:T(8,128)(2,1)} %pack.1.refs_1_), channel_id=1, source_target_pairs={{0,1},{1,0},{2,3},{3,2},{4,5},{5,4},{6,7},{7,6},{8,9},{9,8},{10,11... | collective-permute-start | bytes 2359304 | tf_op jit(solution)/shard_map/ppermute | solution.py:400
  5.2 3.9 %collective-permute-start.2 = (bf16[192,2048]{1,0:T(8,128)(2,1)}, bf16[192,2048]{1,0:T(8,128)(2,1)}, u32[]{:S(2)}, u32[]{:S(2)}) collective-permute-start(bf16[192,2048]{1,0:T(8,128)(2,1)} %pack.1.refs_1_), channel_id=1, source_target_pairs={{0,2},{1,15},{2,4},{3,1},{4,6},{5,3},{6,8},{7,5},{8,10},{9,7},{10,... | collective-permute-start | bytes 2359304 | tf_op jit(solution)/shard_map/ppermute | solution.py:397
  9.8 3.6 %collective-permute-start = (bf16[2,128]{1,0:T(2,128)(2,1)S(1)}, bf16[2,128]{1,0:T(2,128)(2,1)}, u32[]{:S(2)}, u32[]{:S(2)}) collective-permute-start(bf16[2,128]{1,0:T(2,128)(2,1)S(1)} %get-tuple-element.30), channel_id=1, source_target_pairs={{0,16},{16,32},{32,48},{48,64},{64,80},{80,96},{96,112},{112,128},... | collective-permute-start | bytes 1544 | tf_op jit(solution)/shard_map/ppermute | solution.py:382
  13.4 1.3 collective-permute-start.1
  14.7 3.4 %collective-permute-done.1.after_h = bf16[2,128]{1,0:T(2,128)(2,1)} collective-permute-done((bf16[2,128]{1,0:T(2,128)(2,1)S(1)}, bf16[2,128]{1,0:T(2,128)(2,1)}, u32[]{:S(2)}, u32[]{:S(2)}) %collective-permute-start.1) | collective-permute-done | bytes 544 | tf_op jit(solution)/shard_map/ppermute | solution.py:383
  18.1 5.9 %scan.1 = (f32[1024,128]{1,0:T(8,128)}, f32[1024,128]{1,0:T(8,128)}, f32[1024,128]{1,0:T(8,128)}, f32[32,128]{1,0:T(8,128)}, f32[16,8,128]{2,1,0:T(8,128)}) custom-call(bf16[1024,128]{1,0:T(8,128)(2,1)} %mix_h.1, bf16[2,128]{1,0:T(2,128)(2,1)} %collective-permute-done.before_h, bf16[2,128]{1,0:T(2,128)(2,1)} %collective-permute-done.1.after_h, ...), custom_call_target="tpu_custom_call" | custom-call | tf_op jit(solution)/shard_map/scan/pallas_call | solution.py:408
  25.5 14.1 %all_to_all.20.refs_4_ = f32[16,8,128]{2,1,0:T(8,128)} all-to-all(f32[16,8,128]{2,1,0:T(8,128)} %get-tuple-element.22), channel_id=1, replica_groups=mesh['sp'=16,'tp'=16] {'sp'}, dimensions={0} | all-to-all | bytes 131072 | tf_op jit(solution)/shard_map/all_to_all | solution.py:445
  40.4 3.3 %collective-permute-done.7.refs_7_ = bf16[192,2048]{1,0:T(8,128)(2,1)S(1)} collective-permute-done((bf16[192,2048]{1,0:T(8,128)(2,1)}, bf16[192,2048]{1,0:T(8,128)(2,1)S(1)}, u32[]{:S(2)}, u32[]{:S(2)}) %collective-permute-start.7) | collective-permute-done | bytes 786464 | tf_op jit(solution)/shard_map/ppermute | solution.py:397
  44.6 1.8 %collective-permute-start.11 = (bf16[192,2048]{1,0:T(8,128)(2,1)S(1)}, bf16[192,2048]{1,0:T(8,128)(2,1)}, u32[]{:S(2)}, u32[]{:S(2)}) collective-permute-start(bf16[192,2048]{1,0:T(8,128)(2,1)S(1)} %collective-permute-done.7.refs_7_), channel_id=1, source_target_pairs={{0,2},{1,15},{2,4},{3,1},{4,6},{5,3},{6,8},{7,5},{8,10},{9,7},{10,... | collective-permute-start | bytes 2359304 | tf_op jit(solution)/shard_map/ppermute | solution.py:397
  46.9 5.5 %collective-permute-done.9.refs_9_ = bf16[192,2048]{1,0:T(8,128)(2,1)} collective-permute-done((bf16[192,2048]{1,0:T(8,128)(2,1)}, bf16[192,2048]{1,0:T(8,128)(2,1)}, u32[]{:S(2)}, u32[]{:S(2)}) %collective-permute-start.9) | collective-permute-done | bytes 786464 | tf_op jit(solution)/shard_map/ppermute | solution.py:397
  52.4 1.6 %collective-permute-start.12 = (bf16[192,2048]{1,0:T(8,128)(2,1)}, bf16[192,2048]{1,0:T(8,128)(2,1)}, u32[]{:S(2)}, u32[]{:S(2)}) collective-permute-start(bf16[192,2048]{1,0:T(8,128)(2,1)} %collective-permute-done.9.refs_9_), channel_id=1, source_target_pairs={{0,2},{1,15},{2,4},{3,1},{4,6},{5,3},{6,8},{7,5},{8,10},{9,7},{10,... | collective-permute-start | bytes 2359304 | tf_op jit(solution)/shard_map/ppermute | solution.py:397
  54.0 6.8 %collective-permute-done.11.refs_11_ = bf16[192,2048]{1,0:T(8,128)(2,1)} collective-permute-done((bf16[192,2048]{1,0:T(8,128)(2,1)S(1)}, bf16[192,2048]{1,0:T(8,128)(2,1)}, u32[]{:S(2)}, u32[]{:S(2)}) %collective-permute-start.11) | collective-permute-done | bytes 786464 | tf_op jit(solution)/shard_map/ppermute | solution.py:397
  60.8 1.6 %collective-permute-start.15 = (bf16[192,2048]{1,0:T(8,128)(2,1)}, bf16[192,2048]{1,0:T(8,128)(2,1)}, u32[]{:S(2)}, u32[]{:S(2)}) collective-permute-start(bf16[192,2048]{1,0:T(8,128)(2,1)} %collective-permute-done.11.refs_11_), channel_id=1, source_target_pairs={{0,2},{1,15},{2,4},{3,1},{4,6},{5,3},{6,8},{7,5},{8,10},{9,7},{10,... | collective-permute-start | bytes 2359304 | tf_op jit(solution)/shard_map/ppermute | solution.py:397
  62.5 2.7 %mix.1 = bf16[1024,128]{1,0:T(8,128)(2,1)} custom-call(f32[1024,128]{1,0:T(8,128)} %get-tuple-element.17.refs_0_, f32[1024,128]{1,0:T(8,128)} %get-tuple-element.18.refs_1_, f32[1024,128]{1,0:T(8,128)} %get-tuple-element.19.refs_2_, f32[32,128]{1,0:T(8,128)} %get-tuple-element.20.refs_3_, f32[16,8,128]{2,1,0:T(8,128)} %all_to_all.20.refs_4_, ...), custom_call_target="tpu_custom_call" | custom-call | tf_op jit(solution)/shard_map/mix/pallas_call | solution.py:465
  65.1 7.0 %all-to-all-start.1 = ((bf16[16,64,128]{2,1,0:T(8,128)(2,1)}), bf16[16,64,128]{2,1,0:T(8,128)(2,1)}, u32[]{:S(2)}, u32[]{:S(2)}) async-start(bf16[16,64,128]{2,1,0:T(8,128)(2,1)} %bitcast.17), calls=%async_computation.1 | async-start | bytes 524288 | tf_op jit(solution)/shard_map/all_to_all | solution.py:466
  75.7 9.1 %all-to-all-done.1.mixed_h = bf16[16,64,128]{2,1,0:T(8,128)(2,1)} async-done(((bf16[16,64,128]{2,1,0:T(8,128)(2,1)}), bf16[16,64,128]{2,1,0:T(8,128)(2,1)}, u32[]{:S(2)}, u32[]{:S(2)}) %all-to-all-start.1) | async-done | bytes 262176 | tf_op jit(solution)/shard_map/all_to_all | solution.py:466
  84.8 5.5 %proj.1 = (bf16[64,2048]{1,0:T(8,128)(2,1)}, bf16[256,2048]{1,0:T(8,128)(2,1)}, bf16[192,256]{1,0:T(8,128)(2,1)}) custom-call(bf16[16,64,128]{2,1,0:T(8,128)(2,1)} %all-to-all-done.1.mixed_h, bf16[2048,2048]{1,0:T(8,128)(2,1)} %weights_h.1, bf16[64,2048]{1,0:T(8,128)(2,1)} %residual_h.1, f32[3,2048]{1,0:T(4,128)} %gain.1, s32[2,64]{1,0:T(2,128)} %copy.20.routes_h, ...), custom_call_target="tpu_custom_call" | custom-call | tf_op jit(solution)/shard_map/proj/pallas_call | solution.py:500
  90.4 7.8 %all-to-all-start.2 = ((bf16[16,16,2048]{2,1,0:T(8,128)(2,1)}), bf16[16,16,2048]{2,1,0:T(8,128)(2,1)S(1)}, u32[]{:S(2)}, u32[]{:S(2)}) async-start(bf16[16,16,2048]{2,1,0:T(8,128)(2,1)} %bitcast.18), calls=%async_computation.2 | async-start | bytes 2097152 | tf_op jit(solution)/shard_map/all_to_all | solution.py:503
  99.6 1.2 collective-permute-done.8.refs_8_
  100.8 15.8 %all-to-all-done.2 = bf16[16,16,2048]{2,1,0:T(8,128)(2,1)S(1)} async-done(((bf16[16,16,2048]{2,1,0:T(8,128)(2,1)}), bf16[16,16,2048]{2,1,0:T(8,128)(2,1)S(1)}, u32[]{:S(2)}, u32[]{:S(2)}) %all-to-all-start.2) | async-done | bytes 1048608 | tf_op jit(solution)/shard_map/all_to_all | solution.py:503
  118.9 6.5 %experts.1 = bf16[256,2048]{1,0:T(8,128)(2,1)S(1)} custom-call(bf16[256,2048]{1,0:T(8,128)(2,1)S(1)} %bitcast.14, bf16[192,2048]{1,0:T(8,128)(2,1)S(1)} %copy-done, bf16[192,2048]{1,0:T(8,128)(2,1)} %collective-permute-done.3.refs_2_, bf16[192,2048]{1,0:T(8,128)(2,1)} %collective-permute-done.2.refs_3_, bf16[192,2048]{1,0:T(8,128)(2,1)} %collective-permute-done.5.refs_4_, ...), custom_call_target="tpu_custom_call" | custom-call | tf_op jit(solution)/shard_map/experts/pallas_call | solution.py:517
  125.4 19.2 %all_to_all.21 = bf16[16,16,2048]{2,1,0:T(8,128)(2,1)S(1)} all-to-all(bf16[16,16,2048]{2,1,0:T(8,128)(2,1)S(1)} %bitcast.15), channel_id=1, replica_groups=mesh['sp'=16,'tp'=16] {'sp'}, dimensions={0} | all-to-all | bytes 2097152 | tf_op jit(solution)/shard_map/all_to_all | solution.py:518
  144.6 1.3 combine.1
  (42 shorter events, 11.6 us)
Async XLA Ops:
  1.9 22.1 %collective-permute-start.3 = (bf16[192,2048]{1,0:T(8,128)(2,1)}, bf16[192,2048]{1,0:T(8,128)(2,1)}, u32[]{:S(2)}, u32[]{:S(2)}) collective-permute-start(bf16[192,2048]{1,0:T(8,128)(2,1)} %pack.1.refs_1_), channel_id=1, source_target_pairs={{0,1},{1,0},{2,3},{3,2},{4,5},{5,4},{6,7},{7,6},{8,9},{9,8},{10,11... | collective-permute-start | bytes 2359304 | tf_op jit(solution)/shard_map/ppermute | solution.py:400
  5.2 19.6 %collective-permute-start.2 = (bf16[192,2048]{1,0:T(8,128)(2,1)}, bf16[192,2048]{1,0:T(8,128)(2,1)}, u32[]{:S(2)}, u32[]{:S(2)}) collective-permute-start(bf16[192,2048]{1,0:T(8,128)(2,1)} %pack.1.refs_1_), channel_id=1, source_target_pairs={{0,2},{1,15},{2,4},{3,1},{4,6},{5,3},{6,8},{7,5},{8,10},{9,7},{10,... | collective-permute-start | bytes 2359304 | tf_op jit(solution)/shard_map/ppermute | solution.py:397
  9.8 4.9 %collective-permute-start = (bf16[2,128]{1,0:T(2,128)(2,1)S(1)}, bf16[2,128]{1,0:T(2,128)(2,1)}, u32[]{:S(2)}, u32[]{:S(2)}) collective-permute-start(bf16[2,128]{1,0:T(2,128)(2,1)S(1)} %get-tuple-element.30), channel_id=1, source_target_pairs={{0,16},{16,32},{32,48},{48,64},{64,80},{80,96},{96,112},{112,128},... | collective-permute-start | bytes 1544 | tf_op jit(solution)/shard_map/ppermute | solution.py:382
  13.4 4.7 %collective-permute-start.1 = (bf16[2,128]{1,0:T(2,128)(2,1)S(1)}, bf16[2,128]{1,0:T(2,128)(2,1)}, u32[]{:S(2)}, u32[]{:S(2)}) collective-permute-start(bf16[2,128]{1,0:T(2,128)(2,1)S(1)} %get-tuple-element.29), channel_id=1, source_target_pairs={{16,0},{32,16},{48,32},{64,48},{80,64},{96,80},{112,96},{128,112},... | collective-permute-start | bytes 1544 | tf_op jit(solution)/shard_map/ppermute | solution.py:383
  24.0 15.7 %collective-permute-start.4 = (bf16[192,2048]{1,0:T(8,128)(2,1)}, bf16[192,2048]{1,0:T(8,128)(2,1)}, u32[]{:S(2)}, u32[]{:S(2)}) collective-permute-start(bf16[192,2048]{1,0:T(8,128)(2,1)} %collective-permute-done.3.refs_2_), channel_id=1, source_target_pairs={{0,2},{1,15},{2,4},{3,1},{4,6},{5,3},{6,8},{7,5},{8,10},{9,7},{10,... | collective-permute-start | bytes 2359304 | tf_op jit(solution)/shard_map/ppermute | solution.py:397
  24.8 18.9 %collective-permute-start.7 = (bf16[192,2048]{1,0:T(8,128)(2,1)}, bf16[192,2048]{1,0:T(8,128)(2,1)S(1)}, u32[]{:S(2)}, u32[]{:S(2)}) collective-permute-start(bf16[192,2048]{1,0:T(8,128)(2,1)} %collective-permute-done.2.refs_3_), channel_id=1, source_target_pairs={{0,2},{1,15},{2,4},{3,1},{4,6},{5,3},{6,8},{7,5},{8,10},{9,7},{10,... | collective-permute-start | bytes 2359304 | tf_op jit(solution)/shard_map/ppermute | solution.py:397
  39.7 12.7 %collective-permute-start.9 = (bf16[192,2048]{1,0:T(8,128)(2,1)}, bf16[192,2048]{1,0:T(8,128)(2,1)}, u32[]{:S(2)}, u32[]{:S(2)}) collective-permute-start(bf16[192,2048]{1,0:T(8,128)(2,1)} %collective-permute-done.4.refs_5_), channel_id=1, source_target_pairs={{0,2},{1,15},{2,4},{3,1},{4,6},{5,3},{6,8},{7,5},{8,10},{9,7},{10,... | collective-permute-start | bytes 2359304 | tf_op jit(solution)/shard_map/ppermute | solution.py:397
  44.6 16.3 %collective-permute-start.11 = (bf16[192,2048]{1,0:T(8,128)(2,1)S(1)}, bf16[192,2048]{1,0:T(8,128)(2,1)}, u32[]{:S(2)}, u32[]{:S(2)}) collective-permute-start(bf16[192,2048]{1,0:T(8,128)(2,1)S(1)} %collective-permute-done.7.refs_7_), channel_id=1, source_target_pairs={{0,2},{1,15},{2,4},{3,1},{4,6},{5,3},{6,8},{7,5},{8,10},{9,7},{10,... | collective-permute-start | bytes 2359304 | tf_op jit(solution)/shard_map/ppermute | solution.py:397
  46.4 52.0 %collective-permute-start.5 = (bf16[192,2048]{1,0:T(8,128)(2,1)}, bf16[192,2048]{1,0:T(8,128)(2,1)}, u32[]{:S(2)}, u32[]{:S(2)}) collective-permute-start(bf16[192,2048]{1,0:T(8,128)(2,1)} %collective-permute-done.2.refs_3_), channel_id=1, source_target_pairs={{0,1},{1,0},{2,3},{3,2},{4,5},{5,4},{6,7},{7,6},{8,9},{9,8},{10,11... | collective-permute-start | bytes 2359304 | tf_op jit(solution)/shard_map/ppermute | solution.py:400
  46.4 52.4 %collective-permute-start.6 = (bf16[192,2048]{1,0:T(8,128)(2,1)}, bf16[192,2048]{1,0:T(8,128)(2,1)}, u32[]{:S(2)}, u32[]{:S(2)}) collective-permute-start(bf16[192,2048]{1,0:T(8,128)(2,1)} %collective-permute-done.4.refs_5_), channel_id=1, source_target_pairs={{0,1},{1,0},{2,3},{3,2},{4,5},{5,4},{6,7},{7,6},{8,9},{9,8},{10,11... | collective-permute-start | bytes 2359304 | tf_op jit(solution)/shard_map/ppermute | solution.py:400
  52.4 46.7 %collective-permute-start.12 = (bf16[192,2048]{1,0:T(8,128)(2,1)}, bf16[192,2048]{1,0:T(8,128)(2,1)}, u32[]{:S(2)}, u32[]{:S(2)}) collective-permute-start(bf16[192,2048]{1,0:T(8,128)(2,1)} %collective-permute-done.9.refs_9_), channel_id=1, source_target_pairs={{0,2},{1,15},{2,4},{3,1},{4,6},{5,3},{6,8},{7,5},{8,10},{9,7},{10,... | collective-permute-start | bytes 2359304 | tf_op jit(solution)/shard_map/ppermute | solution.py:397
  60.8 38.5 %collective-permute-start.15 = (bf16[192,2048]{1,0:T(8,128)(2,1)}, bf16[192,2048]{1,0:T(8,128)(2,1)}, u32[]{:S(2)}, u32[]{:S(2)}) collective-permute-start(bf16[192,2048]{1,0:T(8,128)(2,1)} %collective-permute-done.11.refs_11_), channel_id=1, source_target_pairs={{0,2},{1,15},{2,4},{3,1},{4,6},{5,3},{6,8},{7,5},{8,10},{9,7},{10,... | collective-permute-start | bytes 2359304 | tf_op jit(solution)/shard_map/ppermute | solution.py:397
  65.1 19.7 %all-to-all-start.1 = ((bf16[16,64,128]{2,1,0:T(8,128)(2,1)}), bf16[16,64,128]{2,1,0:T(8,128)(2,1)}, u32[]{:S(2)}, u32[]{:S(2)}) async-start(bf16[16,64,128]{2,1,0:T(8,128)(2,1)} %bitcast.17), calls=%async_computation.1 | async-start | bytes 524288 | tf_op jit(solution)/shard_map/all_to_all | solution.py:466
  90.4 26.2 %all-to-all-start.2 = ((bf16[16,16,2048]{2,1,0:T(8,128)(2,1)}), bf16[16,16,2048]{2,1,0:T(8,128)(2,1)S(1)}, u32[]{:S(2)}, u32[]{:S(2)}) async-start(bf16[16,16,2048]{2,1,0:T(8,128)(2,1)} %bitcast.18), calls=%async_computation.2 | async-start | bytes 2097152 | tf_op jit(solution)/shard_map/all_to_all | solution.py:503
  98.2 2.6 %collective-permute-start.8 = (bf16[192,2048]{1,0:T(8,128)(2,1)}, bf16[192,2048]{1,0:T(8,128)(2,1)S(1)}, u32[]{:S(2)}, u32[]{:S(2)}) collective-permute-start(bf16[192,2048]{1,0:T(8,128)(2,1)} %copy-done.1), channel_id=1, source_target_pairs={{0,1},{1,0},{2,3},{3,2},{4,5},{5,4},{6,7},{7,6},{8,9},{9,8},{10,11... | collective-permute-start | bytes 2359304 | tf_op jit(solution)/shard_map/ppermute | solution.py:400
  98.4 18.2 %collective-permute-start.10 = (bf16[192,2048]{1,0:T(8,128)(2,1)}, bf16[192,2048]{1,0:T(8,128)(2,1)S(1)}, u32[]{:S(2)}, u32[]{:S(2)}) collective-permute-start(bf16[192,2048]{1,0:T(8,128)(2,1)} %collective-permute-done.9.refs_9_), channel_id=1, source_target_pairs={{0,1},{1,0},{2,3},{3,2},{4,5},{5,4},{6,7},{7,6},{8,9},{9,8},{10,11... | collective-permute-start | bytes 2359304 | tf_op jit(solution)/shard_map/ppermute | solution.py:400
  98.8 17.8 %collective-permute-start.13 = (bf16[192,2048]{1,0:T(8,128)(2,1)}, bf16[192,2048]{1,0:T(8,128)(2,1)S(1)}, u32[]{:S(2)}, u32[]{:S(2)}) collective-permute-start(bf16[192,2048]{1,0:T(8,128)(2,1)} %collective-permute-done.11.refs_11_), channel_id=1, source_target_pairs={{0,1},{1,0},{2,3},{3,2},{4,5},{5,4},{6,7},{7,6},{8,9},{9,8},{10,11... | collective-permute-start | bytes 2359304 | tf_op jit(solution)/shard_map/ppermute | solution.py:400
  99.1 17.5 %collective-permute-start.14 = (bf16[192,2048]{1,0:T(8,128)(2,1)}, bf16[192,2048]{1,0:T(8,128)(2,1)}, u32[]{:S(2)}, u32[]{:S(2)}) collective-permute-start(bf16[192,2048]{1,0:T(8,128)(2,1)} %collective-permute-done.12.refs_12_), channel_id=1, source_target_pairs={{0,1},{1,0},{2,3},{3,2},{4,5},{5,4},{6,7},{7,6},{8,9},{9,8},{10,11... | collective-permute-start | bytes 2359304 | tf_op jit(solution)/shard_map/ppermute | solution.py:400
  99.3 17.3 %collective-permute-start.16 = (bf16[192,2048]{1,0:T(8,128)(2,1)}, bf16[192,2048]{1,0:T(8,128)(2,1)}, u32[]{:S(2)}, u32[]{:S(2)}) collective-permute-start(bf16[192,2048]{1,0:T(8,128)(2,1)} %collective-permute-done.15.refs_15_), channel_id=1, source_target_pairs={{0,1},{1,0},{2,3},{3,2},{4,5},{5,4},{6,7},{7,6},{8,9},{9,8},{10,11... | collective-permute-start | bytes 2359304 | tf_op jit(solution)/shard_map/ppermute | solution.py:400
  116.6 1.1 copy-start
  117.8 1.1 copy-start.2
  118.9 25.7 %copy-start.3 = (bf16[64,2048]{1,0:T(8,128)(2,1)S(1)}, bf16[64,2048]{1,0:T(8,128)(2,1)}, u32[]{:S(2)}) copy-start(bf16[64,2048]{1,0:T(8,128)(2,1)} %get-tuple-element.27.stream) | copy-start | bytes 786436
  118.9 25.7 %copy-start.4 = (f32[3,2048]{1,0:T(4,128)S(1)}, f32[3,2048]{1,0:T(4,128)}, u32[]{:S(2)}) copy-start(f32[3,2048]{1,0:T(4,128)} %gain.1) | copy-start | bytes 73732
  118.9 25.7 %copy-start.5 = (bf16[192,256]{1,0:T(8,128)(2,1)S(1)}, bf16[192,256]{1,0:T(8,128)(2,1)}, u32[]{:S(2)}) copy-start(bf16[192,256]{1,0:T(8,128)(2,1)} %get-tuple-element.28.table) | copy-start | bytes 294916
  (2 other events, 1.5 us)
